TPU v7x, 128 devices: a whole 4x4x4 slice. The times are simulated.
128 devices in a mesh: sp: 32 (over z, y, core), tp: 4 (over x).
Axes of the slice: x: 4, y: 4, z: 4, core: 2. Of those that a mesh axis runs over, the one named last changes fastest.
Arguments:
- query_rows: bfloat16 [16384, 1024], P('sp', 'tp'), may hold values from -6 to 6
- key_rows: bfloat16 [16384, 512], P('sp', 'tp'), may hold values from -6 to 6
- value_rows: bfloat16 [16384, 512], P('sp', 'tp'), may hold values from -12 to 12
- query_gain: float32 [128], replicated, may hold values from 0.2 to 6.5
- key_gain: float32 [128], replicated, may hold values from 0.2 to 6.5
- residual: bfloat16 [16384, 2048], P(('sp', 'tp')), may hold values from -6 to 6
- out_weight: bfloat16 [1024, 2048], P('tp'), may hold values from -3 to 3
- mix_gain: float32 [2048], replicated, may hold values from 0.1 to 1.9
- gate_weight: bfloat16 [2048, 5632], P('sp', 'tp'), may hold values from -0.125 to 0.125
- up_weight: bfloat16 [2048, 5632], P('sp', 'tp'), may hold values from -0.125 to 0.125
- down_weight: bfloat16 [5632, 2048], P('tp', 'sp'), may hold values from -0.15625 to 0.15625
Outputs:
- layer_out: bfloat16 [16384, 2048], P(('sp', 'tp'))
All inputs are finite; a program needn't handle non-finite values.
Results may differ from a plain program's by a relative error of at most 0.015.
The roundings to bfloat16 on the way count: a program that leaves them out, or rounds other values in their place, can miss the bound.
Values may be sent and summed in bfloat16 or wider, within the bound.
No kernel may reach another device: no remote copies, remote signals or barrier semaphores. Data moves between devices by JAX's collectives and lax.ppermute only.
A program may use at most 128 MiB of HBM per device.

v0:
```python
import jax
import jax.numpy as jnp
from jax import lax
from jax.sharding import PartitionSpec as P

GRID = 64


norm_eps = 1e-06
theta_base = 10000.0


def sent_together(arrays, axis, dim, along):
    widths = [a.shape[along] for a in arrays]
    both = jnp.concatenate(arrays, axis=along)
    filled = lax.all_gather(both, axis, axis=dim, tiled=True)
    return tuple(jnp.split(filled, [sum(widths[:k]) for k in range(1, len(widths))], axis=along))


def cut_along(value, dim, devices):
    before, after = (value.shape[:dim], value.shape[dim + 1 :])
    return jnp.moveaxis(value.reshape(*before, devices, -1, *after), dim, 0)


def summed_on_arrival(value, axis, dim):
    devices = lax.axis_size(axis)
    blocks = lax.all_to_all(cut_along(value, dim, devices), axis, 0, 0, tiled=True)
    return jnp.sum(blocks.astype(jnp.float32), axis=0)


def joined_along(blocks, dim):
    blocks = jnp.moveaxis(blocks, 0, dim)
    shape = blocks.shape
    return blocks.reshape(*shape[:dim], shape[dim] * shape[dim + 1], *shape[dim + 2 :])


def from_everyone(value, axis):
    copies = jnp.broadcast_to(value, (lax.axis_size(axis), *value.shape))
    return lax.all_to_all(copies, axis, split_axis=0, concat_axis=0, tiled=True)


def gather_directly(value, axis, dim):
    return joined_along(from_everyone(value, axis), dim)


def spin(halfway, angles):
    cosine = jnp.cos(angles)[:, None, :]
    sine_val = jnp.sin(angles)[:, None, :]
    quarter = halfway.shape[-1] // 2
    leading = halfway[..., :quarter]
    trailing = halfway[..., quarter:]
    return [leading * cosine - trailing * sine_val, trailing * cosine + leading * sine_val]


def rotate_grid(vectors, positions):
    head_dim = vectors.shape[-1]
    quarter = head_dim // 4
    frequency = jnp.power(
        theta_base, -2.0 * jnp.arange(quarter, dtype=jnp.float32) / (head_dim // 2)
    )
    row_angle = (positions // GRID).astype(jnp.float32)[:, None] * frequency
    col_angle = (positions % GRID).astype(jnp.float32)[:, None] * frequency
    lower_half = vectors[..., : 2 * quarter]
    upper_half = vectors[..., 2 * quarter :]
    return jnp.concatenate(spin(lower_half, row_angle) + spin(upper_half, col_angle), axis=-1)


def prepare_heads(raw_heads, head_gain, positions):
    floated = raw_heads.astype(jnp.float32)
    scaled = floated * lax.rsqrt(jnp.mean(floated * floated, axis=-1, keepdims=True) + norm_eps)
    return rotate_grid(scaled * head_gain, positions).astype(jnp.bfloat16)


def row_norm(row_data, row_gain):
    floated = row_data.astype(jnp.float32)
    scaled = floated * lax.rsqrt(jnp.mean(floated * floated, axis=-1, keepdims=True) + norm_eps)
    return (scaled * row_gain).astype(jnp.bfloat16)


def on_device(
    query_rows,
    key_rows,
    value_rows,
    query_gain,
    key_gain,
    residual,
    out_weight,
    mix_gain,
    gate_weight,
    up_weight,
    down_weight,
):
    tok_rows = query_rows.shape[0]
    head_dim = query_gain.shape[0]
    local_kv = key_rows.shape[1] // head_dim
    local_q = query_rows.shape[1] // head_dim
    group_size = local_q // local_kv
    positions = lax.axis_index("sp") * tok_rows + jnp.arange(tok_rows, dtype=jnp.int32)
    q_heads = prepare_heads(query_rows.reshape(tok_rows, local_q, head_dim), query_gain, positions)
    q_stack = (
        q_heads.reshape(tok_rows, local_kv, group_size, head_dim)
        .transpose(1, 2, 0, 3)
        .reshape(local_kv, group_size * tok_rows, head_dim)
    )
    k_heads = prepare_heads(
        key_rows.reshape(tok_rows, local_kv, head_dim), key_gain, positions
    ).reshape(tok_rows, local_kv * head_dim)
    score_scale = head_dim ** (-0.5)
    start_state = (
        jnp.full((local_kv, group_size * tok_rows), -jnp.inf, jnp.float32),
        jnp.zeros((local_kv, group_size * tok_rows), jnp.float32),
        jnp.zeros((local_kv, group_size * tok_rows, head_dim), jnp.float32),
    )
    key_piece, value_piece = sent_together((k_heads, value_rows), "sp", 0, 1)
    count_rows = key_piece.shape[0]
    key_blocks = key_piece.reshape(count_rows // tok_rows, tok_rows, local_kv, head_dim).transpose(
        0, 2, 1, 3
    )
    value_blocks = value_piece.reshape(
        count_rows // tok_rows, tok_rows, local_kv, head_dim
    ).transpose(0, 2, 1, 3)

    def inner(state, blocks):
        key_block, value_block = blocks
        running_max, running_sum, weighted = state
        scores = (
            jnp.einsum("kqd,ksd->kqs", q_stack, key_block, preferred_element_type=jnp.float32)
            * score_scale
        )
        new_max = jnp.maximum(running_max, jnp.max(scores, axis=-1))
        weights = jnp.exp(scores - new_max[..., None])
        factor = jnp.exp(running_max - new_max)
        running_sum = running_sum * factor + jnp.sum(weights, axis=-1)
        weighted = weighted * factor[..., None] + jnp.einsum(
            "kqs,ksd->kqd",
            weights.astype(jnp.bfloat16),
            value_block,
            preferred_element_type=jnp.float32,
        )
        return ((new_max, running_sum, weighted), None)

    result, unused = lax.scan(inner, start_state, (key_blocks, value_blocks))
    final_max, final_sum, weighted = result
    attended = (weighted / final_sum[..., None]).reshape(local_kv, group_size, tok_rows, head_dim)
    attended = (
        attended.transpose(2, 0, 1, 3).reshape(tok_rows, local_q * head_dim).astype(jnp.bfloat16)
    )
    attn_sum = summed_on_arrival(
        jnp.dot(attended, out_weight, preferred_element_type=jnp.float32).astype(jnp.bfloat16),
        "tp",
        0,
    )
    own_rows = (residual.astype(jnp.float32) + attn_sum).astype(jnp.bfloat16)
    normed_all = gather_directly(row_norm(own_rows, mix_gain), "tp", 0)
    gate_piece, up_piece = sent_together((gate_weight, up_weight), "sp", 0, 1)
    gate_act = jnp.dot(normed_all, gate_piece, preferred_element_type=jnp.float32)
    up_act = jnp.dot(normed_all, up_piece, preferred_element_type=jnp.float32)
    down_whole = lax.all_gather(down_weight, "sp", axis=1, tiled=True)
    hidden = (jax.nn.silu(gate_act) * up_act).astype(jnp.bfloat16)
    unit_sum = summed_on_arrival(
        jnp.dot(hidden, down_whole, preferred_element_type=jnp.float32).astype(jnp.bfloat16),
        "tp",
        0,
    )
    return (own_rows.astype(jnp.float32) + 0.5 * unit_sum).astype(jnp.bfloat16)


def solution(mesh):
    placed = (
        P("sp", "tp"),
        P("sp", "tp"),
        P("sp", "tp"),
        P(),
        P(),
        P(("sp", "tp"), None),
        P("tp", None),
        P(),
        P("sp", "tp"),
        P("sp", "tp"),
        P("tp", "sp"),
    )
    return jax.shard_map(
        on_device, mesh=mesh, in_specs=placed, out_specs=P(("sp", "tp"), None), check_vma=False
    )
```

profile of v0, /device:TPU:8, one launch (start us, length us, event | category | flops | bytes accessed | tf_op | source)
XLA Modules:
  0.0 330.9 jit_solution(5153312041854904211)
XLA Ops:
  9.6 1.9 concatenate.43
  13.2 1.9 multiply_cosine_fusion.1
  16.7 1.8 fusion.37
  18.6 1.6 maximum_bitcast_fusion
  20.2 46.6 %all-gather.4.cloned.1.call-done = bf16[16384,256]{1,0:T(8,128)(2,1)} async-done(((bf16[512,256]{1,0:T(8,128)(2,1)}), bf16[16384,256]{1,0:T(8,128)(2,1)}) %all-gather.4.cloned.1.call-update) | async-done | bytes 8388624 | tf_op jit(solution)/shard_map/all_gather | solution.py:16
  66.9 5.7 %fusion.67 = (bf16[16384,128]{1,0:T(8,128)(2,1)}, bf16[16384,128]{1,0:T(8,128)(2,1)}) fusion(bf16[16384,256]{1,0:T(8,128)(2,1)} %all-gather.4.cloned.1.call-done), kind=kLoop, calls=%fused_computation.105 | loop fusion | bytes 16777216 | tf_op jit(solution)/shard_map/split | solution.py:17
  72.6 135.9 %while.15 = (s32[]{:T(128)}, f32[1,1024]{1,0:T(1,128)S(1)}, f32[1,1024]{1,0:T(1,128)S(1)}, f32[1,1024,128]{2,1,0:T(8,128)}, bf16[32,1,512,128]{3,2,1,0:T(8,128)(...) while((s32[]{:T(128)}, f32[1,1024]{1,0:T(1,128)S(1)}, ...), condition=%wide.region_5.6_spmd.clone, body=%wide.region_2.5_spmd.clone.sunk | while | flops 273028096 | bytes 7930985 | solution.py:142
  74.4 2.3 fusion.84
  76.6 1.3 multiply_reduce_fusion.3
  78.4 2.5 fusion.84
  82.7 2.5 fusion.84
  85.2 1.4 multiply_reduce_fusion.3
  86.9 2.5 fusion.84
  89.4 1.3 multiply_reduce_fusion.3
  91.2 2.5 fusion.84
  95.4 2.5 fusion.84
  97.9 1.3 multiply_reduce_fusion.3
  99.7 2.5 fusion.84
  103.9 2.5 fusion.84
  106.4 1.4 multiply_reduce_fusion.3
  108.2 2.5 fusion.84
  110.7 1.4 multiply_reduce_fusion.3
  112.5 2.5 fusion.84
  115.0 1.4 multiply_reduce_fusion.3
  116.8 2.5 fusion.84
  119.3 1.3 multiply_reduce_fusion.3
  121.0 2.5 fusion.84
  125.3 2.5 fusion.84
  129.5 2.5 fusion.84
  132.0 1.3 multiply_reduce_fusion.3
  133.8 2.5 fusion.84
  138.0 2.5 fusion.84
  140.5 1.3 multiply_reduce_fusion.3
  142.2 2.5 fusion.84
  144.7 1.3 multiply_reduce_fusion.3
  146.5 2.5 fusion.84
  150.7 2.5 fusion.84
  153.2 1.3 multiply_reduce_fusion.3
  155.0 2.5 fusion.84
  159.2 2.5 fusion.84
  161.7 1.3 multiply_reduce_fusion.3
  163.4 2.5 fusion.84
  165.9 1.4 multiply_reduce_fusion.3
  167.7 2.6 fusion.84
  170.3 1.3 multiply_reduce_fusion.3
  172.1 2.5 fusion.84
  174.6 1.4 multiply_reduce_fusion.3
  176.4 2.5 fusion.84
  178.8 1.3 multiply_reduce_fusion.3
  180.6 2.5 fusion.84
  184.8 2.5 fusion.84
  187.3 1.3 multiply_reduce_fusion.3
  189.1 2.5 fusion.84
  193.3 2.5 fusion.84
  195.8 1.3 multiply_reduce_fusion.3
  197.6 2.5 fusion.84
  201.8 2.5 fusion.84
  204.3 1.3 multiply_reduce_fusion.3
  206.0 2.5 fusion.84
  210.7 31.0 %all_to_all.15 = bf16[4,128,2048]{2,1,0:T(8,128)(2,1)S(1)} all-to-all(bf16[4,128,2048]{2,1,0:T(8,128)(2,1)S(1)} %bitcast.73), channel_id=1, replica_groups=mesh['sp'=32,'tp'=4] {'tp'}, dimensions={0} | all-to-all | bytes 4194304 | tf_op jit(solution)/shard_map/all_to_all | solution.py:27
  242.8 29.3 %all_to_all.16 = bf16[4,128,2048]{2,1,0:T(8,128)(2,1)} all-to-all(bf16[4,128,2048]{2,1,0:T(8,128)(2,1)S(1)} %broadcast_in_dim.11), channel_id=1, replica_groups=mesh['sp'=32,'tp'=4] {'tp'}, dimensions={0} | all-to-all | bytes 4194304 | tf_op jit(solution)/shard_map/all_to_all | solution.py:39
  272.1 8.4 %fusion.20 = f32[512,1408]{1,0:T(8,128)} fusion(bf16[512,2048]{1,0:T(8,128)(2,1)} %bitcast.79, bf16[2048,2816]{1,0:T(8,128)(2,1)} %all-gather.6.cloned.1.call-done), kind=kOutput, calls=%fused_computation.26 | convolution fusion | flops 2952790016 | bytes 10747904 | tf_op jit(solution)/shard_map/dot_general | solution.py:156
  280.4 13.8 %convolution_convert_fusion.1 = bf16[512,2048]{1,0:T(8,128)(2,1)} fusion(bf16[1408,2048]{0,1:T(8,128)(2,1)} %all-gather.8.cloned.1.call-done, bf16[512,2048]{1,0:T(8,128)(2,1)} %bitcast.80, bf16[2048,2816]{1,0:T(8,128)(2,1)} %all-gather.6.cloned.1.call-done, f32[512,1408]{1,0:T(8,128)} %fusion.20), kind=kOutput, calls=%fused_computation.33 | convolution fusion | flops 5910953984 | bytes 18612224 | tf_op jit(solution)/shard_map/dot_general | solution.py:161
  294.3 28.7 %all_to_all.17 = bf16[4,128,2048]{2,1,0:T(8,128)(2,1)S(1)} all-to-all(bf16[4,128,2048]{2,1,0:T(8,128)(2,1)} %bitcast.81), channel_id=1, replica_groups=mesh['sp'=32,'tp'=4] {'tp'}, dimensions={0} | all-to-all | bytes 4194304 | tf_op jit(solution)/shard_map/all_to_all | solution.py:27
  (192 shorter events, 40.0 us)
Async XLA Ops:
  6.5 203.4 %copy-start = (bf16[256,2048]{1,0:T(8,128)(2,1)S(1)}, bf16[256,2048]{1,0:T(8,128)(2,1)}, u32[]{:S(2)}) copy-start(bf16[256,2048]{1,0:T(8,128)(2,1)} %param.19) | copy-start | bytes 3145732
  6.5 5.1 %copy-start.4 = (bf16[64,1408]{1,0:T(8,128)(2,1)S(1)}, bf16[64,1408]{1,0:T(8,128)(2,1)}, u32[]{:S(2)}) copy-start(bf16[64,1408]{1,0:T(8,128)(2,1)} %param.21) | copy-start | bytes 540676
  6.5 5.1 %copy-start.3 = (bf16[64,1408]{1,0:T(8,128)(2,1)S(1)}, bf16[64,1408]{1,0:T(8,128)(2,1)}, u32[]{:S(2)}) copy-start(bf16[64,1408]{1,0:T(8,128)(2,1)} %param.22) | copy-start | bytes 540676
  6.5 8.5 %copy-start.2 = (bf16[512,256]{1,0:T(8,128)(2,1)S(1)}, bf16[512,256]{1,0:T(8,128)(2,1)}, u32[]{:S(2)}) copy-start(bf16[512,256]{1,0:T(8,128)(2,1)} %param.13) | copy-start | bytes 786436
  6.5 60.3 %all-gather.4.cloned.1.call-start = ((), (), s32[]{:S(2)}) async-start(), calls=%async_computation.3 | async-start | bytes 8650752 | tf_op jit(solution)/shard_map/all_gather | solution.py:16
  9.5 6.5 %copy-start.6 = (f32[128]{0:T(128)S(1)}, f32[128]{0:T(128)}, u32[]{:S(2)}) copy-start(f32[128]{0:T(128)} %param.16) | copy-start | bytes 1540
  11.6 260.5 %all-gather.6.cloned.1.call-start = ((), (), s32[]{:S(2)}) async-start(), calls=%async_computation.4 | async-start | bytes 11894784 | tf_op jit(solution)/shard_map/all_gather | solution.py:16
  12.4 268.0 %all-gather.8.cloned.1.call-start = ((), (), s32[]{:S(2)}) async-start(), calls=%async_computation.5 | async-start | bytes 5947392 | tf_op jit(solution)/shard_map/all_gather | solution.py:158
  210.7 31.4 %copy-start.1 = (bf16[128,2048]{1,0:T(8,128)(2,1)S(1)}, bf16[128,2048]{1,0:T(8,128)(2,1)}, u32[]{:S(2)}) copy-start(bf16[128,2048]{1,0:T(8,128)(2,1)} %param.18) | copy-start | bytes 1572868
  241.7 0.7 copy-start.5
Sparse Core Ops, SparseCore 0:
  11.7 55.1 all-gather.3
  69.1 59.7 all-gather.5
  131.2 46.9 all-gather.7
where the time goes:
time: 333 us; the launch traced here: 331 us
  matrix products  145 us (44%)
  blocking collectives  89 us (27%)
  waiting for transfers between devices  47.4 us (14%)
  other arithmetic  25.2 us (8%)
  between operations  13.4 us (4%)
  local copies, waits for them, and re-layouts  10 us (3%)
    dot_general x32, matrix products, inner(): jnp.einsum('kqs,ksd->kqd', weights.astype(jnp.bfloat16), value_block, pre...  79 us
    all_to_all x2, blocking collectives, summed_on_arrival(): lax.all_to_all(cut_along(value, dim, devices), axis, 0, 0, tiled=True)  59.7 us
    all_gather x2, waiting for transfers between devices, sent_together(): filled = lax.all_gather(both, axis, axis=dim, tiled=True)  46.6 us
    dot_general x32, matrix products, inner(): jnp.einsum('kqd,ksd->kqs', q_stack, key_block, preferred_element_type=jnp...  43.1 us
    all_to_all x1, blocking collectives, from_everyone(): return lax.all_to_all(copies, axis, split_axis=0, concat_axis=0, tiled=True)  29.3 us
    dot_general x1, matrix products, on_device(): jnp.dot(hidden, down_whole, preferred_element_type=jnp.float32)  13.8 us
    reduce_sum x32, other arithmetic, inner(): running_sum = running_sum * factor + jnp.sum(weights, axis=-1)  11.9 us
    dot_general x1, matrix products, on_device(): jnp.dot(normed_all, gate_piece, preferred_element_type=jnp.float32)  8.35 us
  transfers between devices with their start and end apart: 3, of which 1 were waited for; matrix products, arithmetic and copies ran while one was open for 48% of the time, Pallas kernels for 0%

commit v1 on v0

v1 whole, which is shorter than its diff:
```python
import functools

import jax
import jax.numpy as jnp
from jax import lax
from jax.experimental import pallas as pl
from jax.experimental.pallas import tpu as pltpu
from jax.sharding import PartitionSpec as P

GRID = 64
norm_eps = 1e-06
theta_base = 10000.0
LOG2E = 1.4426950408889634
f32 = jnp.float32
bf16 = jnp.bfloat16


def angle_tables(first_row, rows, head_dim):
    quarter = head_dim // 4
    frequency = jnp.power(theta_base, -2.0 * jnp.arange(quarter, dtype=f32) / (head_dim // 2))
    places = jnp.concatenate([first_row + jnp.arange(rows, dtype=jnp.int32), jnp.arange(GRID, dtype=jnp.int32)])
    angles = places.astype(f32)[:, None] * frequency
    cosine, sine = lax.optimization_barrier((jnp.cos(angles), jnp.sin(angles)))
    is_row = (jnp.arange(rows + GRID) < rows)[:, None]
    zero = jnp.zeros_like(cosine)

    def placed(lead, trail):
        return jnp.concatenate(
            [
                jnp.where(is_row, lead, zero),
                jnp.where(is_row, trail, zero),
                jnp.where(is_row, zero, lead),
                jnp.where(is_row, zero, trail),
            ],
            axis=1,
        )

    return placed(cosine, cosine), placed(-sine, sine)


def prepare_kernel(q_ref, k_ref, v_ref, qg_ref, kg_ref, cos_ref, sin_ref, q_out, kv_out, *, rows, head_dim, heads):
    tok = rows * GRID

    def spread(ref):
        both = ref[0:rows, :][:, None, :] + ref[rows : rows + GRID, :][None, :, :]
        return both.reshape(tok, head_dim)

    cosine = spread(cos_ref)
    sine = spread(sin_ref)
    lane = lax.broadcasted_iota(jnp.int32, (tok, head_dim), 1)
    first = (lane % (head_dim // 2)) < head_dim // 4
    quarter = head_dim // 4

    def prepared(raw, gain):
        x = raw.astype(f32)
        x = x * lax.rsqrt(jnp.mean(x * x, axis=-1, keepdims=True) + norm_eps) * gain
        partner = jnp.where(first, pltpu.roll(x, head_dim - quarter, 1), pltpu.roll(x, quarter, 1))
        return (x * cosine + partner * sine).astype(bf16)

    for h in range(heads):
        q_out[h * tok : (h + 1) * tok, :] = prepared(q_ref[:, h * head_dim : (h + 1) * head_dim], qg_ref[...])
    kv_out[:, 0:head_dim] = prepared(k_ref[...], kg_ref[...])
    kv_out[:, head_dim:] = v_ref[...]


def prepare(query_rows, key_rows, value_rows, query_gain, key_gain):
    tok, width = query_rows.shape
    head_dim = query_gain.shape[0]
    rows = tok // GRID
    cosine, sine = angle_tables(lax.axis_index("sp") * rows, rows, head_dim)
    return pl.pallas_call(
        functools.partial(prepare_kernel, rows=rows, head_dim=head_dim, heads=width // head_dim),
        out_shape=(
            jax.ShapeDtypeStruct((tok * (width // head_dim), head_dim), bf16),
            jax.ShapeDtypeStruct((tok, 2 * head_dim), bf16),
        ),
        name="prepare",
    )(query_rows, key_rows, value_rows, query_gain[None, :], key_gain[None, :], cosine, sine)


def flash_kernel(q_ref, kv_ref, o_ref, m_ref, acc_ref, *, tile, scale):
    step = pl.program_id(0)
    head_dim = q_ref.shape[1]

    @pl.when(step == 0)
    def _():
        m_ref[...] = jnp.full_like(m_ref, -jnp.inf)
        acc_ref[...] = jnp.zeros_like(acc_ref)

    keys = kv_ref[:, 0:head_dim]
    values = kv_ref[:, head_dim:]
    values = jnp.concatenate([values, jnp.ones_like(values)], axis=1)
    for t in range(q_ref.shape[0] // tile):
        part = slice(t * tile, (t + 1) * tile)
        s = lax.dot_general(q_ref[part, :], keys, (((1,), (1,)), ((), ())), preferred_element_type=f32) * scale
        old = m_ref[part, :]
        new = jnp.maximum(old, jnp.max(s, axis=1, keepdims=True))
        w = jnp.exp2(s - new[:, 0:1]).astype(bf16)
        factor = jnp.exp2(old - new)
        m_ref[part, :] = new
        acc_ref[part, :] = acc_ref[part, :] * factor[:, 0:1] + jnp.dot(w, values, preferred_element_type=f32)

    @pl.when(step == pl.num_programs(0) - 1)
    def _():
        tok = o_ref.shape[0]
        for h in range(q_ref.shape[0] // tok):
            a = acc_ref[h * tok : (h + 1) * tok, :]
            o_ref[:, h * head_dim : (h + 1) * head_dim] = (a[:, 0:head_dim] / a[:, head_dim:]).astype(bf16)


def flash(q, kv, tok, tile=256, block=1024):
    rows, head_dim = q.shape
    heads = rows // tok
    keys = kv.shape[0]
    return pl.pallas_call(
        functools.partial(flash_kernel, tile=tile, scale=head_dim**-0.5 * LOG2E),
        grid=(keys // block,),
        in_specs=[
            pl.BlockSpec((rows, head_dim), lambda i: (0, 0)),
            pl.BlockSpec((block, 2 * head_dim), lambda i: (i, 0)),
        ],
        out_specs=pl.BlockSpec((tok, heads * head_dim), lambda i: (0, 0)),
        out_shape=jax.ShapeDtypeStruct((tok, heads * head_dim), bf16),
        scratch_shapes=[pltpu.VMEM((rows, 128), f32), pltpu.VMEM((rows, 2 * head_dim), f32)],
        compiler_params=pltpu.CompilerParams(dimension_semantics=("arbitrary",)),
        cost_estimate=pl.CostEstimate(
            flops=4 * rows * keys * head_dim, bytes_accessed=4 * keys * head_dim, transcendentals=rows * keys
        ),
        name="flash",
    )(q, kv)


def project_kernel(place, *refs, parts, tile):
    att = refs[0:parts]
    weight = refs[parts : 2 * parts]
    res = refs[2 * parts : 3 * parts]
    gain_ref, own_ref, norm_ref, up_ref = refs[3 * parts :]
    step = pl.program_id(0)
    sub = res[0].shape[0]
    cols = pl.ds(pl.multiple_of(step * tile, tile), tile)
    total = None
    for a, w in zip(att, weight):
        rolled = jnp.concatenate(
            [a[pl.ds(pl.multiple_of(((place[0] + r) % parts) * sub, sub), sub), :] for r in range(parts)], axis=0
        )
        part = jnp.dot(rolled, w[...], preferred_element_type=f32).astype(bf16).astype(f32)
        total = part if total is None else total + part
    for r in range(parts):
        updated = (res[r][...].astype(f32) + total[r * sub : (r + 1) * sub, :]).astype(bf16)
        up_ref[r * sub : (r + 1) * sub, cols] = updated

    @pl.when(step == pl.num_programs(0) - 1)
    def _():
        own_ref[...] = up_ref[0:sub, :]
        for r in range(2 * parts):
            some = slice(r * sub // 2, (r + 1) * sub // 2)
            x = up_ref[some, :].astype(f32)
            x = x * lax.rsqrt(jnp.mean(x * x, axis=-1, keepdims=True) + norm_eps)
            norm_ref[some, :] = (x * gain_ref[...]).astype(bf16)


def project(place, att, weight, res, gain, tile=512):
    parts = len(att)
    tok, part_width = att[0].shape
    sub, width = res[0].shape
    return pl.pallas_call(
        functools.partial(project_kernel, parts=parts, tile=tile),
        grid_spec=pltpu.PrefetchScalarGridSpec(
            num_scalar_prefetch=1,
            grid=(width // tile,),
            in_specs=[pl.BlockSpec((tok, part_width), lambda i, p: (0, 0))] * parts
            + [pl.BlockSpec((part_width, tile), lambda i, p: (0, i))] * parts
            + [pl.BlockSpec((sub, tile), lambda i, p: (0, i))] * parts
            + [pl.BlockSpec((1, width), lambda i, p: (0, 0))],
            out_specs=(
                pl.BlockSpec((sub, width), lambda i, p: (0, 0)),
                pl.BlockSpec((tok, width), lambda i, p: (0, 0)),
            ),
            scratch_shapes=[pltpu.VMEM((tok, width), bf16)],
        ),
        out_shape=(jax.ShapeDtypeStruct((sub, width), bf16), jax.ShapeDtypeStruct((tok, width), bf16)),
        compiler_params=pltpu.CompilerParams(dimension_semantics=("arbitrary",)),
        name="project",
    )(place, *att, *weight, *res, gain[None, :])


def hidden_kernel(x_ref, g_ref, u_ref, h_ref):
    both = jnp.concatenate([g_ref[...], u_ref[...]], axis=1)
    r = jnp.dot(x_ref[...], both, preferred_element_type=f32)
    tile = g_ref.shape[1]
    gate = r[:, 0:tile]
    h_ref[...] = (gate / (1.0 + jnp.exp(-gate)) * r[:, tile:]).astype(bf16)


def down_kernel(h_ref, d_ref, o_ref):
    o_ref[...] = lax.dot_general(
        h_ref[...], d_ref[...], (((1,), (1,)), ((), ())), preferred_element_type=f32
    ).astype(bf16)


def feed_forward(x, weights, units, tile=128, out_tile=256):
    tok, width = x.shape
    count = units // tile
    hidden = pl.pallas_call(
        hidden_kernel,
        grid=(count,),
        in_specs=[
            pl.BlockSpec((tok, width), lambda i: (0, 0)),
            pl.BlockSpec((width, tile), lambda i: (0, i)),
            pl.BlockSpec((width, tile), lambda i: (0, i + count)),
        ],
        out_specs=pl.BlockSpec((tok, tile), lambda i: (0, i)),
        out_shape=jax.ShapeDtypeStruct((tok, units), bf16),
        compiler_params=pltpu.CompilerParams(dimension_semantics=("arbitrary",)),
        name="hidden",
    )(x, weights, weights)
    return pl.pallas_call(
        down_kernel,
        grid=(width // out_tile,),
        in_specs=[
            pl.BlockSpec((tok, units), lambda i: (0, 0)),
            pl.BlockSpec((out_tile, units), lambda i: (i, 2)),
        ],
        out_specs=pl.BlockSpec((tok, out_tile), lambda i: (0, i)),
        out_shape=jax.ShapeDtypeStruct((tok, width), bf16),
        compiler_params=pltpu.CompilerParams(dimension_semantics=("arbitrary",)),
        name="down",
    )(hidden, weights)


def shifted(value, by):
    count = lax.axis_size("tp")
    return lax.ppermute(value, "tp", [(i, (i + by) % count) for i in range(count)])


def on_device(
    query_rows,
    key_rows,
    value_rows,
    query_gain,
    key_gain,
    residual,
    out_weight,
    mix_gain,
    gate_weight,
    up_weight,
    down_weight,
):
    tok = query_rows.shape[0]
    parts = lax.axis_size("tp")
    units = gate_weight.shape[1]
    place = lax.axis_index("tp")[None]
    q, kv = prepare(query_rows, key_rows, value_rows, query_gain, key_gain)
    kv_all = lax.all_gather(kv, "sp", axis=0, tiled=True)
    own_weights = jnp.concatenate([gate_weight, up_weight, down_weight.T], axis=1)
    own_weights, _ = lax.optimization_barrier((own_weights, kv))
    weights = lax.all_gather(own_weights, "sp", axis=0, tiled=True)
    out_parts = [out_weight] + [shifted(out_weight, -r) for r in range(1, parts)]
    res_parts = [residual] + [shifted(residual, -r) for r in range(1, parts)]
    attended = flash(q, kv_all, tok)
    att_parts = [attended] + [shifted(attended, -r) for r in range(1, parts)]
    own_rows, normed = project(place, att_parts, out_parts, res_parts, mix_gain)
    unit_part = feed_forward(normed, weights, units)
    sub = tok // parts
    unit_sum = unit_part[0:sub].astype(f32)
    for r in range(1, parts):
        unit_sum = unit_sum + shifted(unit_part[r * sub : (r + 1) * sub], r).astype(f32)
    return (own_rows.astype(f32) + 0.5 * unit_sum).astype(bf16)


def solution(mesh):
    placed = (
        P("sp", "tp"),
        P("sp", "tp"),
        P("sp", "tp"),
        P(),
        P(),
        P(("sp", "tp"), None),
        P("tp", None),
        P(),
        P("sp", "tp"),
        P("sp", "tp"),
        P("tp", "sp"),
    )
    return jax.shard_map(
        on_device, mesh=mesh, in_specs=placed, out_specs=P(("sp", "tp"), None), check_vma=False
    )
```

time: 333 us -> 204 us (0.61)
  matrix products: 145 us -> 0 us
  blocking collectives: 89 us -> 0 us
  Pallas kernels: 0 us -> 66.7 us
  waiting for transfers between devices: 47.4 us -> 94.9 us
  other arithmetic: 25.2 us -> 5.41 us
  starting transfers between devices: 0.12 us -> 19.7 us
  local copies, waits for them, and re-layouts: 10 us -> 1.6 us
    dot_general x67 -> x0, matrix products: 145 us -> none  [the longest x32 79 us: inner(): jnp.einsum('kqs,ksd->kqd', weights.astype(jnp.bfloat16), value_block, pre...]
    all_to_all x3 -> x0, blocking collectives: 89 us -> none  [the longest x2 59.7 us: summed_on_arrival(): lax.all_to_all(cut_along(value, dim, devices), axis, 0, 0, tiled=True)]
    pallas_call x0 -> x5, Pallas kernels: none -> 66.7 us  [the longest x1 33.1 us: flash(): pl.pallas_call(functools.partial(flash_kernel, tile=tile, scale=head_dim...]
    ppermute x0 -> x12, waiting for transfers between devices: none -> 42.2 us  [shifted(): lax.ppermute(value, 'tp', [(i, (i + by) % count) for i in range(count)])]
    ppermute x0 -> x12, starting transfers between devices: none -> 19.7 us  [shifted(): lax.ppermute(value, 'tp', [(i, (i + by) % count) for i in range(count)])]
    reduce_sum x37 -> x0, other arithmetic: 13.6 us -> none  [the longest x32 11.9 us: inner(): running_sum = running_sum * factor + jnp.sum(weights, axis=-1)]
    all_gather x3 -> x2, waiting for transfers between devices: 46.6 us -> 52.6 us  [the longest x1 36.6 us: on_device(): kv_all = lax.all_gather(kv, 'sp', axis=0, tiled=True)]
    split x1 -> x0, local copies, waits for them, and re-layouts: 5.74 us -> none  [sent_together(): jnp.split(filled, [sum(widths[:k]) for k in range(1, len(widths))], axis=...]
  transfers between devices with their start and end apart: 3 -> 14, of which waited for: 1 -> 7; matrix products, arithmetic and copies ran while one was open for 48% -> 1% of each run, Pallas kernels for 0% -> 21%
where the time goes in v1:
time: 204 us; the launch traced here: 202 us
  waiting for transfers between devices  94.9 us (47%)
  Pallas kernels  66.7 us (33%)
  starting transfers between devices  19.7 us (10%)
  between operations  13.5 us (7%)
  other arithmetic  5.41 us (3%)
    ppermute x12, waiting for transfers between devices, shifted(): lax.ppermute(value, 'tp', [(i, (i + by) % count) for i in range(count)])  42.2 us
    all_gather x1, waiting for transfers between devices, on_device(): kv_all = lax.all_gather(kv, 'sp', axis=0, tiled=True)  36.6 us
    pallas_call x1, Pallas kernels, flash(): pl.pallas_call(functools.partial(flash_kernel, tile=tile, scale=head_dim...  33.1 us
    ppermute x12, starting transfers between devices, shifted(): lax.ppermute(value, 'tp', [(i, (i + by) % count) for i in range(count)])  19.7 us
    all_gather x1, waiting for transfers between devices, on_device(): weights = lax.all_gather(own_weights, 'sp', axis=0, tiled=True)  16 us
    pallas_call x1, Pallas kernels, feed_forward(): pl.pallas_call(hidden_kernel, grid=(count,), in_specs=[pl.BlockSpec((tok,...  13.6 us
    pallas_call x1, Pallas kernels, feed_forward(): pl.pallas_call(down_kernel, grid=(width // out_tile,), in_specs=[pl.Block...  9.2 us
    pallas_call x1, Pallas kernels, project(): pl.pallas_call(functools.partial(project_kernel, parts=parts, tile=tile),...  8.25 us
  transfers between devices with their start and end apart: 14, of which 7 were waited for; matrix products, arithmetic and copies ran while one was open for 1% of the time, Pallas kernels for 21%

profile of v1, /device:TPU:8, one launch (start us, length us, event | category | flops | bytes accessed | tf_op | source)
XLA Modules:
  0.0 201.8 jit_solution(2816607341778733021)
XLA Ops:
  6.5 0.0 copy-start
  6.5 0.0 all-gather.3.cloned.1.call-start
  6.6 0.1 add_convert_fusion.1
  6.7 0.2 multiply_sine_fusion
  6.9 0.1 negate_select_fusion.1
  7.0 0.8 pad_maximum_fusion.1
  7.7 2.6 %prepare.1 = (bf16[1024,128]{1,0:T(8,128)(2,1)}, bf16[512,256]{1,0:T(8,128)(2,1)}) custom-call(bf16[512,256]{1,0:T(8,128)(2,1)} %q_ref.1, bf16[512,128]{1,0:T(8,128)(2,1)} %k_ref.1, bf16[512,128]{1,0:T(8,128)(2,1)} %v_ref.1, f32[1,128]{1,0:T(1,128)} %bitcast.7, f32[1,128]{1,0:T(1,128)} %bitcast.8, f32[72,128]{1,0:T(8,128)} %get-tuple-element.32.cos_ref, ...), custom_call_target="tpu_custom_call" | custom-call | tf_op jit(solution)/shard_map/prepare/pallas_call | solution.py:71
  10.3 0.0 all-gather.3.cloned.1.call-update
  10.3 0.0 all-gather.5.cloned.1.call-start
  10.4 2.0 pad_maximum_fusion
  12.4 0.0 all-gather.5.cloned.1.call-update
  12.4 2.8 %collective-permute-start.6 = (bf16[128,2048]{1,0:T(8,128)(2,1)}, bf16[128,2048]{1,0:T(8,128)(2,1)}, u32[]{:S(2)}, u32[]{:S(2)}) collective-permute-start(bf16[128,2048]{1,0:T(8,128)(2,1)} %refs_8_.1), channel_id=1, source_target_pairs={{0,3},{1,0},{2,1},{3,2},{4,7},{5,4},{6,5},{7,6},{8,11},{9,8},{10,9... | collective-permute-start | bytes 1572872 | tf_op jit(solution)/shard_map/ppermute | solution.py:233
  15.2 0.0 copy-done
  15.2 0.8 collective-permute-start.3
  16.0 0.5 collective-permute-start.4
  16.6 0.9 collective-permute-start.5
  17.4 3.9 %collective-permute-start.7 = (bf16[128,2048]{1,0:T(8,128)(2,1)}, bf16[128,2048]{1,0:T(8,128)(2,1)}, u32[]{:S(2)}, u32[]{:S(2)}) collective-permute-start(bf16[128,2048]{1,0:T(8,128)(2,1)} %refs_8_.1), channel_id=1, source_target_pairs={{0,2},{1,3},{2,0},{3,1},{4,6},{5,7},{6,4},{7,5},{8,10},{9,11},{10,... | collective-permute-start | bytes 1572872 | tf_op jit(solution)/shard_map/ppermute | solution.py:233
  21.4 6.5 %collective-permute-done.6.refs_9_ = bf16[128,2048]{1,0:T(8,128)(2,1)} collective-permute-done((bf16[128,2048]{1,0:T(8,128)(2,1)}, bf16[128,2048]{1,0:T(8,128)(2,1)}, u32[]{:S(2)}, u32[]{:S(2)}) %collective-permute-start.6) | collective-permute-done | bytes 524320 | tf_op jit(solution)/shard_map/ppermute | solution.py:233
  27.8 1.2 collective-permute-start.8
  29.1 36.6 %all-gather.3.cloned.1.call-done.kv_ref = bf16[16384,256]{1,0:T(8,128)(2,1)} async-done(((bf16[512,256]{1,0:T(8,128)(2,1)}), bf16[16384,256]{1,0:T(8,128)(2,1)}) %all-gather.3.cloned.1.call-update) | async-done | bytes 8388624 | tf_op jit(solution)/shard_map/all_gather | solution.py:254
  65.6 33.1 %flash.1.refs_0_ = bf16[512,256]{1,0:T(8,128)(2,1)} custom-call(bf16[1024,128]{1,0:T(8,128)(2,1)} %get-tuple-element.14.q_ref, bf16[16384,256]{1,0:T(8,128)(2,1)} %all-gather.3.cloned.1.call-done.kv_ref), custom_call_target="tpu_custom_call" | custom-call | flops 8589934592 | bytes 8388608 | tf_op jit(solution)/shard_map/flash/pallas_call | solution.py:115
  98.7 0.0 collective-permute-done.7.refs_10_
  98.7 2.7 %collective-permute-start = (bf16[512,256]{1,0:T(8,128)(2,1)}, bf16[512,256]{1,0:T(8,128)(2,1)S(1)}, u32[]{:S(2)}, u32[]{:S(2)}) collective-permute-start(bf16[512,256]{1,0:T(8,128)(2,1)} %flash.1.refs_0_), channel_id=1, source_target_pairs={{0,3},{1,0},{2,1},{3,2},{4,7},{5,4},{6,5},{7,6},{8,11},{9,8},{10,9... | collective-permute-start | bytes 786440 | tf_op jit(solution)/shard_map/ppermute | solution.py:233
  101.4 0.0 collective-permute-done.8.refs_11_
  101.4 0.8 collective-permute-start.1
  102.3 0.0 collective-permute-done.3.refs_5_
  102.3 0.0 copy-start.1
  102.3 0.9 collective-permute-start.2
  103.2 0.0 collective-permute-done.4.refs_6_
  103.2 0.0 copy-start.2
  103.2 0.0 collective-permute-done.5.refs_7_
  103.2 10.2 %collective-permute-done.refs_1_ = bf16[512,256]{1,0:T(8,128)(2,1)S(1)} collective-permute-done((bf16[512,256]{1,0:T(8,128)(2,1)}, bf16[512,256]{1,0:T(8,128)(2,1)S(1)}, u32[]{:S(2)}, u32[]{:S(2)}) %collective-permute-start) | collective-permute-done | bytes 262176 | tf_op jit(solution)/shard_map/ppermute | solution.py:233
  113.4 0.0 copy-start.4
  113.4 0.0 collective-permute-done.1.refs_2_
  113.4 3.7 %collective-permute-done.2.refs_3_ = bf16[512,256]{1,0:T(8,128)(2,1)} collective-permute-done((bf16[512,256]{1,0:T(8,128)(2,1)}, bf16[512,256]{1,0:T(8,128)(2,1)}, u32[]{:S(2)}, u32[]{:S(2)}) %collective-permute-start.2) | collective-permute-done | bytes 262176 | tf_op jit(solution)/shard_map/ppermute | solution.py:233
  117.1 0.0 copy-done.1
  117.1 0.0 copy-done.2
  117.1 0.0 copy-done.4
  117.1 8.2 %project.1 = (bf16[128,2048]{1,0:T(8,128)(2,1)}, bf16[512,2048]{1,0:T(8,128)(2,1)}) custom-call(s32[1]{0:T(128)} %bitcast.place, bf16[512,256]{1,0:T(8,128)(2,1)} %flash.1.refs_0_, bf16[512,256]{1,0:T(8,128)(2,1)} %copy-done.4, bf16[512,256]{1,0:T(8,128)(2,1)} %collective-permute-done.1.refs_2_, bf16[512,256]{1,0:T(8,128)(2,1)} %collective-permute-done.2.refs_3_, ...), custom_call_target="tpu_custom_call" | custom-call | tf_op jit(solution)/shard_map/project/pallas_call | solution.py:166
  125.3 16.0 %all-gather.5.cloned.1.call-done.g_ref.u_ref.d_ref = bf16[2048,4224]{1,0:T(8,128)(2,1)} async-done(((bf16[64,4224]{1,0:T(8,128)(2,1)}), bf16[2048,4224]{1,0:T(8,128)(2,1)}) %all-gather.5.cloned.1.call-update) | async-done | bytes 17301520 | tf_op jit(solution)/shard_map/all_gather | solution.py:257
  141.4 13.6 %hidden.1.h_ref = bf16[512,1408]{1,0:T(8,128)(2,1)} custom-call(bf16[512,2048]{1,0:T(8,128)(2,1)} %get-tuple-element.17.x_ref, bf16[2048,4224]{1,0:T(8,128)(2,1)} %all-gather.5.cloned.1.call-done.g_ref.u_ref.d_ref, bf16[2048,4224]{1,0:T(8,128)(2,1)} %all-gather.5.cloned.1.call-done.g_ref.u_ref.d_ref), custom_call_target="tpu_custom_call" | custom-call | tf_op jit(solution)/shard_map/hidden/pallas_call | solution.py:204
  154.9 9.2 %down.1 = bf16[512,2048]{1,0:T(8,128)(2,1)} custom-call(bf16[512,1408]{1,0:T(8,128)(2,1)} %hidden.1.h_ref, bf16[2048,4224]{1,0:T(8,128)(2,1)} %all-gather.5.cloned.1.call-done.g_ref.u_ref.d_ref), custom_call_target="tpu_custom_call" | custom-call | tf_op jit(solution)/shard_map/down/pallas_call | solution.py:217
  164.1 0.0 copy-start.3
  164.1 1.6 fusion
  165.7 3.0 %collective-permute-start.10 = (bf16[128,2048]{1,0:T(8,128)(2,1)S(1)}, bf16[128,2048]{1,0:T(8,128)(2,1)S(1)}, u32[]{:S(2)}, u32[]{:S(2)}) collective-permute-start(bf16[128,2048]{1,0:T(8,128)(2,1)S(1)} %get-tuple-element.21), channel_id=1, source_target_pairs={{0,2},{1,3},{2,0},{3,1},{4,6},{5,7},{6,4},{7,5},{8,10},{9,11},{10,... | collective-permute-start | bytes 1572872 | tf_op jit(solution)/shard_map/ppermute | solution.py:233
  168.8 1.2 collective-permute-start.11
  169.9 0.9 collective-permute-start.9
  170.8 11.3 %collective-permute-done.10 = bf16[128,2048]{1,0:T(8,128)(2,1)S(1)} collective-permute-done((bf16[128,2048]{1,0:T(8,128)(2,1)S(1)}, bf16[128,2048]{1,0:T(8,128)(2,1)S(1)}, u32[]{:S(2)}, u32[]{:S(2)}) %collective-permute-start.10) | collective-permute-done | bytes 524320 | tf_op jit(solution)/shard_map/ppermute | solution.py:233
  182.1 10.5 %collective-permute-done.11 = bf16[128,2048]{1,0:T(8,128)(2,1)S(1)} collective-permute-done((bf16[128,2048]{1,0:T(8,128)(2,1)S(1)}, bf16[128,2048]{1,0:T(8,128)(2,1)S(1)}, u32[]{:S(2)}, u32[]{:S(2)}) %collective-permute-start.11) | collective-permute-done | bytes 524320 | tf_op jit(solution)/shard_map/ppermute | solution.py:233
  192.7 0.0 collective-permute-done.9
  192.7 0.0 copy-done.3
  192.7 2.3 %add_convert_fusion = bf16[128,2048]{1,0:T(8,128)(2,1)} fusion(bf16[128,2048]{1,0:T(8,128)(2,1)S(1)} %collective-permute-done.11, bf16[128,2048]{1,0:T(8,128)(2,1)S(1)} %collective-permute-done.10, bf16[128,2048]{1,0:T(8,128)(2,1)S(1)} %collective-permute-done.9, bf16[128,2048]{1,0:T(8,128)(2,1)S(1)} %copy-done.3, bf16[512,2048]{1,0:T(8,128)(2,1)} %down.1), kind=kLoop, calls=%fused_computation | loop fusion | flops 2883584 | bytes 3145728 | tf_op jit(solution)/shard_map/convert_element_type | solution.py:268
  (4 shorter events, 0.0 us)
Async XLA Ops:
  6.5 8.7 %copy-start = (bf16[256,2048]{1,0:T(8,128)(2,1)S(1)}, bf16[256,2048]{1,0:T(8,128)(2,1)}, u32[]{:S(2)}) copy-start(bf16[256,2048]{1,0:T(8,128)(2,1)} %refs_4_.1) | copy-start | bytes 3145732
  6.5 59.1 %all-gather.3.cloned.1.call-start = ((), (), s32[]{:S(2)}) async-start(), calls=%async_computation | async-start | bytes 8650752 | tf_op jit(solution)/shard_map/all_gather | solution.py:254
  10.3 131.0 %all-gather.5.cloned.1.call-start = ((), (), s32[]{:S(2)}) async-start(), calls=%async_computation.1 | async-start | bytes 17842176 | tf_op jit(solution)/shard_map/all_gather | solution.py:257
  12.4 15.5 %collective-permute-start.6 = (bf16[128,2048]{1,0:T(8,128)(2,1)}, bf16[128,2048]{1,0:T(8,128)(2,1)}, u32[]{:S(2)}, u32[]{:S(2)}) collective-permute-start(bf16[128,2048]{1,0:T(8,128)(2,1)} %refs_8_.1), channel_id=1, source_target_pairs={{0,3},{1,0},{2,1},{3,2},{4,7},{5,4},{6,5},{7,6},{8,11},{9,8},{10,9... | collective-permute-start | bytes 1572872 | tf_op jit(solution)/shard_map/ppermute | solution.py:233
  15.2 87.1 %collective-permute-start.3 = (bf16[256,2048]{1,0:T(8,128)(2,1)S(1)}, bf16[256,2048]{1,0:T(8,128)(2,1)S(1)}, u32[]{:S(2)}, u32[]{:S(2)}) collective-permute-start(bf16[256,2048]{1,0:T(8,128)(2,1)S(1)} %copy-done), channel_id=1, source_target_pairs={{0,3},{1,0},{2,1},{3,2},{4,7},{5,4},{6,5},{7,6},{8,11},{9,8},{10,9... | collective-permute-start | bytes 3145736 | tf_op jit(solution)/shard_map/ppermute | solution.py:233
  16.0 87.1 %collective-permute-start.4 = (bf16[256,2048]{1,0:T(8,128)(2,1)S(1)}, bf16[256,2048]{1,0:T(8,128)(2,1)S(1)}, u32[]{:S(2)}, u32[]{:S(2)}) collective-permute-start(bf16[256,2048]{1,0:T(8,128)(2,1)S(1)} %copy-done), channel_id=1, source_target_pairs={{0,2},{1,3},{2,0},{3,1},{4,6},{5,7},{6,4},{7,5},{8,10},{9,11},{10,... | collective-permute-start | bytes 3145736 | tf_op jit(solution)/shard_map/ppermute | solution.py:233
  16.6 86.6 %collective-permute-start.5 = (bf16[256,2048]{1,0:T(8,128)(2,1)S(1)}, bf16[256,2048]{1,0:T(8,128)(2,1)}, u32[]{:S(2)}, u32[]{:S(2)}) collective-permute-start(bf16[256,2048]{1,0:T(8,128)(2,1)S(1)} %copy-done), channel_id=1, source_target_pairs={{0,1},{1,2},{2,3},{3,0},{4,5},{5,6},{6,7},{7,4},{8,9},{9,10},{10,1... | collective-permute-start | bytes 3145736 | tf_op jit(solution)/shard_map/ppermute | solution.py:233
  17.4 81.3 %collective-permute-start.7 = (bf16[128,2048]{1,0:T(8,128)(2,1)}, bf16[128,2048]{1,0:T(8,128)(2,1)}, u32[]{:S(2)}, u32[]{:S(2)}) collective-permute-start(bf16[128,2048]{1,0:T(8,128)(2,1)} %refs_8_.1), channel_id=1, source_target_pairs={{0,2},{1,3},{2,0},{3,1},{4,6},{5,7},{6,4},{7,5},{8,10},{9,11},{10,... | collective-permute-start | bytes 1572872 | tf_op jit(solution)/shard_map/ppermute | solution.py:233
  27.8 73.6 %collective-permute-start.8 = (bf16[128,2048]{1,0:T(8,128)(2,1)}, bf16[128,2048]{1,0:T(8,128)(2,1)}, u32[]{:S(2)}, u32[]{:S(2)}) collective-permute-start(bf16[128,2048]{1,0:T(8,128)(2,1)} %refs_8_.1), channel_id=1, source_target_pairs={{0,1},{1,2},{2,3},{3,0},{4,5},{5,6},{6,7},{7,4},{8,9},{9,10},{10,1... | collective-permute-start | bytes 1572872 | tf_op jit(solution)/shard_map/ppermute | solution.py:233
  98.7 14.6 %collective-permute-start = (bf16[512,256]{1,0:T(8,128)(2,1)}, bf16[512,256]{1,0:T(8,128)(2,1)S(1)}, u32[]{:S(2)}, u32[]{:S(2)}) collective-permute-start(bf16[512,256]{1,0:T(8,128)(2,1)} %flash.1.refs_0_), channel_id=1, source_target_pairs={{0,3},{1,0},{2,1},{3,2},{4,7},{5,4},{6,5},{7,6},{8,11},{9,8},{10,9... | collective-permute-start | bytes 786440 | tf_op jit(solution)/shard_map/ppermute | solution.py:233
  101.4 11.9 %collective-permute-start.1 = (bf16[512,256]{1,0:T(8,128)(2,1)}, bf16[512,256]{1,0:T(8,128)(2,1)}, u32[]{:S(2)}, u32[]{:S(2)}) collective-permute-start(bf16[512,256]{1,0:T(8,128)(2,1)} %flash.1.refs_0_), channel_id=1, source_target_pairs={{0,2},{1,3},{2,0},{3,1},{4,6},{5,7},{6,4},{7,5},{8,10},{9,11},{10,... | collective-permute-start | bytes 786440 | tf_op jit(solution)/shard_map/ppermute | solution.py:233
  102.3 14.8 %copy-start.1 = (bf16[256,2048]{1,0:T(8,128)(2,1)}, bf16[256,2048]{1,0:T(8,128)(2,1)S(1)}, u32[]{:S(2)}) copy-start(bf16[256,2048]{1,0:T(8,128)(2,1)S(1)} %collective-permute-done.3.refs_5_) | copy-start | bytes 3145732
  102.3 14.8 %collective-permute-start.2 = (bf16[512,256]{1,0:T(8,128)(2,1)}, bf16[512,256]{1,0:T(8,128)(2,1)}, u32[]{:S(2)}, u32[]{:S(2)}) collective-permute-start(bf16[512,256]{1,0:T(8,128)(2,1)} %flash.1.refs_0_), channel_id=1, source_target_pairs={{0,1},{1,2},{2,3},{3,0},{4,5},{5,6},{6,7},{7,4},{8,9},{9,10},{10,1... | collective-permute-start | bytes 786440 | tf_op jit(solution)/shard_map/ppermute | solution.py:233
  103.2 13.9 %copy-start.2 = (bf16[256,2048]{1,0:T(8,128)(2,1)}, bf16[256,2048]{1,0:T(8,128)(2,1)S(1)}, u32[]{:S(2)}) copy-start(bf16[256,2048]{1,0:T(8,128)(2,1)S(1)} %collective-permute-done.4.refs_6_) | copy-start | bytes 3145732
  113.4 3.7 %copy-start.4 = (bf16[512,256]{1,0:T(8,128)(2,1)}, bf16[512,256]{1,0:T(8,128)(2,1)S(1)}, u32[]{:S(2)}) copy-start(bf16[512,256]{1,0:T(8,128)(2,1)S(1)} %collective-permute-done.refs_1_) | copy-start | bytes 786436
  164.1 28.5 %copy-start.3 = (bf16[128,2048]{1,0:T(8,128)(2,1)S(1)}, bf16[128,2048]{1,0:T(8,128)(2,1)}, u32[]{:S(2)}) copy-start(bf16[128,2048]{1,0:T(8,128)(2,1)} %get-tuple-element.16) | copy-start | bytes 1572868
  165.7 16.4 %collective-permute-start.10 = (bf16[128,2048]{1,0:T(8,128)(2,1)S(1)}, bf16[128,2048]{1,0:T(8,128)(2,1)S(1)}, u32[]{:S(2)}, u32[]{:S(2)}) collective-permute-start(bf16[128,2048]{1,0:T(8,128)(2,1)S(1)} %get-tuple-element.21), channel_id=1, source_target_pairs={{0,2},{1,3},{2,0},{3,1},{4,6},{5,7},{6,4},{7,5},{8,10},{9,11},{10,... | collective-permute-start | bytes 1572872 | tf_op jit(solution)/shard_map/ppermute | solution.py:233
  168.8 23.9 %collective-permute-start.11 = (bf16[128,2048]{1,0:T(8,128)(2,1)S(1)}, bf16[128,2048]{1,0:T(8,128)(2,1)S(1)}, u32[]{:S(2)}, u32[]{:S(2)}) collective-permute-start(bf16[128,2048]{1,0:T(8,128)(2,1)S(1)} %get-tuple-element.20), channel_id=1, source_target_pairs={{0,3},{1,0},{2,1},{3,2},{4,7},{5,4},{6,5},{7,6},{8,11},{9,8},{10,9... | collective-permute-start | bytes 1572872 | tf_op jit(solution)/shard_map/ppermute | solution.py:233
  169.9 22.7 %collective-permute-start.9 = (bf16[128,2048]{1,0:T(8,128)(2,1)S(1)}, bf16[128,2048]{1,0:T(8,128)(2,1)S(1)}, u32[]{:S(2)}, u32[]{:S(2)}) collective-permute-start(bf16[128,2048]{1,0:T(8,128)(2,1)S(1)} %get-tuple-element.19), channel_id=1, source_target_pairs={{0,1},{1,2},{2,3},{3,0},{4,5},{5,6},{6,7},{7,4},{8,9},{9,10},{10,1... | collective-permute-start | bytes 1572872 | tf_op jit(solution)/shard_map/ppermute | solution.py:233
Sparse Core Ops, SparseCore 0:
  10.5 55.1 all-gather.2
  67.9 73.4 all-gather.4

commit v2 on v1

v2 whole, which is shorter than its diff:
```python
import functools

import jax
import jax.numpy as jnp
from jax import lax
from jax.experimental import pallas as pl
from jax.experimental.pallas import tpu as pltpu
from jax.sharding import PartitionSpec as P

GRID = 64
norm_eps = 1e-06
theta_base = 10000.0
LOG2E = 1.4426950408889634
f32 = jnp.float32
bf16 = jnp.bfloat16


def angle_tables(first_row, rows, head_dim):
    quarter = head_dim // 4
    frequency = jnp.power(theta_base, -2.0 * jnp.arange(quarter, dtype=f32) / (head_dim // 2))
    places = jnp.concatenate([first_row + jnp.arange(rows, dtype=jnp.int32), jnp.arange(GRID, dtype=jnp.int32)])
    angles = places.astype(f32)[:, None] * frequency
    cosine, sine = lax.optimization_barrier((jnp.cos(angles), jnp.sin(angles)))
    is_row = (jnp.arange(rows + GRID) < rows)[:, None]
    zero = jnp.zeros_like(cosine)

    def placed(lead, trail):
        return jnp.concatenate(
            [
                jnp.where(is_row, lead, zero),
                jnp.where(is_row, trail, zero),
                jnp.where(is_row, zero, lead),
                jnp.where(is_row, zero, trail),
            ],
            axis=1,
        )

    return placed(cosine, cosine), placed(-sine, sine)


def prepare_kernel(
    core, q_hbm, k_hbm, v_hbm, g_hbm, u_hbm, d_hbm, w_hbm, r_hbm, qg_ref, kg_ref, cos_ref, sin_ref,
    q_out, a_out, b_out, woven, sent, kept,
    q_ref, k_ref, v_ref, g_ref, u_ref, d_ref, sems, *, rows, head_dim, heads, tile,
):
    tok = rows * GRID
    half = kept.shape[0]
    first_half = pl.ds(pl.multiple_of(core[0] * half, half), half)
    other_half = pl.ds(pl.multiple_of((1 - core[0]) * half, half), half)
    moves = [
        (k_hbm, k_ref),
        (v_hbm, v_ref),
        (q_hbm, q_ref),
        (g_hbm, g_ref),
        (u_hbm, u_ref),
        (d_hbm, d_ref),
        (w_hbm.at[first_half, :], sent.at[pl.ds(0, half), :]),
        (r_hbm, sent.at[pl.ds(half, r_hbm.shape[0]), :]),
        (w_hbm.at[other_half, :], kept),
    ]
    copies = [pltpu.make_async_copy(x, y, sems.at[n]) for n, (x, y) in enumerate(moves)]
    for c in copies:
        c.start()

    def spread(ref):
        both = ref[0:rows, :][:, None, :] + ref[rows : rows + GRID, :][None, :, :]
        return both.reshape(tok, head_dim)

    cosine = spread(cos_ref)
    sine = spread(sin_ref)
    lane = lax.broadcasted_iota(jnp.int32, (tok, head_dim), 1)
    first = (lane % (head_dim // 2)) < head_dim // 4
    quarter = head_dim // 4

    def prepared(raw, gain):
        x = raw.astype(f32)
        x = x * lax.rsqrt(jnp.mean(x * x, axis=-1, keepdims=True) + norm_eps) * gain
        partner = jnp.where(first, pltpu.roll(x, head_dim - quarter, 1), pltpu.roll(x, quarter, 1))
        return (x * cosine + partner * sine).astype(bf16)

    copies[0].wait()
    copies[1].wait()
    keys = prepared(k_ref[...], kg_ref[...])
    for n, out in enumerate((a_out, b_out)):
        part = slice(n * tok // 2, (n + 1) * tok // 2)
        out[:, 0:head_dim] = keys[part, :]
        out[:, head_dim:] = v_ref[part, :]
    copies[2].wait()
    for h in range(heads):
        q_out[h * tok : (h + 1) * tok, :] = prepared(q_ref[:, h * head_dim : (h + 1) * head_dim], qg_ref[...])
    for n in (3, 4, 5):
        copies[n].wait()
    units = g_ref.shape[1]
    for n in range(units // tile):
        part = slice(n * tile, (n + 1) * tile)
        woven[:, 2 * n * tile : (2 * n + 1) * tile] = g_ref[:, part]
        woven[:, (2 * n + 1) * tile : (2 * n + 2) * tile] = u_ref[:, part]
    woven[:, 2 * units :] = d_ref[...]
    for n in (6, 7, 8):
        copies[n].wait()


def prepare(query_rows, key_rows, value_rows, query_gain, key_gain, gate, up, down, out_weight, residual, tile=128):
    tok, width = query_rows.shape
    head_dim = query_gain.shape[0]
    rows = tok // GRID
    cosine, sine = angle_tables(lax.axis_index("sp") * rows, rows, head_dim)
    hbm = pl.BlockSpec(memory_space=pltpu.HBM)
    vmem = pl.BlockSpec(memory_space=pltpu.VMEM)
    big = (query_rows, key_rows, value_rows, gate, up, down.T)
    half = out_weight.shape[0] // 2
    return pl.pallas_call(
        functools.partial(prepare_kernel, rows=rows, head_dim=head_dim, heads=width // head_dim, tile=tile),
        in_specs=[pl.BlockSpec(memory_space=pltpu.SMEM)] + [hbm] * 8 + [vmem] * 4,
        out_specs=[vmem] * 4 + [hbm] * 2,
        out_shape=(
            jax.ShapeDtypeStruct((tok * (width // head_dim), head_dim), bf16),
            jax.ShapeDtypeStruct((tok // 2, 2 * head_dim), bf16),
            jax.ShapeDtypeStruct((tok // 2, 2 * head_dim), bf16),
            jax.ShapeDtypeStruct((gate.shape[0], 3 * gate.shape[1]), bf16),
            jax.ShapeDtypeStruct((half + residual.shape[0], residual.shape[1]), bf16),
            jax.ShapeDtypeStruct((half, residual.shape[1]), bf16),
        ),
        scratch_shapes=[pltpu.VMEM(x.shape, bf16) for x in big] + [pltpu.SemaphoreType.DMA((9,))],
        compiler_params=pltpu.CompilerParams(vmem_limit_bytes=60 * 1024 * 1024),
        name="prepare",
    )(
        (lax.axis_index("sp") % 2)[None], *big, out_weight, residual, query_gain[None, :], key_gain[None, :], cosine, sine
    )


def flash_kernel(*refs, pieces, scale, first, last):
    q_ref = refs[0]
    kv_refs = refs[1 : 1 + pieces]
    refs = refs[1 + pieces :]
    if not first:
        m_in, acc_in = refs[0:2]
        refs = refs[2:]
    if last:
        o_ref = refs[0]
        refs = refs[1:]
    else:
        m_out, acc_out = refs[0:2]
        refs = refs[2:]
    head_dim = q_ref.shape[1]
    q = q_ref[...]
    if first:
        m = jnp.full((q.shape[0], 128), -jnp.inf, f32)
        acc = jnp.zeros((q.shape[0], 2 * head_dim), f32)
    else:
        m = m_in[...]
        acc = acc_in[...]
    for n in range(pieces):
        keys = kv_refs[n][:, 0:head_dim]
        values = kv_refs[n][:, head_dim:]
        values = jnp.concatenate([values, jnp.ones_like(values)], axis=1)
        s = lax.dot_general(q, keys, (((1,), (1,)), ((), ())), preferred_element_type=f32) * scale
        new = jnp.maximum(m, jnp.max(s, axis=1, keepdims=True))
        w = jnp.exp2(s - new[:, 0:1]).astype(bf16)
        factor = jnp.exp2(m - new)
        acc = acc * factor[:, 0:1] + jnp.dot(w, values, preferred_element_type=f32)
        m = new
    if last:
        o_ref[...] = (acc[:, 0:head_dim] / acc[:, head_dim:]).astype(bf16)
    else:
        m_out[...] = m
        acc_out[...] = acc


def flash(q, kv, state, tok, last, tile=256):
    rows, head_dim = q.shape
    heads = rows // tok
    pieces = len(kv)
    piece = kv[0].shape
    tiles = tok // tile
    held = [pl.BlockSpec((tile, 128), lambda i: (i, 0)), pl.BlockSpec((tile, 2 * head_dim), lambda i: (i, 0))]
    held_shape = (jax.ShapeDtypeStruct((rows, 128), f32), jax.ShapeDtypeStruct((rows, 2 * head_dim), f32))
    first = state is None
    return pl.pallas_call(
        functools.partial(flash_kernel, pieces=pieces, scale=head_dim**-0.5 * LOG2E, first=first, last=last),
        grid=(rows // tile,),
        in_specs=[pl.BlockSpec((tile, head_dim), lambda i: (i, 0))]
        + [pl.BlockSpec(piece, lambda i: (0, 0))] * pieces
        + ([] if first else held),
        out_specs=pl.BlockSpec((tile, head_dim), lambda i: (i % tiles, i // tiles)) if last else tuple(held),
        out_shape=jax.ShapeDtypeStruct((tok, heads * head_dim), bf16) if last else held_shape,
        compiler_params=pltpu.CompilerParams(dimension_semantics=("arbitrary",), vmem_limit_bytes=12 << 20),
        cost_estimate=pl.CostEstimate(
            flops=4 * rows * piece[0] * pieces * head_dim,
            bytes_accessed=4 * piece[0] * pieces * head_dim,
            transcendentals=rows * piece[0] * pieces,
        ),
        name="flash_last" if last else "flash_first" if first else "flash_more",
    )(q, *kv, *([] if first else state))


def project_kernel(place, *refs, parts, tile):
    att = refs[0:parts]
    sent = refs[parts : 2 * parts]
    swapped = refs[2 * parts : 3 * parts]
    gain_ref, own_ref, norm_ref, up_ref = refs[3 * parts :]
    step = pl.program_id(0)
    half = swapped[0].shape[0]
    sub = sent[0].shape[0] - half
    cols = pl.ds(pl.multiple_of(step * tile, tile), tile)
    total = None
    for a, w, o in zip(att, sent, swapped):
        rolled = []
        for r in range(parts):
            rows = pl.ds(pl.multiple_of(((place[0] + r) % parts) * sub, sub), sub)
            halves = [a[rows, pl.ds(pl.multiple_of(c * half, half), half)] for c in (place[1], 1 - place[1])]
            rolled.append(jnp.concatenate(halves, axis=1))
        weight = jnp.concatenate([w[0:half, :], o[...]], axis=0)
        part = jnp.dot(jnp.concatenate(rolled, axis=0), weight, preferred_element_type=f32).astype(bf16).astype(f32)
        total = part if total is None else total + part
    for r in range(parts):
        updated = (sent[r][half:, :].astype(f32) + total[r * sub : (r + 1) * sub, :]).astype(bf16)
        up_ref[r * sub : (r + 1) * sub, cols] = updated

    @pl.when(step == pl.num_programs(0) - 1)
    def _():
        own_ref[...] = up_ref[0:sub, :]
        for r in range(2 * parts):
            some = slice(r * sub // 2, (r + 1) * sub // 2)
            x = up_ref[some, :].astype(f32)
            x = x * lax.rsqrt(jnp.mean(x * x, axis=-1, keepdims=True) + norm_eps)
            norm_ref[some, :] = (x * gain_ref[...]).astype(bf16)


def project(place, att, sent, swapped, gain, tile=512):
    parts = len(att)
    tok, part_width = att[0].shape
    both, width = sent[0].shape
    half = swapped[0].shape[0]
    sub = both - half
    return pl.pallas_call(
        functools.partial(project_kernel, parts=parts, tile=tile),
        grid_spec=pltpu.PrefetchScalarGridSpec(
            num_scalar_prefetch=1,
            grid=(width // tile,),
            in_specs=[pl.BlockSpec((tok, part_width), lambda i, p: (0, 0))] * parts
            + [pl.BlockSpec((both, tile), lambda i, p: (0, i))] * parts
            + [pl.BlockSpec((half, tile), lambda i, p: (0, i))] * parts
            + [pl.BlockSpec((1, width), lambda i, p: (0, 0))],
            out_specs=(
                pl.BlockSpec((sub, width), lambda i, p: (0, 0)),
                pl.BlockSpec((tok, width), lambda i, p: (0, 0)),
            ),
            scratch_shapes=[pltpu.VMEM((tok, width), bf16)],
        ),
        out_shape=(jax.ShapeDtypeStruct((sub, width), bf16), jax.ShapeDtypeStruct((tok, width), bf16)),
        compiler_params=pltpu.CompilerParams(dimension_semantics=("arbitrary",), vmem_limit_bytes=16 << 20),
        name="project",
    )(place, *att, *sent, *swapped, gain[None, :])


def unit_kernel(x_ref, w_hbm, *refs, units, tile, rows):
    outs = refs[:-4]
    pair_ref, down_ref, h_ref, sems = refs[-4:]
    count = units // tile
    blocks = down_ref.shape[0]

    def gate_copy(n):
        return pltpu.make_async_copy(w_hbm.at[:, pl.ds(2 * n * tile, 2 * tile)], pair_ref.at[n], sems.at[n])

    def down_copy(n):
        source = w_hbm.at[pl.ds(n * rows, rows), pl.ds(2 * units, units)]
        return pltpu.make_async_copy(source, down_ref.at[n], sems.at[count + n])

    for n in range(count):
        gate_copy(n).start()
    for n in range(blocks):
        down_copy(n).start()
    for n in range(count):
        gate_copy(n).wait()
        r = jnp.dot(x_ref[...], pair_ref[n], preferred_element_type=f32)
        gate = r[:, 0:tile]
        h_ref[:, n * tile : (n + 1) * tile] = (gate / (1.0 + jnp.exp(-gate)) * r[:, tile:]).astype(bf16)
    sub = outs[0].shape[0]
    for n in range(blocks):
        down_copy(n).wait()
        y = lax.dot_general(h_ref[...], down_ref[n], (((1,), (1,)), ((), ())), preferred_element_type=f32).astype(bf16)
        for p, out in enumerate(outs):
            out[:, n * rows : (n + 1) * rows] = y[p * sub : (p + 1) * sub, :]


def feed_forward(x, weights, units, parts, tile=128, rows=512):
    tok, width = x.shape
    count = units // tile
    blocks = width // rows
    sub = tok // parts
    return pl.pallas_call(
        functools.partial(unit_kernel, units=units, tile=tile, rows=rows),
        in_specs=[pl.BlockSpec(memory_space=pltpu.VMEM), pl.BlockSpec(memory_space=pltpu.HBM)],
        out_specs=[pl.BlockSpec(memory_space=pltpu.VMEM)] * parts,
        out_shape=[jax.ShapeDtypeStruct((sub, width), bf16)] * parts,
        scratch_shapes=[
            pltpu.VMEM((count, width, 2 * tile), bf16),
            pltpu.VMEM((blocks, rows, units), bf16),
            pltpu.VMEM((tok, units), bf16),
            pltpu.SemaphoreType.DMA((count + blocks,)),
        ],
        compiler_params=pltpu.CompilerParams(vmem_limit_bytes=50 << 20),
        name="units",
    )(x, weights)


def line_kernel(*refs, lines):
    each = (len(refs) - lines) // lines
    for n in range(lines):
        for m in range(each):
            piece = refs[n * each + m]
            rows = piece.shape[0]
            refs[lines * each + n][m * rows : (m + 1) * rows, :] = piece[...]


def lined_up(*lines):
    rows, width = lines[0][0].shape
    shape = jax.ShapeDtypeStruct((rows * len(lines[0]), width), bf16)
    return pl.pallas_call(
        functools.partial(line_kernel, lines=len(lines)),
        out_shape=[shape] * len(lines),
        compiler_params=pltpu.CompilerParams(vmem_limit_bytes=8 << 20),
        name="lines",
    )(*[piece for line in lines for piece in line])


def shifted(value, by):
    count = lax.axis_size("tp")
    return lax.ppermute(value, "tp", [(i, (i + by) % count) for i in range(count)])


SIDE = 4


def moved(value, z=0, y=0, other=False):
    pairs = []
    for a in range(SIDE):
        for b in range(SIDE):
            for c in range(2):
                goal = ((a + z) % SIDE * SIDE + (b + y) % SIDE) * 2 + (1 - c if other else c)
                pairs.append(((a * SIDE + b) * 2 + c, goal))
    return lax.ppermute(value, "sp", pairs)


def on_device(
    query_rows,
    key_rows,
    value_rows,
    query_gain,
    key_gain,
    residual,
    out_weight,
    mix_gain,
    gate_weight,
    up_weight,
    down_weight,
):
    tok = query_rows.shape[0]
    parts = lax.axis_size("tp")
    units = gate_weight.shape[1]
    core = lax.axis_index("sp") % 2
    place = jnp.stack([lax.axis_index("tp"), core])
    q, kv_a, kv_b, woven, payload, kept = prepare(
        query_rows, key_rows, value_rows, query_gain, key_gain, gate_weight, up_weight, down_weight, out_weight, residual
    )
    weights = lax.all_gather(woven, "sp", axis=0, tiled=True)

    a_line, b_line = lined_up(
        [kv_a] + [moved(kv_a, y=d) for d in (1, -1, 2)], [kv_b] + [moved(kv_b, z=d) for d in (1, -1, 2)]
    )
    near = [moved(a_line, z=1), moved(a_line, z=-1), moved(b_line, y=1), moved(b_line, y=-1)]
    far = [moved(a_line, z=2), moved(b_line, y=2)]
    lines = [a_line, b_line, moved(a_line, other=True), moved(b_line, other=True)]

    payload, lines = lax.optimization_barrier((payload, lines))
    sent = [payload] + [shifted(payload, -r) for r in range(1, parts)]

    state = flash(q, lines, None, tok, False)
    state, near = lax.optimization_barrier((state, near))
    near_swapped = [moved(v, other=True) for v in near]
    state = flash(q, near, state, tok, False)
    state, far = lax.optimization_barrier((state, far))
    far_swapped = [moved(v, other=True) for v in far]
    state = flash(q, near_swapped, state, tok, False)
    state, sent = lax.optimization_barrier((state, sent))
    swapped = [kept] + [moved(s[: kept.shape[0]], other=True) for s in sent[1:]]
    attended = flash(q, far + far_swapped, state, tok, True)

    att_parts = [attended] + [shifted(attended, -r) for r in range(1, parts)]
    own_rows, normed = project(place, att_parts, sent, swapped, mix_gain)
    unit_parts = feed_forward(normed, weights, units, parts)
    unit_sum = unit_parts[0].astype(f32)
    for r in range(1, parts):
        unit_sum = unit_sum + shifted(unit_parts[r], r).astype(f32)
    return (own_rows.astype(f32) + 0.5 * unit_sum).astype(bf16)


def solution(mesh):
    placed = (
        P("sp", "tp"),
        P("sp", "tp"),
        P("sp", "tp"),
        P(),
        P(),
        P(("sp", "tp"), None),
        P("tp", None),
        P(),
        P("sp", "tp"),
        P("sp", "tp"),
        P("tp", "sp"),
    )
    return jax.shard_map(
        on_device, mesh=mesh, in_specs=placed, out_specs=P(("sp", "tp"), None), check_vma=False
    )
```

time: 204 us -> 260 us (1.27)
  Pallas kernels: 66.7 us -> 109 us
  starting transfers between devices: 19.7 us -> 37.4 us
  waiting for transfers between devices: 94.9 us -> 82.1 us
  local copies, waits for them, and re-layouts: 1.6 us -> 11.3 us
  other arithmetic: 5.41 us -> 2.47 us
    all_gather x2 -> x1, waiting for transfers between devices: 52.6 us -> 0.01 us  [on_device(): weights = lax.all_gather(woven, 'sp', axis=0, tiled=True)]
    pallas_call x1, Pallas kernels: 2.58 us -> 50.6 us  [prepare(): pl.pallas_call(functools.partial(prepare_kernel, rows=rows, head_dim=head...]
    ppermute x0 -> x23, waiting for transfers between devices: none -> 28.2 us  [moved(): return lax.ppermute(value, 'sp', pairs)]
    ppermute x0 -> x23, starting transfers between devices: none -> 20.6 us  [moved(): return lax.ppermute(value, 'sp', pairs)]
    ppermute x12 -> x9, waiting for transfers between devices: 42.2 us -> 53.9 us  [shifted(): lax.ppermute(value, 'tp', [(i, (i + by) % count) for i in range(count)])]
    unnamed x10 -> x22, local copies, waits for them, and re-layouts: 0.02 us -> 8.76 us
    pallas_call x3 -> x6, Pallas kernels: 55.9 us -> 51.7 us  [the longest x4 30.4 us: flash(): pl.pallas_call(functools.partial(flash_kernel, pieces=pieces, scale=head_...]
    ppermute x12 -> x9, starting transfers between devices: 19.7 us -> 16.8 us  [shifted(): lax.ppermute(value, 'tp', [(i, (i + by) % count) for i in range(count)])]
  transfers between devices with their start and end apart: 14 -> 33, of which waited for: 7 -> 14; matrix products, arithmetic and copies ran while one was open for 1% -> 1% of each run, Pallas kernels for 21% -> 14%
where the time goes in v2:
time: 260 us; the launch traced here: 256 us
  Pallas kernels  109 us (42%)
  waiting for transfers between devices  82.1 us (32%)
  starting transfers between devices  37.4 us (14%)
  between operations  13.6 us (5%)
  local copies, waits for them, and re-layouts  11.3 us (4%)
    ppermute x9, waiting for transfers between devices, shifted(): lax.ppermute(value, 'tp', [(i, (i + by) % count) for i in range(count)])  53.9 us
    pallas_call x1, Pallas kernels, prepare(): pl.pallas_call(functools.partial(prepare_kernel, rows=rows, head_dim=head...  50.6 us
    pallas_call x4, Pallas kernels, flash(): pl.pallas_call(functools.partial(flash_kernel, pieces=pieces, scale=head_...  30.4 us
    ppermute x23, waiting for transfers between devices, moved(): return lax.ppermute(value, 'sp', pairs)  28.2 us
    pallas_call x1, Pallas kernels, feed_forward(): pl.pallas_call(functools.partial(unit_kernel, units=units, tile=tile, row...  21.3 us
    ppermute x23, starting transfers between devices, moved(): return lax.ppermute(value, 'sp', pairs)  20.6 us
    ppermute x9, starting transfers between devices, shifted(): lax.ppermute(value, 'tp', [(i, (i + by) % count) for i in range(count)])  16.8 us
    unnamed x22, local copies, waits for them, and re-layouts  8.76 us
  transfers between devices with their start and end apart: 33, of which 14 were waited for; matrix products, arithmetic and copies ran while one was open for 1% of the time, Pallas kernels for 14%

profile of v2, /device:TPU:8, one launch (start us, length us, event | category | flops | bytes accessed | tf_op | source)
XLA Modules:
  0.0 255.6 jit_solution(90291701947488654)
XLA Ops:
  6.7 0.2 multiply_sine_fusion
  7.0 0.8 pad_maximum_fusion
  7.8 50.6 %prepare.1 = (bf16[1024,128]{1,0:T(8,128)(2,1)}, bf16[256,256]{1,0:T(8,128)(2,1)}, bf16[256,256]{1,0:T(8,128)(2,1)}, bf16[64,4224]{1,0:T(8,128)(2,1)}, bf16[256,...) custom-call(s32[1]{0:T(128)} %bitcast.1.core, bf16[512,256]{1,0:T(8,128)(2,1)} %q_hbm.1, bf16[512,128]{1,0:T(8,128)(2,1)} %k_hbm.1, ...), custom_call_target="tpu_custom_call" | custom-call | tf_op jit(solution)/shard_map/prepare/pallas_call | solution.py:112
  58.4 1.6 collective-permute-start
  60.1 0.4 collective-permute-start.1
  60.5 2.3 collective-permute-start.2
  62.8 1.9 collective-permute-start.3
  64.7 2.1 collective-permute-start.4
  66.9 1.9 collective-permute-start.5
  68.8 1.5 collective-permute-done.3.refs_5_
  70.3 2.1 collective-permute-done.4.refs_6_
  72.4 1.7 collective-permute-done.5.refs_7_
  74.1 0.9 copy-done.7
  75.0 0.9 copy-done.8
  76.1 0.5 collective-permute-start.7
  76.6 1.0 collective-permute-start.10
  77.5 1.1 collective-permute-start.11
  78.6 0.8 collective-permute-start.8
  79.4 2.5 collective-permute-start.9
  81.8 0.4 collective-permute-start.12
  82.2 1.0 copy-done.10
  83.2 7.0 %flash_first.1 = (f32[1024,128]{1,0:T(8,128)S(1)}, f32[1024,256]{1,0:T(8,128)S(1)}) custom-call(bf16[1024,128]{1,0:T(8,128)(2,1)S(1)} %copy-done.10, bf16[1024,256]{1,0:T(8,128)(2,1)S(1)} %get-tuple-element.56.refs_1_, bf16[1024,256]{1,0:T(8,128)(2,1)S(1)} %get-tuple-element.57.refs_2_, bf16[1024,256]{1,0:T(8,128)(2,1)S(1)} %collective-permute-done.6.refs_3_, ...), custom_call_target="tpu_custom_call" | custom-call | flops 2147483648 | bytes 2097152 | tf_op jit(solution)/shard_map/flash_first/pallas_call | solution.py:179
  90.2 4.4 %collective-permute-done.10.refs_3_ = bf16[1024,256]{1,0:T(8,128)(2,1)S(1)} collective-permute-done((bf16[1024,256]{1,0:T(8,128)(2,1)S(1)}, bf16[1024,256]{1,0:T(8,128)(2,1)S(1)}, u32[]{:S(2)}, u32[]{:S(2)}) %collective-permute-start.10) | collective-permute-done | bytes 524320 | tf_op jit(solution)/shard_map/ppermute | solution.py:343
  94.6 1.8 collective-permute-start.13
  96.4 3.9 %collective-permute-done.9.refs_2_ = bf16[1024,256]{1,0:T(8,128)(2,1)S(1)} collective-permute-done((bf16[1024,256]{1,0:T(8,128)(2,1)S(1)}, bf16[1024,256]{1,0:T(8,128)(2,1)S(1)}, u32[]{:S(2)}, u32[]{:S(2)}) %collective-permute-start.9) | collective-permute-done | bytes 524320 | tf_op jit(solution)/shard_map/ppermute | solution.py:343
  100.3 0.5 collective-permute-start.17
  100.9 2.3 collective-permute-start.20
  103.1 11.7 %collective-permute-done.12.refs_1_ = bf16[1024,256]{1,0:T(8,128)(2,1)S(1)} collective-permute-done((bf16[1024,256]{1,0:T(8,128)(2,1)S(1)}, bf16[1024,256]{1,0:T(8,128)(2,1)S(1)}, u32[]{:S(2)}, u32[]{:S(2)}) %collective-permute-start.12) | collective-permute-done | bytes 524320 | tf_op jit(solution)/shard_map/ppermute | solution.py:343
  114.9 3.1 %collective-permute-start.21 = (bf16[256,2048]{1,0:T(8,128)(2,1)}, bf16[256,2048]{1,0:T(8,128)(2,1)S(1)}, u32[]{:S(2)}, u32[]{:S(2)}) collective-permute-start(bf16[256,2048]{1,0:T(8,128)(2,1)} %get-tuple-element.79.refs_4_), channel_id=1, source_target_pairs={{0,2},{1,3},{2,0},{3,1},{4,6},{5,7},{6,4},{7,5},{8,10},{9,11},{10,... | collective-permute-start | bytes 3145736 | tf_op jit(solution)/shard_map/ppermute | solution.py:330
  118.0 2.7 %collective-permute-done.13.refs_2_ = bf16[1024,256]{1,0:T(8,128)(2,1)S(1)} collective-permute-done((bf16[1024,256]{1,0:T(8,128)(2,1)S(1)}, bf16[1024,256]{1,0:T(8,128)(2,1)S(1)}, u32[]{:S(2)}, u32[]{:S(2)}) %collective-permute-start.13) | collective-permute-done | bytes 524320 | tf_op jit(solution)/shard_map/ppermute | solution.py:343
  120.7 1.5 collective-permute-start.22
  122.2 0.5 collective-permute-start.19
  122.7 7.7 %flash_more.2 = (f32[1024,128]{1,0:T(8,128)S(1)}, f32[1024,256]{1,0:T(8,128)S(1)}) custom-call(bf16[1024,128]{1,0:T(8,128)(2,1)S(1)} %copy-done.10, bf16[1024,256]{1,0:T(8,128)(2,1)S(1)} %collective-permute-done.8.refs_1_, bf16[1024,256]{1,0:T(8,128)(2,1)S(1)} %collective-permute-done.9.refs_2_, bf16[1024,256]{1,0:T(8,128)(2,1)S(1)} %collective-permute-done.10.refs_3_, ...), custom_call_target="tpu_custom_call" | custom-call | flops 2147483648 | bytes 2097152 | tf_op jit(solution)/shard_map/flash_more/pallas_call | solution.py:179
  130.4 0.3 collective-permute-start.14
  130.8 0.4 collective-permute-start.15
  131.2 7.7 %flash_more.3 = (f32[1024,128]{1,0:T(8,128)S(1)}, f32[1024,256]{1,0:T(8,128)S(1)}) custom-call(bf16[1024,128]{1,0:T(8,128)(2,1)S(1)} %copy-done.10, bf16[1024,256]{1,0:T(8,128)(2,1)S(1)} %collective-permute-done.16.refs_1_, bf16[1024,256]{1,0:T(8,128)(2,1)S(1)} %collective-permute-done.17.refs_2_, bf16[1024,256]{1,0:T(8,128)(2,1)S(1)} %collective-permute-done.18.refs_3_, ...), custom_call_target="tpu_custom_call" | custom-call | flops 2147483648 | bytes 2097152 | tf_op jit(solution)/shard_map/flash_more/pallas_call | solution.py:179
  138.9 9.6 %collective-permute-done.20.refs_5_ = bf16[256,2048]{1,0:T(8,128)(2,1)S(1)} collective-permute-done((bf16[256,2048]{1,0:T(8,128)(2,1)}, bf16[256,2048]{1,0:T(8,128)(2,1)S(1)}, u32[]{:S(2)}, u32[]{:S(2)}) %collective-permute-start.20) | collective-permute-done | bytes 1048608 | tf_op jit(solution)/shard_map/ppermute | solution.py:330
  148.6 13.1 %collective-permute-done.22.refs_7_ = bf16[256,2048]{1,0:T(8,128)(2,1)S(1)} collective-permute-done((bf16[256,2048]{1,0:T(8,128)(2,1)}, bf16[256,2048]{1,0:T(8,128)(2,1)S(1)}, u32[]{:S(2)}, u32[]{:S(2)}) %collective-permute-start.22) | collective-permute-done | bytes 1048608 | tf_op jit(solution)/shard_map/ppermute | solution.py:330
  161.6 0.8 slice.9
  162.5 7.9 %flash_last.1.refs_0_ = bf16[512,256]{1,0:T(8,128)(2,1)S(1)} custom-call(bf16[1024,128]{1,0:T(8,128)(2,1)S(1)} %copy-done.10, bf16[1024,256]{1,0:T(8,128)(2,1)S(1)} %collective-permute-done.12.refs_1_, bf16[1024,256]{1,0:T(8,128)(2,1)S(1)} %collective-permute-done.13.refs_2_, bf16[1024,256]{1,0:T(8,128)(2,1)S(1)} %collective-permute-done.14.refs_3_, ...), custom_call_target="tpu_custom_call" | custom-call | flops 2147483648 | bytes 2097152 | tf_op jit(solution)/shard_map/flash_last/pallas_call | solution.py:179
  170.4 0.7 collective-permute-start.23
  171.1 0.8 slice.10
  171.9 0.2 collective-permute-start.27
  172.1 0.8 slice.11
  172.9 0.3 collective-permute-start.28
  173.3 2.9 %collective-permute-start.24 = (bf16[512,256]{1,0:T(8,128)(2,1)S(1)}, bf16[512,256]{1,0:T(8,128)(2,1)}, u32[]{:S(2)}, u32[]{:S(2)}) collective-permute-start(bf16[512,256]{1,0:T(8,128)(2,1)S(1)} %flash_last.1.refs_0_), channel_id=1, source_target_pairs={{0,2},{1,3},{2,0},{3,1},{4,6},{5,7},{6,4},{7,5},{8,10},{9,11},{10,... | collective-permute-start | bytes 786440 | tf_op jit(solution)/shard_map/ppermute | solution.py:330
  176.2 3.5 %collective-permute-done.23.refs_1_ = bf16[512,256]{1,0:T(8,128)(2,1)S(1)} collective-permute-done((bf16[512,256]{1,0:T(8,128)(2,1)S(1)}, bf16[512,256]{1,0:T(8,128)(2,1)S(1)}, u32[]{:S(2)}, u32[]{:S(2)}) %collective-permute-start.23) | collective-permute-done | bytes 262176 | tf_op jit(solution)/shard_map/ppermute | solution.py:330
  179.6 0.7 copy-done.5
  180.3 0.9 collective-permute-start.25
  181.4 1.9 collective-permute-done.24.refs_2_
  183.3 5.8 %collective-permute-done.25.refs_3_ = bf16[512,256]{1,0:T(8,128)(2,1)} collective-permute-done((bf16[512,256]{1,0:T(8,128)(2,1)S(1)}, bf16[512,256]{1,0:T(8,128)(2,1)}, u32[]{:S(2)}, u32[]{:S(2)}) %collective-permute-start.25) | collective-permute-done | bytes 262176 | tf_op jit(solution)/shard_map/ppermute | solution.py:330
  189.1 1.2 copy-done.1
  190.3 1.0 copy-done.2
  191.4 0.9 copy-done.6
  192.3 6.3 %project.1 = (bf16[128,2048]{1,0:T(8,128)(2,1)S(1)}, bf16[512,2048]{1,0:T(8,128)(2,1)S(1)}) custom-call(s32[2]{0:T(128)S(1)} %pad_add_fusion.place, bf16[512,256]{1,0:T(8,128)(2,1)S(1)} %flash_last.1.refs_0_, bf16[512,256]{1,0:T(8,128)(2,1)S(1)} %copy-done.6, bf16[512,256]{1,0:T(8,128)(2,1)} %collective-permute-done.24.refs_2_, ...), custom_call_target="tpu_custom_call" | custom-call | tf_op jit(solution)/shard_map/project/pallas_call | solution.py:236
  198.6 1.3 copy-done
  199.9 0.8 copy-done.3
  200.7 21.3 %units.1 = (bf16[128,2048]{1,0:T(8,128)(2,1)S(1)}, bf16[128,2048]{1,0:T(8,128)(2,1)S(1)}, bf16[128,2048]{1,0:T(8,128)(2,1)S(1)}, bf16[128,2048]{1,0:T(8,128)(2,1)S(1)}) custom-call(bf16[512,2048]{1,0:T(8,128)(2,1)} %copy-done, bf16[2048,4224]{1,0:T(8,128)(2,1)} %all-gather.2.cloned.1.call-done.w_hbm), custom_call_target="tpu_custom_call" | custom-call | tf_op jit(solution)/shard_map/units/pallas_call | solution.py:292
  222.0 1.3 collective-permute-start.29
  223.3 1.6 collective-permute-start.30
  224.9 2.5 collective-permute-start.31
  227.5 8.6 %collective-permute-done.29 = bf16[128,2048]{1,0:T(8,128)(2,1)S(1)} collective-permute-done((bf16[128,2048]{1,0:T(8,128)(2,1)S(1)}, bf16[128,2048]{1,0:T(8,128)(2,1)S(1)}, u32[]{:S(2)}, u32[]{:S(2)}) %collective-permute-start.29) | collective-permute-done | bytes 524320 | tf_op jit(solution)/shard_map/ppermute | solution.py:330
  236.1 11.4 %collective-permute-done.30 = bf16[128,2048]{1,0:T(8,128)(2,1)S(1)} collective-permute-done((bf16[128,2048]{1,0:T(8,128)(2,1)S(1)}, bf16[128,2048]{1,0:T(8,128)(2,1)S(1)}, u32[]{:S(2)}, u32[]{:S(2)}) %collective-permute-start.30) | collective-permute-done | bytes 524320 | tf_op jit(solution)/shard_map/ppermute | solution.py:330
  247.5 1.2 add_convert_fusion
  (46 shorter events, 0.6 us)
Async XLA Ops:
  6.5 194.2 %all-gather.2.cloned.1.call-start = ((), (), s32[]{:S(2)}) async-start(), calls=%async_computation | async-start | bytes 17842176 | tf_op jit(solution)/shard_map/all_gather | solution.py:367
  58.4 8.4 %collective-permute-start = (bf16[256,256]{1,0:T(8,128)(2,1)}, bf16[256,256]{1,0:T(8,128)(2,1)S(1)}, u32[]{:S(2)}, u32[]{:S(2)}) collective-permute-start(bf16[256,256]{1,0:T(8,128)(2,1)} %get-tuple-element.52.refs_0_), channel_id=1, source_target_pairs={{0,8},{4,12},{8,16},{12,20},{16,24},{20,28},{24,0},{28,4},{32,40},... | collective-permute-start | bytes 393224 | tf_op jit(solution)/shard_map/ppermute | solution.py:343
  60.1 8.7 %collective-permute-start.1 = (bf16[256,256]{1,0:T(8,128)(2,1)}, bf16[256,256]{1,0:T(8,128)(2,1)S(1)}, u32[]{:S(2)}, u32[]{:S(2)}) collective-permute-start(bf16[256,256]{1,0:T(8,128)(2,1)} %get-tuple-element.52.refs_0_), channel_id=1, source_target_pairs={{0,24},{4,28},{8,0},{12,4},{16,8},{20,12},{24,16},{28,20},{32,56},... | collective-permute-start | bytes 393224 | tf_op jit(solution)/shard_map/ppermute | solution.py:343
  60.5 8.2 %collective-permute-start.2 = (bf16[256,256]{1,0:T(8,128)(2,1)}, bf16[256,256]{1,0:T(8,128)(2,1)S(1)}, u32[]{:S(2)}, u32[]{:S(2)}) collective-permute-start(bf16[256,256]{1,0:T(8,128)(2,1)} %get-tuple-element.52.refs_0_), channel_id=1, source_target_pairs={{0,16},{4,20},{8,24},{12,28},{16,0},{20,4},{24,8},{28,12},{32,48},... | collective-permute-start | bytes 393224 | tf_op jit(solution)/shard_map/ppermute | solution.py:343
  62.8 7.5 %collective-permute-start.3 = (bf16[256,256]{1,0:T(8,128)(2,1)}, bf16[256,256]{1,0:T(8,128)(2,1)S(1)}, u32[]{:S(2)}, u32[]{:S(2)}) collective-permute-start(bf16[256,256]{1,0:T(8,128)(2,1)} %get-tuple-element.53.refs_4_), channel_id=1, source_target_pairs={{0,32},{4,36},{8,40},{12,44},{16,48},{20,52},{24,56},{28,60},{32,6... | collective-permute-start | bytes 393224 | tf_op jit(solution)/shard_map/ppermute | solution.py:343
  64.7 7.7 %collective-permute-start.4 = (bf16[256,256]{1,0:T(8,128)(2,1)}, bf16[256,256]{1,0:T(8,128)(2,1)S(1)}, u32[]{:S(2)}, u32[]{:S(2)}) collective-permute-start(bf16[256,256]{1,0:T(8,128)(2,1)} %get-tuple-element.53.refs_4_), channel_id=1, source_target_pairs={{0,96},{4,100},{8,104},{12,108},{16,112},{20,116},{24,120},{28,124... | collective-permute-start | bytes 393224 | tf_op jit(solution)/shard_map/ppermute | solution.py:343
  66.9 7.2 %collective-permute-start.5 = (bf16[256,256]{1,0:T(8,128)(2,1)}, bf16[256,256]{1,0:T(8,128)(2,1)S(1)}, u32[]{:S(2)}, u32[]{:S(2)}) collective-permute-start(bf16[256,256]{1,0:T(8,128)(2,1)} %get-tuple-element.53.refs_4_), channel_id=1, source_target_pairs={{0,64},{4,68},{8,72},{12,76},{16,80},{20,84},{24,88},{28,92},{32,9... | collective-permute-start | bytes 393224 | tf_op jit(solution)/shard_map/ppermute | solution.py:343
  74.1 0.9 copy-start.7
  75.0 0.9 copy-start.8
  76.0 3.4 %collective-permute-start.6 = (bf16[1024,256]{1,0:T(8,128)(2,1)S(1)}, bf16[1024,256]{1,0:T(8,128)(2,1)S(1)}, u32[]{:S(2)}, u32[]{:S(2)}) collective-permute-start(bf16[1024,256]{1,0:T(8,128)(2,1)S(1)} %get-tuple-element.56.refs_1_), channel_id=1, source_target_pairs={{0,4},{4,0},{8,12},{12,8},{16,20},{20,16},{24,28},{28,24},{32,36},... | collective-permute-start | bytes 1572872 | tf_op jit(solution)/shard_map/ppermute | solution.py:343
  76.1 5.8 %collective-permute-start.7 = (bf16[1024,256]{1,0:T(8,128)(2,1)S(1)}, bf16[1024,256]{1,0:T(8,128)(2,1)S(1)}, u32[]{:S(2)}, u32[]{:S(2)}) collective-permute-start(bf16[1024,256]{1,0:T(8,128)(2,1)S(1)} %get-tuple-element.57.refs_2_), channel_id=1, source_target_pairs={{0,4},{4,0},{8,12},{12,8},{16,20},{20,16},{24,28},{28,24},{32,36},... | collective-permute-start | bytes 1572872 | tf_op jit(solution)/shard_map/ppermute | solution.py:343
  76.6 18.1 %collective-permute-start.10 = (bf16[1024,256]{1,0:T(8,128)(2,1)S(1)}, bf16[1024,256]{1,0:T(8,128)(2,1)S(1)}, u32[]{:S(2)}, u32[]{:S(2)}) collective-permute-start(bf16[1024,256]{1,0:T(8,128)(2,1)S(1)} %get-tuple-element.57.refs_2_), channel_id=1, source_target_pairs={{0,8},{4,12},{8,16},{12,20},{16,24},{20,28},{24,0},{28,4},{32,40},... | collective-permute-start | bytes 1572872 | tf_op jit(solution)/shard_map/ppermute | solution.py:343
  77.5 18.9 %collective-permute-start.11 = (bf16[1024,256]{1,0:T(8,128)(2,1)S(1)}, bf16[1024,256]{1,0:T(8,128)(2,1)S(1)}, u32[]{:S(2)}, u32[]{:S(2)}) collective-permute-start(bf16[1024,256]{1,0:T(8,128)(2,1)S(1)} %get-tuple-element.57.refs_2_), channel_id=1, source_target_pairs={{0,24},{4,28},{8,0},{12,4},{16,8},{20,12},{24,16},{28,20},{32,56},... | collective-permute-start | bytes 1572872 | tf_op jit(solution)/shard_map/ppermute | solution.py:343
  78.6 17.8 %collective-permute-start.8 = (bf16[1024,256]{1,0:T(8,128)(2,1)S(1)}, bf16[1024,256]{1,0:T(8,128)(2,1)S(1)}, u32[]{:S(2)}, u32[]{:S(2)}) collective-permute-start(bf16[1024,256]{1,0:T(8,128)(2,1)S(1)} %get-tuple-element.56.refs_1_), channel_id=1, source_target_pairs={{0,32},{4,36},{8,40},{12,44},{16,48},{20,52},{24,56},{28,60},{32,6... | collective-permute-start | bytes 1572872 | tf_op jit(solution)/shard_map/ppermute | solution.py:343
  79.4 21.0 %collective-permute-start.9 = (bf16[1024,256]{1,0:T(8,128)(2,1)S(1)}, bf16[1024,256]{1,0:T(8,128)(2,1)S(1)}, u32[]{:S(2)}, u32[]{:S(2)}) collective-permute-start(bf16[1024,256]{1,0:T(8,128)(2,1)S(1)} %get-tuple-element.56.refs_1_), channel_id=1, source_target_pairs={{0,96},{4,100},{8,104},{12,108},{16,112},{20,116},{24,120},{28,124... | collective-permute-start | bytes 1572872 | tf_op jit(solution)/shard_map/ppermute | solution.py:343
  81.8 33.0 %collective-permute-start.12 = (bf16[1024,256]{1,0:T(8,128)(2,1)S(1)}, bf16[1024,256]{1,0:T(8,128)(2,1)S(1)}, u32[]{:S(2)}, u32[]{:S(2)}) collective-permute-start(bf16[1024,256]{1,0:T(8,128)(2,1)S(1)} %get-tuple-element.56.refs_1_), channel_id=1, source_target_pairs={{0,64},{4,68},{8,72},{12,76},{16,80},{20,84},{24,88},{28,92},{32,9... | collective-permute-start | bytes 1572872 | tf_op jit(solution)/shard_map/ppermute | solution.py:343
  82.2 1.0 copy-start.10
  83.2 105.9 %copy-start.9 = (f32[2048]{0:T(1024)S(1)}, f32[2048]{0:T(1024)}, u32[]{:S(2)}) copy-start(f32[2048]{0:T(1024)} %param.18) | copy-start | bytes 24580
  94.6 26.1 %collective-permute-start.13 = (bf16[1024,256]{1,0:T(8,128)(2,1)S(1)}, bf16[1024,256]{1,0:T(8,128)(2,1)S(1)}, u32[]{:S(2)}, u32[]{:S(2)}) collective-permute-start(bf16[1024,256]{1,0:T(8,128)(2,1)S(1)} %get-tuple-element.57.refs_2_), channel_id=1, source_target_pairs={{0,16},{4,20},{8,24},{12,28},{16,0},{20,4},{24,8},{28,12},{32,48},... | collective-permute-start | bytes 1572872 | tf_op jit(solution)/shard_map/ppermute | solution.py:343
  100.3 21.9 %collective-permute-start.16 = (bf16[1024,256]{1,0:T(8,128)(2,1)S(1)}, bf16[1024,256]{1,0:T(8,128)(2,1)S(1)}, u32[]{:S(2)}, u32[]{:S(2)}) collective-permute-start(bf16[1024,256]{1,0:T(8,128)(2,1)S(1)} %collective-permute-done.8.refs_1_), channel_id=1, source_target_pairs={{0,4},{4,0},{8,12},{12,8},{16,20},{20,16},{24,28},{28,24},{32,36},... | collective-permute-start | bytes 1572872 | tf_op jit(solution)/shard_map/ppermute | solution.py:343
  100.3 21.9 %collective-permute-start.17 = (bf16[1024,256]{1,0:T(8,128)(2,1)S(1)}, bf16[1024,256]{1,0:T(8,128)(2,1)S(1)}, u32[]{:S(2)}, u32[]{:S(2)}) collective-permute-start(bf16[1024,256]{1,0:T(8,128)(2,1)S(1)} %collective-permute-done.9.refs_2_), channel_id=1, source_target_pairs={{0,4},{4,0},{8,12},{12,8},{16,20},{20,16},{24,28},{28,24},{32,36},... | collective-permute-start | bytes 1572872 | tf_op jit(solution)/shard_map/ppermute | solution.py:343
  100.9 47.7 %collective-permute-start.20 = (bf16[256,2048]{1,0:T(8,128)(2,1)}, bf16[256,2048]{1,0:T(8,128)(2,1)S(1)}, u32[]{:S(2)}, u32[]{:S(2)}) collective-permute-start(bf16[256,2048]{1,0:T(8,128)(2,1)} %get-tuple-element.79.refs_4_), channel_id=1, source_target_pairs={{0,3},{1,0},{2,1},{3,2},{4,7},{5,4},{6,5},{7,6},{8,11},{9,8},{10,9... | collective-permute-start | bytes 3145736 | tf_op jit(solution)/shard_map/ppermute | solution.py:330
  114.9 33.7 %collective-permute-start.21 = (bf16[256,2048]{1,0:T(8,128)(2,1)}, bf16[256,2048]{1,0:T(8,128)(2,1)S(1)}, u32[]{:S(2)}, u32[]{:S(2)}) collective-permute-start(bf16[256,2048]{1,0:T(8,128)(2,1)} %get-tuple-element.79.refs_4_), channel_id=1, source_target_pairs={{0,2},{1,3},{2,0},{3,1},{4,6},{5,7},{6,4},{7,5},{8,10},{9,11},{10,... | collective-permute-start | bytes 3145736 | tf_op jit(solution)/shard_map/ppermute | solution.py:330
  120.7 40.9 %collective-permute-start.22 = (bf16[256,2048]{1,0:T(8,128)(2,1)}, bf16[256,2048]{1,0:T(8,128)(2,1)S(1)}, u32[]{:S(2)}, u32[]{:S(2)}) collective-permute-start(bf16[256,2048]{1,0:T(8,128)(2,1)} %get-tuple-element.79.refs_4_), channel_id=1, source_target_pairs={{0,1},{1,2},{2,3},{3,0},{4,5},{5,6},{6,7},{7,4},{8,9},{9,10},{10,1... | collective-permute-start | bytes 3145736 | tf_op jit(solution)/shard_map/ppermute | solution.py:330
  122.2 8.2 %collective-permute-start.18 = (bf16[1024,256]{1,0:T(8,128)(2,1)S(1)}, bf16[1024,256]{1,0:T(8,128)(2,1)S(1)}, u32[]{:S(2)}, u32[]{:S(2)}) collective-permute-start(bf16[1024,256]{1,0:T(8,128)(2,1)S(1)} %collective-permute-done.10.refs_3_), channel_id=1, source_target_pairs={{0,4},{4,0},{8,12},{12,8},{16,20},{20,16},{24,28},{28,24},{32,36},... | collective-permute-start | bytes 1572872 | tf_op jit(solution)/shard_map/ppermute | solution.py:343
  122.2 8.6 %collective-permute-start.19 = (bf16[1024,256]{1,0:T(8,128)(2,1)S(1)}, bf16[1024,256]{1,0:T(8,128)(2,1)S(1)}, u32[]{:S(2)}, u32[]{:S(2)}) collective-permute-start(bf16[1024,256]{1,0:T(8,128)(2,1)S(1)} %collective-permute-done.11.refs_4_), channel_id=1, source_target_pairs={{0,4},{4,0},{8,12},{12,8},{16,20},{20,16},{24,28},{28,24},{32,36},... | collective-permute-start | bytes 1572872 | tf_op jit(solution)/shard_map/ppermute | solution.py:343
  130.4 32.0 %collective-permute-start.14 = (bf16[1024,256]{1,0:T(8,128)(2,1)S(1)}, bf16[1024,256]{1,0:T(8,128)(2,1)S(1)}, u32[]{:S(2)}, u32[]{:S(2)}) collective-permute-start(bf16[1024,256]{1,0:T(8,128)(2,1)S(1)} %collective-permute-done.12.refs_1_), channel_id=1, source_target_pairs={{0,4},{4,0},{8,12},{12,8},{16,20},{20,16},{24,28},{28,24},{32,36},... | collective-permute-start | bytes 1572872 | tf_op jit(solution)/shard_map/ppermute | solution.py:343
  130.8 31.7 %collective-permute-start.15 = (bf16[1024,256]{1,0:T(8,128)(2,1)S(1)}, bf16[1024,256]{1,0:T(8,128)(2,1)S(1)}, u32[]{:S(2)}, u32[]{:S(2)}) collective-permute-start(bf16[1024,256]{1,0:T(8,128)(2,1)S(1)} %collective-permute-done.13.refs_2_), channel_id=1, source_target_pairs={{0,4},{4,0},{8,12},{12,8},{16,20},{20,16},{24,28},{28,24},{32,36},... | collective-permute-start | bytes 1572872 | tf_op jit(solution)/shard_map/ppermute | solution.py:343
  162.5 26.6 %collective-permute-start.26 = (bf16[128,2048]{1,0:T(8,128)(2,1)}, bf16[128,2048]{1,0:T(8,128)(2,1)}, u32[]{:S(2)}, u32[]{:S(2)}) collective-permute-start(bf16[128,2048]{1,0:T(8,128)(2,1)} %slice.9), channel_id=1, source_target_pairs={{0,4},{4,0},{8,12},{12,8},{16,20},{20,16},{24,28},{28,24},{32,36},... | collective-permute-start | bytes 1572872 | tf_op jit(solution)/shard_map/ppermute | solution.py:343
  170.4 9.2 %collective-permute-start.23 = (bf16[512,256]{1,0:T(8,128)(2,1)S(1)}, bf16[512,256]{1,0:T(8,128)(2,1)S(1)}, u32[]{:S(2)}, u32[]{:S(2)}) collective-permute-start(bf16[512,256]{1,0:T(8,128)(2,1)S(1)} %flash_last.1.refs_0_), channel_id=1, source_target_pairs={{0,3},{1,0},{2,1},{3,2},{4,7},{5,4},{6,5},{7,6},{8,11},{9,8},{10,9... | collective-permute-start | bytes 786440 | tf_op jit(solution)/shard_map/ppermute | solution.py:330
  171.9 17.2 %collective-permute-start.27 = (bf16[128,2048]{1,0:T(8,128)(2,1)}, bf16[128,2048]{1,0:T(8,128)(2,1)}, u32[]{:S(2)}, u32[]{:S(2)}) collective-permute-start(bf16[128,2048]{1,0:T(8,128)(2,1)} %slice.10), channel_id=1, source_target_pairs={{0,4},{4,0},{8,12},{12,8},{16,20},{20,16},{24,28},{28,24},{32,36},... | collective-permute-start | bytes 1572872 | tf_op jit(solution)/shard_map/ppermute | solution.py:343
  172.9 16.1 %collective-permute-start.28 = (bf16[128,2048]{1,0:T(8,128)(2,1)}, bf16[128,2048]{1,0:T(8,128)(2,1)}, u32[]{:S(2)}, u32[]{:S(2)}) collective-permute-start(bf16[128,2048]{1,0:T(8,128)(2,1)} %slice.11), channel_id=1, source_target_pairs={{0,4},{4,0},{8,12},{12,8},{16,20},{20,16},{24,28},{28,24},{32,36},... | collective-permute-start | bytes 1572872 | tf_op jit(solution)/shard_map/ppermute | solution.py:343
  173.3 10.0 %collective-permute-start.24 = (bf16[512,256]{1,0:T(8,128)(2,1)S(1)}, bf16[512,256]{1,0:T(8,128)(2,1)}, u32[]{:S(2)}, u32[]{:S(2)}) collective-permute-start(bf16[512,256]{1,0:T(8,128)(2,1)S(1)} %flash_last.1.refs_0_), channel_id=1, source_target_pairs={{0,2},{1,3},{2,0},{3,1},{4,6},{5,7},{6,4},{7,5},{8,10},{9,11},{10,... | collective-permute-start | bytes 786440 | tf_op jit(solution)/shard_map/ppermute | solution.py:330
  179.6 0.7 copy-start.5
  180.3 8.7 %collective-permute-start.25 = (bf16[512,256]{1,0:T(8,128)(2,1)S(1)}, bf16[512,256]{1,0:T(8,128)(2,1)}, u32[]{:S(2)}, u32[]{:S(2)}) collective-permute-start(bf16[512,256]{1,0:T(8,128)(2,1)S(1)} %flash_last.1.refs_0_), channel_id=1, source_target_pairs={{0,1},{1,2},{2,3},{3,0},{4,5},{5,6},{6,7},{7,4},{8,9},{9,10},{10,1... | collective-permute-start | bytes 786440 | tf_op jit(solution)/shard_map/ppermute | solution.py:330
  189.1 1.2 copy-start.1
  190.3 1.0 copy-start.2
  191.4 0.9 copy-start.6
  198.6 1.3 copy-start
  199.9 0.8 copy-start.3
  200.7 46.8 %copy-start.4 = (bf16[128,2048]{1,0:T(8,128)(2,1)S(1)}, bf16[128,2048]{1,0:T(8,128)(2,1)}, u32[]{:S(2)}) copy-start(bf16[128,2048]{1,0:T(8,128)(2,1)} %copy-done.3) | copy-start | bytes 1572868
  222.0 14.0 %collective-permute-start.29 = (bf16[128,2048]{1,0:T(8,128)(2,1)S(1)}, bf16[128,2048]{1,0:T(8,128)(2,1)S(1)}, u32[]{:S(2)}, u32[]{:S(2)}) collective-permute-start(bf16[128,2048]{1,0:T(8,128)(2,1)S(1)} %get-tuple-element.88), channel_id=1, source_target_pairs={{0,1},{1,2},{2,3},{3,0},{4,5},{5,6},{6,7},{7,4},{8,9},{9,10},{10,1... | collective-permute-start | bytes 1572872 | tf_op jit(solution)/shard_map/ppermute | solution.py:330
  223.3 24.2 %collective-permute-start.30 = (bf16[128,2048]{1,0:T(8,128)(2,1)S(1)}, bf16[128,2048]{1,0:T(8,128)(2,1)S(1)}, u32[]{:S(2)}, u32[]{:S(2)}) collective-permute-start(bf16[128,2048]{1,0:T(8,128)(2,1)S(1)} %get-tuple-element.89), channel_id=1, source_target_pairs={{0,2},{1,3},{2,0},{3,1},{4,6},{5,7},{6,4},{7,5},{8,10},{9,11},{10,... | collective-permute-start | bytes 1572872 | tf_op jit(solution)/shard_map/ppermute | solution.py:330
  224.9 22.6 %collective-permute-start.31 = (bf16[128,2048]{1,0:T(8,128)(2,1)S(1)}, bf16[128,2048]{1,0:T(8,128)(2,1)S(1)}, u32[]{:S(2)}, u32[]{:S(2)}) collective-permute-start(bf16[128,2048]{1,0:T(8,128)(2,1)S(1)} %get-tuple-element.90), channel_id=1, source_target_pairs={{0,3},{1,0},{2,1},{3,2},{4,7},{5,4},{6,5},{7,6},{8,11},{9,8},{10,9... | collective-permute-start | bytes 1572872 | tf_op jit(solution)/shard_map/ppermute | solution.py:330
Sparse Core Ops, SparseCore 0:
  58.5 87.5 all-gather.1

commit v3 on v2

--- a/solution.py
+++ b/solution.py
@@ -41,7 +41,7 @@
 def prepare_kernel(
     core, q_hbm, k_hbm, v_hbm, g_hbm, u_hbm, d_hbm, w_hbm, r_hbm, qg_ref, kg_ref, cos_ref, sin_ref,
     q_out, a_out, b_out, woven, sent, kept,
-    q_ref, k_ref, v_ref, g_ref, u_ref, d_ref, sems, *, rows, head_dim, heads, tile,
+    q_ref, k_ref, v_ref, g_ref, u_ref, d_ref, w_ref, r_ref, sems, *, rows, head_dim, heads, tile,
 ):
     tok = rows * GRID
     half = kept.shape[0]
@@ -54,12 +54,15 @@
         (g_hbm, g_ref),
         (u_hbm, u_ref),
         (d_hbm, d_ref),
-        (w_hbm.at[first_half, :], sent.at[pl.ds(0, half), :]),
-        (r_hbm, sent.at[pl.ds(half, r_hbm.shape[0]), :]),
-        (w_hbm.at[other_half, :], kept),
+        (w_hbm.at[first_half, :], w_ref.at[pl.ds(0, half), :]),
+        (w_hbm.at[other_half, :], w_ref.at[pl.ds(half, half), :]),
+        (r_hbm, r_ref),
+        (w_ref.at[pl.ds(0, half), :], sent.at[pl.ds(0, half), :]),
+        (w_ref.at[pl.ds(half, half), :], kept),
+        (r_ref, sent.at[pl.ds(half, r_hbm.shape[0]), :]),
     ]
     copies = [pltpu.make_async_copy(x, y, sems.at[n]) for n, (x, y) in enumerate(moves)]
-    for c in copies:
+    for c in copies[:9]:
         c.start()
 
     def spread(ref):
@@ -85,6 +88,9 @@
         part = slice(n * tok // 2, (n + 1) * tok // 2)
         out[:, 0:head_dim] = keys[part, :]
         out[:, head_dim:] = v_ref[part, :]
+    for n in (6, 7, 8):
+        copies[n].wait()
+        copies[n + 3].start()
     copies[2].wait()
     for h in range(heads):
         q_out[h * tok : (h + 1) * tok, :] = prepared(q_ref[:, h * head_dim : (h + 1) * head_dim], qg_ref[...])
@@ -96,7 +102,7 @@
         woven[:, 2 * n * tile : (2 * n + 1) * tile] = g_ref[:, part]
         woven[:, (2 * n + 1) * tile : (2 * n + 2) * tile] = u_ref[:, part]
     woven[:, 2 * units :] = d_ref[...]
-    for n in (6, 7, 8):
+    for n in (9, 10, 11):
         copies[n].wait()
 
 
@@ -121,7 +127,7 @@
             jax.ShapeDtypeStruct((half + residual.shape[0], residual.shape[1]), bf16),
             jax.ShapeDtypeStruct((half, residual.shape[1]), bf16),
         ),
-        scratch_shapes=[pltpu.VMEM(x.shape, bf16) for x in big] + [pltpu.SemaphoreType.DMA((9,))],
+        scratch_shapes=[pltpu.VMEM(x.shape, bf16) for x in (*big, out_weight, residual)] + [pltpu.SemaphoreType.DMA((12,))],
         compiler_params=pltpu.CompilerParams(vmem_limit_bytes=60 * 1024 * 1024),
         name="prepare",
     )(
@@ -150,11 +156,17 @@
     else:
         m = m_in[...]
         acc = acc_in[...]
+
+    def scores(n):
+        return lax.dot_general(q, kv_refs[n][:, 0:head_dim], (((1,), (1,)), ((), ())), preferred_element_type=f32)
+
+    following = scores(0)
     for n in range(pieces):
-        keys = kv_refs[n][:, 0:head_dim]
         values = kv_refs[n][:, head_dim:]
         values = jnp.concatenate([values, jnp.ones_like(values)], axis=1)
-        s = lax.dot_general(q, keys, (((1,), (1,)), ((), ())), preferred_element_type=f32) * scale
+        s = following * scale
+        if n + 1 < pieces:
+            following = scores(n + 1)
         new = jnp.maximum(m, jnp.max(s, axis=1, keepdims=True))
         w = jnp.exp2(s - new[:, 0:1]).astype(bf16)
         factor = jnp.exp2(m - new)
@@ -254,7 +266,7 @@
     )(place, *att, *sent, *swapped, gain[None, :])
 
 
-def unit_kernel(x_ref, w_hbm, *refs, units, tile, rows):
+def unit_kernel(x_ref, w_hbm, *refs, units, tile, rows, ahead=3):
     outs = refs[:-4]
     pair_ref, down_ref, h_ref, sems = refs[-4:]
     count = units // tile
@@ -267,18 +279,23 @@
         source = w_hbm.at[pl.ds(n * rows, rows), pl.ds(2 * units, units)]
         return pltpu.make_async_copy(source, down_ref.at[n], sems.at[count + n])
 
+    copies = [gate_copy(n) for n in range(count)] + [down_copy(n) for n in range(blocks)]
+
+    def arrive(n):
+        copies[n].wait()
+        if n + ahead < len(copies):
+            copies[n + ahead].start()
+
+    for n in range(ahead):
+        copies[n].start()
     for n in range(count):
-        gate_copy(n).start()
-    for n in range(blocks):
-        down_copy(n).start()
-    for n in range(count):
-        gate_copy(n).wait()
+        arrive(n)
         r = jnp.dot(x_ref[...], pair_ref[n], preferred_element_type=f32)
         gate = r[:, 0:tile]
         h_ref[:, n * tile : (n + 1) * tile] = (gate / (1.0 + jnp.exp(-gate)) * r[:, tile:]).astype(bf16)
     sub = outs[0].shape[0]
     for n in range(blocks):
-        down_copy(n).wait()
+        arrive(count + n)
         y = lax.dot_general(h_ref[...], down_ref[n], (((1,), (1,)), ((), ())), preferred_element_type=f32).astype(bf16)
         for p, out in enumerate(outs):
             out[:, n * rows : (n + 1) * rows] = y[p * sub : (p + 1) * sub, :]
@@ -373,7 +390,6 @@
     far = [moved(a_line, z=2), moved(b_line, y=2)]
     lines = [a_line, b_line, moved(a_line, other=True), moved(b_line, other=True)]
 
-    payload, lines = lax.optimization_barrier((payload, lines))
     sent = [payload] + [shifted(payload, -r) for r in range(1, parts)]
 
     state = flash(q, lines, None, tok, False)
@@ -383,9 +399,9 @@
     state, far = lax.optimization_barrier((state, far))
     far_swapped = [moved(v, other=True) for v in far]
     state = flash(q, near_swapped, state, tok, False)
-    state, sent = lax.optimization_barrier((state, sent))
+    attended = flash(q, far + far_swapped, state, tok, True)
+    attended, sent = lax.optimization_barrier((attended, sent))
     swapped = [kept] + [moved(s[: kept.shape[0]], other=True) for s in sent[1:]]
-    attended = flash(q, far + far_swapped, state, tok, True)
 
     att_parts = [attended] + [shifted(attended, -r) for r in range(1, parts)]
     own_rows, normed = project(place, att_parts, sent, swapped, mix_gain)

time: 260 us -> 214 us (0.82)
  the two profiles are of different devices: /device:TPU:8 before, /device:TPU:0 now
where the time goes in v3:
time: 214 us; the launch traced here: 213 us
  waiting for transfers between devices  95.4 us (45%)
  Pallas kernels  59.3 us (28%)
  starting transfers between devices  31 us (14%)
  between operations  13.6 us (6%)
  local copies, waits for them, and re-layouts  11.3 us (5%)
  other arithmetic  2.47 us (1%)
    ppermute x9, waiting for transfers between devices, shifted(): lax.ppermute(value, 'tp', [(i, (i + by) % count) for i in range(count)])  60.1 us
    ppermute x23, waiting for transfers between devices, moved(): return lax.ppermute(value, 'sp', pairs)  35.2 us
    pallas_call x4, Pallas kernels, flash(): pl.pallas_call(functools.partial(flash_kernel, pieces=pieces, scale=head_...  27.2 us
    ppermute x23, starting transfers between devices, moved(): return lax.ppermute(value, 'sp', pairs)  21.8 us
    pallas_call x1, Pallas kernels, feed_forward(): pl.pallas_call(functools.partial(unit_kernel, units=units, tile=tile, row...  21.3 us
    ppermute x9, starting transfers between devices, shifted(): lax.ppermute(value, 'tp', [(i, (i + by) % count) for i in range(count)])  9.22 us
    unnamed x22, local copies, waits for them, and re-layouts  8.76 us
    pallas_call x1, Pallas kernels, project(): pl.pallas_call(functools.partial(project_kernel, parts=parts, tile=tile),...  6.31 us
  transfers between devices with their start and end apart: 33, of which 15 were waited for; matrix products, arithmetic and copies ran while one was open for 1% of the time, Pallas kernels for 16%

profile of v3, /device:TPU:0, one launch (start us, length us, event | category | flops | bytes accessed | tf_op | source)
XLA Modules:
  0.0 213.1 jit_solution(11054286852769628489)
XLA Ops:
  6.7 0.2 multiply_sine_fusion
  6.9 0.1 negate_select_fusion.1
  7.0 0.8 pad_maximum_fusion
  7.8 4.5 %prepare.1 = (bf16[1024,128]{1,0:T(8,128)(2,1)}, bf16[256,256]{1,0:T(8,128)(2,1)}, bf16[256,256]{1,0:T(8,128)(2,1)}, bf16[64,4224]{1,0:T(8,128)(2,1)}, bf16[256,...) custom-call(s32[1]{0:T(128)} %bitcast.1.core, bf16[512,256]{1,0:T(8,128)(2,1)} %q_hbm.1, bf16[512,128]{1,0:T(8,128)(2,1)} %k_hbm.1, ...), custom_call_target="tpu_custom_call" | custom-call | tf_op jit(solution)/shard_map/prepare/pallas_call | solution.py:118
  12.3 1.8 collective-permute-start
  14.0 1.5 collective-permute-start.1
  15.6 2.1 collective-permute-start.2
  17.7 1.9 collective-permute-start.3
  19.6 2.1 collective-permute-start.4
  21.7 1.9 collective-permute-start.5
  23.6 1.6 collective-permute-done.3.refs_5_
  25.2 2.6 %collective-permute-done.4.refs_6_ = bf16[256,256]{1,0:T(8,128)(2,1)S(1)} collective-permute-done((bf16[256,256]{1,0:T(8,128)(2,1)}, bf16[256,256]{1,0:T(8,128)(2,1)S(1)}, u32[]{:S(2)}, u32[]{:S(2)}) %collective-permute-start.4) | collective-permute-done | bytes 131104 | tf_op jit(solution)/shard_map/ppermute | solution.py:360
  27.8 1.2 collective-permute-done.5.refs_7_
  28.9 0.9 copy-done.7
  29.9 0.9 copy-done.8
  30.8 0.1 collective-permute-start.6
  30.9 0.5 collective-permute-start.7
  31.4 0.7 collective-permute-start.10
  32.1 2.6 %collective-permute-start.11 = (bf16[1024,256]{1,0:T(8,128)(2,1)S(1)}, bf16[1024,256]{1,0:T(8,128)(2,1)S(1)}, u32[]{:S(2)}, u32[]{:S(2)}) collective-permute-start(bf16[1024,256]{1,0:T(8,128)(2,1)S(1)} %get-tuple-element.48.refs_2_), channel_id=1, source_target_pairs={{0,24},{4,28},{8,0},{12,4},{16,8},{20,12},{24,16},{28,20},{32,56},... | collective-permute-start | bytes 1572872 | tf_op jit(solution)/shard_map/ppermute | solution.py:360
  34.7 0.8 collective-permute-start.8
  35.4 2.5 %collective-permute-start.9 = (bf16[1024,256]{1,0:T(8,128)(2,1)S(1)}, bf16[1024,256]{1,0:T(8,128)(2,1)S(1)}, u32[]{:S(2)}, u32[]{:S(2)}) collective-permute-start(bf16[1024,256]{1,0:T(8,128)(2,1)S(1)} %get-tuple-element.47.refs_1_), channel_id=1, source_target_pairs={{0,96},{4,100},{8,104},{12,108},{16,112},{20,116},{24,120},{28,124... | collective-permute-start | bytes 1572872 | tf_op jit(solution)/shard_map/ppermute | solution.py:360
  37.9 1.0 collective-permute-start.12
  38.9 0.9 copy-done.10
  39.9 6.2 %flash_first.1 = (f32[1024,128]{1,0:T(8,128)S(1)}, f32[1024,256]{1,0:T(8,128)S(1)}) custom-call(bf16[1024,128]{1,0:T(8,128)(2,1)S(1)} %copy-done.10, bf16[1024,256]{1,0:T(8,128)(2,1)S(1)} %get-tuple-element.47.refs_1_, bf16[1024,256]{1,0:T(8,128)(2,1)S(1)} %get-tuple-element.48.refs_2_, bf16[1024,256]{1,0:T(8,128)(2,1)S(1)} %collective-permute-done.6.refs_3_, ...), custom_call_target="tpu_custom_call" | custom-call | flops 2147483648 | bytes 2097152 | tf_op jit(solution)/shard_map/flash_first/pallas_call | solution.py:191
  46.1 4.5 %collective-permute-done.10.refs_3_ = bf16[1024,256]{1,0:T(8,128)(2,1)S(1)} collective-permute-done((bf16[1024,256]{1,0:T(8,128)(2,1)S(1)}, bf16[1024,256]{1,0:T(8,128)(2,1)S(1)}, u32[]{:S(2)}, u32[]{:S(2)}) %collective-permute-start.10) | collective-permute-done | bytes 524320 | tf_op jit(solution)/shard_map/ppermute | solution.py:360
  50.6 0.8 collective-permute-start.13
  51.4 0.5 collective-permute-done.8.refs_1_
  51.9 2.7 %collective-permute-done.9.refs_2_ = bf16[1024,256]{1,0:T(8,128)(2,1)S(1)} collective-permute-done((bf16[1024,256]{1,0:T(8,128)(2,1)S(1)}, bf16[1024,256]{1,0:T(8,128)(2,1)S(1)}, u32[]{:S(2)}, u32[]{:S(2)}) %collective-permute-start.9) | collective-permute-done | bytes 524320 | tf_op jit(solution)/shard_map/ppermute | solution.py:360
  54.6 0.5 collective-permute-start.17
  55.1 16.0 %collective-permute-done.12.refs_1_ = bf16[1024,256]{1,0:T(8,128)(2,1)S(1)} collective-permute-done((bf16[1024,256]{1,0:T(8,128)(2,1)S(1)}, bf16[1024,256]{1,0:T(8,128)(2,1)S(1)}, u32[]{:S(2)}, u32[]{:S(2)}) %collective-permute-start.12) | collective-permute-done | bytes 524320 | tf_op jit(solution)/shard_map/ppermute | solution.py:360
  71.1 6.2 %collective-permute-done.13.refs_2_ = bf16[1024,256]{1,0:T(8,128)(2,1)S(1)} collective-permute-done((bf16[1024,256]{1,0:T(8,128)(2,1)S(1)}, bf16[1024,256]{1,0:T(8,128)(2,1)S(1)}, u32[]{:S(2)}, u32[]{:S(2)}) %collective-permute-start.13) | collective-permute-done | bytes 524320 | tf_op jit(solution)/shard_map/ppermute | solution.py:360
  77.2 2.7 %collective-permute-start.20 = (bf16[256,2048]{1,0:T(8,128)(2,1)}, bf16[256,2048]{1,0:T(8,128)(2,1)S(1)}, u32[]{:S(2)}, u32[]{:S(2)}) collective-permute-start(bf16[256,2048]{1,0:T(8,128)(2,1)} %get-tuple-element.67.refs_4_), channel_id=1, source_target_pairs={{0,3},{1,0},{2,1},{3,2},{4,7},{5,4},{6,5},{7,6},{8,11},{9,8},{10,9... | collective-permute-start | bytes 3145736 | tf_op jit(solution)/shard_map/ppermute | solution.py:347
  79.9 0.8 collective-permute-start.21
  80.8 0.9 collective-permute-start.22
  81.6 6.9 %flash_more.2 = (f32[1024,128]{1,0:T(8,128)S(1)}, f32[1024,256]{1,0:T(8,128)S(1)}) custom-call(bf16[1024,128]{1,0:T(8,128)(2,1)S(1)} %copy-done.10, bf16[1024,256]{1,0:T(8,128)(2,1)S(1)} %collective-permute-done.8.refs_1_, bf16[1024,256]{1,0:T(8,128)(2,1)S(1)} %collective-permute-done.9.refs_2_, bf16[1024,256]{1,0:T(8,128)(2,1)S(1)} %collective-permute-done.10.refs_3_, ...), custom_call_target="tpu_custom_call" | custom-call | flops 2147483648 | bytes 2097152 | tf_op jit(solution)/shard_map/flash_more/pallas_call | solution.py:191
  88.6 0.1 collective-permute-start.14
  88.7 0.5 collective-permute-start.15
  89.2 6.9 %flash_more.3 = (f32[1024,128]{1,0:T(8,128)S(1)}, f32[1024,256]{1,0:T(8,128)S(1)}) custom-call(bf16[1024,128]{1,0:T(8,128)(2,1)S(1)} %copy-done.10, bf16[1024,256]{1,0:T(8,128)(2,1)S(1)} %collective-permute-done.16.refs_1_, bf16[1024,256]{1,0:T(8,128)(2,1)S(1)} %collective-permute-done.17.refs_2_, bf16[1024,256]{1,0:T(8,128)(2,1)S(1)} %collective-permute-done.18.refs_3_, ...), custom_call_target="tpu_custom_call" | custom-call | flops 2147483648 | bytes 2097152 | tf_op jit(solution)/shard_map/flash_more/pallas_call | solution.py:191
  96.1 7.1 %flash_last.1.refs_0_ = bf16[512,256]{1,0:T(8,128)(2,1)S(1)} custom-call(bf16[1024,128]{1,0:T(8,128)(2,1)S(1)} %copy-done.10, bf16[1024,256]{1,0:T(8,128)(2,1)S(1)} %collective-permute-done.12.refs_1_, bf16[1024,256]{1,0:T(8,128)(2,1)S(1)} %collective-permute-done.13.refs_2_, bf16[1024,256]{1,0:T(8,128)(2,1)S(1)} %collective-permute-done.14.refs_3_, ...), custom_call_target="tpu_custom_call" | custom-call | flops 2147483648 | bytes 2097152 | tf_op jit(solution)/shard_map/flash_last/pallas_call | solution.py:191
  103.2 20.3 %collective-permute-done.20.refs_5_ = bf16[256,2048]{1,0:T(8,128)(2,1)S(1)} collective-permute-done((bf16[256,2048]{1,0:T(8,128)(2,1)}, bf16[256,2048]{1,0:T(8,128)(2,1)S(1)}, u32[]{:S(2)}, u32[]{:S(2)}) %collective-permute-start.20) | collective-permute-done | bytes 1048608 | tf_op jit(solution)/shard_map/ppermute | solution.py:347
  123.5 3.6 %collective-permute-done.22.refs_7_ = bf16[256,2048]{1,0:T(8,128)(2,1)S(1)} collective-permute-done((bf16[256,2048]{1,0:T(8,128)(2,1)}, bf16[256,2048]{1,0:T(8,128)(2,1)S(1)}, u32[]{:S(2)}, u32[]{:S(2)}) %collective-permute-start.22) | collective-permute-done | bytes 1048608 | tf_op jit(solution)/shard_map/ppermute | solution.py:347
  127.1 0.8 slice.9
  127.9 0.6 collective-permute-start.23
  128.5 0.8 slice.10
  129.4 0.2 collective-permute-start.27
  129.6 0.8 slice.11
  130.5 0.3 collective-permute-start.28
  130.7 0.9 collective-permute-start.24
  131.6 5.5 %collective-permute-done.23.refs_1_ = bf16[512,256]{1,0:T(8,128)(2,1)S(1)} collective-permute-done((bf16[512,256]{1,0:T(8,128)(2,1)S(1)}, bf16[512,256]{1,0:T(8,128)(2,1)S(1)}, u32[]{:S(2)}, u32[]{:S(2)}) %collective-permute-start.23) | collective-permute-done | bytes 262176 | tf_op jit(solution)/shard_map/ppermute | solution.py:347
  137.1 0.7 copy-done.5
  137.9 2.9 %collective-permute-done.24.refs_2_ = bf16[512,256]{1,0:T(8,128)(2,1)} collective-permute-done((bf16[512,256]{1,0:T(8,128)(2,1)S(1)}, bf16[512,256]{1,0:T(8,128)(2,1)}, u32[]{:S(2)}, u32[]{:S(2)}) %collective-permute-start.24) | collective-permute-done | bytes 262176 | tf_op jit(solution)/shard_map/ppermute | solution.py:347
  140.8 5.8 %collective-permute-done.25.refs_3_ = bf16[512,256]{1,0:T(8,128)(2,1)} collective-permute-done((bf16[512,256]{1,0:T(8,128)(2,1)S(1)}, bf16[512,256]{1,0:T(8,128)(2,1)}, u32[]{:S(2)}, u32[]{:S(2)}) %collective-permute-start.25) | collective-permute-done | bytes 262176 | tf_op jit(solution)/shard_map/ppermute | solution.py:347
  146.7 1.2 copy-done.1
  147.9 1.0 copy-done.2
  148.9 0.9 copy-done.6
  149.9 6.3 %project.1 = (bf16[128,2048]{1,0:T(8,128)(2,1)S(1)}, bf16[512,2048]{1,0:T(8,128)(2,1)S(1)}) custom-call(s32[2]{0:T(128)S(1)} %pad_add_fusion.place, bf16[512,256]{1,0:T(8,128)(2,1)S(1)} %flash_last.1.refs_0_, bf16[512,256]{1,0:T(8,128)(2,1)S(1)} %copy-done.6, bf16[512,256]{1,0:T(8,128)(2,1)} %collective-permute-done.24.refs_2_, ...), custom_call_target="tpu_custom_call" | custom-call | tf_op jit(solution)/shard_map/project/pallas_call | solution.py:248
  156.2 1.3 copy-done
  157.5 0.8 copy-done.3
  158.3 21.3 %units.1 = (bf16[128,2048]{1,0:T(8,128)(2,1)S(1)}, bf16[128,2048]{1,0:T(8,128)(2,1)S(1)}, bf16[128,2048]{1,0:T(8,128)(2,1)S(1)}, bf16[128,2048]{1,0:T(8,128)(2,1)S(1)}) custom-call(bf16[512,2048]{1,0:T(8,128)(2,1)} %copy-done, bf16[2048,4224]{1,0:T(8,128)(2,1)} %all-gather.2.cloned.1.call-done.w_hbm), custom_call_target="tpu_custom_call" | custom-call | tf_op jit(solution)/shard_map/units/pallas_call | solution.py:309
  179.7 2.0 collective-permute-start.30
  181.6 1.3 collective-permute-start.31
  183.0 21.4 %collective-permute-done.29 = bf16[128,2048]{1,0:T(8,128)(2,1)S(1)} collective-permute-done((bf16[128,2048]{1,0:T(8,128)(2,1)S(1)}, bf16[128,2048]{1,0:T(8,128)(2,1)S(1)}, u32[]{:S(2)}, u32[]{:S(2)}) %collective-permute-start.29) | collective-permute-done | bytes 524320 | tf_op jit(solution)/shard_map/ppermute | solution.py:347
  204.4 0.6 collective-permute-done.31
  205.0 1.2 add_convert_fusion
  (46 shorter events, 0.4 us)
Async XLA Ops:
  6.5 151.7 %all-gather.2.cloned.1.call-start = ((), (), s32[]{:S(2)}) async-start(), calls=%async_computation | async-start | bytes 17842176 | tf_op jit(solution)/shard_map/all_gather | solution.py:384
  12.3 9.4 %collective-permute-start = (bf16[256,256]{1,0:T(8,128)(2,1)}, bf16[256,256]{1,0:T(8,128)(2,1)S(1)}, u32[]{:S(2)}, u32[]{:S(2)}) collective-permute-start(bf16[256,256]{1,0:T(8,128)(2,1)} %get-tuple-element.45.refs_0_), channel_id=1, source_target_pairs={{0,8},{4,12},{8,16},{12,20},{16,24},{20,28},{24,0},{28,4},{32,40},... | collective-permute-start | bytes 393224 | tf_op jit(solution)/shard_map/ppermute | solution.py:360
  14.0 9.6 %collective-permute-start.1 = (bf16[256,256]{1,0:T(8,128)(2,1)}, bf16[256,256]{1,0:T(8,128)(2,1)S(1)}, u32[]{:S(2)}, u32[]{:S(2)}) collective-permute-start(bf16[256,256]{1,0:T(8,128)(2,1)} %get-tuple-element.45.refs_0_), channel_id=1, source_target_pairs={{0,24},{4,28},{8,0},{12,4},{16,8},{20,12},{24,16},{28,20},{32,56},... | collective-permute-start | bytes 393224 | tf_op jit(solution)/shard_map/ppermute | solution.py:360
  15.6 8.0 %collective-permute-start.2 = (bf16[256,256]{1,0:T(8,128)(2,1)}, bf16[256,256]{1,0:T(8,128)(2,1)S(1)}, u32[]{:S(2)}, u32[]{:S(2)}) collective-permute-start(bf16[256,256]{1,0:T(8,128)(2,1)} %get-tuple-element.45.refs_0_), channel_id=1, source_target_pairs={{0,16},{4,20},{8,24},{12,28},{16,0},{20,4},{24,8},{28,12},{32,48},... | collective-permute-start | bytes 393224 | tf_op jit(solution)/shard_map/ppermute | solution.py:360
  17.7 7.5 %collective-permute-start.3 = (bf16[256,256]{1,0:T(8,128)(2,1)}, bf16[256,256]{1,0:T(8,128)(2,1)S(1)}, u32[]{:S(2)}, u32[]{:S(2)}) collective-permute-start(bf16[256,256]{1,0:T(8,128)(2,1)} %get-tuple-element.46.refs_4_), channel_id=1, source_target_pairs={{0,32},{4,36},{8,40},{12,44},{16,48},{20,52},{24,56},{28,60},{32,6... | collective-permute-start | bytes 393224 | tf_op jit(solution)/shard_map/ppermute | solution.py:360
  19.6 8.2 %collective-permute-start.4 = (bf16[256,256]{1,0:T(8,128)(2,1)}, bf16[256,256]{1,0:T(8,128)(2,1)S(1)}, u32[]{:S(2)}, u32[]{:S(2)}) collective-permute-start(bf16[256,256]{1,0:T(8,128)(2,1)} %get-tuple-element.46.refs_4_), channel_id=1, source_target_pairs={{0,96},{4,100},{8,104},{12,108},{16,112},{20,116},{24,120},{28,124... | collective-permute-start | bytes 393224 | tf_op jit(solution)/shard_map/ppermute | solution.py:360
  21.7 7.2 %collective-permute-start.5 = (bf16[256,256]{1,0:T(8,128)(2,1)}, bf16[256,256]{1,0:T(8,128)(2,1)S(1)}, u32[]{:S(2)}, u32[]{:S(2)}) collective-permute-start(bf16[256,256]{1,0:T(8,128)(2,1)} %get-tuple-element.46.refs_4_), channel_id=1, source_target_pairs={{0,64},{4,68},{8,72},{12,76},{16,80},{20,84},{24,88},{28,92},{32,9... | collective-permute-start | bytes 393224 | tf_op jit(solution)/shard_map/ppermute | solution.py:360
  28.9 0.9 copy-start.7
  29.9 0.9 copy-start.8
  30.8 4.6 %collective-permute-start.6 = (bf16[1024,256]{1,0:T(8,128)(2,1)S(1)}, bf16[1024,256]{1,0:T(8,128)(2,1)S(1)}, u32[]{:S(2)}, u32[]{:S(2)}) collective-permute-start(bf16[1024,256]{1,0:T(8,128)(2,1)S(1)} %get-tuple-element.47.refs_1_), channel_id=1, source_target_pairs={{0,4},{4,0},{8,12},{12,8},{16,20},{20,16},{24,28},{28,24},{32,36},... | collective-permute-start | bytes 1572872 | tf_op jit(solution)/shard_map/ppermute | solution.py:360
  30.9 7.0 %collective-permute-start.7 = (bf16[1024,256]{1,0:T(8,128)(2,1)S(1)}, bf16[1024,256]{1,0:T(8,128)(2,1)S(1)}, u32[]{:S(2)}, u32[]{:S(2)}) collective-permute-start(bf16[1024,256]{1,0:T(8,128)(2,1)S(1)} %get-tuple-element.48.refs_2_), channel_id=1, source_target_pairs={{0,4},{4,0},{8,12},{12,8},{16,20},{20,16},{24,28},{28,24},{32,36},... | collective-permute-start | bytes 1572872 | tf_op jit(solution)/shard_map/ppermute | solution.py:360
  31.4 19.2 %collective-permute-start.10 = (bf16[1024,256]{1,0:T(8,128)(2,1)S(1)}, bf16[1024,256]{1,0:T(8,128)(2,1)S(1)}, u32[]{:S(2)}, u32[]{:S(2)}) collective-permute-start(bf16[1024,256]{1,0:T(8,128)(2,1)S(1)} %get-tuple-element.48.refs_2_), channel_id=1, source_target_pairs={{0,8},{4,12},{8,16},{12,20},{16,24},{20,28},{24,0},{28,4},{32,40},... | collective-permute-start | bytes 1572872 | tf_op jit(solution)/shard_map/ppermute | solution.py:360
  32.1 19.3 %collective-permute-start.11 = (bf16[1024,256]{1,0:T(8,128)(2,1)S(1)}, bf16[1024,256]{1,0:T(8,128)(2,1)S(1)}, u32[]{:S(2)}, u32[]{:S(2)}) collective-permute-start(bf16[1024,256]{1,0:T(8,128)(2,1)S(1)} %get-tuple-element.48.refs_2_), channel_id=1, source_target_pairs={{0,24},{4,28},{8,0},{12,4},{16,8},{20,12},{24,16},{28,20},{32,56},... | collective-permute-start | bytes 1572872 | tf_op jit(solution)/shard_map/ppermute | solution.py:360
  34.7 17.2 %collective-permute-start.8 = (bf16[1024,256]{1,0:T(8,128)(2,1)S(1)}, bf16[1024,256]{1,0:T(8,128)(2,1)S(1)}, u32[]{:S(2)}, u32[]{:S(2)}) collective-permute-start(bf16[1024,256]{1,0:T(8,128)(2,1)S(1)} %get-tuple-element.47.refs_1_), channel_id=1, source_target_pairs={{0,32},{4,36},{8,40},{12,44},{16,48},{20,52},{24,56},{28,60},{32,6... | collective-permute-start | bytes 1572872 | tf_op jit(solution)/shard_map/ppermute | solution.py:360
  35.4 19.2 %collective-permute-start.9 = (bf16[1024,256]{1,0:T(8,128)(2,1)S(1)}, bf16[1024,256]{1,0:T(8,128)(2,1)S(1)}, u32[]{:S(2)}, u32[]{:S(2)}) collective-permute-start(bf16[1024,256]{1,0:T(8,128)(2,1)S(1)} %get-tuple-element.47.refs_1_), channel_id=1, source_target_pairs={{0,96},{4,100},{8,104},{12,108},{16,112},{20,116},{24,120},{28,124... | collective-permute-start | bytes 1572872 | tf_op jit(solution)/shard_map/ppermute | solution.py:360
  37.9 33.2 %collective-permute-start.12 = (bf16[1024,256]{1,0:T(8,128)(2,1)S(1)}, bf16[1024,256]{1,0:T(8,128)(2,1)S(1)}, u32[]{:S(2)}, u32[]{:S(2)}) collective-permute-start(bf16[1024,256]{1,0:T(8,128)(2,1)S(1)} %get-tuple-element.47.refs_1_), channel_id=1, source_target_pairs={{0,64},{4,68},{8,72},{12,76},{16,80},{20,84},{24,88},{28,92},{32,9... | collective-permute-start | bytes 1572872 | tf_op jit(solution)/shard_map/ppermute | solution.py:360
  38.9 0.9 copy-start.10
  39.9 106.8 %copy-start.9 = (f32[2048]{0:T(1024)S(1)}, f32[2048]{0:T(1024)}, u32[]{:S(2)}) copy-start(f32[2048]{0:T(1024)} %param.18) | copy-start | bytes 24580
  50.6 26.6 %collective-permute-start.13 = (bf16[1024,256]{1,0:T(8,128)(2,1)S(1)}, bf16[1024,256]{1,0:T(8,128)(2,1)S(1)}, u32[]{:S(2)}, u32[]{:S(2)}) collective-permute-start(bf16[1024,256]{1,0:T(8,128)(2,1)S(1)} %get-tuple-element.48.refs_2_), channel_id=1, source_target_pairs={{0,16},{4,20},{8,24},{12,28},{16,0},{20,4},{24,8},{28,12},{32,48},... | collective-permute-start | bytes 1572872 | tf_op jit(solution)/shard_map/ppermute | solution.py:360
  54.6 25.3 %collective-permute-start.16 = (bf16[1024,256]{1,0:T(8,128)(2,1)S(1)}, bf16[1024,256]{1,0:T(8,128)(2,1)S(1)}, u32[]{:S(2)}, u32[]{:S(2)}) collective-permute-start(bf16[1024,256]{1,0:T(8,128)(2,1)S(1)} %collective-permute-done.8.refs_1_), channel_id=1, source_target_pairs={{0,4},{4,0},{8,12},{12,8},{16,20},{20,16},{24,28},{28,24},{32,36},... | collective-permute-start | bytes 1572872 | tf_op jit(solution)/shard_map/ppermute | solution.py:360
  54.6 26.2 %collective-permute-start.17 = (bf16[1024,256]{1,0:T(8,128)(2,1)S(1)}, bf16[1024,256]{1,0:T(8,128)(2,1)S(1)}, u32[]{:S(2)}, u32[]{:S(2)}) collective-permute-start(bf16[1024,256]{1,0:T(8,128)(2,1)S(1)} %collective-permute-done.9.refs_2_), channel_id=1, source_target_pairs={{0,4},{4,0},{8,12},{12,8},{16,20},{20,16},{24,28},{28,24},{32,36},... | collective-permute-start | bytes 1572872 | tf_op jit(solution)/shard_map/ppermute | solution.py:360
  55.1 33.5 %collective-permute-start.18 = (bf16[1024,256]{1,0:T(8,128)(2,1)S(1)}, bf16[1024,256]{1,0:T(8,128)(2,1)S(1)}, u32[]{:S(2)}, u32[]{:S(2)}) collective-permute-start(bf16[1024,256]{1,0:T(8,128)(2,1)S(1)} %collective-permute-done.10.refs_3_), channel_id=1, source_target_pairs={{0,4},{4,0},{8,12},{12,8},{16,20},{20,16},{24,28},{28,24},{32,36},... | collective-permute-start | bytes 1572872 | tf_op jit(solution)/shard_map/ppermute | solution.py:360
  71.1 17.6 %collective-permute-start.19 = (bf16[1024,256]{1,0:T(8,128)(2,1)S(1)}, bf16[1024,256]{1,0:T(8,128)(2,1)S(1)}, u32[]{:S(2)}, u32[]{:S(2)}) collective-permute-start(bf16[1024,256]{1,0:T(8,128)(2,1)S(1)} %collective-permute-done.11.refs_4_), channel_id=1, source_target_pairs={{0,4},{4,0},{8,12},{12,8},{16,20},{20,16},{24,28},{28,24},{32,36},... | collective-permute-start | bytes 1572872 | tf_op jit(solution)/shard_map/ppermute | solution.py:360
  77.2 46.3 %collective-permute-start.20 = (bf16[256,2048]{1,0:T(8,128)(2,1)}, bf16[256,2048]{1,0:T(8,128)(2,1)S(1)}, u32[]{:S(2)}, u32[]{:S(2)}) collective-permute-start(bf16[256,2048]{1,0:T(8,128)(2,1)} %get-tuple-element.67.refs_4_), channel_id=1, source_target_pairs={{0,3},{1,0},{2,1},{3,2},{4,7},{5,4},{6,5},{7,6},{8,11},{9,8},{10,9... | collective-permute-start | bytes 3145736 | tf_op jit(solution)/shard_map/ppermute | solution.py:347
  79.9 43.6 %collective-permute-start.21 = (bf16[256,2048]{1,0:T(8,128)(2,1)}, bf16[256,2048]{1,0:T(8,128)(2,1)S(1)}, u32[]{:S(2)}, u32[]{:S(2)}) collective-permute-start(bf16[256,2048]{1,0:T(8,128)(2,1)} %get-tuple-element.67.refs_4_), channel_id=1, source_target_pairs={{0,2},{1,3},{2,0},{3,1},{4,6},{5,7},{6,4},{7,5},{8,10},{9,11},{10,... | collective-permute-start | bytes 3145736 | tf_op jit(solution)/shard_map/ppermute | solution.py:347
  80.8 46.3 %collective-permute-start.22 = (bf16[256,2048]{1,0:T(8,128)(2,1)}, bf16[256,2048]{1,0:T(8,128)(2,1)S(1)}, u32[]{:S(2)}, u32[]{:S(2)}) collective-permute-start(bf16[256,2048]{1,0:T(8,128)(2,1)} %get-tuple-element.67.refs_4_), channel_id=1, source_target_pairs={{0,1},{1,2},{2,3},{3,0},{4,5},{5,6},{6,7},{7,4},{8,9},{9,10},{10,1... | collective-permute-start | bytes 3145736 | tf_op jit(solution)/shard_map/ppermute | solution.py:347
  88.6 7.5 %collective-permute-start.14 = (bf16[1024,256]{1,0:T(8,128)(2,1)S(1)}, bf16[1024,256]{1,0:T(8,128)(2,1)S(1)}, u32[]{:S(2)}, u32[]{:S(2)}) collective-permute-start(bf16[1024,256]{1,0:T(8,128)(2,1)S(1)} %collective-permute-done.12.refs_1_), channel_id=1, source_target_pairs={{0,4},{4,0},{8,12},{12,8},{16,20},{20,16},{24,28},{28,24},{32,36},... | collective-permute-start | bytes 1572872 | tf_op jit(solution)/shard_map/ppermute | solution.py:360
  88.7 7.4 %collective-permute-start.15 = (bf16[1024,256]{1,0:T(8,128)(2,1)S(1)}, bf16[1024,256]{1,0:T(8,128)(2,1)S(1)}, u32[]{:S(2)}, u32[]{:S(2)}) collective-permute-start(bf16[1024,256]{1,0:T(8,128)(2,1)S(1)} %collective-permute-done.13.refs_2_), channel_id=1, source_target_pairs={{0,4},{4,0},{8,12},{12,8},{16,20},{20,16},{24,28},{28,24},{32,36},... | collective-permute-start | bytes 1572872 | tf_op jit(solution)/shard_map/ppermute | solution.py:360
  127.9 18.7 %collective-permute-start.26 = (bf16[128,2048]{1,0:T(8,128)(2,1)}, bf16[128,2048]{1,0:T(8,128)(2,1)}, u32[]{:S(2)}, u32[]{:S(2)}) collective-permute-start(bf16[128,2048]{1,0:T(8,128)(2,1)} %slice.9), channel_id=1, source_target_pairs={{0,4},{4,0},{8,12},{12,8},{16,20},{20,16},{24,28},{28,24},{32,36},... | collective-permute-start | bytes 1572872 | tf_op jit(solution)/shard_map/ppermute | solution.py:360
  127.9 9.2 %collective-permute-start.23 = (bf16[512,256]{1,0:T(8,128)(2,1)S(1)}, bf16[512,256]{1,0:T(8,128)(2,1)S(1)}, u32[]{:S(2)}, u32[]{:S(2)}) collective-permute-start(bf16[512,256]{1,0:T(8,128)(2,1)S(1)} %flash_last.1.refs_0_), channel_id=1, source_target_pairs={{0,3},{1,0},{2,1},{3,2},{4,7},{5,4},{6,5},{7,6},{8,11},{9,8},{10,9... | collective-permute-start | bytes 786440 | tf_op jit(solution)/shard_map/ppermute | solution.py:347
  129.4 17.2 %collective-permute-start.27 = (bf16[128,2048]{1,0:T(8,128)(2,1)}, bf16[128,2048]{1,0:T(8,128)(2,1)}, u32[]{:S(2)}, u32[]{:S(2)}) collective-permute-start(bf16[128,2048]{1,0:T(8,128)(2,1)} %slice.10), channel_id=1, source_target_pairs={{0,4},{4,0},{8,12},{12,8},{16,20},{20,16},{24,28},{28,24},{32,36},... | collective-permute-start | bytes 1572872 | tf_op jit(solution)/shard_map/ppermute | solution.py:360
  130.5 16.2 %collective-permute-start.28 = (bf16[128,2048]{1,0:T(8,128)(2,1)}, bf16[128,2048]{1,0:T(8,128)(2,1)}, u32[]{:S(2)}, u32[]{:S(2)}) collective-permute-start(bf16[128,2048]{1,0:T(8,128)(2,1)} %slice.11), channel_id=1, source_target_pairs={{0,4},{4,0},{8,12},{12,8},{16,20},{20,16},{24,28},{28,24},{32,36},... | collective-permute-start | bytes 1572872 | tf_op jit(solution)/shard_map/ppermute | solution.py:360
  130.7 10.0 %collective-permute-start.24 = (bf16[512,256]{1,0:T(8,128)(2,1)S(1)}, bf16[512,256]{1,0:T(8,128)(2,1)}, u32[]{:S(2)}, u32[]{:S(2)}) collective-permute-start(bf16[512,256]{1,0:T(8,128)(2,1)S(1)} %flash_last.1.refs_0_), channel_id=1, source_target_pairs={{0,2},{1,3},{2,0},{3,1},{4,6},{5,7},{6,4},{7,5},{8,10},{9,11},{10,... | collective-permute-start | bytes 786440 | tf_op jit(solution)/shard_map/ppermute | solution.py:347
  137.1 0.7 copy-start.5
  137.8 8.8 %collective-permute-start.25 = (bf16[512,256]{1,0:T(8,128)(2,1)S(1)}, bf16[512,256]{1,0:T(8,128)(2,1)}, u32[]{:S(2)}, u32[]{:S(2)}) collective-permute-start(bf16[512,256]{1,0:T(8,128)(2,1)S(1)} %flash_last.1.refs_0_), channel_id=1, source_target_pairs={{0,1},{1,2},{2,3},{3,0},{4,5},{5,6},{6,7},{7,4},{8,9},{9,10},{10,1... | collective-permute-start | bytes 786440 | tf_op jit(solution)/shard_map/ppermute | solution.py:347
  146.6 1.2 copy-start.1
  147.9 1.0 copy-start.2
  148.9 0.9 copy-start.6
  156.2 1.3 copy-start
  157.5 0.8 copy-start.3
  158.3 46.7 %copy-start.4 = (bf16[128,2048]{1,0:T(8,128)(2,1)S(1)}, bf16[128,2048]{1,0:T(8,128)(2,1)}, u32[]{:S(2)}) copy-start(bf16[128,2048]{1,0:T(8,128)(2,1)} %copy-done.3) | copy-start | bytes 1572868
  179.6 24.8 %collective-permute-start.29 = (bf16[128,2048]{1,0:T(8,128)(2,1)S(1)}, bf16[128,2048]{1,0:T(8,128)(2,1)S(1)}, u32[]{:S(2)}, u32[]{:S(2)}) collective-permute-start(bf16[128,2048]{1,0:T(8,128)(2,1)S(1)} %get-tuple-element.76), channel_id=1, source_target_pairs={{0,1},{1,2},{2,3},{3,0},{4,5},{5,6},{6,7},{7,4},{8,9},{9,10},{10,1... | collective-permute-start | bytes 1572872 | tf_op jit(solution)/shard_map/ppermute | solution.py:347
  179.7 24.7 %collective-permute-start.30 = (bf16[128,2048]{1,0:T(8,128)(2,1)S(1)}, bf16[128,2048]{1,0:T(8,128)(2,1)S(1)}, u32[]{:S(2)}, u32[]{:S(2)}) collective-permute-start(bf16[128,2048]{1,0:T(8,128)(2,1)S(1)} %get-tuple-element.77), channel_id=1, source_target_pairs={{0,2},{1,3},{2,0},{3,1},{4,6},{5,7},{6,4},{7,5},{8,10},{9,11},{10,... | collective-permute-start | bytes 1572872 | tf_op jit(solution)/shard_map/ppermute | solution.py:347
  181.6 23.3 %collective-permute-start.31 = (bf16[128,2048]{1,0:T(8,128)(2,1)S(1)}, bf16[128,2048]{1,0:T(8,128)(2,1)S(1)}, u32[]{:S(2)}, u32[]{:S(2)}) collective-permute-start(bf16[128,2048]{1,0:T(8,128)(2,1)S(1)} %get-tuple-element.78), channel_id=1, source_target_pairs={{0,3},{1,0},{2,1},{3,2},{4,7},{5,4},{6,5},{7,6},{8,11},{9,8},{10,9... | collective-permute-start | bytes 1572872 | tf_op jit(solution)/shard_map/ppermute | solution.py:347
Sparse Core Ops, SparseCore 0:
  12.4 89.8 all-gather.1

commit v4 on v3

--- a/solution.py
+++ b/solution.py
@@ -206,14 +206,14 @@
     )(q, *kv, *([] if first else state))
 
 
-def project_kernel(place, *refs, parts, tile):
+def project_kernel(place, *refs, parts, tile, res_rows):
     att = refs[0:parts]
     sent = refs[parts : 2 * parts]
     swapped = refs[2 * parts : 3 * parts]
     gain_ref, own_ref, norm_ref, up_ref = refs[3 * parts :]
     step = pl.program_id(0)
-    half = swapped[0].shape[0]
-    sub = sent[0].shape[0] - half
+    sub = res_rows
+    half = sent[0].shape[0] - sub
     cols = pl.ds(pl.multiple_of(step * tile, tile), tile)
     total = None
     for a, w, o in zip(att, sent, swapped):
@@ -222,7 +222,7 @@
             rows = pl.ds(pl.multiple_of(((place[0] + r) % parts) * sub, sub), sub)
             halves = [a[rows, pl.ds(pl.multiple_of(c * half, half), half)] for c in (place[1], 1 - place[1])]
             rolled.append(jnp.concatenate(halves, axis=1))
-        weight = jnp.concatenate([w[0:half, :], o[...]], axis=0)
+        weight = jnp.concatenate([w[0:half, :], o[0:half, :]], axis=0)
         part = jnp.dot(jnp.concatenate(rolled, axis=0), weight, preferred_element_type=f32).astype(bf16).astype(f32)
         total = part if total is None else total + part
     for r in range(parts):
@@ -246,7 +246,7 @@
     half = swapped[0].shape[0]
     sub = both - half
     return pl.pallas_call(
-        functools.partial(project_kernel, parts=parts, tile=tile),
+        functools.partial(project_kernel, parts=parts, tile=tile, res_rows=sub),
         grid_spec=pltpu.PrefetchScalarGridSpec(
             num_scalar_prefetch=1,
             grid=(width // tile,),
@@ -266,48 +266,69 @@
     )(place, *att, *sent, *swapped, gain[None, :])
 
 
-def unit_kernel(x_ref, w_hbm, *refs, units, tile, rows, ahead=3):
+def unit_kernel(x_ref, w_hbm, *refs, units, tile, rows, split, ahead):
     outs = refs[:-4]
     pair_ref, down_ref, h_ref, sems = refs[-4:]
     count = units // tile
     blocks = down_ref.shape[0]
-
-    def gate_copy(n):
-        return pltpu.make_async_copy(w_hbm.at[:, pl.ds(2 * n * tile, 2 * tile)], pair_ref.at[n], sems.at[n])
-
-    def down_copy(n):
-        source = w_hbm.at[pl.ds(n * rows, rows), pl.ds(2 * units, units)]
-        return pltpu.make_async_copy(source, down_ref.at[n], sems.at[count + n])
-
-    copies = [gate_copy(n) for n in range(count)] + [down_copy(n) for n in range(blocks)]
+    width = x_ref.shape[1]
+
+    def tile_copies(n):
+        found = []
+        for m in range(split):
+            if n < count:
+                part = pl.ds(m * width // split, width // split)
+                source = w_hbm.at[part, pl.ds(2 * n * tile, 2 * tile)]
+                target = pair_ref.at[n, part, :]
+            else:
+                b = n - count
+                source = w_hbm.at[pl.ds(b * rows + m * rows // split, rows // split), pl.ds(2 * units, units)]
+                target = down_ref.at[b, pl.ds(m * rows // split, rows // split), :]
+            found.append(pltpu.make_async_copy(source, target, sems.at[n * split + m]))
+        return found
+
+    copies = [tile_copies(n) for n in range(count + blocks)]
+
+    def begin(n):
+        if n < count + blocks:
+            for c in copies[n]:
+                c.start()
 
     def arrive(n):
-        copies[n].wait()
-        if n + ahead < len(copies):
-            copies[n + ahead].start()
+        for c in copies[n]:
+            c.wait()
+        begin(n + ahead)
+
+    def product(n):
+        return jnp.dot(x_ref[...], pair_ref[n], preferred_element_type=f32)
 
     for n in range(ahead):
-        copies[n].start()
+        begin(n)
+    arrive(0)
+    following = product(0)
     for n in range(count):
-        arrive(n)
-        r = jnp.dot(x_ref[...], pair_ref[n], preferred_element_type=f32)
+        arrive(n + 1)
+        r = following
+        if n + 1 < count:
+            following = product(n + 1)
         gate = r[:, 0:tile]
         h_ref[:, n * tile : (n + 1) * tile] = (gate / (1.0 + jnp.exp(-gate)) * r[:, tile:]).astype(bf16)
     sub = outs[0].shape[0]
     for n in range(blocks):
-        arrive(count + n)
+        if n > 0:
+            arrive(count + n)
         y = lax.dot_general(h_ref[...], down_ref[n], (((1,), (1,)), ((), ())), preferred_element_type=f32).astype(bf16)
         for p, out in enumerate(outs):
             out[:, n * rows : (n + 1) * rows] = y[p * sub : (p + 1) * sub, :]
 
 
-def feed_forward(x, weights, units, parts, tile=128, rows=512):
+def feed_forward(x, weights, units, parts, tile=128, rows=512, split=4, ahead=4):
     tok, width = x.shape
     count = units // tile
     blocks = width // rows
     sub = tok // parts
     return pl.pallas_call(
-        functools.partial(unit_kernel, units=units, tile=tile, rows=rows),
+        functools.partial(unit_kernel, units=units, tile=tile, rows=rows, split=split, ahead=ahead),
         in_specs=[pl.BlockSpec(memory_space=pltpu.VMEM), pl.BlockSpec(memory_space=pltpu.HBM)],
         out_specs=[pl.BlockSpec(memory_space=pltpu.VMEM)] * parts,
         out_shape=[jax.ShapeDtypeStruct((sub, width), bf16)] * parts,
@@ -315,7 +336,7 @@
             pltpu.VMEM((count, width, 2 * tile), bf16),
             pltpu.VMEM((blocks, rows, units), bf16),
             pltpu.VMEM((tok, units), bf16),
-            pltpu.SemaphoreType.DMA((count + blocks,)),
+            pltpu.SemaphoreType.DMA(((count + blocks) * split,)),
         ],
         compiler_params=pltpu.CompilerParams(vmem_limit_bytes=50 << 20),
         name="units",
@@ -383,14 +404,20 @@
     )
     weights = lax.all_gather(woven, "sp", axis=0, tiled=True)
 
-    a_line, b_line = lined_up(
-        [kv_a] + [moved(kv_a, y=d) for d in (1, -1, 2)], [kv_b] + [moved(kv_b, z=d) for d in (1, -1, 2)]
-    )
+    a_parts = [kv_a]
+    b_parts = [kv_b]
+    for d in (1, -1, 2):
+        a_parts.append(moved(kv_a, y=d))
+    for d in (1, -1, 2):
+        b_parts.append(moved(kv_b, z=d))
+    a_line, b_line = lined_up(a_parts, b_parts)
     near = [moved(a_line, z=1), moved(a_line, z=-1), moved(b_line, y=1), moved(b_line, y=-1)]
     far = [moved(a_line, z=2), moved(b_line, y=2)]
     lines = [a_line, b_line, moved(a_line, other=True), moved(b_line, other=True)]
 
-    sent = [payload] + [shifted(payload, -r) for r in range(1, parts)]
+    sent = [payload]
+    for r in range(1, parts):
+        sent.append(shifted(payload, -r))
 
     state = flash(q, lines, None, tok, False)
     state, near = lax.optimization_barrier((state, near))
@@ -399,9 +426,9 @@
     state, far = lax.optimization_barrier((state, far))
     far_swapped = [moved(v, other=True) for v in far]
     state = flash(q, near_swapped, state, tok, False)
+    state, sent = lax.optimization_barrier((state, sent))
+    swapped = [kept] + [moved(s, other=True) for s in sent[1:]]
     attended = flash(q, far + far_swapped, state, tok, True)
-    attended, sent = lax.optimization_barrier((attended, sent))
-    swapped = [kept] + [moved(s[: kept.shape[0]], other=True) for s in sent[1:]]
 
     att_parts = [attended] + [shifted(attended, -r) for r in range(1, parts)]
     own_rows, normed = project(place, att_parts, sent, swapped, mix_gain)
@@ -426,6 +453,4 @@
         P("sp", "tp"),
         P("tp", "sp"),
     )
-    return jax.shard_map(
-        on_device, mesh=mesh, in_specs=placed, out_specs=P(("sp", "tp"), None), check_vma=False
-    )
+    return jax.shard_map(on_device, mesh=mesh, in_specs=placed, out_specs=P(("sp", "tp"), None), check_vma=False)

time: 214 us -> 211 us (0.986)
  the two profiles are of different devices: /device:TPU:0 before, /device:TPU:8 now
where the time goes in v4:
time: 211 us; the launch traced here: 207 us
  waiting for transfers between devices  87.3 us (41%)
  Pallas kernels  59.8 us (28%)
  starting transfers between devices  36.8 us (17%)
  between operations  13.6 us (6%)
  local copies, waits for them, and re-layouts  7.54 us (4%)
  other arithmetic  2.47 us (1%)
    ppermute x9, waiting for transfers between devices, shifted(): lax.ppermute(value, 'tp', [(i, (i + by) % count) for i in range(count)])  58.8 us
    ppermute x23, waiting for transfers between devices, moved(): return lax.ppermute(value, 'sp', pairs)  28.4 us
    pallas_call x4, Pallas kernels, flash(): pl.pallas_call(functools.partial(flash_kernel, pieces=pieces, scale=head_...  27.2 us
    pallas_call x1, Pallas kernels, feed_forward(): pl.pallas_call(functools.partial(unit_kernel, units=units, tile=tile, row...  21.7 us
    ppermute x23, starting transfers between devices, moved(): return lax.ppermute(value, 'sp', pairs)  20.5 us
    ppermute x9, starting transfers between devices, shifted(): lax.ppermute(value, 'tp', [(i, (i + by) % count) for i in range(count)])  16.3 us
    unnamed x22, local copies, waits for them, and re-layouts  7.53 us
    pallas_call x1, Pallas kernels, project(): pl.pallas_call(functools.partial(project_kernel, parts=parts, tile=tile,...  6.35 us
  transfers between devices with their start and end apart: 33, of which 12 were waited for; matrix products, arithmetic and copies ran while one was open for 0% of the time, Pallas kernels for 16%

profile of v4, /device:TPU:8, one launch (start us, length us, event | category | flops | bytes accessed | tf_op | source)
XLA Modules:
  0.0 207.5 jit_solution(6445948481916119613)
XLA Ops:
  6.6 0.1 add_convert_fusion.1
  6.7 0.2 multiply_sine_fusion
  6.9 0.1 negate_select_fusion.1
  7.0 0.8 pad_maximum_fusion
  7.8 4.5 %prepare.1 = (bf16[1024,128]{1,0:T(8,128)(2,1)}, bf16[256,256]{1,0:T(8,128)(2,1)}, bf16[256,256]{1,0:T(8,128)(2,1)}, bf16[64,4224]{1,0:T(8,128)(2,1)}, bf16[256,...) custom-call(s32[1]{0:T(128)} %bitcast.1.core, bf16[512,256]{1,0:T(8,128)(2,1)} %q_hbm.1, bf16[512,128]{1,0:T(8,128)(2,1)} %k_hbm.1, ...), custom_call_target="tpu_custom_call" | custom-call | tf_op jit(solution)/shard_map/prepare/pallas_call | solution.py:118
  12.3 1.6 collective-permute-start
  13.9 0.4 collective-permute-start.1
  14.4 2.3 %collective-permute-start.2 = (bf16[256,256]{1,0:T(8,128)(2,1)}, bf16[256,256]{1,0:T(8,128)(2,1)S(1)}, u32[]{:S(2)}, u32[]{:S(2)}) collective-permute-start(bf16[256,256]{1,0:T(8,128)(2,1)} %get-tuple-element.46.refs_0_), channel_id=1, source_target_pairs={{0,16},{4,20},{8,24},{12,28},{16,0},{20,4},{24,8},{28,12},{32,48},... | collective-permute-start | bytes 393224 | tf_op jit(solution)/shard_map/ppermute | solution.py:381
  16.7 1.9 collective-permute-start.3
  18.6 2.1 %collective-permute-start.4 = (bf16[256,256]{1,0:T(8,128)(2,1)}, bf16[256,256]{1,0:T(8,128)(2,1)S(1)}, u32[]{:S(2)}, u32[]{:S(2)}) collective-permute-start(bf16[256,256]{1,0:T(8,128)(2,1)} %get-tuple-element.47.refs_4_), channel_id=1, source_target_pairs={{0,96},{4,100},{8,104},{12,108},{16,112},{20,116},{24,120},{28,124... | collective-permute-start | bytes 393224 | tf_op jit(solution)/shard_map/ppermute | solution.py:381
  20.7 1.9 collective-permute-start.5
  22.6 0.0 collective-permute-done.2.refs_3_
  22.6 1.5 collective-permute-done.3.refs_5_
  24.1 2.1 %collective-permute-done.4.refs_6_ = bf16[256,256]{1,0:T(8,128)(2,1)S(1)} collective-permute-done((bf16[256,256]{1,0:T(8,128)(2,1)}, bf16[256,256]{1,0:T(8,128)(2,1)S(1)}, u32[]{:S(2)}, u32[]{:S(2)}) %collective-permute-start.4) | collective-permute-done | bytes 131104 | tf_op jit(solution)/shard_map/ppermute | solution.py:381
  26.3 1.7 collective-permute-done.5.refs_7_
  27.9 0.9 copy-done.7
  28.8 0.9 copy-done.8
  29.7 0.1 lines.1
  29.8 0.1 collective-permute-start.6
  29.9 0.5 collective-permute-start.7
  30.4 1.0 collective-permute-start.10
  31.4 1.1 collective-permute-start.11
  32.4 0.8 collective-permute-start.8
  33.2 2.5 %collective-permute-start.9 = (bf16[1024,256]{1,0:T(8,128)(2,1)S(1)}, bf16[1024,256]{1,0:T(8,128)(2,1)S(1)}, u32[]{:S(2)}, u32[]{:S(2)}) collective-permute-start(bf16[1024,256]{1,0:T(8,128)(2,1)S(1)} %get-tuple-element.48.refs_1_), channel_id=1, source_target_pairs={{0,96},{4,100},{8,104},{12,108},{16,112},{20,116},{24,120},{28,124... | collective-permute-start | bytes 1572872 | tf_op jit(solution)/shard_map/ppermute | solution.py:381
  35.7 0.4 collective-permute-start.12
  36.0 12.4 %collective-permute-done.10.refs_3_ = bf16[1024,256]{1,0:T(8,128)(2,1)S(1)} collective-permute-done((bf16[1024,256]{1,0:T(8,128)(2,1)S(1)}, bf16[1024,256]{1,0:T(8,128)(2,1)S(1)}, u32[]{:S(2)}, u32[]{:S(2)}) %collective-permute-start.10) | collective-permute-done | bytes 524320 | tf_op jit(solution)/shard_map/ppermute | solution.py:381
  48.5 1.8 collective-permute-start.13
  50.3 0.9 copy-done.10
  51.2 6.2 %flash_first.1 = (f32[1024,128]{1,0:T(8,128)S(1)}, f32[1024,256]{1,0:T(8,128)S(1)}) custom-call(bf16[1024,128]{1,0:T(8,128)(2,1)S(1)} %copy-done.10, bf16[1024,256]{1,0:T(8,128)(2,1)S(1)} %get-tuple-element.48.refs_1_, bf16[1024,256]{1,0:T(8,128)(2,1)S(1)} %get-tuple-element.49.refs_2_, bf16[1024,256]{1,0:T(8,128)(2,1)S(1)} %collective-permute-done.6.refs_3_, ...), custom_call_target="tpu_custom_call" | custom-call | flops 2147483648 | bytes 2097152 | tf_op jit(solution)/shard_map/flash_first/pallas_call | solution.py:191
  57.5 0.1 collective-permute-start.16
  57.6 0.5 collective-permute-start.17
  58.1 2.8 %collective-permute-start.20 = (bf16[256,2048]{1,0:T(8,128)(2,1)}, bf16[256,2048]{1,0:T(8,128)(2,1)S(1)}, u32[]{:S(2)}, u32[]{:S(2)}) collective-permute-start(bf16[256,2048]{1,0:T(8,128)(2,1)} %get-tuple-element.69.refs_4_), channel_id=1, source_target_pairs={{0,3},{1,0},{2,1},{3,2},{4,7},{5,4},{6,5},{7,6},{8,11},{9,8},{10,9... | collective-permute-start | bytes 3145736 | tf_op jit(solution)/shard_map/ppermute | solution.py:368
  60.9 7.8 %collective-permute-done.12.refs_1_ = bf16[1024,256]{1,0:T(8,128)(2,1)S(1)} collective-permute-done((bf16[1024,256]{1,0:T(8,128)(2,1)S(1)}, bf16[1024,256]{1,0:T(8,128)(2,1)S(1)}, u32[]{:S(2)}, u32[]{:S(2)}) %collective-permute-start.12) | collective-permute-done | bytes 524320 | tf_op jit(solution)/shard_map/ppermute | solution.py:381
  68.7 3.1 %collective-permute-start.21 = (bf16[256,2048]{1,0:T(8,128)(2,1)}, bf16[256,2048]{1,0:T(8,128)(2,1)S(1)}, u32[]{:S(2)}, u32[]{:S(2)}) collective-permute-start(bf16[256,2048]{1,0:T(8,128)(2,1)} %get-tuple-element.69.refs_4_), channel_id=1, source_target_pairs={{0,2},{1,3},{2,0},{3,1},{4,6},{5,7},{6,4},{7,5},{8,10},{9,11},{10,... | collective-permute-start | bytes 3145736 | tf_op jit(solution)/shard_map/ppermute | solution.py:368
  71.8 2.7 %collective-permute-done.13.refs_2_ = bf16[1024,256]{1,0:T(8,128)(2,1)S(1)} collective-permute-done((bf16[1024,256]{1,0:T(8,128)(2,1)S(1)}, bf16[1024,256]{1,0:T(8,128)(2,1)S(1)}, u32[]{:S(2)}, u32[]{:S(2)}) %collective-permute-start.13) | collective-permute-done | bytes 524320 | tf_op jit(solution)/shard_map/ppermute | solution.py:381
  74.6 1.5 collective-permute-start.22
  76.0 0.5 collective-permute-start.19
  76.5 6.9 %flash_more.2 = (f32[1024,128]{1,0:T(8,128)S(1)}, f32[1024,256]{1,0:T(8,128)S(1)}) custom-call(bf16[1024,128]{1,0:T(8,128)(2,1)S(1)} %copy-done.10, bf16[1024,256]{1,0:T(8,128)(2,1)S(1)} %collective-permute-done.8.refs_1_, bf16[1024,256]{1,0:T(8,128)(2,1)S(1)} %collective-permute-done.9.refs_2_, bf16[1024,256]{1,0:T(8,128)(2,1)S(1)} %collective-permute-done.10.refs_3_, ...), custom_call_target="tpu_custom_call" | custom-call | flops 2147483648 | bytes 2097152 | tf_op jit(solution)/shard_map/flash_more/pallas_call | solution.py:191
  83.5 0.2 collective-permute-start.14
  83.7 0.4 collective-permute-start.15
  84.1 6.9 %flash_more.3 = (f32[1024,128]{1,0:T(8,128)S(1)}, f32[1024,256]{1,0:T(8,128)S(1)}) custom-call(bf16[1024,128]{1,0:T(8,128)(2,1)S(1)} %copy-done.10, bf16[1024,256]{1,0:T(8,128)(2,1)S(1)} %collective-permute-done.16.refs_1_, bf16[1024,256]{1,0:T(8,128)(2,1)S(1)} %collective-permute-done.17.refs_2_, bf16[1024,256]{1,0:T(8,128)(2,1)S(1)} %collective-permute-done.18.refs_3_, ...), custom_call_target="tpu_custom_call" | custom-call | flops 2147483648 | bytes 2097152 | tf_op jit(solution)/shard_map/flash_more/pallas_call | solution.py:191
  91.0 15.3 %collective-permute-done.20.refs_5_ = bf16[256,2048]{1,0:T(8,128)(2,1)S(1)} collective-permute-done((bf16[256,2048]{1,0:T(8,128)(2,1)}, bf16[256,2048]{1,0:T(8,128)(2,1)S(1)}, u32[]{:S(2)}, u32[]{:S(2)}) %collective-permute-start.20) | collective-permute-done | bytes 1048608 | tf_op jit(solution)/shard_map/ppermute | solution.py:368
  106.4 9.2 %collective-permute-done.22.refs_7_ = bf16[256,2048]{1,0:T(8,128)(2,1)} collective-permute-done((bf16[256,2048]{1,0:T(8,128)(2,1)}, bf16[256,2048]{1,0:T(8,128)(2,1)}, u32[]{:S(2)}, u32[]{:S(2)}) %collective-permute-start.22) | collective-permute-done | bytes 1048608 | tf_op jit(solution)/shard_map/ppermute | solution.py:368
  115.6 0.5 collective-permute-start.27
  116.1 7.1 %flash_last.1.refs_0_ = bf16[512,256]{1,0:T(8,128)(2,1)S(1)} custom-call(bf16[1024,128]{1,0:T(8,128)(2,1)S(1)} %copy-done.10, bf16[1024,256]{1,0:T(8,128)(2,1)S(1)} %collective-permute-done.12.refs_1_, bf16[1024,256]{1,0:T(8,128)(2,1)S(1)} %collective-permute-done.13.refs_2_, bf16[1024,256]{1,0:T(8,128)(2,1)S(1)} %collective-permute-done.14.refs_3_, ...), custom_call_target="tpu_custom_call" | custom-call | flops 2147483648 | bytes 2097152 | tf_op jit(solution)/shard_map/flash_last/pallas_call | solution.py:191
  123.2 0.7 collective-permute-start.23
  123.9 2.9 %collective-permute-start.24 = (bf16[512,256]{1,0:T(8,128)(2,1)S(1)}, bf16[512,256]{1,0:T(8,128)(2,1)}, u32[]{:S(2)}, u32[]{:S(2)}) collective-permute-start(bf16[512,256]{1,0:T(8,128)(2,1)S(1)} %flash_last.1.refs_0_), channel_id=1, source_target_pairs={{0,2},{1,3},{2,0},{3,1},{4,6},{5,7},{6,4},{7,5},{8,10},{9,11},{10,... | collective-permute-start | bytes 786440 | tf_op jit(solution)/shard_map/ppermute | solution.py:368
  126.8 5.7 %collective-permute-done.23.refs_1_ = bf16[512,256]{1,0:T(8,128)(2,1)S(1)} collective-permute-done((bf16[512,256]{1,0:T(8,128)(2,1)S(1)}, bf16[512,256]{1,0:T(8,128)(2,1)S(1)}, u32[]{:S(2)}, u32[]{:S(2)}) %collective-permute-start.23) | collective-permute-done | bytes 262176 | tf_op jit(solution)/shard_map/ppermute | solution.py:368
  132.4 0.7 copy-done.5
  133.1 0.9 collective-permute-start.25
  134.1 0.1 pad_add_fusion.place
  134.1 7.7 %collective-permute-done.25.refs_3_ = bf16[512,256]{1,0:T(8,128)(2,1)} collective-permute-done((bf16[512,256]{1,0:T(8,128)(2,1)S(1)}, bf16[512,256]{1,0:T(8,128)(2,1)}, u32[]{:S(2)}, u32[]{:S(2)}) %collective-permute-start.25) | collective-permute-done | bytes 262176 | tf_op jit(solution)/shard_map/ppermute | solution.py:368
  141.9 1.0 copy-done.4
  142.9 0.9 copy-done.6
  143.9 6.4 %project.1 = (bf16[128,2048]{1,0:T(8,128)(2,1)S(1)}, bf16[512,2048]{1,0:T(8,128)(2,1)S(1)}) custom-call(s32[2]{0:T(128)S(1)} %pad_add_fusion.place, bf16[512,256]{1,0:T(8,128)(2,1)S(1)} %flash_last.1.refs_0_, bf16[512,256]{1,0:T(8,128)(2,1)S(1)} %copy-done.6, bf16[512,256]{1,0:T(8,128)(2,1)} %collective-permute-done.24.refs_2_, ...), custom_call_target="tpu_custom_call" | custom-call | tf_op jit(solution)/shard_map/project/pallas_call | solution.py:248
  150.3 1.3 copy-done
  151.6 0.8 copy-done.2
  152.4 21.7 %units.1 = (bf16[128,2048]{1,0:T(8,128)(2,1)S(1)}, bf16[128,2048]{1,0:T(8,128)(2,1)S(1)}, bf16[128,2048]{1,0:T(8,128)(2,1)S(1)}, bf16[128,2048]{1,0:T(8,128)(2,1)S(1)}) custom-call(bf16[512,2048]{1,0:T(8,128)(2,1)} %copy-done, bf16[2048,4224]{1,0:T(8,128)(2,1)} %all-gather.2.cloned.1.call-done.w_hbm), custom_call_target="tpu_custom_call" | custom-call | tf_op jit(solution)/shard_map/units/pallas_call | solution.py:330
  174.1 0.2 collective-permute-start.29
  174.3 1.8 collective-permute-start.30
  176.1 2.3 %collective-permute-start.31 = (bf16[128,2048]{1,0:T(8,128)(2,1)S(1)}, bf16[128,2048]{1,0:T(8,128)(2,1)S(1)}, u32[]{:S(2)}, u32[]{:S(2)}) collective-permute-start(bf16[128,2048]{1,0:T(8,128)(2,1)S(1)} %get-tuple-element.80), channel_id=1, source_target_pairs={{0,3},{1,0},{2,1},{3,2},{4,7},{5,4},{6,5},{7,6},{8,11},{9,8},{10,9... | collective-permute-start | bytes 1572872 | tf_op jit(solution)/shard_map/ppermute | solution.py:368
  178.5 20.3 %collective-permute-done.29 = bf16[128,2048]{1,0:T(8,128)(2,1)S(1)} collective-permute-done((bf16[128,2048]{1,0:T(8,128)(2,1)S(1)}, bf16[128,2048]{1,0:T(8,128)(2,1)S(1)}, u32[]{:S(2)}, u32[]{:S(2)}) %collective-permute-start.29) | collective-permute-done | bytes 524320 | tf_op jit(solution)/shard_map/ppermute | solution.py:368
  198.8 0.6 collective-permute-done.31
  199.4 1.2 add_convert_fusion
  (43 shorter events, 0.2 us)
Async XLA Ops:
  6.5 145.8 %all-gather.2.cloned.1.call-start = ((), (), s32[]{:S(2)}) async-start(), calls=%async_computation | async-start | bytes 17842176 | tf_op jit(solution)/shard_map/all_gather | solution.py:405
  7.8 134.1 %copy-start.9 = (f32[2048]{0:T(1024)S(1)}, f32[2048]{0:T(1024)}, u32[]{:S(2)}) copy-start(f32[2048]{0:T(1024)} %param.18) | copy-start | bytes 24580
  12.2 129.7 %copy-start.1 = (bf16[256,2048]{1,0:T(8,128)(2,1)S(1)}, bf16[256,2048]{1,0:T(8,128)(2,1)}, u32[]{:S(2)}) copy-start(bf16[256,2048]{1,0:T(8,128)(2,1)} %get-tuple-element.69.refs_4_) | copy-start | bytes 3145732
  12.3 8.4 %collective-permute-start = (bf16[256,256]{1,0:T(8,128)(2,1)}, bf16[256,256]{1,0:T(8,128)(2,1)S(1)}, u32[]{:S(2)}, u32[]{:S(2)}) collective-permute-start(bf16[256,256]{1,0:T(8,128)(2,1)} %get-tuple-element.46.refs_0_), channel_id=1, source_target_pairs={{0,8},{4,12},{8,16},{12,20},{16,24},{20,28},{24,0},{28,4},{32,40},... | collective-permute-start | bytes 393224 | tf_op jit(solution)/shard_map/ppermute | solution.py:381
  13.9 8.7 %collective-permute-start.1 = (bf16[256,256]{1,0:T(8,128)(2,1)}, bf16[256,256]{1,0:T(8,128)(2,1)S(1)}, u32[]{:S(2)}, u32[]{:S(2)}) collective-permute-start(bf16[256,256]{1,0:T(8,128)(2,1)} %get-tuple-element.46.refs_0_), channel_id=1, source_target_pairs={{0,24},{4,28},{8,0},{12,4},{16,8},{20,12},{24,16},{28,20},{32,56},... | collective-permute-start | bytes 393224 | tf_op jit(solution)/shard_map/ppermute | solution.py:381
  14.4 8.2 %collective-permute-start.2 = (bf16[256,256]{1,0:T(8,128)(2,1)}, bf16[256,256]{1,0:T(8,128)(2,1)S(1)}, u32[]{:S(2)}, u32[]{:S(2)}) collective-permute-start(bf16[256,256]{1,0:T(8,128)(2,1)} %get-tuple-element.46.refs_0_), channel_id=1, source_target_pairs={{0,16},{4,20},{8,24},{12,28},{16,0},{20,4},{24,8},{28,12},{32,48},... | collective-permute-start | bytes 393224 | tf_op jit(solution)/shard_map/ppermute | solution.py:381
  16.7 7.5 %collective-permute-start.3 = (bf16[256,256]{1,0:T(8,128)(2,1)}, bf16[256,256]{1,0:T(8,128)(2,1)S(1)}, u32[]{:S(2)}, u32[]{:S(2)}) collective-permute-start(bf16[256,256]{1,0:T(8,128)(2,1)} %get-tuple-element.47.refs_4_), channel_id=1, source_target_pairs={{0,32},{4,36},{8,40},{12,44},{16,48},{20,52},{24,56},{28,60},{32,6... | collective-permute-start | bytes 393224 | tf_op jit(solution)/shard_map/ppermute | solution.py:381
  18.6 7.7 %collective-permute-start.4 = (bf16[256,256]{1,0:T(8,128)(2,1)}, bf16[256,256]{1,0:T(8,128)(2,1)S(1)}, u32[]{:S(2)}, u32[]{:S(2)}) collective-permute-start(bf16[256,256]{1,0:T(8,128)(2,1)} %get-tuple-element.47.refs_4_), channel_id=1, source_target_pairs={{0,96},{4,100},{8,104},{12,108},{16,112},{20,116},{24,120},{28,124... | collective-permute-start | bytes 393224 | tf_op jit(solution)/shard_map/ppermute | solution.py:381
  20.7 7.2 %collective-permute-start.5 = (bf16[256,256]{1,0:T(8,128)(2,1)}, bf16[256,256]{1,0:T(8,128)(2,1)S(1)}, u32[]{:S(2)}, u32[]{:S(2)}) collective-permute-start(bf16[256,256]{1,0:T(8,128)(2,1)} %get-tuple-element.47.refs_4_), channel_id=1, source_target_pairs={{0,64},{4,68},{8,72},{12,76},{16,80},{20,84},{24,88},{28,92},{32,9... | collective-permute-start | bytes 393224 | tf_op jit(solution)/shard_map/ppermute | solution.py:381
  27.9 0.9 copy-start.7
  28.8 0.9 copy-start.8
  29.8 3.4 %collective-permute-start.6 = (bf16[1024,256]{1,0:T(8,128)(2,1)S(1)}, bf16[1024,256]{1,0:T(8,128)(2,1)S(1)}, u32[]{:S(2)}, u32[]{:S(2)}) collective-permute-start(bf16[1024,256]{1,0:T(8,128)(2,1)S(1)} %get-tuple-element.48.refs_1_), channel_id=1, source_target_pairs={{0,4},{4,0},{8,12},{12,8},{16,20},{20,16},{24,28},{28,24},{32,36},... | collective-permute-start | bytes 1572872 | tf_op jit(solution)/shard_map/ppermute | solution.py:381
  29.9 5.8 %collective-permute-start.7 = (bf16[1024,256]{1,0:T(8,128)(2,1)S(1)}, bf16[1024,256]{1,0:T(8,128)(2,1)S(1)}, u32[]{:S(2)}, u32[]{:S(2)}) collective-permute-start(bf16[1024,256]{1,0:T(8,128)(2,1)S(1)} %get-tuple-element.49.refs_2_), channel_id=1, source_target_pairs={{0,4},{4,0},{8,12},{12,8},{16,20},{20,16},{24,28},{28,24},{32,36},... | collective-permute-start | bytes 1572872 | tf_op jit(solution)/shard_map/ppermute | solution.py:381
  30.4 18.1 %collective-permute-start.10 = (bf16[1024,256]{1,0:T(8,128)(2,1)S(1)}, bf16[1024,256]{1,0:T(8,128)(2,1)S(1)}, u32[]{:S(2)}, u32[]{:S(2)}) collective-permute-start(bf16[1024,256]{1,0:T(8,128)(2,1)S(1)} %get-tuple-element.49.refs_2_), channel_id=1, source_target_pairs={{0,8},{4,12},{8,16},{12,20},{16,24},{20,28},{24,0},{28,4},{32,40},... | collective-permute-start | bytes 1572872 | tf_op jit(solution)/shard_map/ppermute | solution.py:381
  31.4 26.1 %collective-permute-start.11 = (bf16[1024,256]{1,0:T(8,128)(2,1)S(1)}, bf16[1024,256]{1,0:T(8,128)(2,1)S(1)}, u32[]{:S(2)}, u32[]{:S(2)}) collective-permute-start(bf16[1024,256]{1,0:T(8,128)(2,1)S(1)} %get-tuple-element.49.refs_2_), channel_id=1, source_target_pairs={{0,24},{4,28},{8,0},{12,4},{16,8},{20,12},{24,16},{28,20},{32,56},... | collective-permute-start | bytes 1572872 | tf_op jit(solution)/shard_map/ppermute | solution.py:381
  32.4 25.0 %collective-permute-start.8 = (bf16[1024,256]{1,0:T(8,128)(2,1)S(1)}, bf16[1024,256]{1,0:T(8,128)(2,1)S(1)}, u32[]{:S(2)}, u32[]{:S(2)}) collective-permute-start(bf16[1024,256]{1,0:T(8,128)(2,1)S(1)} %get-tuple-element.48.refs_1_), channel_id=1, source_target_pairs={{0,32},{4,36},{8,40},{12,44},{16,48},{20,52},{24,56},{28,60},{32,6... | collective-permute-start | bytes 1572872 | tf_op jit(solution)/shard_map/ppermute | solution.py:381
  33.2 24.3 %collective-permute-start.9 = (bf16[1024,256]{1,0:T(8,128)(2,1)S(1)}, bf16[1024,256]{1,0:T(8,128)(2,1)S(1)}, u32[]{:S(2)}, u32[]{:S(2)}) collective-permute-start(bf16[1024,256]{1,0:T(8,128)(2,1)S(1)} %get-tuple-element.48.refs_1_), channel_id=1, source_target_pairs={{0,96},{4,100},{8,104},{12,108},{16,112},{20,116},{24,120},{28,124... | collective-permute-start | bytes 1572872 | tf_op jit(solution)/shard_map/ppermute | solution.py:381
  35.7 33.0 %collective-permute-start.12 = (bf16[1024,256]{1,0:T(8,128)(2,1)S(1)}, bf16[1024,256]{1,0:T(8,128)(2,1)S(1)}, u32[]{:S(2)}, u32[]{:S(2)}) collective-permute-start(bf16[1024,256]{1,0:T(8,128)(2,1)S(1)} %get-tuple-element.48.refs_1_), channel_id=1, source_target_pairs={{0,64},{4,68},{8,72},{12,76},{16,80},{20,84},{24,88},{28,92},{32,9... | collective-permute-start | bytes 1572872 | tf_op jit(solution)/shard_map/ppermute | solution.py:381
  48.5 26.1 %collective-permute-start.13 = (bf16[1024,256]{1,0:T(8,128)(2,1)S(1)}, bf16[1024,256]{1,0:T(8,128)(2,1)S(1)}, u32[]{:S(2)}, u32[]{:S(2)}) collective-permute-start(bf16[1024,256]{1,0:T(8,128)(2,1)S(1)} %get-tuple-element.49.refs_2_), channel_id=1, source_target_pairs={{0,16},{4,20},{8,24},{12,28},{16,0},{20,4},{24,8},{28,12},{32,48},... | collective-permute-start | bytes 1572872 | tf_op jit(solution)/shard_map/ppermute | solution.py:381
  50.3 0.9 copy-start.10
  57.5 18.5 %collective-permute-start.16 = (bf16[1024,256]{1,0:T(8,128)(2,1)S(1)}, bf16[1024,256]{1,0:T(8,128)(2,1)S(1)}, u32[]{:S(2)}, u32[]{:S(2)}) collective-permute-start(bf16[1024,256]{1,0:T(8,128)(2,1)S(1)} %collective-permute-done.8.refs_1_), channel_id=1, source_target_pairs={{0,4},{4,0},{8,12},{12,8},{16,20},{20,16},{24,28},{28,24},{32,36},... | collective-permute-start | bytes 1572872 | tf_op jit(solution)/shard_map/ppermute | solution.py:381
  57.6 18.4 %collective-permute-start.17 = (bf16[1024,256]{1,0:T(8,128)(2,1)S(1)}, bf16[1024,256]{1,0:T(8,128)(2,1)S(1)}, u32[]{:S(2)}, u32[]{:S(2)}) collective-permute-start(bf16[1024,256]{1,0:T(8,128)(2,1)S(1)} %collective-permute-done.9.refs_2_), channel_id=1, source_target_pairs={{0,4},{4,0},{8,12},{12,8},{16,20},{20,16},{24,28},{28,24},{32,36},... | collective-permute-start | bytes 1572872 | tf_op jit(solution)/shard_map/ppermute | solution.py:381
  58.1 48.3 %collective-permute-start.20 = (bf16[256,2048]{1,0:T(8,128)(2,1)}, bf16[256,2048]{1,0:T(8,128)(2,1)S(1)}, u32[]{:S(2)}, u32[]{:S(2)}) collective-permute-start(bf16[256,2048]{1,0:T(8,128)(2,1)} %get-tuple-element.69.refs_4_), channel_id=1, source_target_pairs={{0,3},{1,0},{2,1},{3,2},{4,7},{5,4},{6,5},{7,6},{8,11},{9,8},{10,9... | collective-permute-start | bytes 3145736 | tf_op jit(solution)/shard_map/ppermute | solution.py:368
  68.7 37.7 %collective-permute-start.21 = (bf16[256,2048]{1,0:T(8,128)(2,1)}, bf16[256,2048]{1,0:T(8,128)(2,1)S(1)}, u32[]{:S(2)}, u32[]{:S(2)}) collective-permute-start(bf16[256,2048]{1,0:T(8,128)(2,1)} %get-tuple-element.69.refs_4_), channel_id=1, source_target_pairs={{0,2},{1,3},{2,0},{3,1},{4,6},{5,7},{6,4},{7,5},{8,10},{9,11},{10,... | collective-permute-start | bytes 3145736 | tf_op jit(solution)/shard_map/ppermute | solution.py:368
  74.6 41.0 %collective-permute-start.22 = (bf16[256,2048]{1,0:T(8,128)(2,1)}, bf16[256,2048]{1,0:T(8,128)(2,1)}, u32[]{:S(2)}, u32[]{:S(2)}) collective-permute-start(bf16[256,2048]{1,0:T(8,128)(2,1)} %get-tuple-element.69.refs_4_), channel_id=1, source_target_pairs={{0,1},{1,2},{2,3},{3,0},{4,5},{5,6},{6,7},{7,4},{8,9},{9,10},{10,1... | collective-permute-start | bytes 3145736 | tf_op jit(solution)/shard_map/ppermute | solution.py:368
  76.0 7.5 %collective-permute-start.18 = (bf16[1024,256]{1,0:T(8,128)(2,1)S(1)}, bf16[1024,256]{1,0:T(8,128)(2,1)S(1)}, u32[]{:S(2)}, u32[]{:S(2)}) collective-permute-start(bf16[1024,256]{1,0:T(8,128)(2,1)S(1)} %collective-permute-done.10.refs_3_), channel_id=1, source_target_pairs={{0,4},{4,0},{8,12},{12,8},{16,20},{20,16},{24,28},{28,24},{32,36},... | collective-permute-start | bytes 1572872 | tf_op jit(solution)/shard_map/ppermute | solution.py:381
  76.0 7.6 %collective-permute-start.19 = (bf16[1024,256]{1,0:T(8,128)(2,1)S(1)}, bf16[1024,256]{1,0:T(8,128)(2,1)S(1)}, u32[]{:S(2)}, u32[]{:S(2)}) collective-permute-start(bf16[1024,256]{1,0:T(8,128)(2,1)S(1)} %collective-permute-done.11.refs_4_), channel_id=1, source_target_pairs={{0,4},{4,0},{8,12},{12,8},{16,20},{20,16},{24,28},{28,24},{32,36},... | collective-permute-start | bytes 1572872 | tf_op jit(solution)/shard_map/ppermute | solution.py:381
  83.5 32.6 %collective-permute-start.14 = (bf16[1024,256]{1,0:T(8,128)(2,1)S(1)}, bf16[1024,256]{1,0:T(8,128)(2,1)S(1)}, u32[]{:S(2)}, u32[]{:S(2)}) collective-permute-start(bf16[1024,256]{1,0:T(8,128)(2,1)S(1)} %collective-permute-done.12.refs_1_), channel_id=1, source_target_pairs={{0,4},{4,0},{8,12},{12,8},{16,20},{20,16},{24,28},{28,24},{32,36},... | collective-permute-start | bytes 1572872 | tf_op jit(solution)/shard_map/ppermute | solution.py:381
  83.7 32.4 %collective-permute-start.15 = (bf16[1024,256]{1,0:T(8,128)(2,1)S(1)}, bf16[1024,256]{1,0:T(8,128)(2,1)S(1)}, u32[]{:S(2)}, u32[]{:S(2)}) collective-permute-start(bf16[1024,256]{1,0:T(8,128)(2,1)S(1)} %collective-permute-done.13.refs_2_), channel_id=1, source_target_pairs={{0,4},{4,0},{8,12},{12,8},{16,20},{20,16},{24,28},{28,24},{32,36},... | collective-permute-start | bytes 1572872 | tf_op jit(solution)/shard_map/ppermute | solution.py:381
  115.6 26.3 %collective-permute-start.26 = (bf16[256,2048]{1,0:T(8,128)(2,1)S(1)}, bf16[256,2048]{1,0:T(8,128)(2,1)}, u32[]{:S(2)}, u32[]{:S(2)}) collective-permute-start(bf16[256,2048]{1,0:T(8,128)(2,1)S(1)} %collective-permute-done.20.refs_5_), channel_id=1, source_target_pairs={{0,4},{4,0},{8,12},{12,8},{16,20},{20,16},{24,28},{28,24},{32,36},... | collective-permute-start | bytes 3145736 | tf_op jit(solution)/shard_map/ppermute | solution.py:381
  115.6 26.3 %collective-permute-start.27 = (bf16[256,2048]{1,0:T(8,128)(2,1)S(1)}, bf16[256,2048]{1,0:T(8,128)(2,1)}, u32[]{:S(2)}, u32[]{:S(2)}) collective-permute-start(bf16[256,2048]{1,0:T(8,128)(2,1)S(1)} %collective-permute-done.21.refs_6_), channel_id=1, source_target_pairs={{0,4},{4,0},{8,12},{12,8},{16,20},{20,16},{24,28},{28,24},{32,36},... | collective-permute-start | bytes 3145736 | tf_op jit(solution)/shard_map/ppermute | solution.py:381
  116.1 25.8 %collective-permute-start.28 = (bf16[256,2048]{1,0:T(8,128)(2,1)}, bf16[256,2048]{1,0:T(8,128)(2,1)}, u32[]{:S(2)}, u32[]{:S(2)}) collective-permute-start(bf16[256,2048]{1,0:T(8,128)(2,1)} %collective-permute-done.22.refs_7_), channel_id=1, source_target_pairs={{0,4},{4,0},{8,12},{12,8},{16,20},{20,16},{24,28},{28,24},{32,36},... | collective-permute-start | bytes 3145736 | tf_op jit(solution)/shard_map/ppermute | solution.py:381
  123.2 9.2 %collective-permute-start.23 = (bf16[512,256]{1,0:T(8,128)(2,1)S(1)}, bf16[512,256]{1,0:T(8,128)(2,1)S(1)}, u32[]{:S(2)}, u32[]{:S(2)}) collective-permute-start(bf16[512,256]{1,0:T(8,128)(2,1)S(1)} %flash_last.1.refs_0_), channel_id=1, source_target_pairs={{0,3},{1,0},{2,1},{3,2},{4,7},{5,4},{6,5},{7,6},{8,11},{9,8},{10,9... | collective-permute-start | bytes 786440 | tf_op jit(solution)/shard_map/ppermute | solution.py:368
  123.9 10.3 %collective-permute-start.24 = (bf16[512,256]{1,0:T(8,128)(2,1)S(1)}, bf16[512,256]{1,0:T(8,128)(2,1)}, u32[]{:S(2)}, u32[]{:S(2)}) collective-permute-start(bf16[512,256]{1,0:T(8,128)(2,1)S(1)} %flash_last.1.refs_0_), channel_id=1, source_target_pairs={{0,2},{1,3},{2,0},{3,1},{4,6},{5,7},{6,4},{7,5},{8,10},{9,11},{10,... | collective-permute-start | bytes 786440 | tf_op jit(solution)/shard_map/ppermute | solution.py:368
  132.4 0.7 copy-start.5
  133.1 8.7 %collective-permute-start.25 = (bf16[512,256]{1,0:T(8,128)(2,1)S(1)}, bf16[512,256]{1,0:T(8,128)(2,1)}, u32[]{:S(2)}, u32[]{:S(2)}) collective-permute-start(bf16[512,256]{1,0:T(8,128)(2,1)S(1)} %flash_last.1.refs_0_), channel_id=1, source_target_pairs={{0,1},{1,2},{2,3},{3,0},{4,5},{5,6},{6,7},{7,4},{8,9},{9,10},{10,1... | collective-permute-start | bytes 786440 | tf_op jit(solution)/shard_map/ppermute | solution.py:368
  141.9 1.0 copy-start.4
  142.9 0.9 copy-start.6
  150.3 1.3 copy-start
  151.6 0.8 copy-start.2
  152.3 47.1 %copy-start.3 = (bf16[128,2048]{1,0:T(8,128)(2,1)S(1)}, bf16[128,2048]{1,0:T(8,128)(2,1)}, u32[]{:S(2)}) copy-start(bf16[128,2048]{1,0:T(8,128)(2,1)} %copy-done.2) | copy-start | bytes 1572868
  174.1 24.7 %collective-permute-start.29 = (bf16[128,2048]{1,0:T(8,128)(2,1)S(1)}, bf16[128,2048]{1,0:T(8,128)(2,1)S(1)}, u32[]{:S(2)}, u32[]{:S(2)}) collective-permute-start(bf16[128,2048]{1,0:T(8,128)(2,1)S(1)} %get-tuple-element.78), channel_id=1, source_target_pairs={{0,1},{1,2},{2,3},{3,0},{4,5},{5,6},{6,7},{7,4},{8,9},{9,10},{10,1... | collective-permute-start | bytes 1572872 | tf_op jit(solution)/shard_map/ppermute | solution.py:368
  174.3 24.5 %collective-permute-start.30 = (bf16[128,2048]{1,0:T(8,128)(2,1)S(1)}, bf16[128,2048]{1,0:T(8,128)(2,1)S(1)}, u32[]{:S(2)}, u32[]{:S(2)}) collective-permute-start(bf16[128,2048]{1,0:T(8,128)(2,1)S(1)} %get-tuple-element.79), channel_id=1, source_target_pairs={{0,2},{1,3},{2,0},{3,1},{4,6},{5,7},{6,4},{7,5},{8,10},{9,11},{10,... | collective-permute-start | bytes 1572872 | tf_op jit(solution)/shard_map/ppermute | solution.py:368
  176.1 23.3 %collective-permute-start.31 = (bf16[128,2048]{1,0:T(8,128)(2,1)S(1)}, bf16[128,2048]{1,0:T(8,128)(2,1)S(1)}, u32[]{:S(2)}, u32[]{:S(2)}) collective-permute-start(bf16[128,2048]{1,0:T(8,128)(2,1)S(1)} %get-tuple-element.80), channel_id=1, source_target_pairs={{0,3},{1,0},{2,1},{3,2},{4,7},{5,4},{6,5},{7,6},{8,11},{9,8},{10,9... | collective-permute-start | bytes 1572872 | tf_op jit(solution)/shard_map/ppermute | solution.py:368
Sparse Core Ops, SparseCore 0:
  12.4 87.5 all-gather.1

commit v5 on v3

v5 whole, which is shorter than its diff:
```python
import functools

import jax
import jax.numpy as jnp
from jax import lax
from jax.experimental import pallas as pl
from jax.experimental.pallas import tpu as pltpu
from jax.sharding import PartitionSpec as P

GRID = 64
norm_eps = 1e-06
theta_base = 10000.0
LOG2E = 1.4426950408889634
f32 = jnp.float32
bf16 = jnp.bfloat16


def angle_tables(first_row, rows, head_dim):
    quarter = head_dim // 4
    frequency = jnp.power(theta_base, -2.0 * jnp.arange(quarter, dtype=f32) / (head_dim // 2))
    places = jnp.concatenate([first_row + jnp.arange(rows, dtype=jnp.int32), jnp.arange(GRID, dtype=jnp.int32)])
    angles = places.astype(f32)[:, None] * frequency
    cosine, sine = lax.optimization_barrier((jnp.cos(angles), jnp.sin(angles)))
    is_row = (jnp.arange(rows + GRID) < rows)[:, None]
    zero = jnp.zeros_like(cosine)

    def placed(lead, trail):
        return jnp.concatenate(
            [
                jnp.where(is_row, lead, zero),
                jnp.where(is_row, trail, zero),
                jnp.where(is_row, zero, lead),
                jnp.where(is_row, zero, trail),
            ],
            axis=1,
        )

    return placed(cosine, cosine), placed(-sine, sine)


def prepare_kernel(
    core, q_hbm, k_hbm, v_hbm, g_hbm, u_hbm, d_hbm, w_hbm, r_hbm, qg_ref, kg_ref, cos_ref, sin_ref,
    q_out, kv_out, woven, sent, kept,
    q_ref, k_ref, v_ref, g_ref, u_ref, d_ref, w_ref, r_ref, sems, *, rows, head_dim, heads, tile,
):
    tok = rows * GRID
    half = kept.shape[0]
    first_half = pl.ds(pl.multiple_of(core[0] * half, half), half)
    other_half = pl.ds(pl.multiple_of((1 - core[0]) * half, half), half)
    moves = [
        (k_hbm, k_ref),
        (v_hbm, v_ref),
        (q_hbm, q_ref),
        (g_hbm, g_ref),
        (u_hbm, u_ref),
        (d_hbm, d_ref),
        (w_hbm.at[first_half, :], w_ref.at[pl.ds(0, half), :]),
        (w_hbm.at[other_half, :], w_ref.at[pl.ds(half, half), :]),
        (r_hbm, r_ref),
        (w_ref.at[pl.ds(0, half), :], sent.at[pl.ds(0, half), :]),
        (w_ref.at[pl.ds(half, half), :], kept),
        (r_ref, sent.at[pl.ds(half, r_hbm.shape[0]), :]),
    ]
    copies = [pltpu.make_async_copy(x, y, sems.at[n]) for n, (x, y) in enumerate(moves)]
    for c in copies[:9]:
        c.start()

    def spread(ref):
        both = ref[0:rows, :][:, None, :] + ref[rows : rows + GRID, :][None, :, :]
        return both.reshape(tok, head_dim)

    cosine = spread(cos_ref)
    sine = spread(sin_ref)
    lane = lax.broadcasted_iota(jnp.int32, (tok, head_dim), 1)
    first = (lane % (head_dim // 2)) < head_dim // 4
    quarter = head_dim // 4

    def prepared(raw, gain):
        x = raw.astype(f32)
        x = x * lax.rsqrt(jnp.mean(x * x, axis=-1, keepdims=True) + norm_eps) * gain
        partner = jnp.where(first, pltpu.roll(x, head_dim - quarter, 1), pltpu.roll(x, quarter, 1))
        return (x * cosine + partner * sine).astype(bf16)

    copies[0].wait()
    copies[1].wait()
    kv_out[:, 0:head_dim] = prepared(k_ref[...], kg_ref[...])
    kv_out[:, head_dim:] = v_ref[...]
    for n in (6, 7, 8):
        copies[n].wait()
        copies[n + 3].start()
    copies[2].wait()
    for h in range(heads):
        q_out[h * tok : (h + 1) * tok, :] = prepared(q_ref[:, h * head_dim : (h + 1) * head_dim], qg_ref[...])
    for n in (3, 4, 5):
        copies[n].wait()
    units = g_ref.shape[1]
    for n in range(units // tile):
        part = slice(n * tile, (n + 1) * tile)
        woven[:, 2 * n * tile : (2 * n + 1) * tile] = g_ref[:, part]
        woven[:, (2 * n + 1) * tile : (2 * n + 2) * tile] = u_ref[:, part]
    woven[:, 2 * units :] = d_ref[...]
    for n in (9, 10, 11):
        copies[n].wait()


def prepare(query_rows, key_rows, value_rows, query_gain, key_gain, gate, up, down, out_weight, residual, tile=128):
    tok, width = query_rows.shape
    head_dim = query_gain.shape[0]
    rows = tok // GRID
    cosine, sine = angle_tables(lax.axis_index("sp") * rows, rows, head_dim)
    hbm = pl.BlockSpec(memory_space=pltpu.HBM)
    vmem = pl.BlockSpec(memory_space=pltpu.VMEM)
    big = (query_rows, key_rows, value_rows, gate, up, down.T)
    half = out_weight.shape[0] // 2
    return pl.pallas_call(
        functools.partial(prepare_kernel, rows=rows, head_dim=head_dim, heads=width // head_dim, tile=tile),
        in_specs=[pl.BlockSpec(memory_space=pltpu.SMEM)] + [hbm] * 8 + [vmem] * 4,
        out_specs=[vmem] * 3 + [hbm] * 2,
        out_shape=(
            jax.ShapeDtypeStruct((tok * (width // head_dim), head_dim), bf16),
            jax.ShapeDtypeStruct((tok, 2 * head_dim), bf16),
            jax.ShapeDtypeStruct((gate.shape[0], 3 * gate.shape[1]), bf16),
            jax.ShapeDtypeStruct((half + residual.shape[0], residual.shape[1]), bf16),
            jax.ShapeDtypeStruct((half, residual.shape[1]), bf16),
        ),
        scratch_shapes=[pltpu.VMEM(x.shape, bf16) for x in (*big, out_weight, residual)] + [pltpu.SemaphoreType.DMA((12,))],
        compiler_params=pltpu.CompilerParams(vmem_limit_bytes=60 * 1024 * 1024),
        name="prepare",
    )(
        (lax.axis_index("sp") % 2)[None], *big, out_weight, residual, query_gain[None, :], key_gain[None, :], cosine, sine
    )


def flash_kernel(*refs, pieces, scale, first, last, block=1024):
    q_ref = refs[0]
    kv_refs = refs[1 : 1 + pieces]
    refs = refs[1 + pieces :]
    if not first:
        m_in, acc_in = refs[0:2]
        refs = refs[2:]
    if last:
        o_ref = refs[0]
        refs = refs[1:]
    else:
        m_out, acc_out = refs[0:2]
        refs = refs[2:]
    head_dim = q_ref.shape[1]
    q = q_ref[...]
    if first:
        m = jnp.full((q.shape[0], 128), -jnp.inf, f32)
        acc = jnp.zeros((q.shape[0], 2 * head_dim), f32)
    else:
        m = m_in[...]
        acc = acc_in[...]

    parts = [(ref, slice(r, r + block)) for ref in kv_refs for r in range(0, ref.shape[0], block)]

    def scores(n):
        ref, rows = parts[n]
        return lax.dot_general(q, ref[rows, 0:head_dim], (((1,), (1,)), ((), ())), preferred_element_type=f32)

    following = scores(0)
    for n, (ref, rows) in enumerate(parts):
        values = ref[rows, head_dim:]
        values = jnp.concatenate([values, jnp.ones_like(values)], axis=1)
        s = following * scale
        if n + 1 < len(parts):
            following = scores(n + 1)
        new = jnp.maximum(m, jnp.max(s, axis=1, keepdims=True))
        w = jnp.exp2(s - new[:, 0:1]).astype(bf16)
        factor = jnp.exp2(m - new)
        acc = acc * factor[:, 0:1] + jnp.dot(w, values, preferred_element_type=f32)
        m = new
    if last:
        o_ref[...] = (acc[:, 0:head_dim] / acc[:, head_dim:]).astype(bf16)
    else:
        m_out[...] = m
        acc_out[...] = acc


def flash(q, kv, state, tok, last, tile=256):
    rows, head_dim = q.shape
    heads = rows // tok
    pieces = len(kv)
    piece = kv[0].shape
    tiles = tok // tile
    held = [pl.BlockSpec((tile, 128), lambda i: (i, 0)), pl.BlockSpec((tile, 2 * head_dim), lambda i: (i, 0))]
    held_shape = (jax.ShapeDtypeStruct((rows, 128), f32), jax.ShapeDtypeStruct((rows, 2 * head_dim), f32))
    first = state is None
    return pl.pallas_call(
        functools.partial(flash_kernel, pieces=pieces, scale=head_dim**-0.5 * LOG2E, first=first, last=last),
        grid=(rows // tile,),
        in_specs=[pl.BlockSpec((tile, head_dim), lambda i: (i, 0))]
        + [pl.BlockSpec(piece, lambda i: (0, 0))] * pieces
        + ([] if first else held),
        out_specs=pl.BlockSpec((tile, head_dim), lambda i: (i % tiles, i // tiles)) if last else tuple(held),
        out_shape=jax.ShapeDtypeStruct((tok, heads * head_dim), bf16) if last else held_shape,
        compiler_params=pltpu.CompilerParams(dimension_semantics=("arbitrary",), vmem_limit_bytes=12 << 20),
        cost_estimate=pl.CostEstimate(
            flops=4 * rows * piece[0] * pieces * head_dim,
            bytes_accessed=4 * piece[0] * pieces * head_dim,
            transcendentals=rows * piece[0] * pieces,
        ),
        name="flash_last" if last else "flash_first" if first else "flash_more",
    )(q, *kv, *([] if first else state))


def layer_kernel(place, *refs, parts, tile, sub, units, unit_tile):
    att = refs[0:parts]
    sent = refs[parts : 2 * parts]
    swapped = refs[2 * parts : 3 * parts]
    gain_ref, w_hbm, own_ref = refs[3 * parts : 3 * parts + 3]
    outs = refs[3 * parts + 3 : -5]
    x_ref, pair_ref, down_ref, h_ref, sems = refs[-5:]
    step = pl.program_id(0)
    half = sent[0].shape[0] - sub
    count = units // unit_tile
    blocks, rows, _ = down_ref.shape

    def copies():
        found = []
        for n in range(count):
            source = w_hbm.at[:, pl.ds(2 * n * unit_tile, 2 * unit_tile)]
            found.append(pltpu.make_async_copy(source, pair_ref.at[n], sems.at[n]))
        for n in range(blocks):
            source = w_hbm.at[pl.ds(n * rows, rows), pl.ds(2 * units, units)]
            found.append(pltpu.make_async_copy(source, down_ref.at[n], sems.at[count + n]))
        return found

    @pl.when(step == 0)
    def _():
        for c in copies():
            c.start()

    cols = pl.ds(pl.multiple_of(step * tile, tile), tile)
    total = None
    for a, w, o in zip(att, sent, swapped):
        rolled = []
        for r in range(parts):
            some = pl.ds(pl.multiple_of(((place[0] + r) % parts) * sub, sub), sub)
            halves = [a[some, pl.ds(pl.multiple_of(c * half, half), half)] for c in (place[1], 1 - place[1])]
            rolled.append(jnp.concatenate(halves, axis=1))
        weight = jnp.concatenate([w[0:half, :], o[0:half, :]], axis=0)
        part = jnp.dot(jnp.concatenate(rolled, axis=0), weight, preferred_element_type=f32).astype(bf16).astype(f32)
        total = part if total is None else total + part
    for r in range(parts):
        updated = (sent[r][half:, :].astype(f32) + total[r * sub : (r + 1) * sub, :]).astype(bf16)
        x_ref[r * sub : (r + 1) * sub, cols] = updated

    @pl.when(step == pl.num_programs(0) - 1)
    def _():
        own_ref[...] = x_ref[0:sub, :]
        for r in range(2 * parts):
            some = slice(r * sub // 2, (r + 1) * sub // 2)
            x = x_ref[some, :].astype(f32)
            x = x * lax.rsqrt(jnp.mean(x * x, axis=-1, keepdims=True) + norm_eps)
            x_ref[some, :] = (x * gain_ref[...]).astype(bf16)
        for c in copies():
            c.wait()

        def product(n):
            return jnp.dot(x_ref[...], pair_ref[n], preferred_element_type=f32)

        following = product(0)
        for n in range(count):
            r = following
            if n + 1 < count:
                following = product(n + 1)
            gate = r[:, 0:unit_tile]
            hidden = gate / (1.0 + jnp.exp(-gate)) * r[:, unit_tile:]
            h_ref[:, n * unit_tile : (n + 1) * unit_tile] = hidden.astype(bf16)
        for n in range(blocks):
            y = lax.dot_general(h_ref[...], down_ref[n], (((1,), (1,)), ((), ())), preferred_element_type=f32).astype(bf16)
            for p, out in enumerate(outs):
                out[:, n * rows : (n + 1) * rows] = y[p * sub : (p + 1) * sub, :]


def layer(place, att, sent, swapped, gain, weights, units, tile=512, unit_tile=128, rows=512):
    parts = len(att)
    tok, part_width = att[0].shape
    both, width = sent[0].shape
    sub = tok // parts
    count = units // unit_tile
    blocks = width // rows
    return pl.pallas_call(
        functools.partial(layer_kernel, parts=parts, tile=tile, sub=sub, units=units, unit_tile=unit_tile),
        grid_spec=pltpu.PrefetchScalarGridSpec(
            num_scalar_prefetch=1,
            grid=(width // tile,),
            in_specs=[pl.BlockSpec((tok, part_width), lambda i, p: (0, 0))] * parts
            + [pl.BlockSpec((both, tile), lambda i, p: (0, i))] * parts
            + [pl.BlockSpec((s.shape[0], tile), lambda i, p: (0, i)) for s in swapped]
            + [pl.BlockSpec((1, width), lambda i, p: (0, 0)), pl.BlockSpec(memory_space=pltpu.HBM)],
            out_specs=[pl.BlockSpec((sub, width), lambda i, p: (0, 0))] * (1 + parts),
            scratch_shapes=[
                pltpu.VMEM((tok, width), bf16),
                pltpu.VMEM((count, width, 2 * unit_tile), bf16),
                pltpu.VMEM((blocks, rows, units), bf16),
                pltpu.VMEM((tok, units), bf16),
                pltpu.SemaphoreType.DMA((count + blocks,)),
            ],
        ),
        out_shape=[jax.ShapeDtypeStruct((sub, width), bf16)] * (1 + parts),
        compiler_params=pltpu.CompilerParams(dimension_semantics=("arbitrary",), vmem_limit_bytes=50 << 20),
        name="layer",
    )(place, *att, *sent, *swapped, gain[None, :], weights)


def line_kernel(*refs):
    rows = refs[0].shape[0]
    for n, piece in enumerate(refs[:-1]):
        refs[-1][n * rows : (n + 1) * rows, :] = piece[...]


def lined_up(*pieces):
    rows, width = pieces[0].shape
    return pl.pallas_call(
        line_kernel,
        out_shape=jax.ShapeDtypeStruct((rows * len(pieces), width), bf16),
        compiler_params=pltpu.CompilerParams(vmem_limit_bytes=8 << 20),
        name="lines",
    )(*pieces)


def shifted(value, by):
    count = lax.axis_size("tp")
    return lax.ppermute(value, "tp", [(i, (i + by) % count) for i in range(count)])


SIDE = 4


def sp_index(z, y, core):
    return (z % SIDE * SIDE + y % SIDE) * 2 + core


def crossed(value, by, turned):
    pairs = []
    for z in range(SIDE):
        for y in range(SIDE):
            for core in range(2):
                along_y = (core == 0) != turned
                goal = sp_index(z, y + by, core) if along_y else sp_index(z + by, y, core)
                pairs.append((sp_index(z, y, core), goal))
    return lax.ppermute(value, "sp", pairs)


def other_core(value):
    count = 2 * SIDE * SIDE
    return lax.ppermute(value, "sp", [(n, n ^ 1) for n in range(count)])


def on_device(
    query_rows,
    key_rows,
    value_rows,
    query_gain,
    key_gain,
    residual,
    out_weight,
    mix_gain,
    gate_weight,
    up_weight,
    down_weight,
):
    tok = query_rows.shape[0]
    parts = lax.axis_size("tp")
    units = gate_weight.shape[1]
    core = lax.axis_index("sp") % 2
    place = jnp.stack([lax.axis_index("tp"), core])
    q, kv, woven, payload, kept = prepare(
        query_rows, key_rows, value_rows, query_gain, key_gain, gate_weight, up_weight, down_weight, out_weight, residual
    )
    weights = lax.all_gather(woven, "sp", axis=0, tiled=True)

    steps = (2, 1, -1)
    line = [kv]
    for d in steps:
        line.append(crossed(kv, d, False))
    line = lined_up(*line)
    turned = []
    for d in steps:
        turned.append(crossed(line, d, True))
    far, *near = turned

    sent = [payload]
    for r in range(1, parts):
        sent.append(shifted(payload, -r))

    state = flash(q, [line, other_core(line)], None, tok, False)
    state, near = lax.optimization_barrier((state, near))
    near_swapped = [other_core(v) for v in near]
    state = flash(q, near, state, tok, False)
    state = flash(q, near_swapped, state, tok, False)
    state, far, sent = lax.optimization_barrier((state, far, sent))
    far_swapped = other_core(far)
    swapped = [kept]
    for r in range(1, parts):
        swapped.append(other_core(sent[r]))
    state = flash(q, [far], state, tok, False)
    attended = flash(q, [far_swapped], state, tok, True)

    att_parts = [attended] + [shifted(attended, -r) for r in range(1, parts)]
    own_rows, *unit_parts = layer(place, att_parts, sent, swapped, mix_gain, weights, units)
    unit_sum = unit_parts[0].astype(f32)
    for r in range(1, parts):
        unit_sum = unit_sum + shifted(unit_parts[r], r).astype(f32)
    return (own_rows.astype(f32) + 0.5 * unit_sum).astype(bf16)


def solution(mesh):
    placed = (
        P("sp", "tp"),
        P("sp", "tp"),
        P("sp", "tp"),
        P(),
        P(),
        P(("sp", "tp"), None),
        P("tp", None),
        P(),
        P("sp", "tp"),
        P("sp", "tp"),
        P("tp", "sp"),
    )
    return jax.shard_map(on_device, mesh=mesh, in_specs=placed, out_specs=P(("sp", "tp"), None), check_vma=False)
```

time: 214 us -> 185 us (0.86)
  the two profiles are of different devices: /device:TPU:0 before, /device:TPU:8 now
where the time goes in v5:
time: 185 us; the launch traced here: 183 us
  waiting for transfers between devices  79.2 us (43%)
  Pallas kernels  55.6 us (30%)
  starting transfers between devices  29.4 us (16%)
  between operations  13.6 us (7%)
  local copies, waits for them, and re-layouts  2.92 us (2%)
  other arithmetic  2.48 us (1%)
    ppermute x9, waiting for transfers between devices, shifted(): lax.ppermute(value, 'tp', [(i, (i + by) % count) for i in range(count)])  60.5 us
    pallas_call x5, Pallas kernels, flash(): pl.pallas_call(functools.partial(flash_kernel, pieces=pieces, scale=head_...  28.8 us
    pallas_call x1, Pallas kernels, layer(): pl.pallas_call(functools.partial(layer_kernel, parts=parts, tile=tile, su...  22.3 us
    ppermute x6, waiting for transfers between devices, crossed(): return lax.ppermute(value, 'sp', pairs)  18.3 us
    ppermute x9, starting transfers between devices, shifted(): lax.ppermute(value, 'tp', [(i, (i + by) % count) for i in range(count)])  16.2 us
    ppermute x6, starting transfers between devices, crossed(): return lax.ppermute(value, 'sp', pairs)  8.86 us
    pallas_call x1, Pallas kernels, prepare(): pl.pallas_call(functools.partial(prepare_kernel, rows=rows, head_dim=head...  4.5 us
    ppermute x7, starting transfers between devices, other_core(): return lax.ppermute(value, 'sp', [(n, n ^ 1) for n in range(count)])  4.33 us
  transfers between devices with their start and end apart: 23, of which 13 were waited for; matrix products, arithmetic and copies ran while one was open for 0% of the time, Pallas kernels for 16%

profile of v5, /device:TPU:8, one launch (start us, length us, event | category | flops | bytes accessed | tf_op | source)
XLA Modules:
  0.0 183.2 jit_solution(8666233621809638970)
XLA Ops:
  6.5 0.0 all-gather.2.cloned.1.call-start
  6.6 0.1 add_convert_fusion.1
  6.7 0.2 multiply_sine_fusion
  6.9 0.1 negate_select_fusion.1
  7.0 0.8 pad_maximum_fusion
  7.7 4.5 %prepare.1 = (bf16[1024,128]{1,0:T(8,128)(2,1)}, bf16[512,256]{1,0:T(8,128)(2,1)}, bf16[64,4224]{1,0:T(8,128)(2,1)}, bf16[256,2048]{1,0:T(8,128)(2,1)}, bf16[128,2048]{1,0:T(8,128)(2,1)}) custom-call(s32[1]{0:T(128)} %bitcast.1.core, bf16[512,256]{1,0:T(8,128)(2,1)} %q_hbm.1, bf16[512,128]{1,0:T(8,128)(2,1)} %k_hbm.1, bf16[512,128]{1,0:T(8,128)(2,1)} %v_hbm.1, ...), custom_call_target="tpu_custom_call" | custom-call | tf_op jit(solution)/shard_map/prepare/pallas_call | solution.py:115
  12.3 0.0 copy-start.1
  12.3 0.0 all-gather.2.cloned.1.call-update
  12.3 0.4 collective-permute-start.2
  12.7 1.7 collective-permute-start.1
  14.4 3.5 %collective-permute-start = (bf16[512,256]{1,0:T(8,128)(2,1)}, bf16[512,256]{1,0:T(8,128)(2,1)S(1)}, u32[]{:S(2)}, u32[]{:S(2)}) collective-permute-start(bf16[512,256]{1,0:T(8,128)(2,1)} %get-tuple-element.39.refs_0_), channel_id=1, source_target_pairs={{0,16},{4,68},{8,24},{12,76},{16,0},{20,84},{24,8},{28,92},{32,48}... | collective-permute-start | bytes 786440 | tf_op jit(solution)/shard_map/ppermute | solution.py:345
  17.9 1.0 collective-permute-done.2.refs_3_
  18.9 1.5 collective-permute-done.1.refs_2_
  20.4 2.3 %collective-permute-done.refs_1_ = bf16[512,256]{1,0:T(8,128)(2,1)S(1)} collective-permute-done((bf16[512,256]{1,0:T(8,128)(2,1)}, bf16[512,256]{1,0:T(8,128)(2,1)S(1)}, u32[]{:S(2)}, u32[]{:S(2)}) %collective-permute-start) | collective-permute-done | bytes 262176 | tf_op jit(solution)/shard_map/ppermute | solution.py:345
  22.8 0.9 copy-done
  23.7 0.1 lines.1.refs_1_
  23.8 2.7 %collective-permute-start.3 = (bf16[2048,256]{1,0:T(8,128)(2,1)S(1)}, bf16[2048,256]{1,0:T(8,128)(2,1)S(1)}, u32[]{:S(2)}, u32[]{:S(2)}) collective-permute-start(bf16[2048,256]{1,0:T(8,128)(2,1)S(1)} %lines.1.refs_1_), channel_id=1, source_target_pairs={{0,4},{4,0},{8,12},{12,8},{16,20},{20,16},{24,28},{28,24},{32,36},... | collective-permute-start | bytes 3145736 | tf_op jit(solution)/shard_map/ppermute | solution.py:350
  26.5 1.5 collective-permute-start.5
  28.0 0.5 collective-permute-start.4
  28.5 0.3 collective-permute-done.3.refs_2_
  28.8 0.9 copy-done.2
  29.8 6.2 %flash_first.1 = (f32[1024,128]{1,0:T(8,128)S(1)}, f32[1024,256]{1,0:T(8,128)S(1)}) custom-call(bf16[1024,128]{1,0:T(8,128)(2,1)S(1)} %copy-done.2, bf16[2048,256]{1,0:T(8,128)(2,1)S(1)} %lines.1.refs_1_, bf16[2048,256]{1,0:T(8,128)(2,1)S(1)} %collective-permute-done.3.refs_2_), custom_call_target="tpu_custom_call" | custom-call | flops 2147483648 | bytes 2097152 | tf_op jit(solution)/shard_map/flash_first/pallas_call | solution.py:190
  36.0 11.9 %collective-permute-done.5.refs_2_ = bf16[2048,256]{1,0:T(8,128)(2,1)S(1)} collective-permute-done((bf16[2048,256]{1,0:T(8,128)(2,1)S(1)}, bf16[2048,256]{1,0:T(8,128)(2,1)S(1)}, u32[]{:S(2)}, u32[]{:S(2)}) %collective-permute-start.5) | collective-permute-done | bytes 1048608 | tf_op jit(solution)/shard_map/ppermute | solution.py:345
  47.9 1.6 collective-permute-done.4.refs_1_
  49.4 0.0 collective-permute-start.6
  49.5 0.5 collective-permute-start.7
  50.0 1.5 collective-permute-start.11
  51.4 2.7 %collective-permute-start.10 = (bf16[256,2048]{1,0:T(8,128)(2,1)}, bf16[256,2048]{1,0:T(8,128)(2,1)S(1)}, u32[]{:S(2)}, u32[]{:S(2)}) collective-permute-start(bf16[256,2048]{1,0:T(8,128)(2,1)} %get-tuple-element.56.refs_4_), channel_id=1, source_target_pairs={{0,2},{1,3},{2,0},{3,1},{4,6},{5,7},{6,4},{7,5},{8,10},{9,11},{10,... | collective-permute-start | bytes 3145736 | tf_op jit(solution)/shard_map/ppermute | solution.py:327
  54.2 1.4 collective-permute-start.9
  55.6 0.0 collective-permute-done.6.refs_1_
  55.6 1.2 collective-permute-start.8
  56.9 6.9 %flash_more.3 = (f32[1024,128]{1,0:T(8,128)S(1)}, f32[1024,256]{1,0:T(8,128)S(1)}) custom-call(bf16[1024,128]{1,0:T(8,128)(2,1)S(1)} %copy-done.2, bf16[2048,256]{1,0:T(8,128)(2,1)S(1)} %collective-permute-done.4.refs_1_, bf16[2048,256]{1,0:T(8,128)(2,1)S(1)} %collective-permute-done.5.refs_2_, f32[1024,128]{1,0:T(8,128)S(1)} %get-tuple-element.44.refs_3_, ...), custom_call_target="tpu_custom_call" | custom-call | flops 2147483648 | bytes 2097152 | tf_op jit(solution)/shard_map/flash_more/pallas_call | solution.py:190
  63.8 0.0 collective-permute-done.7.refs_2_
  63.8 6.9 %flash_more.4 = (f32[1024,128]{1,0:T(8,128)S(1)}, f32[1024,256]{1,0:T(8,128)S(1)}) custom-call(bf16[1024,128]{1,0:T(8,128)(2,1)S(1)} %copy-done.2, bf16[2048,256]{1,0:T(8,128)(2,1)S(1)} %collective-permute-done.6.refs_1_, bf16[2048,256]{1,0:T(8,128)(2,1)S(1)} %collective-permute-done.7.refs_2_, f32[1024,128]{1,0:T(8,128)S(1)} %get-tuple-element.46.refs_3_, ...), custom_call_target="tpu_custom_call" | custom-call | flops 2147483648 | bytes 2097152 | tf_op jit(solution)/shard_map/flash_more/pallas_call | solution.py:190
  70.8 5.7 %collective-permute-done.11.refs_7_ = bf16[256,2048]{1,0:T(8,128)(2,1)S(1)} collective-permute-done((bf16[256,2048]{1,0:T(8,128)(2,1)}, bf16[256,2048]{1,0:T(8,128)(2,1)S(1)}, u32[]{:S(2)}, u32[]{:S(2)}) %collective-permute-start.11) | collective-permute-done | bytes 1048608 | tf_op jit(solution)/shard_map/ppermute | solution.py:327
  76.4 23.5 %collective-permute-done.10.refs_6_ = bf16[256,2048]{1,0:T(8,128)(2,1)S(1)} collective-permute-done((bf16[256,2048]{1,0:T(8,128)(2,1)}, bf16[256,2048]{1,0:T(8,128)(2,1)S(1)}, u32[]{:S(2)}, u32[]{:S(2)}) %collective-permute-start.10) | collective-permute-done | bytes 1048608 | tf_op jit(solution)/shard_map/ppermute | solution.py:327
  99.9 0.0 collective-permute-done.9.refs_5_
  99.9 0.0 collective-permute-done.8.refs_1_
  99.9 0.1 collective-permute-start.12
  100.0 0.5 collective-permute-start.16
  100.5 0.1 collective-permute-start.17
  100.6 0.4 collective-permute-start.18
  101.0 4.2 %flash_more.5 = (f32[1024,128]{1,0:T(8,128)S(1)}, f32[1024,256]{1,0:T(8,128)S(1)}) custom-call(bf16[1024,128]{1,0:T(8,128)(2,1)S(1)} %copy-done.2, bf16[2048,256]{1,0:T(8,128)(2,1)S(1)} %collective-permute-done.8.refs_1_, f32[1024,128]{1,0:T(8,128)S(1)} %get-tuple-element.52.refs_2_, f32[1024,256]{1,0:T(8,128)S(1)} %get-tuple-element.53.refs_3_), custom_call_target="tpu_custom_call" | custom-call | flops 1073741824 | bytes 1048576 | tf_op jit(solution)/shard_map/flash_more/pallas_call | solution.py:190
  105.3 0.0 collective-permute-done.12.refs_1_
  105.3 4.4 %flash_last.1.refs_0_ = bf16[512,256]{1,0:T(8,128)(2,1)S(1)} custom-call(bf16[1024,128]{1,0:T(8,128)(2,1)S(1)} %copy-done.2, bf16[2048,256]{1,0:T(8,128)(2,1)S(1)} %collective-permute-done.12.refs_1_, f32[1024,128]{1,0:T(8,128)S(1)} %get-tuple-element.54.refs_2_, f32[1024,256]{1,0:T(8,128)S(1)} %get-tuple-element.55.refs_3_), custom_call_target="tpu_custom_call" | custom-call | flops 1073741824 | bytes 1048576 | tf_op jit(solution)/shard_map/flash_last/pallas_call | solution.py:190
  109.7 1.3 collective-permute-start.15
  111.0 2.4 %collective-permute-start.14 = (bf16[512,256]{1,0:T(8,128)(2,1)S(1)}, bf16[512,256]{1,0:T(8,128)(2,1)S(1)}, u32[]{:S(2)}, u32[]{:S(2)}) collective-permute-start(bf16[512,256]{1,0:T(8,128)(2,1)S(1)} %flash_last.1.refs_0_), channel_id=1, source_target_pairs={{0,2},{1,3},{2,0},{3,1},{4,6},{5,7},{6,4},{7,5},{8,10},{9,11},{10,... | collective-permute-start | bytes 786440 | tf_op jit(solution)/shard_map/ppermute | solution.py:327
  113.4 0.0 collective-permute-done.16.refs_9_
  113.4 1.0 copy-done.6
  114.4 1.6 collective-permute-start.13
  116.0 0.1 pad_add_fusion.place
  116.1 0.0 collective-permute-done.17.refs_10_
  116.1 0.0 collective-permute-done.18.refs_11_
  116.1 3.6 %collective-permute-done.15.refs_3_ = bf16[512,256]{1,0:T(8,128)(2,1)S(1)} collective-permute-done((bf16[512,256]{1,0:T(8,128)(2,1)S(1)}, bf16[512,256]{1,0:T(8,128)(2,1)S(1)}, u32[]{:S(2)}, u32[]{:S(2)}) %collective-permute-start.15) | collective-permute-done | bytes 262176 | tf_op jit(solution)/shard_map/ppermute | solution.py:327
  119.7 5.6 %collective-permute-done.14.refs_2_ = bf16[512,256]{1,0:T(8,128)(2,1)S(1)} collective-permute-done((bf16[512,256]{1,0:T(8,128)(2,1)S(1)}, bf16[512,256]{1,0:T(8,128)(2,1)S(1)}, u32[]{:S(2)}, u32[]{:S(2)}) %collective-permute-start.14) | collective-permute-done | bytes 262176 | tf_op jit(solution)/shard_map/ppermute | solution.py:327
  125.3 0.2 collective-permute-done.13.refs_1_
  125.6 22.3 %layer.1 = (bf16[128,2048]{1,0:T(8,128)(2,1)S(1)}, bf16[128,2048]{1,0:T(8,128)(2,1)S(1)}, bf16[128,2048]{1,0:T(8,128)(2,1)S(1)}, bf16[128,2048]{1,0:T(8,128)(2,1)S(1)}, bf16[128,2048]{1,0:T(8,128)(2,1)S(1)}) custom-call(s32[2]{0:T(128)S(1)} %pad_add_fusion.place, bf16[512,256]{1,0:T(8,128)(2,1)S(1)} %flash_last.1.refs_0_, ...), custom_call_target="tpu_custom_call" | custom-call | tf_op jit(solution)/shard_map/layer/pallas_call | solution.py:285
  147.9 2.0 %collective-permute-start.19 = (bf16[128,2048]{1,0:T(8,128)(2,1)S(1)}, bf16[128,2048]{1,0:T(8,128)(2,1)S(1)}, u32[]{:S(2)}, u32[]{:S(2)}) collective-permute-start(bf16[128,2048]{1,0:T(8,128)(2,1)S(1)} %get-tuple-element.64), channel_id=1, source_target_pairs={{0,1},{1,2},{2,3},{3,0},{4,5},{5,6},{6,7},{7,4},{8,9},{9,10},{10,1... | collective-permute-start | bytes 1572872 | tf_op jit(solution)/shard_map/ppermute | solution.py:327
  149.8 2.2 %collective-permute-start.20 = (bf16[128,2048]{1,0:T(8,128)(2,1)S(1)}, bf16[128,2048]{1,0:T(8,128)(2,1)S(1)}, u32[]{:S(2)}, u32[]{:S(2)}) collective-permute-start(bf16[128,2048]{1,0:T(8,128)(2,1)S(1)} %get-tuple-element.65), channel_id=1, source_target_pairs={{0,2},{1,3},{2,0},{3,1},{4,6},{5,7},{6,4},{7,5},{8,10},{9,11},{10,... | collective-permute-start | bytes 1572872 | tf_op jit(solution)/shard_map/ppermute | solution.py:327
  152.0 1.1 collective-permute-start.21
  153.1 9.5 %collective-permute-done.19 = bf16[128,2048]{1,0:T(8,128)(2,1)S(1)} collective-permute-done((bf16[128,2048]{1,0:T(8,128)(2,1)S(1)}, bf16[128,2048]{1,0:T(8,128)(2,1)S(1)}, u32[]{:S(2)}, u32[]{:S(2)}) %collective-permute-start.19) | collective-permute-done | bytes 524320 | tf_op jit(solution)/shard_map/ppermute | solution.py:327
  162.7 12.4 %collective-permute-done.20 = bf16[128,2048]{1,0:T(8,128)(2,1)S(1)} collective-permute-done((bf16[128,2048]{1,0:T(8,128)(2,1)S(1)}, bf16[128,2048]{1,0:T(8,128)(2,1)S(1)}, u32[]{:S(2)}, u32[]{:S(2)}) %collective-permute-start.20) | collective-permute-done | bytes 524320 | tf_op jit(solution)/shard_map/ppermute | solution.py:327
  175.1 0.0 collective-permute-done.21
  175.1 1.2 add_convert_fusion
  (15 shorter events, 0.0 us)
Async XLA Ops:
  6.5 119.0 %all-gather.2.cloned.1.call-start = ((), (), s32[]{:S(2)}) async-start(), calls=%async_computation | async-start | bytes 17842176 | tf_op jit(solution)/shard_map/all_gather | solution.py:374
  12.3 113.3 %copy-start.1 = (f32[2048]{0:T(1024)S(1)}, f32[2048]{0:T(1024)}, u32[]{:S(2)}) copy-start(f32[2048]{0:T(1024)} %param.18) | copy-start | bytes 24580
  12.3 6.7 %collective-permute-start.2 = (bf16[512,256]{1,0:T(8,128)(2,1)}, bf16[512,256]{1,0:T(8,128)(2,1)S(1)}, u32[]{:S(2)}, u32[]{:S(2)}) collective-permute-start(bf16[512,256]{1,0:T(8,128)(2,1)} %get-tuple-element.39.refs_0_), channel_id=1, source_target_pairs={{0,24},{4,100},{8,0},{12,108},{16,8},{20,116},{24,16},{28,124},{32... | collective-permute-start | bytes 786440 | tf_op jit(solution)/shard_map/ppermute | solution.py:345
  12.7 7.7 %collective-permute-start.1 = (bf16[512,256]{1,0:T(8,128)(2,1)}, bf16[512,256]{1,0:T(8,128)(2,1)S(1)}, u32[]{:S(2)}, u32[]{:S(2)}) collective-permute-start(bf16[512,256]{1,0:T(8,128)(2,1)} %get-tuple-element.39.refs_0_), channel_id=1, source_target_pairs={{0,8},{4,36},{8,16},{12,44},{16,24},{20,52},{24,0},{28,60},{32,40}... | collective-permute-start | bytes 786440 | tf_op jit(solution)/shard_map/ppermute | solution.py:345
  14.4 8.4 %collective-permute-start = (bf16[512,256]{1,0:T(8,128)(2,1)}, bf16[512,256]{1,0:T(8,128)(2,1)S(1)}, u32[]{:S(2)}, u32[]{:S(2)}) collective-permute-start(bf16[512,256]{1,0:T(8,128)(2,1)} %get-tuple-element.39.refs_0_), channel_id=1, source_target_pairs={{0,16},{4,68},{8,24},{12,76},{16,0},{20,84},{24,8},{28,92},{32,48}... | collective-permute-start | bytes 786440 | tf_op jit(solution)/shard_map/ppermute | solution.py:345
  22.8 1.0 copy-start
  23.8 5.0 %collective-permute-start.3 = (bf16[2048,256]{1,0:T(8,128)(2,1)S(1)}, bf16[2048,256]{1,0:T(8,128)(2,1)S(1)}, u32[]{:S(2)}, u32[]{:S(2)}) collective-permute-start(bf16[2048,256]{1,0:T(8,128)(2,1)S(1)} %lines.1.refs_1_), channel_id=1, source_target_pairs={{0,4},{4,0},{8,12},{12,8},{16,20},{20,16},{24,28},{28,24},{32,36},... | collective-permute-start | bytes 3145736 | tf_op jit(solution)/shard_map/ppermute | solution.py:350
  26.5 21.3 %collective-permute-start.5 = (bf16[2048,256]{1,0:T(8,128)(2,1)S(1)}, bf16[2048,256]{1,0:T(8,128)(2,1)S(1)}, u32[]{:S(2)}, u32[]{:S(2)}) collective-permute-start(bf16[2048,256]{1,0:T(8,128)(2,1)S(1)} %lines.1.refs_1_), channel_id=1, source_target_pairs={{0,96},{4,28},{8,104},{12,4},{16,112},{20,12},{24,120},{28,20},{32... | collective-permute-start | bytes 3145736 | tf_op jit(solution)/shard_map/ppermute | solution.py:345
  28.0 21.4 %collective-permute-start.4 = (bf16[2048,256]{1,0:T(8,128)(2,1)S(1)}, bf16[2048,256]{1,0:T(8,128)(2,1)S(1)}, u32[]{:S(2)}, u32[]{:S(2)}) collective-permute-start(bf16[2048,256]{1,0:T(8,128)(2,1)S(1)} %lines.1.refs_1_), channel_id=1, source_target_pairs={{0,32},{4,12},{8,40},{12,20},{16,48},{20,28},{24,56},{28,4},{32,64... | collective-permute-start | bytes 3145736 | tf_op jit(solution)/shard_map/ppermute | solution.py:345
  28.8 0.9 copy-start.2
  49.4 6.2 %collective-permute-start.6 = (bf16[2048,256]{1,0:T(8,128)(2,1)S(1)}, bf16[2048,256]{1,0:T(8,128)(2,1)S(1)}, u32[]{:S(2)}, u32[]{:S(2)}) collective-permute-start(bf16[2048,256]{1,0:T(8,128)(2,1)S(1)} %collective-permute-done.4.refs_1_), channel_id=1, source_target_pairs={{0,4},{4,0},{8,12},{12,8},{16,20},{20,16},{24,28},{28,24},{32,36},... | collective-permute-start | bytes 3145736 | tf_op jit(solution)/shard_map/ppermute | solution.py:350
  49.5 14.3 %collective-permute-start.7 = (bf16[2048,256]{1,0:T(8,128)(2,1)S(1)}, bf16[2048,256]{1,0:T(8,128)(2,1)S(1)}, u32[]{:S(2)}, u32[]{:S(2)}) collective-permute-start(bf16[2048,256]{1,0:T(8,128)(2,1)S(1)} %collective-permute-done.5.refs_2_), channel_id=1, source_target_pairs={{0,4},{4,0},{8,12},{12,8},{16,20},{20,16},{24,28},{28,24},{32,36},... | collective-permute-start | bytes 3145736 | tf_op jit(solution)/shard_map/ppermute | solution.py:350
  50.0 26.5 %collective-permute-start.11 = (bf16[256,2048]{1,0:T(8,128)(2,1)}, bf16[256,2048]{1,0:T(8,128)(2,1)S(1)}, u32[]{:S(2)}, u32[]{:S(2)}) collective-permute-start(bf16[256,2048]{1,0:T(8,128)(2,1)} %get-tuple-element.56.refs_4_), channel_id=1, source_target_pairs={{0,1},{1,2},{2,3},{3,0},{4,5},{5,6},{6,7},{7,4},{8,9},{9,10},{10,1... | collective-permute-start | bytes 3145736 | tf_op jit(solution)/shard_map/ppermute | solution.py:327
  51.4 48.5 %collective-permute-start.10 = (bf16[256,2048]{1,0:T(8,128)(2,1)}, bf16[256,2048]{1,0:T(8,128)(2,1)S(1)}, u32[]{:S(2)}, u32[]{:S(2)}) collective-permute-start(bf16[256,2048]{1,0:T(8,128)(2,1)} %get-tuple-element.56.refs_4_), channel_id=1, source_target_pairs={{0,2},{1,3},{2,0},{3,1},{4,6},{5,7},{6,4},{7,5},{8,10},{9,11},{10,... | collective-permute-start | bytes 3145736 | tf_op jit(solution)/shard_map/ppermute | solution.py:327
  54.2 45.7 %collective-permute-start.9 = (bf16[256,2048]{1,0:T(8,128)(2,1)}, bf16[256,2048]{1,0:T(8,128)(2,1)S(1)}, u32[]{:S(2)}, u32[]{:S(2)}) collective-permute-start(bf16[256,2048]{1,0:T(8,128)(2,1)} %get-tuple-element.56.refs_4_), channel_id=1, source_target_pairs={{0,3},{1,0},{2,1},{3,2},{4,7},{5,4},{6,5},{7,6},{8,11},{9,8},{10,9... | collective-permute-start | bytes 3145736 | tf_op jit(solution)/shard_map/ppermute | solution.py:327
  55.6 44.3 %collective-permute-start.8 = (bf16[2048,256]{1,0:T(8,128)(2,1)S(1)}, bf16[2048,256]{1,0:T(8,128)(2,1)S(1)}, u32[]{:S(2)}, u32[]{:S(2)}) collective-permute-start(bf16[2048,256]{1,0:T(8,128)(2,1)S(1)} %lines.1.refs_1_), channel_id=1, source_target_pairs={{0,64},{4,20},{8,72},{12,28},{16,80},{20,4},{24,88},{28,12},{32,96... | collective-permute-start | bytes 3145736 | tf_op jit(solution)/shard_map/ppermute | solution.py:345
  76.4 49.1 %copy-start.3 = (bf16[256,2048]{1,0:T(8,128)(2,1)}, bf16[256,2048]{1,0:T(8,128)(2,1)S(1)}, u32[]{:S(2)}) copy-start(bf16[256,2048]{1,0:T(8,128)(2,1)S(1)} %collective-permute-done.11.refs_7_) | copy-start | bytes 3145732
  99.9 25.6 %copy-start.4 = (bf16[256,2048]{1,0:T(8,128)(2,1)}, bf16[256,2048]{1,0:T(8,128)(2,1)S(1)}, u32[]{:S(2)}) copy-start(bf16[256,2048]{1,0:T(8,128)(2,1)S(1)} %collective-permute-done.10.refs_6_) | copy-start | bytes 3145732
  99.9 13.5 %copy-start.5 = (bf16[256,2048]{1,0:T(8,128)(2,1)}, bf16[256,2048]{1,0:T(8,128)(2,1)S(1)}, u32[]{:S(2)}) copy-start(bf16[256,2048]{1,0:T(8,128)(2,1)S(1)} %collective-permute-done.9.refs_5_) | copy-start | bytes 3145732
  99.9 5.4 %collective-permute-start.12 = (bf16[2048,256]{1,0:T(8,128)(2,1)S(1)}, bf16[2048,256]{1,0:T(8,128)(2,1)S(1)}, u32[]{:S(2)}, u32[]{:S(2)}) collective-permute-start(bf16[2048,256]{1,0:T(8,128)(2,1)S(1)} %collective-permute-done.8.refs_1_), channel_id=1, source_target_pairs={{0,4},{4,0},{8,12},{12,8},{16,20},{20,16},{24,28},{28,24},{32,36},... | collective-permute-start | bytes 3145736 | tf_op jit(solution)/shard_map/ppermute | solution.py:350
  100.0 13.4 %collective-permute-start.16 = (bf16[256,2048]{1,0:T(8,128)(2,1)S(1)}, bf16[256,2048]{1,0:T(8,128)(2,1)S(1)}, u32[]{:S(2)}, u32[]{:S(2)}) collective-permute-start(bf16[256,2048]{1,0:T(8,128)(2,1)S(1)} %collective-permute-done.9.refs_5_), channel_id=1, source_target_pairs={{0,4},{4,0},{8,12},{12,8},{16,20},{20,16},{24,28},{28,24},{32,36},... | collective-permute-start | bytes 3145736 | tf_op jit(solution)/shard_map/ppermute | solution.py:350
  100.5 15.6 %collective-permute-start.17 = (bf16[256,2048]{1,0:T(8,128)(2,1)S(1)}, bf16[256,2048]{1,0:T(8,128)(2,1)}, u32[]{:S(2)}, u32[]{:S(2)}) collective-permute-start(bf16[256,2048]{1,0:T(8,128)(2,1)S(1)} %collective-permute-done.10.refs_6_), channel_id=1, source_target_pairs={{0,4},{4,0},{8,12},{12,8},{16,20},{20,16},{24,28},{28,24},{32,36},... | collective-permute-start | bytes 3145736 | tf_op jit(solution)/shard_map/ppermute | solution.py:350
  100.6 15.5 %collective-permute-start.18 = (bf16[256,2048]{1,0:T(8,128)(2,1)S(1)}, bf16[256,2048]{1,0:T(8,128)(2,1)}, u32[]{:S(2)}, u32[]{:S(2)}) collective-permute-start(bf16[256,2048]{1,0:T(8,128)(2,1)S(1)} %collective-permute-done.11.refs_7_), channel_id=1, source_target_pairs={{0,4},{4,0},{8,12},{12,8},{16,20},{20,16},{24,28},{28,24},{32,36},... | collective-permute-start | bytes 3145736 | tf_op jit(solution)/shard_map/ppermute | solution.py:350
  109.7 10.0 %collective-permute-start.15 = (bf16[512,256]{1,0:T(8,128)(2,1)S(1)}, bf16[512,256]{1,0:T(8,128)(2,1)S(1)}, u32[]{:S(2)}, u32[]{:S(2)}) collective-permute-start(bf16[512,256]{1,0:T(8,128)(2,1)S(1)} %flash_last.1.refs_0_), channel_id=1, source_target_pairs={{0,1},{1,2},{2,3},{3,0},{4,5},{5,6},{6,7},{7,4},{8,9},{9,10},{10,1... | collective-permute-start | bytes 786440 | tf_op jit(solution)/shard_map/ppermute | solution.py:327
  111.0 14.3 %collective-permute-start.14 = (bf16[512,256]{1,0:T(8,128)(2,1)S(1)}, bf16[512,256]{1,0:T(8,128)(2,1)S(1)}, u32[]{:S(2)}, u32[]{:S(2)}) collective-permute-start(bf16[512,256]{1,0:T(8,128)(2,1)S(1)} %flash_last.1.refs_0_), channel_id=1, source_target_pairs={{0,2},{1,3},{2,0},{3,1},{4,6},{5,7},{6,4},{7,5},{8,10},{9,11},{10,... | collective-permute-start | bytes 786440 | tf_op jit(solution)/shard_map/ppermute | solution.py:327
  113.4 1.0 copy-start.6
  114.4 11.1 %collective-permute-start.13 = (bf16[512,256]{1,0:T(8,128)(2,1)S(1)}, bf16[512,256]{1,0:T(8,128)(2,1)S(1)}, u32[]{:S(2)}, u32[]{:S(2)}) collective-permute-start(bf16[512,256]{1,0:T(8,128)(2,1)S(1)} %flash_last.1.refs_0_), channel_id=1, source_target_pairs={{0,3},{1,0},{2,1},{3,2},{4,7},{5,4},{6,5},{7,6},{8,11},{9,8},{10,9... | collective-permute-start | bytes 786440 | tf_op jit(solution)/shard_map/ppermute | solution.py:327
  147.9 14.8 %collective-permute-start.19 = (bf16[128,2048]{1,0:T(8,128)(2,1)S(1)}, bf16[128,2048]{1,0:T(8,128)(2,1)S(1)}, u32[]{:S(2)}, u32[]{:S(2)}) collective-permute-start(bf16[128,2048]{1,0:T(8,128)(2,1)S(1)} %get-tuple-element.64), channel_id=1, source_target_pairs={{0,1},{1,2},{2,3},{3,0},{4,5},{5,6},{6,7},{7,4},{8,9},{9,10},{10,1... | collective-permute-start | bytes 1572872 | tf_op jit(solution)/shard_map/ppermute | solution.py:327
  149.8 25.2 %collective-permute-start.20 = (bf16[128,2048]{1,0:T(8,128)(2,1)S(1)}, bf16[128,2048]{1,0:T(8,128)(2,1)S(1)}, u32[]{:S(2)}, u32[]{:S(2)}) collective-permute-start(bf16[128,2048]{1,0:T(8,128)(2,1)S(1)} %get-tuple-element.65), channel_id=1, source_target_pairs={{0,2},{1,3},{2,0},{3,1},{4,6},{5,7},{6,4},{7,5},{8,10},{9,11},{10,... | collective-permute-start | bytes 1572872 | tf_op jit(solution)/shard_map/ppermute | solution.py:327
  152.0 23.1 %collective-permute-start.21 = (bf16[128,2048]{1,0:T(8,128)(2,1)S(1)}, bf16[128,2048]{1,0:T(8,128)(2,1)S(1)}, u32[]{:S(2)}, u32[]{:S(2)}) collective-permute-start(bf16[128,2048]{1,0:T(8,128)(2,1)S(1)} %get-tuple-element.66), channel_id=1, source_target_pairs={{0,3},{1,0},{2,1},{3,2},{4,7},{5,4},{6,5},{7,6},{8,11},{9,8},{10,9... | collective-permute-start | bytes 1572872 | tf_op jit(solution)/shard_map/ppermute | solution.py:327
Sparse Core Ops, SparseCore 0:
  12.4 89.7 all-gather.1

commit v6 on v5

--- a/solution.py
+++ b/solution.py
@@ -210,7 +210,7 @@
     sent = refs[parts : 2 * parts]
     swapped = refs[2 * parts : 3 * parts]
     gain_ref, w_hbm, own_ref = refs[3 * parts : 3 * parts + 3]
-    outs = refs[3 * parts + 3 : -5]
+    out_1, out_2, rest_ref = refs[3 * parts + 3 : -5]
     x_ref, pair_ref, down_ref, h_ref, sems = refs[-5:]
     step = pl.program_id(0)
     half = sent[0].shape[0] - sub
@@ -269,10 +269,44 @@
             gate = r[:, 0:unit_tile]
             hidden = gate / (1.0 + jnp.exp(-gate)) * r[:, unit_tile:]
             h_ref[:, n * unit_tile : (n + 1) * unit_tile] = hidden.astype(bf16)
-        for n in range(blocks):
-            y = lax.dot_general(h_ref[...], down_ref[n], (((1,), (1,)), ((), ())), preferred_element_type=f32).astype(bf16)
-            for p, out in enumerate(outs):
-                out[:, n * rows : (n + 1) * rows] = y[p * sub : (p + 1) * sub, :]
+        rest_ref[0:sub, :] = h_ref[0:sub, :]
+        rest_ref[sub:, :] = h_ref[3 * sub :, :]
+        down_products(h_ref[sub : 3 * sub, :], down_ref, (out_1, out_2))
+
+
+def down_products(hidden, down_ref, outs):
+    blocks, rows, _ = down_ref.shape
+    sub = outs[0].shape[0]
+    for n in range(blocks):
+        y = lax.dot_general(hidden, down_ref[n], (((1,), (1,)), ((), ())), preferred_element_type=f32).astype(bf16)
+        for p, out in enumerate(outs):
+            out[:, n * rows : (n + 1) * rows] = y[p * sub : (p + 1) * sub, :]
+
+
+def rest_kernel(h_ref, w_hbm, out_0, out_3, down_ref, sems):
+    blocks, rows, units = down_ref.shape
+    copies = []
+    for n in range(blocks):
+        source = w_hbm.at[pl.ds(n * rows, rows), pl.ds(2 * units, units)]
+        copies.append(pltpu.make_async_copy(source, down_ref.at[n], sems.at[n]))
+    for c in copies:
+        c.start()
+    for c in copies:
+        c.wait()
+    down_products(h_ref[...], down_ref, (out_0, out_3))
+
+
+def rest(hidden, weights, rows=512):
+    tok, units = hidden.shape
+    width = weights.shape[0]
+    return pl.pallas_call(
+        rest_kernel,
+        in_specs=[pl.BlockSpec(memory_space=pltpu.VMEM), pl.BlockSpec(memory_space=pltpu.HBM)],
+        out_shape=[jax.ShapeDtypeStruct((tok // 2, width), bf16)] * 2,
+        scratch_shapes=[pltpu.VMEM((width // rows, rows, units), bf16), pltpu.SemaphoreType.DMA((width // rows,))],
+        compiler_params=pltpu.CompilerParams(vmem_limit_bytes=50 << 20),
+        name="rest",
+    )(hidden, weights)
 
 
 def layer(place, att, sent, swapped, gain, weights, units, tile=512, unit_tile=128, rows=512):
@@ -291,7 +325,8 @@
             + [pl.BlockSpec((both, tile), lambda i, p: (0, i))] * parts
             + [pl.BlockSpec((s.shape[0], tile), lambda i, p: (0, i)) for s in swapped]
             + [pl.BlockSpec((1, width), lambda i, p: (0, 0)), pl.BlockSpec(memory_space=pltpu.HBM)],
-            out_specs=[pl.BlockSpec((sub, width), lambda i, p: (0, 0))] * (1 + parts),
+            out_specs=[pl.BlockSpec((sub, width), lambda i, p: (0, 0))] * 3
+            + [pl.BlockSpec((2 * sub, units), lambda i, p: (0, 0))],
             scratch_shapes=[
                 pltpu.VMEM((tok, width), bf16),
                 pltpu.VMEM((count, width, 2 * unit_tile), bf16),
@@ -300,24 +335,28 @@
                 pltpu.SemaphoreType.DMA((count + blocks,)),
             ],
         ),
-        out_shape=[jax.ShapeDtypeStruct((sub, width), bf16)] * (1 + parts),
+        out_shape=[jax.ShapeDtypeStruct((sub, width), bf16)] * 3 + [jax.ShapeDtypeStruct((2 * sub, units), bf16)],
         compiler_params=pltpu.CompilerParams(dimension_semantics=("arbitrary",), vmem_limit_bytes=50 << 20),
         name="layer",
     )(place, *att, *sent, *swapped, gain[None, :], weights)
 
 
 def line_kernel(*refs):
-    rows = refs[0].shape[0]
-    for n, piece in enumerate(refs[:-1]):
-        refs[-1][n * rows : (n + 1) * rows, :] = piece[...]
+    pieces, (whole, *halves) = refs[:-3], refs[-3:]
+    rows = pieces[0].shape[0]
+    each = len(pieces) // 2
+    for n, piece in enumerate(pieces):
+        whole[n * rows : (n + 1) * rows, :] = piece[...]
+        halves[n // each][n % each * rows : (n % each + 1) * rows, :] = piece[...]
 
 
 def lined_up(*pieces):
     rows, width = pieces[0].shape
+    count = rows * len(pieces)
     return pl.pallas_call(
         line_kernel,
-        out_shape=jax.ShapeDtypeStruct((rows * len(pieces), width), bf16),
-        compiler_params=pltpu.CompilerParams(vmem_limit_bytes=8 << 20),
+        out_shape=[jax.ShapeDtypeStruct((n, width), bf16) for n in (count, count // 2, count // 2)],
+        compiler_params=pltpu.CompilerParams(vmem_limit_bytes=10 << 20),
         name="lines",
     )(*pieces)
 
@@ -377,11 +416,13 @@
     line = [kv]
     for d in steps:
         line.append(crossed(kv, d, False))
-    line = lined_up(*line)
-    turned = []
-    for d in steps:
-        turned.append(crossed(line, d, True))
-    far, *near = turned
+    line, *halves = lined_up(*line)
+    near = []
+    for d in (1, -1):
+        near.append(crossed(line, d, True))
+    far = []
+    for n in range(2):
+        far.append(crossed(halves[n], 2, True))
 
     sent = [payload]
     for r in range(1, parts):
@@ -392,19 +433,22 @@
     near_swapped = [other_core(v) for v in near]
     state = flash(q, near, state, tok, False)
     state = flash(q, near_swapped, state, tok, False)
-    state, far, sent = lax.optimization_barrier((state, far, sent))
-    far_swapped = other_core(far)
+    state, far[0] = lax.optimization_barrier((state, far[0]))
+    far_swapped = [other_core(far[0])]
+    state = flash(q, [far[0], far_swapped[0]], state, tok, False)
+    state, far[1], sent = lax.optimization_barrier((state, far[1], sent))
+    far_swapped.append(other_core(far[1]))
     swapped = [kept]
     for r in range(1, parts):
         swapped.append(other_core(sent[r]))
-    state = flash(q, [far], state, tok, False)
-    attended = flash(q, [far_swapped], state, tok, True)
+    attended = flash(q, [far[1], far_swapped[1]], state, tok, True)
 
     att_parts = [attended] + [shifted(attended, -r) for r in range(1, parts)]
-    own_rows, *unit_parts = layer(place, att_parts, sent, swapped, mix_gain, weights, units)
-    unit_sum = unit_parts[0].astype(f32)
-    for r in range(1, parts):
-        unit_sum = unit_sum + shifted(unit_parts[r], r).astype(f32)
+    own_rows, part_1, part_2, hidden = layer(place, att_parts, sent, swapped, mix_gain, weights, units)
+    part_0, part_3 = rest(hidden, weights)
+    unit_sum = part_0.astype(f32)
+    for r, part in ((1, part_1), (2, part_2), (3, part_3)):
+        unit_sum = unit_sum + shifted(part, r).astype(f32)
     return (own_rows.astype(f32) + 0.5 * unit_sum).astype(bf16)
 
 

time: 185 us -> 185 us (level)
  Pallas kernels: 55.6 us -> 58.1 us
    ppermute x9, waiting for transfers between devices: 60.5 us -> 41 us  [shifted(): lax.ppermute(value, 'tp', [(i, (i + by) % count) for i in range(count)])]
    ppermute x6 -> x7, waiting for transfers between devices: 18.3 us -> 35.4 us  [crossed(): return lax.ppermute(value, 'sp', pairs)]
    pallas_call x1 -> x2, Pallas kernels: 0.07 us -> 4.7 us  [the longest x1 4.56 us: rest(): pl.pallas_call(rest_kernel, in_specs=[pl.BlockSpec(memory_space=pltpu.VME...]
    pallas_call x1, Pallas kernels: 22.3 us -> 20.2 us  [layer(): pl.pallas_call(functools.partial(layer_kernel, parts=parts, tile=tile, su...]
    ppermute x6 -> x7, starting transfers between devices: 8.86 us -> 10.2 us  [crossed(): return lax.ppermute(value, 'sp', pairs)]
    ppermute x7 -> x8, starting transfers between devices: 4.33 us -> 4.27 us  [other_core(): return lax.ppermute(value, 'sp', [(n, n ^ 1) for n in range(count)])]
  transfers between devices with their start and end apart: 23 -> 25, of which waited for: 13 -> 16; matrix products, arithmetic and copies ran while one was open for 0% -> 0% of each run, Pallas kernels for 16% -> 16%
where the time goes in v6:
time: 185 us; the launch traced here: 184 us
  waiting for transfers between devices  78.2 us (42%)
  Pallas kernels  58.1 us (31%)
  starting transfers between devices  29.5 us (16%)
  between operations  13.6 us (7%)
  other arithmetic  2.47 us (1%)
  local copies, waits for them, and re-layouts  1.92 us (1%)
    ppermute x9, waiting for transfers between devices, shifted(): lax.ppermute(value, 'tp', [(i, (i + by) % count) for i in range(count)])  41 us
    ppermute x7, waiting for transfers between devices, crossed(): return lax.ppermute(value, 'sp', pairs)  35.4 us
    pallas_call x5, Pallas kernels, flash(): pl.pallas_call(functools.partial(flash_kernel, pieces=pieces, scale=head_...  28.7 us
    pallas_call x1, Pallas kernels, layer(): pl.pallas_call(functools.partial(layer_kernel, parts=parts, tile=tile, su...  20.2 us
    ppermute x9, starting transfers between devices, shifted(): lax.ppermute(value, 'tp', [(i, (i + by) % count) for i in range(count)])  15.1 us
    ppermute x7, starting transfers between devices, crossed(): return lax.ppermute(value, 'sp', pairs)  10.2 us
    pallas_call x1, Pallas kernels, rest(): pl.pallas_call(rest_kernel, in_specs=[pl.BlockSpec(memory_space=pltpu.VME...  4.56 us
    pallas_call x1, Pallas kernels, prepare(): pl.pallas_call(functools.partial(prepare_kernel, rows=rows, head_dim=head...  4.49 us
  transfers between devices with their start and end apart: 25, of which 16 were waited for; matrix products, arithmetic and copies ran while one was open for 0% of the time, Pallas kernels for 16%

profile of v6, /device:TPU:8, one launch (start us, length us, event | category | flops | bytes accessed | tf_op | source)
XLA Modules:
  0.0 183.8 jit_solution(2888714349646339323)
XLA Ops:
  6.6 0.1 add_convert_fusion.1
  6.7 0.2 multiply_sine_fusion
  6.9 0.1 negate_select_fusion.1
  7.0 0.8 pad_maximum_fusion
  7.7 4.5 %prepare.1 = (bf16[1024,128]{1,0:T(8,128)(2,1)}, bf16[512,256]{1,0:T(8,128)(2,1)}, bf16[64,4224]{1,0:T(8,128)(2,1)}, bf16[256,2048]{1,0:T(8,128)(2,1)}, bf16[128,2048]{1,0:T(8,128)(2,1)}) custom-call(s32[1]{0:T(128)} %bitcast.1.core, bf16[512,256]{1,0:T(8,128)(2,1)} %q_hbm.1, bf16[512,128]{1,0:T(8,128)(2,1)} %k_hbm.1, bf16[512,128]{1,0:T(8,128)(2,1)} %v_hbm.1, ...), custom_call_target="tpu_custom_call" | custom-call | tf_op jit(solution)/shard_map/prepare/pallas_call | solution.py:115
  12.2 0.0 copy-start
  12.2 0.0 copy-start.2
  12.3 0.0 all-gather.2.cloned.1.call-update
  12.3 0.4 collective-permute-start.2
  12.7 1.7 collective-permute-start.1
  14.4 3.5 %collective-permute-start = (bf16[512,256]{1,0:T(8,128)(2,1)}, bf16[512,256]{1,0:T(8,128)(2,1)S(1)}, u32[]{:S(2)}, u32[]{:S(2)}) collective-permute-start(bf16[512,256]{1,0:T(8,128)(2,1)} %get-tuple-element.46.refs_0_), channel_id=1, source_target_pairs={{0,16},{4,68},{8,24},{12,76},{16,0},{20,84},{24,8},{28,92},{32,48}... | collective-permute-start | bytes 786440 | tf_op jit(solution)/shard_map/ppermute | solution.py:384
  17.9 1.0 collective-permute-done.2.refs_3_
  18.9 1.5 collective-permute-done.1.refs_2_
  20.4 2.3 %collective-permute-done.refs_1_ = bf16[512,256]{1,0:T(8,128)(2,1)S(1)} collective-permute-done((bf16[512,256]{1,0:T(8,128)(2,1)}, bf16[512,256]{1,0:T(8,128)(2,1)S(1)}, u32[]{:S(2)}, u32[]{:S(2)}) %collective-permute-start) | collective-permute-done | bytes 262176 | tf_op jit(solution)/shard_map/ppermute | solution.py:384
  22.8 0.9 copy-done.1
  23.7 0.1 lines.1
  23.9 2.7 %collective-permute-start.3 = (bf16[2048,256]{1,0:T(8,128)(2,1)S(1)}, bf16[2048,256]{1,0:T(8,128)(2,1)S(1)}, u32[]{:S(2)}, u32[]{:S(2)}) collective-permute-start(bf16[2048,256]{1,0:T(8,128)(2,1)S(1)} %get-tuple-element.47.refs_1_), channel_id=1, source_target_pairs={{0,4},{4,0},{8,12},{12,8},{16,20},{20,16},{24,28},{28,24},{32,36},... | collective-permute-start | bytes 3145736 | tf_op jit(solution)/shard_map/ppermute | solution.py:389
  26.6 1.5 collective-permute-start.5
  28.1 0.5 collective-permute-start.4
  28.6 0.3 collective-permute-done.3.refs_2_
  28.9 0.9 copy-done.3
  29.8 6.2 %flash_first.1 = (f32[1024,128]{1,0:T(8,128)S(1)}, f32[1024,256]{1,0:T(8,128)S(1)}) custom-call(bf16[1024,128]{1,0:T(8,128)(2,1)S(1)} %copy-done.3, bf16[2048,256]{1,0:T(8,128)(2,1)S(1)} %get-tuple-element.47.refs_1_, bf16[2048,256]{1,0:T(8,128)(2,1)S(1)} %collective-permute-done.3.refs_2_), custom_call_target="tpu_custom_call" | custom-call | flops 2147483648 | bytes 2097152 | tf_op jit(solution)/shard_map/flash_first/pallas_call | solution.py:190
  36.1 11.8 %collective-permute-done.5.refs_2_ = bf16[2048,256]{1,0:T(8,128)(2,1)S(1)} collective-permute-done((bf16[2048,256]{1,0:T(8,128)(2,1)S(1)}, bf16[2048,256]{1,0:T(8,128)(2,1)S(1)}, u32[]{:S(2)}, u32[]{:S(2)}) %collective-permute-start.5) | collective-permute-done | bytes 1048608 | tf_op jit(solution)/shard_map/ppermute | solution.py:384
  47.9 1.6 collective-permute-done.4.refs_1_
  49.5 0.0 collective-permute-start.6
  49.5 0.5 collective-permute-start.7
  50.0 1.2 collective-permute-start.8
  51.2 1.5 collective-permute-start.13
  52.7 2.7 %collective-permute-start.12 = (bf16[256,2048]{1,0:T(8,128)(2,1)}, bf16[256,2048]{1,0:T(8,128)(2,1)}, u32[]{:S(2)}, u32[]{:S(2)}) collective-permute-start(bf16[256,2048]{1,0:T(8,128)(2,1)} %get-tuple-element.69.refs_4_), channel_id=1, source_target_pairs={{0,2},{1,3},{2,0},{3,1},{4,6},{5,7},{6,4},{7,5},{8,10},{9,11},{10,... | collective-permute-start | bytes 3145736 | tf_op jit(solution)/shard_map/ppermute | solution.py:366
  55.4 0.0 collective-permute-done.6.refs_1_
  55.4 1.5 collective-permute-start.11
  56.8 6.9 %flash_more.3 = (f32[1024,128]{1,0:T(8,128)S(1)}, f32[1024,256]{1,0:T(8,128)S(1)}) custom-call(bf16[1024,128]{1,0:T(8,128)(2,1)S(1)} %copy-done.3, bf16[2048,256]{1,0:T(8,128)(2,1)S(1)} %collective-permute-done.4.refs_1_, bf16[2048,256]{1,0:T(8,128)(2,1)S(1)} %collective-permute-done.5.refs_2_, f32[1024,128]{1,0:T(8,128)S(1)} %get-tuple-element.52.refs_3_, ...), custom_call_target="tpu_custom_call" | custom-call | flops 2147483648 | bytes 2097152 | tf_op jit(solution)/shard_map/flash_more/pallas_call | solution.py:190
  63.8 6.9 %flash_more.4 = (f32[1024,128]{1,0:T(8,128)S(1)}, f32[1024,256]{1,0:T(8,128)S(1)}) custom-call(bf16[1024,128]{1,0:T(8,128)(2,1)S(1)} %copy-done.3, bf16[2048,256]{1,0:T(8,128)(2,1)S(1)} %collective-permute-done.6.refs_1_, bf16[2048,256]{1,0:T(8,128)(2,1)S(1)} %collective-permute-done.7.refs_2_, f32[1024,128]{1,0:T(8,128)S(1)} %get-tuple-element.54.refs_3_, ...), custom_call_target="tpu_custom_call" | custom-call | flops 2147483648 | bytes 2097152 | tf_op jit(solution)/shard_map/flash_more/pallas_call | solution.py:190
  70.7 1.2 collective-permute-done.8.refs_1_
  72.0 0.0 collective-permute-start.9
  72.0 1.3 collective-permute-start.10
  73.3 0.6 collective-permute-done.9.refs_2_
  73.9 4.2 %flash_more.5 = (f32[1024,128]{1,0:T(8,128)S(1)}, f32[1024,256]{1,0:T(8,128)S(1)}) custom-call(bf16[1024,128]{1,0:T(8,128)(2,1)S(1)} %copy-done.3, bf16[1024,256]{1,0:T(8,128)(2,1)S(1)} %collective-permute-done.8.refs_1_, bf16[1024,256]{1,0:T(8,128)(2,1)S(1)} %collective-permute-done.9.refs_2_, f32[1024,128]{1,0:T(8,128)S(1)} %get-tuple-element.60.refs_3_, ...), custom_call_target="tpu_custom_call" | custom-call | flops 1073741824 | bytes 1048576 | tf_op jit(solution)/shard_map/flash_more/pallas_call | solution.py:190
  78.1 15.9 %collective-permute-done.10.refs_1_ = bf16[1024,256]{1,0:T(8,128)(2,1)S(1)} collective-permute-done((bf16[1024,256]{1,0:T(8,128)(2,1)S(1)}, bf16[1024,256]{1,0:T(8,128)(2,1)S(1)}, u32[]{:S(2)}, u32[]{:S(2)}) %collective-permute-start.10) | collective-permute-done | bytes 524320 | tf_op jit(solution)/shard_map/ppermute | solution.py:384
  94.0 7.4 %collective-permute-done.12.refs_6_ = bf16[256,2048]{1,0:T(8,128)(2,1)} collective-permute-done((bf16[256,2048]{1,0:T(8,128)(2,1)}, bf16[256,2048]{1,0:T(8,128)(2,1)}, u32[]{:S(2)}, u32[]{:S(2)}) %collective-permute-start.12) | collective-permute-done | bytes 1048608 | tf_op jit(solution)/shard_map/ppermute | solution.py:366
  101.5 0.0 collective-permute-done.11.refs_5_
  101.5 0.0 collective-permute-start.14
  101.5 0.5 collective-permute-start.18
  102.0 0.0 collective-permute-start.19
  102.0 0.5 collective-permute-start.20
  102.5 0.9 collective-permute-done.14.refs_2_
  103.4 4.4 %flash_last.1.refs_0_ = bf16[512,256]{1,0:T(8,128)(2,1)S(1)} custom-call(bf16[1024,128]{1,0:T(8,128)(2,1)S(1)} %copy-done.3, bf16[1024,256]{1,0:T(8,128)(2,1)S(1)} %collective-permute-done.10.refs_1_, bf16[1024,256]{1,0:T(8,128)(2,1)S(1)} %collective-permute-done.14.refs_2_, f32[1024,128]{1,0:T(8,128)S(1)} %get-tuple-element.67.refs_3_, ...), custom_call_target="tpu_custom_call" | custom-call | flops 1073741824 | bytes 1048576 | tf_op jit(solution)/shard_map/flash_last/pallas_call | solution.py:190
  107.8 1.8 collective-permute-start.17
  109.5 2.1 %collective-permute-start.16 = (bf16[512,256]{1,0:T(8,128)(2,1)S(1)}, bf16[512,256]{1,0:T(8,128)(2,1)S(1)}, u32[]{:S(2)}, u32[]{:S(2)}) collective-permute-start(bf16[512,256]{1,0:T(8,128)(2,1)S(1)} %flash_last.1.refs_0_), channel_id=1, source_target_pairs={{0,2},{1,3},{2,0},{3,1},{4,6},{5,7},{6,4},{7,5},{8,10},{9,11},{10,... | collective-permute-start | bytes 786440 | tf_op jit(solution)/shard_map/ppermute | solution.py:366
  111.6 6.0 %collective-permute-done.17.refs_3_ = bf16[512,256]{1,0:T(8,128)(2,1)S(1)} collective-permute-done((bf16[512,256]{1,0:T(8,128)(2,1)S(1)}, bf16[512,256]{1,0:T(8,128)(2,1)S(1)}, u32[]{:S(2)}, u32[]{:S(2)}) %collective-permute-start.17) | collective-permute-done | bytes 262176 | tf_op jit(solution)/shard_map/ppermute | solution.py:366
  117.7 1.7 collective-permute-start.15
  119.3 0.1 pad_add_fusion.place
  119.4 4.1 %collective-permute-done.16.refs_2_ = bf16[512,256]{1,0:T(8,128)(2,1)S(1)} collective-permute-done((bf16[512,256]{1,0:T(8,128)(2,1)S(1)}, bf16[512,256]{1,0:T(8,128)(2,1)S(1)}, u32[]{:S(2)}, u32[]{:S(2)}) %collective-permute-start.16) | collective-permute-done | bytes 262176 | tf_op jit(solution)/shard_map/ppermute | solution.py:366
  123.6 1.3 collective-permute-done.15.refs_1_
  124.9 0.0 collective-permute-done.18.refs_9_
  124.9 0.0 collective-permute-done.19.refs_10_
  124.9 0.0 all-gather.2.cloned.1.call-done.refs_13_.w_hbm
  125.0 20.2 %layer.1 = (bf16[128,2048]{1,0:T(8,128)(2,1)S(1)}, bf16[128,2048]{1,0:T(8,128)(2,1)S(1)}, bf16[128,2048]{1,0:T(8,128)(2,1)S(1)}, bf16[256,1408]{1,0:T(8,128)(2,1)S(1)}) custom-call(s32[2]{0:T(128)S(1)} %pad_add_fusion.place, bf16[512,256]{1,0:T(8,128)(2,1)S(1)} %flash_last.1.refs_0_, bf16[512,256]{1,0:T(8,128)(2,1)S(1)} %collective-permute-done.15.refs_1_, ...), custom_call_target="tpu_custom_call" | custom-call | tf_op jit(solution)/shard_map/layer/pallas_call | solution.py:319
  145.2 4.6 %rest.1 = (bf16[128,2048]{1,0:T(8,128)(2,1)S(1)}, bf16[128,2048]{1,0:T(8,128)(2,1)S(1)}) custom-call(bf16[256,1408]{1,0:T(8,128)(2,1)S(1)} %get-tuple-element.76.h_ref, bf16[2048,4224]{1,0:T(8,128)(2,1)} %all-gather.2.cloned.1.call-done.refs_13_.w_hbm), custom_call_target="tpu_custom_call" | custom-call | tf_op jit(solution)/shard_map/rest/pallas_call | solution.py:302
  149.7 2.4 %collective-permute-start.23 = (bf16[128,2048]{1,0:T(8,128)(2,1)S(1)}, bf16[128,2048]{1,0:T(8,128)(2,1)S(1)}, u32[]{:S(2)}, u32[]{:S(2)}) collective-permute-start(bf16[128,2048]{1,0:T(8,128)(2,1)S(1)} %get-tuple-element.80), channel_id=1, source_target_pairs={{0,3},{1,0},{2,1},{3,2},{4,7},{5,4},{6,5},{7,6},{8,11},{9,8},{10,9... | collective-permute-start | bytes 1572872 | tf_op jit(solution)/shard_map/ppermute | solution.py:366
  152.1 1.5 collective-permute-start.22
  153.7 18.6 %collective-permute-done.23 = bf16[128,2048]{1,0:T(8,128)(2,1)S(1)} collective-permute-done((bf16[128,2048]{1,0:T(8,128)(2,1)S(1)}, bf16[128,2048]{1,0:T(8,128)(2,1)S(1)}, u32[]{:S(2)}, u32[]{:S(2)}) %collective-permute-start.23) | collective-permute-done | bytes 524320 | tf_op jit(solution)/shard_map/ppermute | solution.py:366
  172.3 3.4 %collective-permute-done.21 = bf16[128,2048]{1,0:T(8,128)(2,1)S(1)} collective-permute-done((bf16[128,2048]{1,0:T(8,128)(2,1)S(1)}, bf16[128,2048]{1,0:T(8,128)(2,1)S(1)}, u32[]{:S(2)}, u32[]{:S(2)}) %collective-permute-start.21) | collective-permute-done | bytes 524320 | tf_op jit(solution)/shard_map/ppermute | solution.py:366
  175.7 1.2 add_convert_fusion
  (16 shorter events, 0.0 us)
Async XLA Ops:
  6.5 118.4 %all-gather.2.cloned.1.call-start = ((), (), s32[]{:S(2)}) async-start(), calls=%async_computation | async-start | bytes 17842176 | tf_op jit(solution)/shard_map/all_gather | solution.py:413
  12.2 112.7 %copy-start = (bf16[128,2048]{1,0:T(8,128)(2,1)S(1)}, bf16[128,2048]{1,0:T(8,128)(2,1)}, u32[]{:S(2)}) copy-start(bf16[128,2048]{1,0:T(8,128)(2,1)} %get-tuple-element.73.refs_8_) | copy-start | bytes 1572868
  12.2 112.7 %copy-start.2 = (f32[2048]{0:T(1024)S(1)}, f32[2048]{0:T(1024)}, u32[]{:S(2)}) copy-start(f32[2048]{0:T(1024)} %param.18) | copy-start | bytes 24580
  12.3 6.7 %collective-permute-start.2 = (bf16[512,256]{1,0:T(8,128)(2,1)}, bf16[512,256]{1,0:T(8,128)(2,1)S(1)}, u32[]{:S(2)}, u32[]{:S(2)}) collective-permute-start(bf16[512,256]{1,0:T(8,128)(2,1)} %get-tuple-element.46.refs_0_), channel_id=1, source_target_pairs={{0,24},{4,100},{8,0},{12,108},{16,8},{20,116},{24,16},{28,124},{32... | collective-permute-start | bytes 786440 | tf_op jit(solution)/shard_map/ppermute | solution.py:384
  12.7 7.7 %collective-permute-start.1 = (bf16[512,256]{1,0:T(8,128)(2,1)}, bf16[512,256]{1,0:T(8,128)(2,1)S(1)}, u32[]{:S(2)}, u32[]{:S(2)}) collective-permute-start(bf16[512,256]{1,0:T(8,128)(2,1)} %get-tuple-element.46.refs_0_), channel_id=1, source_target_pairs={{0,8},{4,36},{8,16},{12,44},{16,24},{20,52},{24,0},{28,60},{32,40}... | collective-permute-start | bytes 786440 | tf_op jit(solution)/shard_map/ppermute | solution.py:384
  14.4 8.4 %collective-permute-start = (bf16[512,256]{1,0:T(8,128)(2,1)}, bf16[512,256]{1,0:T(8,128)(2,1)S(1)}, u32[]{:S(2)}, u32[]{:S(2)}) collective-permute-start(bf16[512,256]{1,0:T(8,128)(2,1)} %get-tuple-element.46.refs_0_), channel_id=1, source_target_pairs={{0,16},{4,68},{8,24},{12,76},{16,0},{20,84},{24,8},{28,92},{32,48}... | collective-permute-start | bytes 786440 | tf_op jit(solution)/shard_map/ppermute | solution.py:384
  22.8 1.0 copy-start.1
  23.9 5.0 %collective-permute-start.3 = (bf16[2048,256]{1,0:T(8,128)(2,1)S(1)}, bf16[2048,256]{1,0:T(8,128)(2,1)S(1)}, u32[]{:S(2)}, u32[]{:S(2)}) collective-permute-start(bf16[2048,256]{1,0:T(8,128)(2,1)S(1)} %get-tuple-element.47.refs_1_), channel_id=1, source_target_pairs={{0,4},{4,0},{8,12},{12,8},{16,20},{20,16},{24,28},{28,24},{32,36},... | collective-permute-start | bytes 3145736 | tf_op jit(solution)/shard_map/ppermute | solution.py:389
  26.6 21.3 %collective-permute-start.5 = (bf16[2048,256]{1,0:T(8,128)(2,1)S(1)}, bf16[2048,256]{1,0:T(8,128)(2,1)S(1)}, u32[]{:S(2)}, u32[]{:S(2)}) collective-permute-start(bf16[2048,256]{1,0:T(8,128)(2,1)S(1)} %get-tuple-element.47.refs_1_), channel_id=1, source_target_pairs={{0,96},{4,28},{8,104},{12,4},{16,112},{20,12},{24,120},{28,20},{32... | collective-permute-start | bytes 3145736 | tf_op jit(solution)/shard_map/ppermute | solution.py:384
  28.1 21.4 %collective-permute-start.4 = (bf16[2048,256]{1,0:T(8,128)(2,1)S(1)}, bf16[2048,256]{1,0:T(8,128)(2,1)S(1)}, u32[]{:S(2)}, u32[]{:S(2)}) collective-permute-start(bf16[2048,256]{1,0:T(8,128)(2,1)S(1)} %get-tuple-element.47.refs_1_), channel_id=1, source_target_pairs={{0,32},{4,12},{8,40},{12,20},{16,48},{20,28},{24,56},{28,4},{32,64... | collective-permute-start | bytes 3145736 | tf_op jit(solution)/shard_map/ppermute | solution.py:384
  28.9 0.9 copy-start.3
  49.5 5.9 %collective-permute-start.6 = (bf16[2048,256]{1,0:T(8,128)(2,1)S(1)}, bf16[2048,256]{1,0:T(8,128)(2,1)S(1)}, u32[]{:S(2)}, u32[]{:S(2)}) collective-permute-start(bf16[2048,256]{1,0:T(8,128)(2,1)S(1)} %collective-permute-done.4.refs_1_), channel_id=1, source_target_pairs={{0,4},{4,0},{8,12},{12,8},{16,20},{20,16},{24,28},{28,24},{32,36},... | collective-permute-start | bytes 3145736 | tf_op jit(solution)/shard_map/ppermute | solution.py:389
  49.5 14.3 %collective-permute-start.7 = (bf16[2048,256]{1,0:T(8,128)(2,1)S(1)}, bf16[2048,256]{1,0:T(8,128)(2,1)S(1)}, u32[]{:S(2)}, u32[]{:S(2)}) collective-permute-start(bf16[2048,256]{1,0:T(8,128)(2,1)S(1)} %collective-permute-done.5.refs_2_), channel_id=1, source_target_pairs={{0,4},{4,0},{8,12},{12,8},{16,20},{20,16},{24,28},{28,24},{32,36},... | collective-permute-start | bytes 3145736 | tf_op jit(solution)/shard_map/ppermute | solution.py:389
  50.0 21.9 %collective-permute-start.8 = (bf16[1024,256]{1,0:T(8,128)(2,1)S(1)}, bf16[1024,256]{1,0:T(8,128)(2,1)S(1)}, u32[]{:S(2)}, u32[]{:S(2)}) collective-permute-start(bf16[1024,256]{1,0:T(8,128)(2,1)S(1)} %get-tuple-element.58), channel_id=1, source_target_pairs={{0,64},{4,20},{8,72},{12,28},{16,80},{20,4},{24,88},{28,12},{32,96... | collective-permute-start | bytes 1572872 | tf_op jit(solution)/shard_map/ppermute | solution.py:384
  51.2 42.8 %collective-permute-start.13 = (bf16[256,2048]{1,0:T(8,128)(2,1)}, bf16[256,2048]{1,0:T(8,128)(2,1)S(1)}, u32[]{:S(2)}, u32[]{:S(2)}) collective-permute-start(bf16[256,2048]{1,0:T(8,128)(2,1)} %get-tuple-element.69.refs_4_), channel_id=1, source_target_pairs={{0,1},{1,2},{2,3},{3,0},{4,5},{5,6},{6,7},{7,4},{8,9},{9,10},{10,1... | collective-permute-start | bytes 3145736 | tf_op jit(solution)/shard_map/ppermute | solution.py:366
  52.7 48.8 %collective-permute-start.12 = (bf16[256,2048]{1,0:T(8,128)(2,1)}, bf16[256,2048]{1,0:T(8,128)(2,1)}, u32[]{:S(2)}, u32[]{:S(2)}) collective-permute-start(bf16[256,2048]{1,0:T(8,128)(2,1)} %get-tuple-element.69.refs_4_), channel_id=1, source_target_pairs={{0,2},{1,3},{2,0},{3,1},{4,6},{5,7},{6,4},{7,5},{8,10},{9,11},{10,... | collective-permute-start | bytes 3145736 | tf_op jit(solution)/shard_map/ppermute | solution.py:366
  55.4 46.1 %collective-permute-start.11 = (bf16[256,2048]{1,0:T(8,128)(2,1)}, bf16[256,2048]{1,0:T(8,128)(2,1)}, u32[]{:S(2)}, u32[]{:S(2)}) collective-permute-start(bf16[256,2048]{1,0:T(8,128)(2,1)} %get-tuple-element.69.refs_4_), channel_id=1, source_target_pairs={{0,3},{1,0},{2,1},{3,2},{4,7},{5,4},{6,5},{7,6},{8,11},{9,8},{10,9... | collective-permute-start | bytes 3145736 | tf_op jit(solution)/shard_map/ppermute | solution.py:366
  72.0 1.9 %collective-permute-start.9 = (bf16[1024,256]{1,0:T(8,128)(2,1)S(1)}, bf16[1024,256]{1,0:T(8,128)(2,1)S(1)}, u32[]{:S(2)}, u32[]{:S(2)}) collective-permute-start(bf16[1024,256]{1,0:T(8,128)(2,1)S(1)} %collective-permute-done.8.refs_1_), channel_id=1, source_target_pairs={{0,4},{4,0},{8,12},{12,8},{16,20},{20,16},{24,28},{28,24},{32,36},... | collective-permute-start | bytes 1572872 | tf_op jit(solution)/shard_map/ppermute | solution.py:389
  72.0 22.1 %collective-permute-start.10 = (bf16[1024,256]{1,0:T(8,128)(2,1)S(1)}, bf16[1024,256]{1,0:T(8,128)(2,1)S(1)}, u32[]{:S(2)}, u32[]{:S(2)}) collective-permute-start(bf16[1024,256]{1,0:T(8,128)(2,1)S(1)} %get-tuple-element.64), channel_id=1, source_target_pairs={{0,64},{4,20},{8,72},{12,28},{16,80},{20,4},{24,88},{28,12},{32,96... | collective-permute-start | bytes 1572872 | tf_op jit(solution)/shard_map/ppermute | solution.py:384
  94.0 30.9 %copy-start.4 = (bf16[256,2048]{1,0:T(8,128)(2,1)}, bf16[256,2048]{1,0:T(8,128)(2,1)S(1)}, u32[]{:S(2)}) copy-start(bf16[256,2048]{1,0:T(8,128)(2,1)S(1)} %collective-permute-done.13.refs_7_) | copy-start | bytes 3145732
  101.5 1.9 %collective-permute-start.14 = (bf16[1024,256]{1,0:T(8,128)(2,1)S(1)}, bf16[1024,256]{1,0:T(8,128)(2,1)S(1)}, u32[]{:S(2)}, u32[]{:S(2)}) collective-permute-start(bf16[1024,256]{1,0:T(8,128)(2,1)S(1)} %collective-permute-done.10.refs_1_), channel_id=1, source_target_pairs={{0,4},{4,0},{8,12},{12,8},{16,20},{20,16},{24,28},{28,24},{32,36},... | collective-permute-start | bytes 1572872 | tf_op jit(solution)/shard_map/ppermute | solution.py:389
  101.5 23.4 %collective-permute-start.18 = (bf16[256,2048]{1,0:T(8,128)(2,1)}, bf16[256,2048]{1,0:T(8,128)(2,1)}, u32[]{:S(2)}, u32[]{:S(2)}) collective-permute-start(bf16[256,2048]{1,0:T(8,128)(2,1)} %collective-permute-done.11.refs_5_), channel_id=1, source_target_pairs={{0,4},{4,0},{8,12},{12,8},{16,20},{20,16},{24,28},{28,24},{32,36},... | collective-permute-start | bytes 3145736 | tf_op jit(solution)/shard_map/ppermute | solution.py:389
  102.0 22.9 %collective-permute-start.19 = (bf16[256,2048]{1,0:T(8,128)(2,1)}, bf16[256,2048]{1,0:T(8,128)(2,1)}, u32[]{:S(2)}, u32[]{:S(2)}) collective-permute-start(bf16[256,2048]{1,0:T(8,128)(2,1)} %collective-permute-done.12.refs_6_), channel_id=1, source_target_pairs={{0,4},{4,0},{8,12},{12,8},{16,20},{20,16},{24,28},{28,24},{32,36},... | collective-permute-start | bytes 3145736 | tf_op jit(solution)/shard_map/ppermute | solution.py:389
  102.0 22.9 %collective-permute-start.20 = (bf16[256,2048]{1,0:T(8,128)(2,1)S(1)}, bf16[256,2048]{1,0:T(8,128)(2,1)}, u32[]{:S(2)}, u32[]{:S(2)}) collective-permute-start(bf16[256,2048]{1,0:T(8,128)(2,1)S(1)} %collective-permute-done.13.refs_7_), channel_id=1, source_target_pairs={{0,4},{4,0},{8,12},{12,8},{16,20},{20,16},{24,28},{28,24},{32,36},... | collective-permute-start | bytes 3145736 | tf_op jit(solution)/shard_map/ppermute | solution.py:389
  107.8 9.9 %collective-permute-start.17 = (bf16[512,256]{1,0:T(8,128)(2,1)S(1)}, bf16[512,256]{1,0:T(8,128)(2,1)S(1)}, u32[]{:S(2)}, u32[]{:S(2)}) collective-permute-start(bf16[512,256]{1,0:T(8,128)(2,1)S(1)} %flash_last.1.refs_0_), channel_id=1, source_target_pairs={{0,1},{1,2},{2,3},{3,0},{4,5},{5,6},{6,7},{7,4},{8,9},{9,10},{10,1... | collective-permute-start | bytes 786440 | tf_op jit(solution)/shard_map/ppermute | solution.py:366
  109.5 14.0 %collective-permute-start.16 = (bf16[512,256]{1,0:T(8,128)(2,1)S(1)}, bf16[512,256]{1,0:T(8,128)(2,1)S(1)}, u32[]{:S(2)}, u32[]{:S(2)}) collective-permute-start(bf16[512,256]{1,0:T(8,128)(2,1)S(1)} %flash_last.1.refs_0_), channel_id=1, source_target_pairs={{0,2},{1,3},{2,0},{3,1},{4,6},{5,7},{6,4},{7,5},{8,10},{9,11},{10,... | collective-permute-start | bytes 786440 | tf_op jit(solution)/shard_map/ppermute | solution.py:366
  117.7 7.2 %collective-permute-start.15 = (bf16[512,256]{1,0:T(8,128)(2,1)S(1)}, bf16[512,256]{1,0:T(8,128)(2,1)S(1)}, u32[]{:S(2)}, u32[]{:S(2)}) collective-permute-start(bf16[512,256]{1,0:T(8,128)(2,1)S(1)} %flash_last.1.refs_0_), channel_id=1, source_target_pairs={{0,3},{1,0},{2,1},{3,2},{4,7},{5,4},{6,5},{7,6},{8,11},{9,8},{10,9... | collective-permute-start | bytes 786440 | tf_op jit(solution)/shard_map/ppermute | solution.py:366
  149.7 22.6 %collective-permute-start.23 = (bf16[128,2048]{1,0:T(8,128)(2,1)S(1)}, bf16[128,2048]{1,0:T(8,128)(2,1)S(1)}, u32[]{:S(2)}, u32[]{:S(2)}) collective-permute-start(bf16[128,2048]{1,0:T(8,128)(2,1)S(1)} %get-tuple-element.80), channel_id=1, source_target_pairs={{0,3},{1,0},{2,1},{3,2},{4,7},{5,4},{6,5},{7,6},{8,11},{9,8},{10,9... | collective-permute-start | bytes 1572872 | tf_op jit(solution)/shard_map/ppermute | solution.py:366
  152.1 23.6 %collective-permute-start.21 = (bf16[128,2048]{1,0:T(8,128)(2,1)S(1)}, bf16[128,2048]{1,0:T(8,128)(2,1)S(1)}, u32[]{:S(2)}, u32[]{:S(2)}) collective-permute-start(bf16[128,2048]{1,0:T(8,128)(2,1)S(1)} %get-tuple-element.78), channel_id=1, source_target_pairs={{0,1},{1,2},{2,3},{3,0},{4,5},{5,6},{6,7},{7,4},{8,9},{9,10},{10,1... | collective-permute-start | bytes 1572872 | tf_op jit(solution)/shard_map/ppermute | solution.py:366
  152.1 23.6 %collective-permute-start.22 = (bf16[128,2048]{1,0:T(8,128)(2,1)S(1)}, bf16[128,2048]{1,0:T(8,128)(2,1)S(1)}, u32[]{:S(2)}, u32[]{:S(2)}) collective-permute-start(bf16[128,2048]{1,0:T(8,128)(2,1)S(1)} %get-tuple-element.79), channel_id=1, source_target_pairs={{0,2},{1,3},{2,0},{3,1},{4,6},{5,7},{6,4},{7,5},{8,10},{9,11},{10,... | collective-permute-start | bytes 1572872 | tf_op jit(solution)/shard_map/ppermute | solution.py:366
Sparse Core Ops, SparseCore 0:
  12.4 89.1 all-gather.1

commit v7 on v6

--- a/solution.py
+++ b/solution.py
@@ -39,9 +39,9 @@
 
 
 def prepare_kernel(
-    core, q_hbm, k_hbm, v_hbm, g_hbm, u_hbm, d_hbm, w_hbm, r_hbm, qg_ref, kg_ref, cos_ref, sin_ref,
-    q_out, kv_out, woven, sent, kept,
-    q_ref, k_ref, v_ref, g_ref, u_ref, d_ref, w_ref, r_ref, sems, *, rows, head_dim, heads, tile,
+    core, q_hbm, k_hbm, v_hbm, w_hbm, r_hbm, qg_ref, kg_ref, cos_ref, sin_ref,
+    q_out, kv_out, sent, kept,
+    q_ref, k_ref, v_ref, w_ref, r_ref, sems, *, rows, head_dim, heads,
 ):
     tok = rows * GRID
     half = kept.shape[0]
@@ -51,9 +51,6 @@
         (k_hbm, k_ref),
         (v_hbm, v_ref),
         (q_hbm, q_ref),
-        (g_hbm, g_ref),
-        (u_hbm, u_ref),
-        (d_hbm, d_ref),
         (w_hbm.at[first_half, :], w_ref.at[pl.ds(0, half), :]),
         (w_hbm.at[other_half, :], w_ref.at[pl.ds(half, half), :]),
         (r_hbm, r_ref),
@@ -62,7 +59,7 @@
         (r_ref, sent.at[pl.ds(half, r_hbm.shape[0]), :]),
     ]
     copies = [pltpu.make_async_copy(x, y, sems.at[n]) for n, (x, y) in enumerate(moves)]
-    for c in copies[:9]:
+    for c in copies[:6]:
         c.start()
 
     def spread(ref):
@@ -85,49 +82,67 @@
     copies[1].wait()
     kv_out[:, 0:head_dim] = prepared(k_ref[...], kg_ref[...])
     kv_out[:, head_dim:] = v_ref[...]
-    for n in (6, 7, 8):
+    for n in (3, 4, 5):
         copies[n].wait()
         copies[n + 3].start()
     copies[2].wait()
     for h in range(heads):
         q_out[h * tok : (h + 1) * tok, :] = prepared(q_ref[:, h * head_dim : (h + 1) * head_dim], qg_ref[...])
-    for n in (3, 4, 5):
+    for n in (6, 7, 8):
         copies[n].wait()
+
+
+def weave_kernel(g_hbm, u_hbm, d_hbm, woven, g_ref, u_ref, d_ref, sems, *, tile):
+    moves = ((g_hbm, g_ref), (u_hbm, u_ref), (d_hbm, d_ref))
+    copies = [pltpu.make_async_copy(x, y, sems.at[n]) for n, (x, y) in enumerate(moves)]
+    for c in copies:
+        c.start()
+    for c in copies:
+        c.wait()
     units = g_ref.shape[1]
     for n in range(units // tile):
         part = slice(n * tile, (n + 1) * tile)
         woven[:, 2 * n * tile : (2 * n + 1) * tile] = g_ref[:, part]
         woven[:, (2 * n + 1) * tile : (2 * n + 2) * tile] = u_ref[:, part]
     woven[:, 2 * units :] = d_ref[...]
-    for n in (9, 10, 11):
-        copies[n].wait()
-
-
-def prepare(query_rows, key_rows, value_rows, query_gain, key_gain, gate, up, down, out_weight, residual, tile=128):
+
+
+def interleaved(gate, up, down, tile=128):
+    big = (gate, up, down.T)
+    return pl.pallas_call(
+        functools.partial(weave_kernel, tile=tile),
+        in_specs=[pl.BlockSpec(memory_space=pltpu.HBM)] * 3,
+        out_shape=jax.ShapeDtypeStruct((gate.shape[0], 3 * gate.shape[1]), bf16),
+        scratch_shapes=[pltpu.VMEM(x.shape, bf16) for x in big] + [pltpu.SemaphoreType.DMA((3,))],
+        compiler_params=pltpu.CompilerParams(vmem_limit_bytes=60 * 1024 * 1024),
+        name="weave",
+    )(*big)
+
+
+def prepare(query_rows, key_rows, value_rows, query_gain, key_gain, out_weight, residual):
     tok, width = query_rows.shape
     head_dim = query_gain.shape[0]
     rows = tok // GRID
     cosine, sine = angle_tables(lax.axis_index("sp") * rows, rows, head_dim)
     hbm = pl.BlockSpec(memory_space=pltpu.HBM)
     vmem = pl.BlockSpec(memory_space=pltpu.VMEM)
-    big = (query_rows, key_rows, value_rows, gate, up, down.T)
+    big = (query_rows, key_rows, value_rows, out_weight, residual)
     half = out_weight.shape[0] // 2
     return pl.pallas_call(
-        functools.partial(prepare_kernel, rows=rows, head_dim=head_dim, heads=width // head_dim, tile=tile),
-        in_specs=[pl.BlockSpec(memory_space=pltpu.SMEM)] + [hbm] * 8 + [vmem] * 4,
-        out_specs=[vmem] * 3 + [hbm] * 2,
+        functools.partial(prepare_kernel, rows=rows, head_dim=head_dim, heads=width // head_dim),
+        in_specs=[pl.BlockSpec(memory_space=pltpu.SMEM)] + [hbm] * 5 + [vmem] * 4,
+        out_specs=[vmem] * 2 + [hbm] * 2,
         out_shape=(
             jax.ShapeDtypeStruct((tok * (width // head_dim), head_dim), bf16),
             jax.ShapeDtypeStruct((tok, 2 * head_dim), bf16),
-            jax.ShapeDtypeStruct((gate.shape[0], 3 * gate.shape[1]), bf16),
             jax.ShapeDtypeStruct((half + residual.shape[0], residual.shape[1]), bf16),
             jax.ShapeDtypeStruct((half, residual.shape[1]), bf16),
         ),
-        scratch_shapes=[pltpu.VMEM(x.shape, bf16) for x in (*big, out_weight, residual)] + [pltpu.SemaphoreType.DMA((12,))],
+        scratch_shapes=[pltpu.VMEM(x.shape, bf16) for x in big] + [pltpu.SemaphoreType.DMA((9,))],
         compiler_params=pltpu.CompilerParams(vmem_limit_bytes=60 * 1024 * 1024),
         name="prepare",
     )(
-        (lax.axis_index("sp") % 2)[None], *big, out_weight, residual, query_gain[None, :], key_gain[None, :], cosine, sine
+        (lax.axis_index("sp") % 2)[None], *big, query_gain[None, :], key_gain[None, :], cosine, sine
     )
 
 
@@ -201,7 +216,6 @@
             bytes_accessed=4 * piece[0] * pieces * head_dim,
             transcendentals=rows * piece[0] * pieces,
         ),
-        name="flash_last" if last else "flash_first" if first else "flash_more",
     )(q, *kv, *([] if first else state))
 
 
@@ -407,10 +421,10 @@
     units = gate_weight.shape[1]
     core = lax.axis_index("sp") % 2
     place = jnp.stack([lax.axis_index("tp"), core])
-    q, kv, woven, payload, kept = prepare(
-        query_rows, key_rows, value_rows, query_gain, key_gain, gate_weight, up_weight, down_weight, out_weight, residual
-    )
+    woven = interleaved(gate_weight, up_weight, down_weight)
     weights = lax.all_gather(woven, "sp", axis=0, tiled=True)
+    key_rows, woven = lax.optimization_barrier((key_rows, woven))
+    q, kv, payload, kept = prepare(query_rows, key_rows, value_rows, query_gain, key_gain, out_weight, residual)
 
     steps = (2, 1, -1)
     line = [kv]

time: 185 us -> 185 us (level)
  waiting for transfers between devices: 78.2 us -> 74.5 us
  starting transfers between devices: 29.5 us -> 32.2 us
    ppermute x9, waiting for transfers between devices: 41 us -> 38.8 us  [shifted(): lax.ppermute(value, 'tp', [(i, (i + by) % count) for i in range(count)])]
    pallas_call x0 -> x1, Pallas kernels: none -> 2.02 us  [interleaved(): pl.pallas_call(functools.partial(weave_kernel, tile=tile), in_specs=[pl.B...]
  transfers between devices with their start and end apart: 25 -> 25, of which waited for: 16 -> 16; matrix products, arithmetic and copies ran while one was open for 0% -> 1% of each run, Pallas kernels for 16% -> 18%
where the time goes in v7:
time: 185 us
  waiting for transfers between devices  74.5 us (40%)
  Pallas kernels  59.8 us (32%)
  starting transfers between devices  32.2 us (17%)
  between operations  13.6 us (7%)
  other arithmetic  2.47 us (1%)
  local copies, waits for them, and re-layouts  1.92 us (1%)
    ppermute x9, waiting for transfers between devices, shifted(): lax.ppermute(value, 'tp', [(i, (i + by) % count) for i in range(count)])  38.8 us
    ppermute x7, waiting for transfers between devices, crossed(): return lax.ppermute(value, 'sp', pairs)  33.9 us
    pallas_call x5, Pallas kernels, flash(): pl.pallas_call(functools.partial(flash_kernel, pieces=pieces, scale=head_...  28.7 us
    pallas_call x1, Pallas kernels, layer(): pl.pallas_call(functools.partial(layer_kernel, parts=parts, tile=tile, su...  20.2 us
    ppermute x9, starting transfers between devices, shifted(): lax.ppermute(value, 'tp', [(i, (i + by) % count) for i in range(count)])  16.8 us
    ppermute x7, starting transfers between devices, crossed(): return lax.ppermute(value, 'sp', pairs)  9.62 us
    ppermute x8, starting transfers between devices, other_core(): return lax.ppermute(value, 'sp', [(n, n ^ 1) for n in range(count)])  5.83 us
    pallas_call x1, Pallas kernels, rest(): pl.pallas_call(rest_kernel, in_specs=[pl.BlockSpec(memory_space=pltpu.VME...  4.56 us
  transfers between devices with their start and end apart: 25, of which 16 were waited for; matrix products, arithmetic and copies ran while one was open for 1% of the time, Pallas kernels for 18%

profile of v7, /device:TPU:8, one launch (start us, length us, event | category | flops | bytes accessed | tf_op | source)
XLA Modules:
  0.0 184.5 jit_solution(1809712148111929338)
XLA Ops:
  6.5 2.0 %weave.1 = bf16[64,4224]{1,0:T(8,128)(2,1)} custom-call(bf16[64,1408]{1,0:T(8,128)(2,1)} %g_hbm.1, bf16[64,1408]{1,0:T(8,128)(2,1)} %u_hbm.1, bf16[64,1408]{1,0:T(8,128)(2,1)} %bitcast.7), custom_call_target="tpu_custom_call" | custom-call | tf_op jit(solution)/shard_map/weave/pallas_call | solution.py:112
  8.6 0.0 all-gather.2.cloned.1.call-update
  8.6 0.1 add_convert_fusion.1
  8.7 0.2 multiply_sine_fusion
  9.0 0.1 negate_select_fusion.1
  9.0 0.8 pad_maximum_fusion
  9.8 4.1 %prepare.1 = (bf16[1024,128]{1,0:T(8,128)(2,1)}, bf16[512,256]{1,0:T(8,128)(2,1)}, bf16[256,2048]{1,0:T(8,128)(2,1)}, bf16[128,2048]{1,0:T(8,128)(2,1)}) custom-call(s32[1]{0:T(128)} %bitcast.1.core, bf16[512,256]{1,0:T(8,128)(2,1)} %q_hbm.1, bf16[512,128]{1,0:T(8,128)(2,1)} %k_hbm, bf16[512,128]{1,0:T(8,128)(2,1)} %v_hbm.1, bf16[256,2048]{1,0:T(8,128)(2,1)} %w_hbm.1, ...), custom_call_target="tpu_custom_call" | custom-call | tf_op jit(solution)/shard_map/prepare/pallas_call | solution.py:131
  14.0 0.0 copy-start
  14.0 0.4 collective-permute-start.2
  14.4 1.7 collective-permute-start.1
  16.1 3.5 %collective-permute-start = (bf16[512,256]{1,0:T(8,128)(2,1)}, bf16[512,256]{1,0:T(8,128)(2,1)S(1)}, u32[]{:S(2)}, u32[]{:S(2)}) collective-permute-start(bf16[512,256]{1,0:T(8,128)(2,1)} %get-tuple-element.47.refs_0_), channel_id=1, source_target_pairs={{0,16},{4,68},{8,24},{12,76},{16,0},{20,84},{24,8},{28,92},{32,48}... | collective-permute-start | bytes 786440 | tf_op jit(solution)/shard_map/ppermute | solution.py:398
  19.6 1.0 collective-permute-done.2.refs_3_
  20.6 1.5 collective-permute-done.1.refs_2_
  22.1 3.3 %collective-permute-done.refs_1_ = bf16[512,256]{1,0:T(8,128)(2,1)S(1)} collective-permute-done((bf16[512,256]{1,0:T(8,128)(2,1)}, bf16[512,256]{1,0:T(8,128)(2,1)S(1)}, u32[]{:S(2)}, u32[]{:S(2)}) %collective-permute-start) | collective-permute-done | bytes 262176 | tf_op jit(solution)/shard_map/ppermute | solution.py:398
  25.3 1.0 copy-done.1
  26.3 0.1 lines.1
  26.4 3.9 %collective-permute-start.3 = (bf16[2048,256]{1,0:T(8,128)(2,1)S(1)}, bf16[2048,256]{1,0:T(8,128)(2,1)S(1)}, u32[]{:S(2)}, u32[]{:S(2)}) collective-permute-start(bf16[2048,256]{1,0:T(8,128)(2,1)S(1)} %get-tuple-element.48.refs_1_), channel_id=1, source_target_pairs={{0,4},{4,0},{8,12},{12,8},{16,20},{20,16},{24,28},{28,24},{32,36},... | collective-permute-start | bytes 3145736 | tf_op jit(solution)/shard_map/ppermute | solution.py:403
  30.3 2.5 %collective-permute-start.5 = (bf16[2048,256]{1,0:T(8,128)(2,1)S(1)}, bf16[2048,256]{1,0:T(8,128)(2,1)S(1)}, u32[]{:S(2)}, u32[]{:S(2)}) collective-permute-start(bf16[2048,256]{1,0:T(8,128)(2,1)S(1)} %get-tuple-element.48.refs_1_), channel_id=1, source_target_pairs={{0,96},{4,28},{8,104},{12,4},{16,112},{20,12},{24,120},{28,20},{32... | collective-permute-start | bytes 3145736 | tf_op jit(solution)/shard_map/ppermute | solution.py:398
  32.8 0.0 collective-permute-start.4
  32.8 0.0 collective-permute-done.3.refs_2_
  32.8 0.9 copy-done.3
  33.7 6.2 %shard_map.109 = (f32[1024,128]{1,0:T(8,128)S(1)}, f32[1024,256]{1,0:T(8,128)S(1)}) custom-call(bf16[1024,128]{1,0:T(8,128)(2,1)S(1)} %copy-done.3, bf16[2048,256]{1,0:T(8,128)(2,1)S(1)} %get-tuple-element.48.refs_1_, bf16[2048,256]{1,0:T(8,128)(2,1)S(1)} %collective-permute-done.3.refs_2_), custom_call_target="tpu_custom_call" | custom-call | flops 2147483648 | bytes 2097152 | tf_op jit(solution)/shard_map/pallas_call | solution.py:205
  40.0 7.7 %collective-permute-done.5.refs_2_ = bf16[2048,256]{1,0:T(8,128)(2,1)S(1)} collective-permute-done((bf16[2048,256]{1,0:T(8,128)(2,1)S(1)}, bf16[2048,256]{1,0:T(8,128)(2,1)S(1)}, u32[]{:S(2)}, u32[]{:S(2)}) %collective-permute-start.5) | collective-permute-done | bytes 1048608 | tf_op jit(solution)/shard_map/ppermute | solution.py:398
  47.7 2.5 %collective-permute-done.4.refs_1_ = bf16[2048,256]{1,0:T(8,128)(2,1)S(1)} collective-permute-done((bf16[2048,256]{1,0:T(8,128)(2,1)S(1)}, bf16[2048,256]{1,0:T(8,128)(2,1)S(1)}, u32[]{:S(2)}, u32[]{:S(2)}) %collective-permute-start.4) | collective-permute-done | bytes 1048608 | tf_op jit(solution)/shard_map/ppermute | solution.py:398
  50.1 0.5 collective-permute-start.7
  50.6 0.4 collective-permute-start.8
  51.0 1.5 collective-permute-start.13
  52.5 2.7 %collective-permute-start.12 = (bf16[256,2048]{1,0:T(8,128)(2,1)}, bf16[256,2048]{1,0:T(8,128)(2,1)}, u32[]{:S(2)}, u32[]{:S(2)}) collective-permute-start(bf16[256,2048]{1,0:T(8,128)(2,1)} %get-tuple-element.70.refs_4_), channel_id=1, source_target_pairs={{0,2},{1,3},{2,0},{3,1},{4,6},{5,7},{6,4},{7,5},{8,10},{9,11},{10,... | collective-permute-start | bytes 3145736 | tf_op jit(solution)/shard_map/ppermute | solution.py:380
  55.2 0.0 collective-permute-done.6.refs_1_
  55.2 1.4 collective-permute-start.11
  56.7 6.9 %shard_map.110 = (f32[1024,128]{1,0:T(8,128)S(1)}, f32[1024,256]{1,0:T(8,128)S(1)}) custom-call(bf16[1024,128]{1,0:T(8,128)(2,1)S(1)} %copy-done.3, bf16[2048,256]{1,0:T(8,128)(2,1)S(1)} %collective-permute-done.4.refs_1_, bf16[2048,256]{1,0:T(8,128)(2,1)S(1)} %collective-permute-done.5.refs_2_, f32[1024,128]{1,0:T(8,128)S(1)} %get-tuple-element.53.refs_3_, ...), custom_call_target="tpu_custom_call" | custom-call | flops 2147483648 | bytes 2097152 | tf_op jit(solution)/shard_map/pallas_call | solution.py:205
  63.6 6.9 %shard_map.111 = (f32[1024,128]{1,0:T(8,128)S(1)}, f32[1024,256]{1,0:T(8,128)S(1)}) custom-call(bf16[1024,128]{1,0:T(8,128)(2,1)S(1)} %copy-done.3, bf16[2048,256]{1,0:T(8,128)(2,1)S(1)} %collective-permute-done.6.refs_1_, bf16[2048,256]{1,0:T(8,128)(2,1)S(1)} %collective-permute-done.7.refs_2_, f32[1024,128]{1,0:T(8,128)S(1)} %get-tuple-element.55.refs_3_, ...), custom_call_target="tpu_custom_call" | custom-call | flops 2147483648 | bytes 2097152 | tf_op jit(solution)/shard_map/pallas_call | solution.py:205
  70.6 2.1 %collective-permute-done.8.refs_1_ = bf16[1024,256]{1,0:T(8,128)(2,1)S(1)} collective-permute-done((bf16[1024,256]{1,0:T(8,128)(2,1)S(1)}, bf16[1024,256]{1,0:T(8,128)(2,1)S(1)}, u32[]{:S(2)}, u32[]{:S(2)}) %collective-permute-start.8) | collective-permute-done | bytes 524320 | tf_op jit(solution)/shard_map/ppermute | solution.py:398
  72.7 0.0 collective-permute-start.9
  72.7 1.2 collective-permute-start.10
  73.8 0.7 collective-permute-done.9.refs_2_
  74.6 4.3 %shard_map.112 = (f32[1024,128]{1,0:T(8,128)S(1)}, f32[1024,256]{1,0:T(8,128)S(1)}) custom-call(bf16[1024,128]{1,0:T(8,128)(2,1)S(1)} %copy-done.3, bf16[1024,256]{1,0:T(8,128)(2,1)S(1)} %collective-permute-done.8.refs_1_, bf16[1024,256]{1,0:T(8,128)(2,1)S(1)} %collective-permute-done.9.refs_2_, f32[1024,128]{1,0:T(8,128)S(1)} %get-tuple-element.61.refs_3_, ...), custom_call_target="tpu_custom_call" | custom-call | flops 1073741824 | bytes 1048576 | tf_op jit(solution)/shard_map/pallas_call | solution.py:205
  78.8 15.9 %collective-permute-done.10.refs_1_ = bf16[1024,256]{1,0:T(8,128)(2,1)S(1)} collective-permute-done((bf16[1024,256]{1,0:T(8,128)(2,1)S(1)}, bf16[1024,256]{1,0:T(8,128)(2,1)S(1)}, u32[]{:S(2)}, u32[]{:S(2)}) %collective-permute-start.10) | collective-permute-done | bytes 524320 | tf_op jit(solution)/shard_map/ppermute | solution.py:398
  94.7 0.0 collective-permute-done.13.refs_7_
  94.7 6.0 %collective-permute-done.12.refs_6_ = bf16[256,2048]{1,0:T(8,128)(2,1)} collective-permute-done((bf16[256,2048]{1,0:T(8,128)(2,1)}, bf16[256,2048]{1,0:T(8,128)(2,1)}, u32[]{:S(2)}, u32[]{:S(2)}) %collective-permute-start.12) | collective-permute-done | bytes 1048608 | tf_op jit(solution)/shard_map/ppermute | solution.py:380
  100.7 0.2 collective-permute-done.11.refs_5_
  100.9 0.9 collective-permute-start.14
  101.9 0.0 collective-permute-start.18
  101.9 0.5 collective-permute-start.19
  102.4 0.0 collective-permute-start.20
  102.4 1.0 collective-permute-done.14.refs_2_
  103.4 4.4 %shard_map.113.refs_0_ = bf16[512,256]{1,0:T(8,128)(2,1)S(1)} custom-call(bf16[1024,128]{1,0:T(8,128)(2,1)S(1)} %copy-done.3, bf16[1024,256]{1,0:T(8,128)(2,1)S(1)} %collective-permute-done.10.refs_1_, bf16[1024,256]{1,0:T(8,128)(2,1)S(1)} %collective-permute-done.14.refs_2_, f32[1024,128]{1,0:T(8,128)S(1)} %get-tuple-element.68.refs_3_, ...), custom_call_target="tpu_custom_call" | custom-call | flops 1073741824 | bytes 1048576 | tf_op jit(solution)/shard_map/pallas_call | solution.py:205
  107.8 2.0 %collective-permute-start.17 = (bf16[512,256]{1,0:T(8,128)(2,1)S(1)}, bf16[512,256]{1,0:T(8,128)(2,1)S(1)}, u32[]{:S(2)}, u32[]{:S(2)}) collective-permute-start(bf16[512,256]{1,0:T(8,128)(2,1)S(1)} %shard_map.113.refs_0_), channel_id=1, source_target_pairs={{0,1},{1,2},{2,3},{3,0},{4,5},{5,6},{6,7},{7,4},{8,9},{9,10},{10,1... | collective-permute-start | bytes 786440 | tf_op jit(solution)/shard_map/ppermute | solution.py:380
  109.8 2.5 %collective-permute-start.16 = (bf16[512,256]{1,0:T(8,128)(2,1)S(1)}, bf16[512,256]{1,0:T(8,128)(2,1)S(1)}, u32[]{:S(2)}, u32[]{:S(2)}) collective-permute-start(bf16[512,256]{1,0:T(8,128)(2,1)S(1)} %shard_map.113.refs_0_), channel_id=1, source_target_pairs={{0,2},{1,3},{2,0},{3,1},{4,6},{5,7},{6,4},{7,5},{8,10},{9,11},{10,... | collective-permute-start | bytes 786440 | tf_op jit(solution)/shard_map/ppermute | solution.py:380
  112.3 5.3 %collective-permute-done.17.refs_3_ = bf16[512,256]{1,0:T(8,128)(2,1)S(1)} collective-permute-done((bf16[512,256]{1,0:T(8,128)(2,1)S(1)}, bf16[512,256]{1,0:T(8,128)(2,1)S(1)}, u32[]{:S(2)}, u32[]{:S(2)}) %collective-permute-start.17) | collective-permute-done | bytes 262176 | tf_op jit(solution)/shard_map/ppermute | solution.py:380
  117.6 2.4 %collective-permute-start.15 = (bf16[512,256]{1,0:T(8,128)(2,1)S(1)}, bf16[512,256]{1,0:T(8,128)(2,1)S(1)}, u32[]{:S(2)}, u32[]{:S(2)}) collective-permute-start(bf16[512,256]{1,0:T(8,128)(2,1)S(1)} %shard_map.113.refs_0_), channel_id=1, source_target_pairs={{0,3},{1,0},{2,1},{3,2},{4,7},{5,4},{6,5},{7,6},{8,11},{9,8},{10,9... | collective-permute-start | bytes 786440 | tf_op jit(solution)/shard_map/ppermute | solution.py:380
  120.1 0.1 pad_add_fusion.place
  120.1 4.2 %collective-permute-done.16.refs_2_ = bf16[512,256]{1,0:T(8,128)(2,1)S(1)} collective-permute-done((bf16[512,256]{1,0:T(8,128)(2,1)S(1)}, bf16[512,256]{1,0:T(8,128)(2,1)S(1)}, u32[]{:S(2)}, u32[]{:S(2)}) %collective-permute-start.16) | collective-permute-done | bytes 262176 | tf_op jit(solution)/shard_map/ppermute | solution.py:380
  124.3 1.1 collective-permute-done.15.refs_1_
  125.4 0.0 collective-permute-done.18.refs_9_
  125.4 0.0 collective-permute-done.19.refs_10_
  125.4 0.0 all-gather.2.cloned.1.call-done.refs_13_.w_hbm
  125.4 20.2 %layer.1 = (bf16[128,2048]{1,0:T(8,128)(2,1)S(1)}, bf16[128,2048]{1,0:T(8,128)(2,1)S(1)}, bf16[128,2048]{1,0:T(8,128)(2,1)S(1)}, bf16[256,1408]{1,0:T(8,128)(2,1)S(1)}) custom-call(s32[2]{0:T(128)S(1)} %pad_add_fusion.place, bf16[512,256]{1,0:T(8,128)(2,1)S(1)} %shard_map.113.refs_0_, bf16[512,256]{1,0:T(8,128)(2,1)S(1)} %collective-permute-done.15.refs_1_, ...), custom_call_target="tpu_custom_call" | custom-call | tf_op jit(solution)/shard_map/layer/pallas_call | solution.py:333
  145.7 4.6 %rest.1 = (bf16[128,2048]{1,0:T(8,128)(2,1)S(1)}, bf16[128,2048]{1,0:T(8,128)(2,1)S(1)}) custom-call(bf16[256,1408]{1,0:T(8,128)(2,1)S(1)} %get-tuple-element.76.h_ref, bf16[2048,4224]{1,0:T(8,128)(2,1)} %all-gather.2.cloned.1.call-done.refs_13_.w_hbm), custom_call_target="tpu_custom_call" | custom-call | tf_op jit(solution)/shard_map/rest/pallas_call | solution.py:316
  150.2 2.6 %collective-permute-start.23 = (bf16[128,2048]{1,0:T(8,128)(2,1)S(1)}, bf16[128,2048]{1,0:T(8,128)(2,1)S(1)}, u32[]{:S(2)}, u32[]{:S(2)}) collective-permute-start(bf16[128,2048]{1,0:T(8,128)(2,1)S(1)} %get-tuple-element.80), channel_id=1, source_target_pairs={{0,3},{1,0},{2,1},{3,2},{4,7},{5,4},{6,5},{7,6},{8,11},{9,8},{10,9... | collective-permute-start | bytes 1572872 | tf_op jit(solution)/shard_map/ppermute | solution.py:380
  152.9 1.5 collective-permute-start.22
  154.4 10.7 %collective-permute-done.23 = bf16[128,2048]{1,0:T(8,128)(2,1)S(1)} collective-permute-done((bf16[128,2048]{1,0:T(8,128)(2,1)S(1)}, bf16[128,2048]{1,0:T(8,128)(2,1)S(1)}, u32[]{:S(2)}, u32[]{:S(2)}) %collective-permute-start.23) | collective-permute-done | bytes 524320 | tf_op jit(solution)/shard_map/ppermute | solution.py:380
  165.1 11.3 %collective-permute-done.21 = bf16[128,2048]{1,0:T(8,128)(2,1)S(1)} collective-permute-done((bf16[128,2048]{1,0:T(8,128)(2,1)S(1)}, bf16[128,2048]{1,0:T(8,128)(2,1)S(1)}, u32[]{:S(2)}, u32[]{:S(2)}) %collective-permute-start.21) | collective-permute-done | bytes 524320 | tf_op jit(solution)/shard_map/ppermute | solution.py:380
  176.4 1.2 add_convert_fusion
  (17 shorter events, 0.1 us)
Async XLA Ops:
  6.5 118.9 %all-gather.2.cloned.1.call-start = ((), (), s32[]{:S(2)}) async-start(), calls=%async_computation | async-start | bytes 17842176 | tf_op jit(solution)/shard_map/all_gather | solution.py:425
  9.8 115.6 %copy-start.2 = (f32[2048]{0:T(1024)S(1)}, f32[2048]{0:T(1024)}, u32[]{:S(2)}) copy-start(f32[2048]{0:T(1024)} %param.18) | copy-start | bytes 24580
  14.0 111.5 %copy-start = (bf16[128,2048]{1,0:T(8,128)(2,1)S(1)}, bf16[128,2048]{1,0:T(8,128)(2,1)}, u32[]{:S(2)}) copy-start(bf16[128,2048]{1,0:T(8,128)(2,1)} %get-tuple-element.74.refs_8_) | copy-start | bytes 1572868
  14.0 6.7 %collective-permute-start.2 = (bf16[512,256]{1,0:T(8,128)(2,1)}, bf16[512,256]{1,0:T(8,128)(2,1)S(1)}, u32[]{:S(2)}, u32[]{:S(2)}) collective-permute-start(bf16[512,256]{1,0:T(8,128)(2,1)} %get-tuple-element.47.refs_0_), channel_id=1, source_target_pairs={{0,24},{4,100},{8,0},{12,108},{16,8},{20,116},{24,16},{28,124},{32... | collective-permute-start | bytes 786440 | tf_op jit(solution)/shard_map/ppermute | solution.py:398
  14.4 7.7 %collective-permute-start.1 = (bf16[512,256]{1,0:T(8,128)(2,1)}, bf16[512,256]{1,0:T(8,128)(2,1)S(1)}, u32[]{:S(2)}, u32[]{:S(2)}) collective-permute-start(bf16[512,256]{1,0:T(8,128)(2,1)} %get-tuple-element.47.refs_0_), channel_id=1, source_target_pairs={{0,8},{4,36},{8,16},{12,44},{16,24},{20,52},{24,0},{28,60},{32,40}... | collective-permute-start | bytes 786440 | tf_op jit(solution)/shard_map/ppermute | solution.py:398
  16.1 9.3 %collective-permute-start = (bf16[512,256]{1,0:T(8,128)(2,1)}, bf16[512,256]{1,0:T(8,128)(2,1)S(1)}, u32[]{:S(2)}, u32[]{:S(2)}) collective-permute-start(bf16[512,256]{1,0:T(8,128)(2,1)} %get-tuple-element.47.refs_0_), channel_id=1, source_target_pairs={{0,16},{4,68},{8,24},{12,76},{16,0},{20,84},{24,8},{28,92},{32,48}... | collective-permute-start | bytes 786440 | tf_op jit(solution)/shard_map/ppermute | solution.py:398
  25.3 1.0 copy-start.1
  26.4 6.3 %collective-permute-start.3 = (bf16[2048,256]{1,0:T(8,128)(2,1)S(1)}, bf16[2048,256]{1,0:T(8,128)(2,1)S(1)}, u32[]{:S(2)}, u32[]{:S(2)}) collective-permute-start(bf16[2048,256]{1,0:T(8,128)(2,1)S(1)} %get-tuple-element.48.refs_1_), channel_id=1, source_target_pairs={{0,4},{4,0},{8,12},{12,8},{16,20},{20,16},{24,28},{28,24},{32,36},... | collective-permute-start | bytes 3145736 | tf_op jit(solution)/shard_map/ppermute | solution.py:403
  30.3 17.3 %collective-permute-start.5 = (bf16[2048,256]{1,0:T(8,128)(2,1)S(1)}, bf16[2048,256]{1,0:T(8,128)(2,1)S(1)}, u32[]{:S(2)}, u32[]{:S(2)}) collective-permute-start(bf16[2048,256]{1,0:T(8,128)(2,1)S(1)} %get-tuple-element.48.refs_1_), channel_id=1, source_target_pairs={{0,96},{4,28},{8,104},{12,4},{16,112},{20,12},{24,120},{28,20},{32... | collective-permute-start | bytes 3145736 | tf_op jit(solution)/shard_map/ppermute | solution.py:398
  32.8 17.3 %collective-permute-start.4 = (bf16[2048,256]{1,0:T(8,128)(2,1)S(1)}, bf16[2048,256]{1,0:T(8,128)(2,1)S(1)}, u32[]{:S(2)}, u32[]{:S(2)}) collective-permute-start(bf16[2048,256]{1,0:T(8,128)(2,1)S(1)} %get-tuple-element.48.refs_1_), channel_id=1, source_target_pairs={{0,32},{4,12},{8,40},{12,20},{16,48},{20,28},{24,56},{28,4},{32,64... | collective-permute-start | bytes 3145736 | tf_op jit(solution)/shard_map/ppermute | solution.py:398
  32.8 1.0 copy-start.3
  50.1 5.1 %collective-permute-start.6 = (bf16[2048,256]{1,0:T(8,128)(2,1)S(1)}, bf16[2048,256]{1,0:T(8,128)(2,1)S(1)}, u32[]{:S(2)}, u32[]{:S(2)}) collective-permute-start(bf16[2048,256]{1,0:T(8,128)(2,1)S(1)} %collective-permute-done.4.refs_1_), channel_id=1, source_target_pairs={{0,4},{4,0},{8,12},{12,8},{16,20},{20,16},{24,28},{28,24},{32,36},... | collective-permute-start | bytes 3145736 | tf_op jit(solution)/shard_map/ppermute | solution.py:403
  50.1 13.5 %collective-permute-start.7 = (bf16[2048,256]{1,0:T(8,128)(2,1)S(1)}, bf16[2048,256]{1,0:T(8,128)(2,1)S(1)}, u32[]{:S(2)}, u32[]{:S(2)}) collective-permute-start(bf16[2048,256]{1,0:T(8,128)(2,1)S(1)} %collective-permute-done.5.refs_2_), channel_id=1, source_target_pairs={{0,4},{4,0},{8,12},{12,8},{16,20},{20,16},{24,28},{28,24},{32,36},... | collective-permute-start | bytes 3145736 | tf_op jit(solution)/shard_map/ppermute | solution.py:403
  50.6 22.0 %collective-permute-start.8 = (bf16[1024,256]{1,0:T(8,128)(2,1)S(1)}, bf16[1024,256]{1,0:T(8,128)(2,1)S(1)}, u32[]{:S(2)}, u32[]{:S(2)}) collective-permute-start(bf16[1024,256]{1,0:T(8,128)(2,1)S(1)} %get-tuple-element.59), channel_id=1, source_target_pairs={{0,64},{4,20},{8,72},{12,28},{16,80},{20,4},{24,88},{28,12},{32,96... | collective-permute-start | bytes 1572872 | tf_op jit(solution)/shard_map/ppermute | solution.py:398
  51.0 43.7 %collective-permute-start.13 = (bf16[256,2048]{1,0:T(8,128)(2,1)}, bf16[256,2048]{1,0:T(8,128)(2,1)S(1)}, u32[]{:S(2)}, u32[]{:S(2)}) collective-permute-start(bf16[256,2048]{1,0:T(8,128)(2,1)} %get-tuple-element.70.refs_4_), channel_id=1, source_target_pairs={{0,1},{1,2},{2,3},{3,0},{4,5},{5,6},{6,7},{7,4},{8,9},{9,10},{10,1... | collective-permute-start | bytes 3145736 | tf_op jit(solution)/shard_map/ppermute | solution.py:380
  52.5 48.2 %collective-permute-start.12 = (bf16[256,2048]{1,0:T(8,128)(2,1)}, bf16[256,2048]{1,0:T(8,128)(2,1)}, u32[]{:S(2)}, u32[]{:S(2)}) collective-permute-start(bf16[256,2048]{1,0:T(8,128)(2,1)} %get-tuple-element.70.refs_4_), channel_id=1, source_target_pairs={{0,2},{1,3},{2,0},{3,1},{4,6},{5,7},{6,4},{7,5},{8,10},{9,11},{10,... | collective-permute-start | bytes 3145736 | tf_op jit(solution)/shard_map/ppermute | solution.py:380
  55.2 45.7 %collective-permute-start.11 = (bf16[256,2048]{1,0:T(8,128)(2,1)}, bf16[256,2048]{1,0:T(8,128)(2,1)}, u32[]{:S(2)}, u32[]{:S(2)}) collective-permute-start(bf16[256,2048]{1,0:T(8,128)(2,1)} %get-tuple-element.70.refs_4_), channel_id=1, source_target_pairs={{0,3},{1,0},{2,1},{3,2},{4,7},{5,4},{6,5},{7,6},{8,11},{9,8},{10,9... | collective-permute-start | bytes 3145736 | tf_op jit(solution)/shard_map/ppermute | solution.py:380
  72.7 1.9 %collective-permute-start.9 = (bf16[1024,256]{1,0:T(8,128)(2,1)S(1)}, bf16[1024,256]{1,0:T(8,128)(2,1)S(1)}, u32[]{:S(2)}, u32[]{:S(2)}) collective-permute-start(bf16[1024,256]{1,0:T(8,128)(2,1)S(1)} %collective-permute-done.8.refs_1_), channel_id=1, source_target_pairs={{0,4},{4,0},{8,12},{12,8},{16,20},{20,16},{24,28},{28,24},{32,36},... | collective-permute-start | bytes 1572872 | tf_op jit(solution)/shard_map/ppermute | solution.py:403
  72.7 22.0 %collective-permute-start.10 = (bf16[1024,256]{1,0:T(8,128)(2,1)S(1)}, bf16[1024,256]{1,0:T(8,128)(2,1)S(1)}, u32[]{:S(2)}, u32[]{:S(2)}) collective-permute-start(bf16[1024,256]{1,0:T(8,128)(2,1)S(1)} %get-tuple-element.65), channel_id=1, source_target_pairs={{0,64},{4,20},{8,72},{12,28},{16,80},{20,4},{24,88},{28,12},{32,96... | collective-permute-start | bytes 1572872 | tf_op jit(solution)/shard_map/ppermute | solution.py:398
  94.7 30.7 %copy-start.4 = (bf16[256,2048]{1,0:T(8,128)(2,1)}, bf16[256,2048]{1,0:T(8,128)(2,1)S(1)}, u32[]{:S(2)}) copy-start(bf16[256,2048]{1,0:T(8,128)(2,1)S(1)} %collective-permute-done.13.refs_7_) | copy-start | bytes 3145732
  100.9 2.5 %collective-permute-start.14 = (bf16[1024,256]{1,0:T(8,128)(2,1)S(1)}, bf16[1024,256]{1,0:T(8,128)(2,1)S(1)}, u32[]{:S(2)}, u32[]{:S(2)}) collective-permute-start(bf16[1024,256]{1,0:T(8,128)(2,1)S(1)} %collective-permute-done.10.refs_1_), channel_id=1, source_target_pairs={{0,4},{4,0},{8,12},{12,8},{16,20},{20,16},{24,28},{28,24},{32,36},... | collective-permute-start | bytes 1572872 | tf_op jit(solution)/shard_map/ppermute | solution.py:403
  101.9 23.5 %collective-permute-start.18 = (bf16[256,2048]{1,0:T(8,128)(2,1)}, bf16[256,2048]{1,0:T(8,128)(2,1)}, u32[]{:S(2)}, u32[]{:S(2)}) collective-permute-start(bf16[256,2048]{1,0:T(8,128)(2,1)} %collective-permute-done.11.refs_5_), channel_id=1, source_target_pairs={{0,4},{4,0},{8,12},{12,8},{16,20},{20,16},{24,28},{28,24},{32,36},... | collective-permute-start | bytes 3145736 | tf_op jit(solution)/shard_map/ppermute | solution.py:403
  101.9 23.5 %collective-permute-start.19 = (bf16[256,2048]{1,0:T(8,128)(2,1)}, bf16[256,2048]{1,0:T(8,128)(2,1)}, u32[]{:S(2)}, u32[]{:S(2)}) collective-permute-start(bf16[256,2048]{1,0:T(8,128)(2,1)} %collective-permute-done.12.refs_6_), channel_id=1, source_target_pairs={{0,4},{4,0},{8,12},{12,8},{16,20},{20,16},{24,28},{28,24},{32,36},... | collective-permute-start | bytes 3145736 | tf_op jit(solution)/shard_map/ppermute | solution.py:403
  102.4 23.0 %collective-permute-start.20 = (bf16[256,2048]{1,0:T(8,128)(2,1)S(1)}, bf16[256,2048]{1,0:T(8,128)(2,1)}, u32[]{:S(2)}, u32[]{:S(2)}) collective-permute-start(bf16[256,2048]{1,0:T(8,128)(2,1)S(1)} %collective-permute-done.13.refs_7_), channel_id=1, source_target_pairs={{0,4},{4,0},{8,12},{12,8},{16,20},{20,16},{24,28},{28,24},{32,36},... | collective-permute-start | bytes 3145736 | tf_op jit(solution)/shard_map/ppermute | solution.py:403
  107.8 9.9 %collective-permute-start.17 = (bf16[512,256]{1,0:T(8,128)(2,1)S(1)}, bf16[512,256]{1,0:T(8,128)(2,1)S(1)}, u32[]{:S(2)}, u32[]{:S(2)}) collective-permute-start(bf16[512,256]{1,0:T(8,128)(2,1)S(1)} %shard_map.113.refs_0_), channel_id=1, source_target_pairs={{0,1},{1,2},{2,3},{3,0},{4,5},{5,6},{6,7},{7,4},{8,9},{9,10},{10,1... | collective-permute-start | bytes 786440 | tf_op jit(solution)/shard_map/ppermute | solution.py:380
  109.8 14.5 %collective-permute-start.16 = (bf16[512,256]{1,0:T(8,128)(2,1)S(1)}, bf16[512,256]{1,0:T(8,128)(2,1)S(1)}, u32[]{:S(2)}, u32[]{:S(2)}) collective-permute-start(bf16[512,256]{1,0:T(8,128)(2,1)S(1)} %shard_map.113.refs_0_), channel_id=1, source_target_pairs={{0,2},{1,3},{2,0},{3,1},{4,6},{5,7},{6,4},{7,5},{8,10},{9,11},{10,... | collective-permute-start | bytes 786440 | tf_op jit(solution)/shard_map/ppermute | solution.py:380
  117.6 7.7 %collective-permute-start.15 = (bf16[512,256]{1,0:T(8,128)(2,1)S(1)}, bf16[512,256]{1,0:T(8,128)(2,1)S(1)}, u32[]{:S(2)}, u32[]{:S(2)}) collective-permute-start(bf16[512,256]{1,0:T(8,128)(2,1)S(1)} %shard_map.113.refs_0_), channel_id=1, source_target_pairs={{0,3},{1,0},{2,1},{3,2},{4,7},{5,4},{6,5},{7,6},{8,11},{9,8},{10,9... | collective-permute-start | bytes 786440 | tf_op jit(solution)/shard_map/ppermute | solution.py:380
  150.2 14.9 %collective-permute-start.23 = (bf16[128,2048]{1,0:T(8,128)(2,1)S(1)}, bf16[128,2048]{1,0:T(8,128)(2,1)S(1)}, u32[]{:S(2)}, u32[]{:S(2)}) collective-permute-start(bf16[128,2048]{1,0:T(8,128)(2,1)S(1)} %get-tuple-element.80), channel_id=1, source_target_pairs={{0,3},{1,0},{2,1},{3,2},{4,7},{5,4},{6,5},{7,6},{8,11},{9,8},{10,9... | collective-permute-start | bytes 1572872 | tf_op jit(solution)/shard_map/ppermute | solution.py:380
  152.8 23.6 %collective-permute-start.21 = (bf16[128,2048]{1,0:T(8,128)(2,1)S(1)}, bf16[128,2048]{1,0:T(8,128)(2,1)S(1)}, u32[]{:S(2)}, u32[]{:S(2)}) collective-permute-start(bf16[128,2048]{1,0:T(8,128)(2,1)S(1)} %get-tuple-element.78), channel_id=1, source_target_pairs={{0,1},{1,2},{2,3},{3,0},{4,5},{5,6},{6,7},{7,4},{8,9},{9,10},{10,1... | collective-permute-start | bytes 1572872 | tf_op jit(solution)/shard_map/ppermute | solution.py:380
  152.9 23.6 %collective-permute-start.22 = (bf16[128,2048]{1,0:T(8,128)(2,1)S(1)}, bf16[128,2048]{1,0:T(8,128)(2,1)S(1)}, u32[]{:S(2)}, u32[]{:S(2)}) collective-permute-start(bf16[128,2048]{1,0:T(8,128)(2,1)S(1)} %get-tuple-element.79), channel_id=1, source_target_pairs={{0,2},{1,3},{2,0},{3,1},{4,6},{5,7},{6,4},{7,5},{8,10},{9,11},{10,... | collective-permute-start | bytes 1572872 | tf_op jit(solution)/shard_map/ppermute | solution.py:380
Sparse Core Ops, SparseCore 0:
  9.6 89.8 all-gather.1

commit v8 on v7

--- a/solution.py
+++ b/solution.py
@@ -219,33 +219,13 @@
     )(q, *kv, *([] if first else state))
 
 
-def layer_kernel(place, *refs, parts, tile, sub, units, unit_tile):
+def project_kernel(place, *refs, parts, tile, sub):
     att = refs[0:parts]
     sent = refs[parts : 2 * parts]
     swapped = refs[2 * parts : 3 * parts]
-    gain_ref, w_hbm, own_ref = refs[3 * parts : 3 * parts + 3]
-    out_1, out_2, rest_ref = refs[3 * parts + 3 : -5]
-    x_ref, pair_ref, down_ref, h_ref, sems = refs[-5:]
+    gain_ref, own_ref, norm_ref, x_ref = refs[3 * parts :]
     step = pl.program_id(0)
     half = sent[0].shape[0] - sub
-    count = units // unit_tile
-    blocks, rows, _ = down_ref.shape
-
-    def copies():
-        found = []
-        for n in range(count):
-            source = w_hbm.at[:, pl.ds(2 * n * unit_tile, 2 * unit_tile)]
-            found.append(pltpu.make_async_copy(source, pair_ref.at[n], sems.at[n]))
-        for n in range(blocks):
-            source = w_hbm.at[pl.ds(n * rows, rows), pl.ds(2 * units, units)]
-            found.append(pltpu.make_async_copy(source, down_ref.at[n], sems.at[count + n]))
-        return found
-
-    @pl.when(step == 0)
-    def _():
-        for c in copies():
-            c.start()
-
     cols = pl.ds(pl.multiple_of(step * tile, tile), tile)
     total = None
     for a, w, o in zip(att, sent, swapped):
@@ -268,24 +248,100 @@
             some = slice(r * sub // 2, (r + 1) * sub // 2)
             x = x_ref[some, :].astype(f32)
             x = x * lax.rsqrt(jnp.mean(x * x, axis=-1, keepdims=True) + norm_eps)
-            x_ref[some, :] = (x * gain_ref[...]).astype(bf16)
-        for c in copies():
+            norm_ref[some, :] = (x * gain_ref[...]).astype(bf16)
+
+
+def project(place, att, sent, swapped, gain, tile=512):
+    parts = len(att)
+    tok, part_width = att[0].shape
+    both, width = sent[0].shape
+    sub = tok // parts
+    return pl.pallas_call(
+        functools.partial(project_kernel, parts=parts, tile=tile, sub=sub),
+        grid_spec=pltpu.PrefetchScalarGridSpec(
+            num_scalar_prefetch=1,
+            grid=(width // tile,),
+            in_specs=[pl.BlockSpec((tok, part_width), lambda i, p: (0, 0))] * parts
+            + [pl.BlockSpec((both, tile), lambda i, p: (0, i))] * parts
+            + [pl.BlockSpec((s.shape[0], tile), lambda i, p: (0, i)) for s in swapped]
+            + [pl.BlockSpec((1, width), lambda i, p: (0, 0))],
+            out_specs=[pl.BlockSpec((sub, width), lambda i, p: (0, 0)), pl.BlockSpec((tok, width), lambda i, p: (0, 0))],
+            scratch_shapes=[pltpu.VMEM((tok, width), bf16)],
+        ),
+        out_shape=[jax.ShapeDtypeStruct((sub, width), bf16), jax.ShapeDtypeStruct((tok, width), bf16)],
+        compiler_params=pltpu.CompilerParams(dimension_semantics=("arbitrary",), vmem_limit_bytes=54 << 20),
+        name="project",
+    )(place, *att, *sent, *swapped, gain[None, :])
+
+
+def unit_kernel(x_ref, w_hbm, out_1, out_2, rest_ref, pair_ref, down_ref, h_ref, sems, *, units, unit_tile, groups, split):
+    sub = out_1.shape[0]
+    width = x_ref.shape[1]
+    count = units // unit_tile
+    blocks, rows, _ = down_ref.shape
+
+    def copies(n):
+        found = []
+        for m in range(split):
+            if n < count:
+                part = pl.ds(m * width // split, width // split)
+                source = w_hbm.at[part, pl.ds(2 * n * unit_tile, 2 * unit_tile)]
+                target = pair_ref.at[n, part, :]
+            else:
+                b = n - count
+                source = w_hbm.at[pl.ds(b * rows + m * rows // split, rows // split), pl.ds(2 * units, units)]
+                target = down_ref.at[b, pl.ds(m * rows // split, rows // split), :]
+            found.append(pltpu.make_async_copy(source, target, sems.at[n * split + m]))
+        return found
+
+    bounds = [sum(groups[:g]) for g in range(len(groups) + 1)] + [count + blocks]
+    waves = [[c for n in range(bounds[g], bounds[g + 1]) for c in copies(n)] for g in range(len(groups) + 1)]
+
+    def arrive(g):
+        for c in waves[g]:
             c.wait()
-
-        def product(n):
-            return jnp.dot(x_ref[...], pair_ref[n], preferred_element_type=f32)
-
-        following = product(0)
-        for n in range(count):
+        if g + 1 < len(waves):
+            for c in waves[g + 1]:
+                c.start()
+
+    def product(n):
+        return jnp.dot(x_ref[...], pair_ref[n], preferred_element_type=f32)
+
+    for c in waves[0]:
+        c.start()
+    for g in range(len(groups)):
+        arrive(g)
+        following = product(bounds[g])
+        for n in range(bounds[g], bounds[g + 1]):
             r = following
-            if n + 1 < count:
+            if n + 1 < bounds[g + 1]:
                 following = product(n + 1)
             gate = r[:, 0:unit_tile]
             hidden = gate / (1.0 + jnp.exp(-gate)) * r[:, unit_tile:]
             h_ref[:, n * unit_tile : (n + 1) * unit_tile] = hidden.astype(bf16)
-        rest_ref[0:sub, :] = h_ref[0:sub, :]
-        rest_ref[sub:, :] = h_ref[3 * sub :, :]
-        down_products(h_ref[sub : 3 * sub, :], down_ref, (out_1, out_2))
+    arrive(len(groups))
+    rest_ref[0:sub, :] = h_ref[0:sub, :]
+    rest_ref[sub:, :] = h_ref[3 * sub :, :]
+    down_products(h_ref[sub : 3 * sub, :], down_ref, (out_1, out_2))
+
+
+def feed_forward(x, weights, units, sub, unit_tile=128, rows=512, groups=(3, 4, 4), split=2):
+    tok, width = x.shape
+    count = units // unit_tile
+    blocks = width // rows
+    return pl.pallas_call(
+        functools.partial(unit_kernel, units=units, unit_tile=unit_tile, groups=groups, split=split),
+        in_specs=[pl.BlockSpec(memory_space=pltpu.VMEM), pl.BlockSpec(memory_space=pltpu.HBM)],
+        out_shape=[jax.ShapeDtypeStruct((sub, width), bf16)] * 2 + [jax.ShapeDtypeStruct((2 * sub, units), bf16)],
+        scratch_shapes=[
+            pltpu.VMEM((count, width, 2 * unit_tile), bf16),
+            pltpu.VMEM((blocks, rows, units), bf16),
+            pltpu.VMEM((tok, units), bf16),
+            pltpu.SemaphoreType.DMA(((count + blocks) * split,)),
+        ],
+        compiler_params=pltpu.CompilerParams(vmem_limit_bytes=50 << 20),
+        name="units",
+    )(x, weights)
 
 
 def down_products(hidden, down_ref, outs):
@@ -323,54 +379,18 @@
     )(hidden, weights)
 
 
-def layer(place, att, sent, swapped, gain, weights, units, tile=512, unit_tile=128, rows=512):
-    parts = len(att)
-    tok, part_width = att[0].shape
-    both, width = sent[0].shape
-    sub = tok // parts
-    count = units // unit_tile
-    blocks = width // rows
-    return pl.pallas_call(
-        functools.partial(layer_kernel, parts=parts, tile=tile, sub=sub, units=units, unit_tile=unit_tile),
-        grid_spec=pltpu.PrefetchScalarGridSpec(
-            num_scalar_prefetch=1,
-            grid=(width // tile,),
-            in_specs=[pl.BlockSpec((tok, part_width), lambda i, p: (0, 0))] * parts
-            + [pl.BlockSpec((both, tile), lambda i, p: (0, i))] * parts
-            + [pl.BlockSpec((s.shape[0], tile), lambda i, p: (0, i)) for s in swapped]
-            + [pl.BlockSpec((1, width), lambda i, p: (0, 0)), pl.BlockSpec(memory_space=pltpu.HBM)],
-            out_specs=[pl.BlockSpec((sub, width), lambda i, p: (0, 0))] * 3
-            + [pl.BlockSpec((2 * sub, units), lambda i, p: (0, 0))],
-            scratch_shapes=[
-                pltpu.VMEM((tok, width), bf16),
-                pltpu.VMEM((count, width, 2 * unit_tile), bf16),
-                pltpu.VMEM((blocks, rows, units), bf16),
-                pltpu.VMEM((tok, units), bf16),
-                pltpu.SemaphoreType.DMA((count + blocks,)),
-            ],
-        ),
-        out_shape=[jax.ShapeDtypeStruct((sub, width), bf16)] * 3 + [jax.ShapeDtypeStruct((2 * sub, units), bf16)],
-        compiler_params=pltpu.CompilerParams(dimension_semantics=("arbitrary",), vmem_limit_bytes=50 << 20),
-        name="layer",
-    )(place, *att, *sent, *swapped, gain[None, :], weights)
-
-
 def line_kernel(*refs):
-    pieces, (whole, *halves) = refs[:-3], refs[-3:]
-    rows = pieces[0].shape[0]
-    each = len(pieces) // 2
-    for n, piece in enumerate(pieces):
-        whole[n * rows : (n + 1) * rows, :] = piece[...]
-        halves[n // each][n % each * rows : (n % each + 1) * rows, :] = piece[...]
+    rows = refs[0].shape[0]
+    for n, piece in enumerate(refs[:-1]):
+        refs[-1][n * rows : (n + 1) * rows, :] = piece[...]
 
 
 def lined_up(*pieces):
     rows, width = pieces[0].shape
-    count = rows * len(pieces)
     return pl.pallas_call(
         line_kernel,
-        out_shape=[jax.ShapeDtypeStruct((n, width), bf16) for n in (count, count // 2, count // 2)],
-        compiler_params=pltpu.CompilerParams(vmem_limit_bytes=10 << 20),
+        out_shape=jax.ShapeDtypeStruct((rows * len(pieces), width), bf16),
+        compiler_params=pltpu.CompilerParams(vmem_limit_bytes=8 << 20),
         name="lines",
     )(*pieces)
 
@@ -421,22 +441,18 @@
     units = gate_weight.shape[1]
     core = lax.axis_index("sp") % 2
     place = jnp.stack([lax.axis_index("tp"), core])
-    woven = interleaved(gate_weight, up_weight, down_weight)
-    weights = lax.all_gather(woven, "sp", axis=0, tiled=True)
-    key_rows, woven = lax.optimization_barrier((key_rows, woven))
+    weights = lax.all_gather(interleaved(gate_weight, up_weight, down_weight), "sp", axis=0, tiled=True)
     q, kv, payload, kept = prepare(query_rows, key_rows, value_rows, query_gain, key_gain, out_weight, residual)
 
     steps = (2, 1, -1)
     line = [kv]
     for d in steps:
         line.append(crossed(kv, d, False))
-    line, *halves = lined_up(*line)
+    line = lined_up(*line)
     near = []
     for d in (1, -1):
         near.append(crossed(line, d, True))
-    far = []
-    for n in range(2):
-        far.append(crossed(halves[n], 2, True))
+    far = crossed(line, 2, True)
 
     sent = [payload]
     for r in range(1, parts):
@@ -447,18 +463,17 @@
     near_swapped = [other_core(v) for v in near]
     state = flash(q, near, state, tok, False)
     state = flash(q, near_swapped, state, tok, False)
-    state, far[0] = lax.optimization_barrier((state, far[0]))
-    far_swapped = [other_core(far[0])]
-    state = flash(q, [far[0], far_swapped[0]], state, tok, False)
-    state, far[1], sent = lax.optimization_barrier((state, far[1], sent))
-    far_swapped.append(other_core(far[1]))
+    state, far, sent = lax.optimization_barrier((state, far, sent))
+    far_swapped = other_core(far)
     swapped = [kept]
     for r in range(1, parts):
         swapped.append(other_core(sent[r]))
-    attended = flash(q, [far[1], far_swapped[1]], state, tok, True)
+    state = flash(q, [far], state, tok, False)
+    attended = flash(q, [far_swapped], state, tok, True)
 
     att_parts = [attended] + [shifted(attended, -r) for r in range(1, parts)]
-    own_rows, part_1, part_2, hidden = layer(place, att_parts, sent, swapped, mix_gain, weights, units)
+    own_rows, normed = project(place, att_parts, sent, swapped, mix_gain)
+    part_1, part_2, hidden = feed_forward(normed, weights, units, own_rows.shape[0])
     part_0, part_3 = rest(hidden, weights)
     unit_sum = part_0.astype(f32)
     for r, part in ((1, part_1), (2, part_2), (3, part_3)):

time: 185 us -> 193 us (1.043); the launches traced: 185 us -> 190 us
  starting transfers between devices: 32.2 us -> 25.8 us
  waiting for transfers between devices: 74.5 us -> 80.8 us
  Pallas kernels: 59.8 us -> 62.5 us
  local copies, waits for them, and re-layouts: 1.92 us -> 4.54 us
    ppermute x9, waiting for transfers between devices: 38.8 us -> 63.7 us  [shifted(): lax.ppermute(value, 'tp', [(i, (i + by) % count) for i in range(count)])]
    ppermute x7 -> x6, waiting for transfers between devices: 33.9 us -> 17.1 us  [crossed(): return lax.ppermute(value, 'sp', pairs)]
    ppermute x8 -> x7, starting transfers between devices: 5.83 us -> 1.61 us  [other_core(): return lax.ppermute(value, 'sp', [(n, n ^ 1) for n in range(count)])]
    ppermute x9, starting transfers between devices: 16.8 us -> 12.9 us  [shifted(): lax.ppermute(value, 'tp', [(i, (i + by) % count) for i in range(count)])]
    pallas_call x2 -> x3, Pallas kernels: 20.3 us -> 23 us  [the longest x1 13.9 us: feed_forward(): pl.pallas_call(functools.partial(unit_kernel, units=units, unit_tile=unit...]
    unnamed x10 -> x18, local copies, waits for them, and re-layouts: 1.92 us -> 4.54 us
    ppermute x7 -> x6, starting transfers between devices: 9.62 us -> 11.2 us  [crossed(): return lax.ppermute(value, 'sp', pairs)]
  transfers between devices with their start and end apart: 25 -> 23, of which waited for: 16 -> 11; matrix products, arithmetic and copies ran while one was open for 1% -> 1% of each run, Pallas kernels for 18% -> 22%
where the time goes in v8:
time: 193 us; the launch traced here: 190 us
  waiting for transfers between devices  80.8 us (42%)
  Pallas kernels  62.5 us (32%)
  starting transfers between devices  25.8 us (13%)
  between operations  13.6 us (7%)
  local copies, waits for them, and re-layouts  4.54 us (2%)
  other arithmetic  3.03 us (2%)
    ppermute x9, waiting for transfers between devices, shifted(): lax.ppermute(value, 'tp', [(i, (i + by) % count) for i in range(count)])  63.7 us
    pallas_call x5, Pallas kernels, flash(): pl.pallas_call(functools.partial(flash_kernel, pieces=pieces, scale=head_...  28.8 us
    ppermute x6, waiting for transfers between devices, crossed(): return lax.ppermute(value, 'sp', pairs)  17.1 us
    pallas_call x1, Pallas kernels, feed_forward(): pl.pallas_call(functools.partial(unit_kernel, units=units, unit_tile=unit...  13.9 us
    ppermute x9, starting transfers between devices, shifted(): lax.ppermute(value, 'tp', [(i, (i + by) % count) for i in range(count)])  12.9 us
    ppermute x6, starting transfers between devices, crossed(): return lax.ppermute(value, 'sp', pairs)  11.2 us
    pallas_call x1, Pallas kernels, project(): pl.pallas_call(functools.partial(project_kernel, parts=parts, tile=tile,...  9.03 us
    unnamed x18, local copies, waits for them, and re-layouts  4.54 us
  transfers between devices with their start and end apart: 23, of which 11 were waited for; matrix products, arithmetic and copies ran while one was open for 1% of the time, Pallas kernels for 22%

profile of v8, /device:TPU:8, one launch (start us, length us, event | category | flops | bytes accessed | tf_op | source)
XLA Modules:
  0.0 190.3 jit_solution(8017191540194399825)
XLA Ops:
  6.5 2.0 %weave.1 = bf16[64,4224]{1,0:T(8,128)(2,1)} custom-call(bf16[64,1408]{1,0:T(8,128)(2,1)} %g_hbm.1, bf16[64,1408]{1,0:T(8,128)(2,1)} %u_hbm.1, bf16[64,1408]{1,0:T(8,128)(2,1)} %bitcast.6), custom_call_target="tpu_custom_call" | custom-call | tf_op jit(solution)/shard_map/weave/pallas_call | solution.py:112
  8.6 0.0 all-gather.2.cloned.1.call-update
  8.6 0.1 add_convert_fusion.1
  8.7 0.2 multiply_sine_fusion
  8.9 0.1 negate_select_fusion.1
  9.0 0.8 pad_maximum_fusion
  9.8 4.1 %prepare.1 = (bf16[1024,128]{1,0:T(8,128)(2,1)}, bf16[512,256]{1,0:T(8,128)(2,1)}, bf16[256,2048]{1,0:T(8,128)(2,1)}, bf16[128,2048]{1,0:T(8,128)(2,1)}) custom-call(s32[1]{0:T(128)} %bitcast.1.core, bf16[512,256]{1,0:T(8,128)(2,1)} %q_hbm.1, bf16[512,128]{1,0:T(8,128)(2,1)} %k_hbm.1, bf16[512,128]{1,0:T(8,128)(2,1)} %v_hbm.1, bf16[256,2048]{1,0:T(8,128)(2,1)} %w_hbm.1, ...), custom_call_target="tpu_custom_call" | custom-call | tf_op jit(solution)/shard_map/prepare/pallas_call | solution.py:131
  13.9 2.4 %collective-permute-start = (bf16[512,256]{1,0:T(8,128)(2,1)}, bf16[512,256]{1,0:T(8,128)(2,1)S(1)}, u32[]{:S(2)}, u32[]{:S(2)}) collective-permute-start(bf16[512,256]{1,0:T(8,128)(2,1)} %get-tuple-element.40.refs_0_), channel_id=1, source_target_pairs={{0,16},{4,68},{8,24},{12,76},{16,0},{20,84},{24,8},{28,92},{32,48}... | collective-permute-start | bytes 786440 | tf_op jit(solution)/shard_map/ppermute | solution.py:418
  16.3 0.0 collective-permute-start.1
  16.3 2.0 %collective-permute-start.2 = (bf16[512,256]{1,0:T(8,128)(2,1)}, bf16[512,256]{1,0:T(8,128)(2,1)S(1)}, u32[]{:S(2)}, u32[]{:S(2)}) collective-permute-start(bf16[512,256]{1,0:T(8,128)(2,1)} %get-tuple-element.40.refs_0_), channel_id=1, source_target_pairs={{0,24},{4,100},{8,0},{12,108},{16,8},{20,116},{24,16},{28,124},{32... | collective-permute-start | bytes 786440 | tf_op jit(solution)/shard_map/ppermute | solution.py:418
  18.3 3.9 %collective-permute-done.refs_1_ = bf16[512,256]{1,0:T(8,128)(2,1)S(1)} collective-permute-done((bf16[512,256]{1,0:T(8,128)(2,1)}, bf16[512,256]{1,0:T(8,128)(2,1)S(1)}, u32[]{:S(2)}, u32[]{:S(2)}) %collective-permute-start) | collective-permute-done | bytes 262176 | tf_op jit(solution)/shard_map/ppermute | solution.py:418
  22.2 5.8 %collective-permute-done.1.refs_2_ = bf16[512,256]{1,0:T(8,128)(2,1)S(1)} collective-permute-done((bf16[512,256]{1,0:T(8,128)(2,1)}, bf16[512,256]{1,0:T(8,128)(2,1)S(1)}, u32[]{:S(2)}, u32[]{:S(2)}) %collective-permute-start.1) | collective-permute-done | bytes 262176 | tf_op jit(solution)/shard_map/ppermute | solution.py:418
  28.0 0.0 collective-permute-done.2.refs_3_
  28.0 1.0 copy-done.1
  29.0 0.1 lines.1.refs_1_
  29.1 0.1 collective-permute-start.3
  29.1 2.2 %collective-permute-start.4 = (bf16[2048,256]{1,0:T(8,128)(2,1)S(1)}, bf16[2048,256]{1,0:T(8,128)(2,1)S(1)}, u32[]{:S(2)}, u32[]{:S(2)}) collective-permute-start(bf16[2048,256]{1,0:T(8,128)(2,1)S(1)} %lines.1.refs_1_), channel_id=1, source_target_pairs={{0,32},{4,12},{8,40},{12,20},{16,48},{20,28},{24,56},{28,4},{32,64... | collective-permute-start | bytes 3145736 | tf_op jit(solution)/shard_map/ppermute | solution.py:418
  31.4 3.0 %collective-permute-start.5 = (bf16[2048,256]{1,0:T(8,128)(2,1)S(1)}, bf16[2048,256]{1,0:T(8,128)(2,1)S(1)}, u32[]{:S(2)}, u32[]{:S(2)}) collective-permute-start(bf16[2048,256]{1,0:T(8,128)(2,1)S(1)} %lines.1.refs_1_), channel_id=1, source_target_pairs={{0,96},{4,28},{8,104},{12,4},{16,112},{20,12},{24,120},{28,20},{32... | collective-permute-start | bytes 3145736 | tf_op jit(solution)/shard_map/ppermute | solution.py:418
  34.4 0.0 collective-permute-done.3.refs_2_
  34.4 1.0 copy-done.3
  35.4 6.2 %shard_map.109 = (f32[1024,128]{1,0:T(8,128)S(1)}, f32[1024,256]{1,0:T(8,128)S(1)}) custom-call(bf16[1024,128]{1,0:T(8,128)(2,1)S(1)} %copy-done.3, bf16[2048,256]{1,0:T(8,128)(2,1)S(1)} %lines.1.refs_1_, bf16[2048,256]{1,0:T(8,128)(2,1)S(1)} %collective-permute-done.3.refs_2_), custom_call_target="tpu_custom_call" | custom-call | flops 2147483648 | bytes 2097152 | tf_op jit(solution)/shard_map/pallas_call | solution.py:205
  41.6 6.8 %collective-permute-done.4.refs_1_ = bf16[2048,256]{1,0:T(8,128)(2,1)S(1)} collective-permute-done((bf16[2048,256]{1,0:T(8,128)(2,1)S(1)}, bf16[2048,256]{1,0:T(8,128)(2,1)S(1)}, u32[]{:S(2)}, u32[]{:S(2)}) %collective-permute-start.4) | collective-permute-done | bytes 1048608 | tf_op jit(solution)/shard_map/ppermute | solution.py:418
  48.4 0.6 collective-permute-done.5.refs_2_
  49.0 0.0 collective-permute-start.6
  49.0 0.5 collective-permute-start.7
  49.5 3.0 %collective-permute-start.10 = (bf16[256,2048]{1,0:T(8,128)(2,1)}, bf16[256,2048]{1,0:T(8,128)(2,1)S(1)}, u32[]{:S(2)}, u32[]{:S(2)}) collective-permute-start(bf16[256,2048]{1,0:T(8,128)(2,1)} %get-tuple-element.57.refs_4_), channel_id=1, source_target_pairs={{0,2},{1,3},{2,0},{3,1},{4,6},{5,7},{6,4},{7,5},{8,10},{9,11},{10,... | collective-permute-start | bytes 3145736 | tf_op jit(solution)/shard_map/ppermute | solution.py:400
  52.5 0.6 collective-permute-start.11
  53.1 2.6 %collective-permute-start.9 = (bf16[256,2048]{1,0:T(8,128)(2,1)}, bf16[256,2048]{1,0:T(8,128)(2,1)S(1)}, u32[]{:S(2)}, u32[]{:S(2)}) collective-permute-start(bf16[256,2048]{1,0:T(8,128)(2,1)} %get-tuple-element.57.refs_4_), channel_id=1, source_target_pairs={{0,3},{1,0},{2,1},{3,2},{4,7},{5,4},{6,5},{7,6},{8,11},{9,8},{10,9... | collective-permute-start | bytes 3145736 | tf_op jit(solution)/shard_map/ppermute | solution.py:400
  55.7 0.0 collective-permute-done.6.refs_1_
  55.7 1.6 collective-permute-start.8
  57.3 6.9 %shard_map.110 = (f32[1024,128]{1,0:T(8,128)S(1)}, f32[1024,256]{1,0:T(8,128)S(1)}) custom-call(bf16[1024,128]{1,0:T(8,128)(2,1)S(1)} %copy-done.3, bf16[2048,256]{1,0:T(8,128)(2,1)S(1)} %collective-permute-done.4.refs_1_, bf16[2048,256]{1,0:T(8,128)(2,1)S(1)} %collective-permute-done.5.refs_2_, f32[1024,128]{1,0:T(8,128)S(1)} %get-tuple-element.45.refs_3_, ...), custom_call_target="tpu_custom_call" | custom-call | flops 2147483648 | bytes 2097152 | tf_op jit(solution)/shard_map/pallas_call | solution.py:205
  64.2 0.0 collective-permute-done.7.refs_2_
  64.3 6.9 %shard_map.111 = (f32[1024,128]{1,0:T(8,128)S(1)}, f32[1024,256]{1,0:T(8,128)S(1)}) custom-call(bf16[1024,128]{1,0:T(8,128)(2,1)S(1)} %copy-done.3, bf16[2048,256]{1,0:T(8,128)(2,1)S(1)} %collective-permute-done.6.refs_1_, bf16[2048,256]{1,0:T(8,128)(2,1)S(1)} %collective-permute-done.7.refs_2_, f32[1024,128]{1,0:T(8,128)S(1)} %get-tuple-element.47.refs_3_, ...), custom_call_target="tpu_custom_call" | custom-call | flops 2147483648 | bytes 2097152 | tf_op jit(solution)/shard_map/pallas_call | solution.py:205
  71.2 6.1 %collective-permute-done.10.refs_6_ = bf16[256,2048]{1,0:T(8,128)(2,1)S(1)} collective-permute-done((bf16[256,2048]{1,0:T(8,128)(2,1)}, bf16[256,2048]{1,0:T(8,128)(2,1)S(1)}, u32[]{:S(2)}, u32[]{:S(2)}) %collective-permute-start.10) | collective-permute-done | bytes 1048608 | tf_op jit(solution)/shard_map/ppermute | solution.py:400
  77.3 21.5 %collective-permute-done.11.refs_7_ = bf16[256,2048]{1,0:T(8,128)(2,1)S(1)} collective-permute-done((bf16[256,2048]{1,0:T(8,128)(2,1)}, bf16[256,2048]{1,0:T(8,128)(2,1)S(1)}, u32[]{:S(2)}, u32[]{:S(2)}) %collective-permute-start.11) | collective-permute-done | bytes 1048608 | tf_op jit(solution)/shard_map/ppermute | solution.py:400
  98.7 0.1 collective-permute-done.9.refs_5_
  98.9 0.0 collective-permute-done.8.refs_1_
  98.9 0.0 collective-permute-start.12
  98.9 0.5 collective-permute-start.16
  99.4 0.1 collective-permute-start.17
  99.5 0.4 collective-permute-start.18
  99.9 4.2 %shard_map.112 = (f32[1024,128]{1,0:T(8,128)S(1)}, f32[1024,256]{1,0:T(8,128)S(1)}) custom-call(bf16[1024,128]{1,0:T(8,128)(2,1)S(1)} %copy-done.3, bf16[2048,256]{1,0:T(8,128)(2,1)S(1)} %collective-permute-done.8.refs_1_, f32[1024,128]{1,0:T(8,128)S(1)} %get-tuple-element.53.refs_2_, f32[1024,256]{1,0:T(8,128)S(1)} %get-tuple-element.54.refs_3_), custom_call_target="tpu_custom_call" | custom-call | flops 1073741824 | bytes 1048576 | tf_op jit(solution)/shard_map/pallas_call | solution.py:205
  104.2 0.0 collective-permute-done.12.refs_1_
  104.2 4.4 %shard_map.113.refs_0_ = bf16[512,256]{1,0:T(8,128)(2,1)S(1)} custom-call(bf16[1024,128]{1,0:T(8,128)(2,1)S(1)} %copy-done.3, bf16[2048,256]{1,0:T(8,128)(2,1)S(1)} %collective-permute-done.12.refs_1_, f32[1024,128]{1,0:T(8,128)S(1)} %get-tuple-element.55.refs_2_, f32[1024,256]{1,0:T(8,128)S(1)} %get-tuple-element.56.refs_3_), custom_call_target="tpu_custom_call" | custom-call | flops 1073741824 | bytes 1048576 | tf_op jit(solution)/shard_map/pallas_call | solution.py:205
  108.6 2.7 %collective-permute-start.13 = (bf16[512,256]{1,0:T(8,128)(2,1)S(1)}, bf16[512,256]{1,0:T(8,128)(2,1)}, u32[]{:S(2)}, u32[]{:S(2)}) collective-permute-start(bf16[512,256]{1,0:T(8,128)(2,1)S(1)} %shard_map.113.refs_0_), channel_id=1, source_target_pairs={{0,3},{1,0},{2,1},{3,2},{4,7},{5,4},{6,5},{7,6},{8,11},{9,8},{10,9... | collective-permute-start | bytes 786440 | tf_op jit(solution)/shard_map/ppermute | solution.py:400
  111.3 0.9 collective-permute-start.14
  112.3 0.0 collective-permute-done.16.refs_9_
  112.3 1.0 copy-done.7
  113.3 0.0 collective-permute-start.15
  113.3 0.6 pad_add_fusion.place
  113.9 8.9 %collective-permute-done.13.refs_1_ = bf16[512,256]{1,0:T(8,128)(2,1)} collective-permute-done((bf16[512,256]{1,0:T(8,128)(2,1)S(1)}, bf16[512,256]{1,0:T(8,128)(2,1)}, u32[]{:S(2)}, u32[]{:S(2)}) %collective-permute-start.13) | collective-permute-done | bytes 262176 | tf_op jit(solution)/shard_map/ppermute | solution.py:400
  122.8 3.8 %collective-permute-done.15.refs_3_ = bf16[512,256]{1,0:T(8,128)(2,1)} collective-permute-done((bf16[512,256]{1,0:T(8,128)(2,1)S(1)}, bf16[512,256]{1,0:T(8,128)(2,1)}, u32[]{:S(2)}, u32[]{:S(2)}) %collective-permute-start.15) | collective-permute-done | bytes 262176 | tf_op jit(solution)/shard_map/ppermute | solution.py:400
  126.6 9.0 %project.1 = (bf16[128,2048]{1,0:T(8,128)(2,1)}, bf16[512,2048]{1,0:T(8,128)(2,1)}) custom-call(s32[2]{0:T(128)} %pad_add_fusion.place, bf16[512,256]{1,0:T(8,128)(2,1)} %copy-done.2, bf16[512,256]{1,0:T(8,128)(2,1)} %collective-permute-done.13.refs_1_, bf16[512,256]{1,0:T(8,128)(2,1)} %collective-permute-done.14.refs_2_, ...), custom_call_target="tpu_custom_call" | custom-call | tf_op jit(solution)/shard_map/project/pallas_call | solution.py:259
  135.6 0.0 all-gather.2.cloned.1.call-done.w_hbm
  135.6 1.6 copy-done
  137.2 13.9 %units.1 = (bf16[128,2048]{1,0:T(8,128)(2,1)S(1)}, bf16[128,2048]{1,0:T(8,128)(2,1)S(1)}, bf16[256,1408]{1,0:T(8,128)(2,1)S(1)}) custom-call(bf16[512,2048]{1,0:T(8,128)(2,1)S(1)} %copy-done, bf16[2048,4224]{1,0:T(8,128)(2,1)} %all-gather.2.cloned.1.call-done.w_hbm), custom_call_target="tpu_custom_call" | custom-call | tf_op jit(solution)/shard_map/units/pallas_call | solution.py:332
  151.2 4.5 %rest.1 = (bf16[128,2048]{1,0:T(8,128)(2,1)S(1)}, bf16[128,2048]{1,0:T(8,128)(2,1)S(1)}) custom-call(bf16[256,1408]{1,0:T(8,128)(2,1)S(1)} %get-tuple-element.64.h_ref, bf16[2048,4224]{1,0:T(8,128)(2,1)} %all-gather.2.cloned.1.call-done.w_hbm), custom_call_target="tpu_custom_call" | custom-call | tf_op jit(solution)/shard_map/rest/pallas_call | solution.py:372
  155.7 0.7 collective-permute-start.21
  156.4 1.4 collective-permute-start.19
  157.8 0.9 collective-permute-start.20
  158.7 11.8 %collective-permute-done.21 = bf16[128,2048]{1,0:T(8,128)(2,1)S(1)} collective-permute-done((bf16[128,2048]{1,0:T(8,128)(2,1)S(1)}, bf16[128,2048]{1,0:T(8,128)(2,1)S(1)}, u32[]{:S(2)}, u32[]{:S(2)}) %collective-permute-start.21) | collective-permute-done | bytes 524320 | tf_op jit(solution)/shard_map/ppermute | solution.py:400
  170.6 11.6 %collective-permute-done.19 = bf16[128,2048]{1,0:T(8,128)(2,1)S(1)} collective-permute-done((bf16[128,2048]{1,0:T(8,128)(2,1)S(1)}, bf16[128,2048]{1,0:T(8,128)(2,1)S(1)}, u32[]{:S(2)}, u32[]{:S(2)}) %collective-permute-start.19) | collective-permute-done | bytes 524320 | tf_op jit(solution)/shard_map/ppermute | solution.py:400
  182.1 0.0 collective-permute-done.20
  182.1 1.3 add_convert_fusion
  (22 shorter events, 0.1 us)
Async XLA Ops:
  6.5 129.1 %all-gather.2.cloned.1.call-start = ((), (), s32[]{:S(2)}) async-start(), calls=%async_computation | async-start | bytes 17842176 | tf_op jit(solution)/shard_map/all_gather | solution.py:444
  13.9 8.3 %collective-permute-start = (bf16[512,256]{1,0:T(8,128)(2,1)}, bf16[512,256]{1,0:T(8,128)(2,1)S(1)}, u32[]{:S(2)}, u32[]{:S(2)}) collective-permute-start(bf16[512,256]{1,0:T(8,128)(2,1)} %get-tuple-element.40.refs_0_), channel_id=1, source_target_pairs={{0,16},{4,68},{8,24},{12,76},{16,0},{20,84},{24,8},{28,92},{32,48}... | collective-permute-start | bytes 786440 | tf_op jit(solution)/shard_map/ppermute | solution.py:418
  16.3 11.7 %collective-permute-start.1 = (bf16[512,256]{1,0:T(8,128)(2,1)}, bf16[512,256]{1,0:T(8,128)(2,1)S(1)}, u32[]{:S(2)}, u32[]{:S(2)}) collective-permute-start(bf16[512,256]{1,0:T(8,128)(2,1)} %get-tuple-element.40.refs_0_), channel_id=1, source_target_pairs={{0,8},{4,36},{8,16},{12,44},{16,24},{20,52},{24,0},{28,60},{32,40}... | collective-permute-start | bytes 786440 | tf_op jit(solution)/shard_map/ppermute | solution.py:418
  16.3 11.7 %collective-permute-start.2 = (bf16[512,256]{1,0:T(8,128)(2,1)}, bf16[512,256]{1,0:T(8,128)(2,1)S(1)}, u32[]{:S(2)}, u32[]{:S(2)}) collective-permute-start(bf16[512,256]{1,0:T(8,128)(2,1)} %get-tuple-element.40.refs_0_), channel_id=1, source_target_pairs={{0,24},{4,100},{8,0},{12,108},{16,8},{20,116},{24,16},{28,124},{32... | collective-permute-start | bytes 786440 | tf_op jit(solution)/shard_map/ppermute | solution.py:418
  28.0 1.0 copy-start.1
  29.1 5.3 %collective-permute-start.3 = (bf16[2048,256]{1,0:T(8,128)(2,1)S(1)}, bf16[2048,256]{1,0:T(8,128)(2,1)S(1)}, u32[]{:S(2)}, u32[]{:S(2)}) collective-permute-start(bf16[2048,256]{1,0:T(8,128)(2,1)S(1)} %lines.1.refs_1_), channel_id=1, source_target_pairs={{0,4},{4,0},{8,12},{12,8},{16,20},{20,16},{24,28},{28,24},{32,36},... | collective-permute-start | bytes 3145736 | tf_op jit(solution)/shard_map/ppermute | solution.py:423
  29.1 19.2 %collective-permute-start.4 = (bf16[2048,256]{1,0:T(8,128)(2,1)S(1)}, bf16[2048,256]{1,0:T(8,128)(2,1)S(1)}, u32[]{:S(2)}, u32[]{:S(2)}) collective-permute-start(bf16[2048,256]{1,0:T(8,128)(2,1)S(1)} %lines.1.refs_1_), channel_id=1, source_target_pairs={{0,32},{4,12},{8,40},{12,20},{16,48},{20,28},{24,56},{28,4},{32,64... | collective-permute-start | bytes 3145736 | tf_op jit(solution)/shard_map/ppermute | solution.py:418
  31.4 17.6 %collective-permute-start.5 = (bf16[2048,256]{1,0:T(8,128)(2,1)S(1)}, bf16[2048,256]{1,0:T(8,128)(2,1)S(1)}, u32[]{:S(2)}, u32[]{:S(2)}) collective-permute-start(bf16[2048,256]{1,0:T(8,128)(2,1)S(1)} %lines.1.refs_1_), channel_id=1, source_target_pairs={{0,96},{4,28},{8,104},{12,4},{16,112},{20,12},{24,120},{28,20},{32... | collective-permute-start | bytes 3145736 | tf_op jit(solution)/shard_map/ppermute | solution.py:418
  34.4 1.0 copy-start.3
  49.0 6.8 %collective-permute-start.6 = (bf16[2048,256]{1,0:T(8,128)(2,1)S(1)}, bf16[2048,256]{1,0:T(8,128)(2,1)S(1)}, u32[]{:S(2)}, u32[]{:S(2)}) collective-permute-start(bf16[2048,256]{1,0:T(8,128)(2,1)S(1)} %collective-permute-done.4.refs_1_), channel_id=1, source_target_pairs={{0,4},{4,0},{8,12},{12,8},{16,20},{20,16},{24,28},{28,24},{32,36},... | collective-permute-start | bytes 3145736 | tf_op jit(solution)/shard_map/ppermute | solution.py:423
  49.0 15.3 %collective-permute-start.7 = (bf16[2048,256]{1,0:T(8,128)(2,1)S(1)}, bf16[2048,256]{1,0:T(8,128)(2,1)S(1)}, u32[]{:S(2)}, u32[]{:S(2)}) collective-permute-start(bf16[2048,256]{1,0:T(8,128)(2,1)S(1)} %collective-permute-done.5.refs_2_), channel_id=1, source_target_pairs={{0,4},{4,0},{8,12},{12,8},{16,20},{20,16},{24,28},{28,24},{32,36},... | collective-permute-start | bytes 3145736 | tf_op jit(solution)/shard_map/ppermute | solution.py:423
  49.5 27.8 %collective-permute-start.10 = (bf16[256,2048]{1,0:T(8,128)(2,1)}, bf16[256,2048]{1,0:T(8,128)(2,1)S(1)}, u32[]{:S(2)}, u32[]{:S(2)}) collective-permute-start(bf16[256,2048]{1,0:T(8,128)(2,1)} %get-tuple-element.57.refs_4_), channel_id=1, source_target_pairs={{0,2},{1,3},{2,0},{3,1},{4,6},{5,7},{6,4},{7,5},{8,10},{9,11},{10,... | collective-permute-start | bytes 3145736 | tf_op jit(solution)/shard_map/ppermute | solution.py:400
  52.5 46.2 %collective-permute-start.11 = (bf16[256,2048]{1,0:T(8,128)(2,1)}, bf16[256,2048]{1,0:T(8,128)(2,1)S(1)}, u32[]{:S(2)}, u32[]{:S(2)}) collective-permute-start(bf16[256,2048]{1,0:T(8,128)(2,1)} %get-tuple-element.57.refs_4_), channel_id=1, source_target_pairs={{0,1},{1,2},{2,3},{3,0},{4,5},{5,6},{6,7},{7,4},{8,9},{9,10},{10,1... | collective-permute-start | bytes 3145736 | tf_op jit(solution)/shard_map/ppermute | solution.py:400
  53.1 45.8 %collective-permute-start.9 = (bf16[256,2048]{1,0:T(8,128)(2,1)}, bf16[256,2048]{1,0:T(8,128)(2,1)S(1)}, u32[]{:S(2)}, u32[]{:S(2)}) collective-permute-start(bf16[256,2048]{1,0:T(8,128)(2,1)} %get-tuple-element.57.refs_4_), channel_id=1, source_target_pairs={{0,3},{1,0},{2,1},{3,2},{4,7},{5,4},{6,5},{7,6},{8,11},{9,8},{10,9... | collective-permute-start | bytes 3145736 | tf_op jit(solution)/shard_map/ppermute | solution.py:400
  55.7 43.1 %collective-permute-start.8 = (bf16[2048,256]{1,0:T(8,128)(2,1)S(1)}, bf16[2048,256]{1,0:T(8,128)(2,1)S(1)}, u32[]{:S(2)}, u32[]{:S(2)}) collective-permute-start(bf16[2048,256]{1,0:T(8,128)(2,1)S(1)} %lines.1.refs_1_), channel_id=1, source_target_pairs={{0,64},{4,20},{8,72},{12,28},{16,80},{20,4},{24,88},{28,12},{32,96... | collective-permute-start | bytes 3145736 | tf_op jit(solution)/shard_map/ppermute | solution.py:418
  77.3 49.3 %copy-start.4 = (bf16[256,2048]{1,0:T(8,128)(2,1)}, bf16[256,2048]{1,0:T(8,128)(2,1)S(1)}, u32[]{:S(2)}) copy-start(bf16[256,2048]{1,0:T(8,128)(2,1)S(1)} %collective-permute-done.10.refs_6_) | copy-start | bytes 3145732
  98.7 27.8 %copy-start.5 = (bf16[256,2048]{1,0:T(8,128)(2,1)}, bf16[256,2048]{1,0:T(8,128)(2,1)S(1)}, u32[]{:S(2)}) copy-start(bf16[256,2048]{1,0:T(8,128)(2,1)S(1)} %collective-permute-done.11.refs_7_) | copy-start | bytes 3145732
  98.9 27.7 %copy-start.6 = (bf16[256,2048]{1,0:T(8,128)(2,1)}, bf16[256,2048]{1,0:T(8,128)(2,1)S(1)}, u32[]{:S(2)}) copy-start(bf16[256,2048]{1,0:T(8,128)(2,1)S(1)} %collective-permute-done.9.refs_5_) | copy-start | bytes 3145732
  98.9 5.3 %collective-permute-start.12 = (bf16[2048,256]{1,0:T(8,128)(2,1)S(1)}, bf16[2048,256]{1,0:T(8,128)(2,1)S(1)}, u32[]{:S(2)}, u32[]{:S(2)}) collective-permute-start(bf16[2048,256]{1,0:T(8,128)(2,1)S(1)} %collective-permute-done.8.refs_1_), channel_id=1, source_target_pairs={{0,4},{4,0},{8,12},{12,8},{16,20},{20,16},{24,28},{28,24},{32,36},... | collective-permute-start | bytes 3145736 | tf_op jit(solution)/shard_map/ppermute | solution.py:423
  98.9 13.4 %collective-permute-start.16 = (bf16[256,2048]{1,0:T(8,128)(2,1)S(1)}, bf16[256,2048]{1,0:T(8,128)(2,1)S(1)}, u32[]{:S(2)}, u32[]{:S(2)}) collective-permute-start(bf16[256,2048]{1,0:T(8,128)(2,1)S(1)} %collective-permute-done.9.refs_5_), channel_id=1, source_target_pairs={{0,4},{4,0},{8,12},{12,8},{16,20},{20,16},{24,28},{28,24},{32,36},... | collective-permute-start | bytes 3145736 | tf_op jit(solution)/shard_map/ppermute | solution.py:423
  99.4 14.5 %collective-permute-start.17 = (bf16[256,2048]{1,0:T(8,128)(2,1)S(1)}, bf16[256,2048]{1,0:T(8,128)(2,1)}, u32[]{:S(2)}, u32[]{:S(2)}) collective-permute-start(bf16[256,2048]{1,0:T(8,128)(2,1)S(1)} %collective-permute-done.10.refs_6_), channel_id=1, source_target_pairs={{0,4},{4,0},{8,12},{12,8},{16,20},{20,16},{24,28},{28,24},{32,36},... | collective-permute-start | bytes 3145736 | tf_op jit(solution)/shard_map/ppermute | solution.py:423
  99.5 14.4 %collective-permute-start.18 = (bf16[256,2048]{1,0:T(8,128)(2,1)S(1)}, bf16[256,2048]{1,0:T(8,128)(2,1)}, u32[]{:S(2)}, u32[]{:S(2)}) collective-permute-start(bf16[256,2048]{1,0:T(8,128)(2,1)S(1)} %collective-permute-done.11.refs_7_), channel_id=1, source_target_pairs={{0,4},{4,0},{8,12},{12,8},{16,20},{20,16},{24,28},{28,24},{32,36},... | collective-permute-start | bytes 3145736 | tf_op jit(solution)/shard_map/ppermute | solution.py:423
  108.6 18.0 %copy-start.2 = (bf16[512,256]{1,0:T(8,128)(2,1)}, bf16[512,256]{1,0:T(8,128)(2,1)S(1)}, u32[]{:S(2)}) copy-start(bf16[512,256]{1,0:T(8,128)(2,1)S(1)} %shard_map.113.refs_0_) | copy-start | bytes 786436
  108.6 14.2 %collective-permute-start.13 = (bf16[512,256]{1,0:T(8,128)(2,1)S(1)}, bf16[512,256]{1,0:T(8,128)(2,1)}, u32[]{:S(2)}, u32[]{:S(2)}) collective-permute-start(bf16[512,256]{1,0:T(8,128)(2,1)S(1)} %shard_map.113.refs_0_), channel_id=1, source_target_pairs={{0,3},{1,0},{2,1},{3,2},{4,7},{5,4},{6,5},{7,6},{8,11},{9,8},{10,9... | collective-permute-start | bytes 786440 | tf_op jit(solution)/shard_map/ppermute | solution.py:400
  111.3 11.5 %collective-permute-start.14 = (bf16[512,256]{1,0:T(8,128)(2,1)S(1)}, bf16[512,256]{1,0:T(8,128)(2,1)}, u32[]{:S(2)}, u32[]{:S(2)}) collective-permute-start(bf16[512,256]{1,0:T(8,128)(2,1)S(1)} %shard_map.113.refs_0_), channel_id=1, source_target_pairs={{0,2},{1,3},{2,0},{3,1},{4,6},{5,7},{6,4},{7,5},{8,10},{9,11},{10,... | collective-permute-start | bytes 786440 | tf_op jit(solution)/shard_map/ppermute | solution.py:400
  112.3 1.0 copy-start.7
  113.3 13.3 %collective-permute-start.15 = (bf16[512,256]{1,0:T(8,128)(2,1)S(1)}, bf16[512,256]{1,0:T(8,128)(2,1)}, u32[]{:S(2)}, u32[]{:S(2)}) collective-permute-start(bf16[512,256]{1,0:T(8,128)(2,1)S(1)} %shard_map.113.refs_0_), channel_id=1, source_target_pairs={{0,1},{1,2},{2,3},{3,0},{4,5},{5,6},{6,7},{7,4},{8,9},{9,10},{10,1... | collective-permute-start | bytes 786440 | tf_op jit(solution)/shard_map/ppermute | solution.py:400
  135.6 1.6 copy-start
  137.2 44.9 %copy-start.8 = (bf16[128,2048]{1,0:T(8,128)(2,1)S(1)}, bf16[128,2048]{1,0:T(8,128)(2,1)}, u32[]{:S(2)}) copy-start(bf16[128,2048]{1,0:T(8,128)(2,1)} %get-tuple-element.62) | copy-start | bytes 1572868
  155.7 14.9 %collective-permute-start.21 = (bf16[128,2048]{1,0:T(8,128)(2,1)S(1)}, bf16[128,2048]{1,0:T(8,128)(2,1)S(1)}, u32[]{:S(2)}, u32[]{:S(2)}) collective-permute-start(bf16[128,2048]{1,0:T(8,128)(2,1)S(1)} %get-tuple-element.68), channel_id=1, source_target_pairs={{0,3},{1,0},{2,1},{3,2},{4,7},{5,4},{6,5},{7,6},{8,11},{9,8},{10,9... | collective-permute-start | bytes 1572872 | tf_op jit(solution)/shard_map/ppermute | solution.py:400
  156.4 25.8 %collective-permute-start.19 = (bf16[128,2048]{1,0:T(8,128)(2,1)S(1)}, bf16[128,2048]{1,0:T(8,128)(2,1)S(1)}, u32[]{:S(2)}, u32[]{:S(2)}) collective-permute-start(bf16[128,2048]{1,0:T(8,128)(2,1)S(1)} %get-tuple-element.66), channel_id=1, source_target_pairs={{0,1},{1,2},{2,3},{3,0},{4,5},{5,6},{6,7},{7,4},{8,9},{9,10},{10,1... | collective-permute-start | bytes 1572872 | tf_op jit(solution)/shard_map/ppermute | solution.py:400
  157.8 24.3 %collective-permute-start.20 = (bf16[128,2048]{1,0:T(8,128)(2,1)S(1)}, bf16[128,2048]{1,0:T(8,128)(2,1)S(1)}, u32[]{:S(2)}, u32[]{:S(2)}) collective-permute-start(bf16[128,2048]{1,0:T(8,128)(2,1)S(1)} %get-tuple-element.67), channel_id=1, source_target_pairs={{0,2},{1,3},{2,0},{3,1},{4,6},{5,7},{6,4},{7,5},{8,10},{9,11},{10,... | collective-permute-start | bytes 1572872 | tf_op jit(solution)/shard_map/ppermute | solution.py:400
Sparse Core Ops, SparseCore 0:
  9.6 88.0 all-gather.1

commit v9 on v7

--- a/solution.py
+++ b/solution.py
@@ -224,8 +224,8 @@
     sent = refs[parts : 2 * parts]
     swapped = refs[2 * parts : 3 * parts]
     gain_ref, w_hbm, own_ref = refs[3 * parts : 3 * parts + 3]
-    out_1, out_2, rest_ref = refs[3 * parts + 3 : -5]
-    x_ref, pair_ref, down_ref, h_ref, sems = refs[-5:]
+    out_1, out_2, rest_ref = refs[3 * parts + 3 : -6]
+    x_ref, att_ref, pair_ref, down_ref, h_ref, sems = refs[-6:]
     step = pl.program_id(0)
     half = sent[0].shape[0] - sub
     count = units // unit_tile
@@ -246,17 +246,18 @@
         for c in copies():
             c.start()
 
+    @pl.when(step == 0)
+    def _():
+        for m, a in enumerate(att):
+            for r in range(parts):
+                some = pl.ds(pl.multiple_of(((place[0] + r) % parts) * sub, sub), sub)
+                for k, c in enumerate((place[1], 1 - place[1])):
+                    head = a[some, pl.ds(pl.multiple_of(c * half, half), half)]
+                    att_ref[r * sub : (r + 1) * sub, (2 * m + k) * half : (2 * m + k + 1) * half] = head
+
     cols = pl.ds(pl.multiple_of(step * tile, tile), tile)
-    total = None
-    for a, w, o in zip(att, sent, swapped):
-        rolled = []
-        for r in range(parts):
-            some = pl.ds(pl.multiple_of(((place[0] + r) % parts) * sub, sub), sub)
-            halves = [a[some, pl.ds(pl.multiple_of(c * half, half), half)] for c in (place[1], 1 - place[1])]
-            rolled.append(jnp.concatenate(halves, axis=1))
-        weight = jnp.concatenate([w[0:half, :], o[0:half, :]], axis=0)
-        part = jnp.dot(jnp.concatenate(rolled, axis=0), weight, preferred_element_type=f32).astype(bf16).astype(f32)
-        total = part if total is None else total + part
+    weight = jnp.concatenate([v for w, o in zip(sent, swapped) for v in (w[0:half, :], o[0:half, :])], axis=0)
+    total = jnp.dot(att_ref[...], weight, preferred_element_type=f32)
     for r in range(parts):
         updated = (sent[r][half:, :].astype(f32) + total[r * sub : (r + 1) * sub, :]).astype(bf16)
         x_ref[r * sub : (r + 1) * sub, cols] = updated
@@ -343,6 +344,7 @@
             + [pl.BlockSpec((2 * sub, units), lambda i, p: (0, 0))],
             scratch_shapes=[
                 pltpu.VMEM((tok, width), bf16),
+                pltpu.VMEM((tok, parts * part_width), bf16),
                 pltpu.VMEM((count, width, 2 * unit_tile), bf16),
                 pltpu.VMEM((blocks, rows, units), bf16),
                 pltpu.VMEM((tok, units), bf16),
@@ -356,21 +358,17 @@
 
 
 def line_kernel(*refs):
-    pieces, (whole, *halves) = refs[:-3], refs[-3:]
-    rows = pieces[0].shape[0]
-    each = len(pieces) // 2
-    for n, piece in enumerate(pieces):
-        whole[n * rows : (n + 1) * rows, :] = piece[...]
-        halves[n // each][n % each * rows : (n % each + 1) * rows, :] = piece[...]
+    rows = refs[0].shape[0]
+    for n, piece in enumerate(refs[:-1]):
+        refs[-1][n * rows : (n + 1) * rows, :] = piece[...]
 
 
 def lined_up(*pieces):
     rows, width = pieces[0].shape
-    count = rows * len(pieces)
     return pl.pallas_call(
         line_kernel,
-        out_shape=[jax.ShapeDtypeStruct((n, width), bf16) for n in (count, count // 2, count // 2)],
-        compiler_params=pltpu.CompilerParams(vmem_limit_bytes=10 << 20),
+        out_shape=jax.ShapeDtypeStruct((rows * len(pieces), width), bf16),
+        compiler_params=pltpu.CompilerParams(vmem_limit_bytes=8 << 20),
         name="lines",
     )(*pieces)
 
@@ -421,22 +419,18 @@
     units = gate_weight.shape[1]
     core = lax.axis_index("sp") % 2
     place = jnp.stack([lax.axis_index("tp"), core])
-    woven = interleaved(gate_weight, up_weight, down_weight)
-    weights = lax.all_gather(woven, "sp", axis=0, tiled=True)
-    key_rows, woven = lax.optimization_barrier((key_rows, woven))
+    weights = lax.all_gather(interleaved(gate_weight, up_weight, down_weight), "sp", axis=0, tiled=True)
     q, kv, payload, kept = prepare(query_rows, key_rows, value_rows, query_gain, key_gain, out_weight, residual)
 
     steps = (2, 1, -1)
     line = [kv]
     for d in steps:
         line.append(crossed(kv, d, False))
-    line, *halves = lined_up(*line)
+    line = lined_up(*line)
     near = []
     for d in (1, -1):
         near.append(crossed(line, d, True))
-    far = []
-    for n in range(2):
-        far.append(crossed(halves[n], 2, True))
+    far = crossed(line, 2, True)
 
     sent = [payload]
     for r in range(1, parts):
@@ -447,15 +441,13 @@
     near_swapped = [other_core(v) for v in near]
     state = flash(q, near, state, tok, False)
     state = flash(q, near_swapped, state, tok, False)
-    state, far[0] = lax.optimization_barrier((state, far[0]))
-    far_swapped = [other_core(far[0])]
-    state = flash(q, [far[0], far_swapped[0]], state, tok, False)
-    state, far[1], sent = lax.optimization_barrier((state, far[1], sent))
-    far_swapped.append(other_core(far[1]))
+    state, far, sent = lax.optimization_barrier((state, far, sent))
+    far_swapped = other_core(far)
     swapped = [kept]
     for r in range(1, parts):
         swapped.append(other_core(sent[r]))
-    attended = flash(q, [far[1], far_swapped[1]], state, tok, True)
+    state = flash(q, [far], state, tok, False)
+    attended = flash(q, [far_swapped], state, tok, True)
 
     att_parts = [attended] + [shifted(attended, -r) for r in range(1, parts)]
     own_rows, part_1, part_2, hidden = layer(place, att_parts, sent, swapped, mix_gain, weights, units)

time: 185 us -> 189 us (1.022)
  waiting for transfers between devices: 74.5 us -> 79.8 us
  starting transfers between devices: 32.2 us -> 29.3 us
    ppermute x9, waiting for transfers between devices: 38.8 us -> 63.7 us  [shifted(): lax.ppermute(value, 'tp', [(i, (i + by) % count) for i in range(count)])]
    ppermute x7 -> x6, waiting for transfers between devices: 33.9 us -> 16.1 us  [crossed(): return lax.ppermute(value, 'sp', pairs)]
    ppermute x7 -> x6, starting transfers between devices: 9.62 us -> 8.4 us  [crossed(): return lax.ppermute(value, 'sp', pairs)]
    ppermute x8 -> x7, starting transfers between devices: 5.83 us -> 5.49 us  [other_core(): return lax.ppermute(value, 'sp', [(n, n ^ 1) for n in range(count)])]
  transfers between devices with their start and end apart: 25 -> 23, of which waited for: 16 -> 12; matrix products, arithmetic and copies ran while one was open for 1% -> 1% of each run, Pallas kernels for 18% -> 18%
where the time goes in v9:
time: 189 us; the launch traced here: 187 us
  waiting for transfers between devices  79.8 us (42%)
  Pallas kernels  59.3 us (31%)
  starting transfers between devices  29.3 us (16%)
  between operations  13.6 us (7%)
  local copies, waits for them, and re-layouts  2.92 us (2%)
  other arithmetic  2.47 us (1%)
    ppermute x9, waiting for transfers between devices, shifted(): lax.ppermute(value, 'tp', [(i, (i + by) % count) for i in range(count)])  63.7 us
    pallas_call x5, Pallas kernels, flash(): pl.pallas_call(functools.partial(flash_kernel, pieces=pieces, scale=head_...  28.8 us
    pallas_call x1, Pallas kernels, layer(): pl.pallas_call(functools.partial(layer_kernel, parts=parts, tile=tile, su...  19.7 us
    ppermute x6, waiting for transfers between devices, crossed(): return lax.ppermute(value, 'sp', pairs)  16.1 us
    ppermute x9, starting transfers between devices, shifted(): lax.ppermute(value, 'tp', [(i, (i + by) % count) for i in range(count)])  15.4 us
    ppermute x6, starting transfers between devices, crossed(): return lax.ppermute(value, 'sp', pairs)  8.4 us
    ppermute x7, starting transfers between devices, other_core(): return lax.ppermute(value, 'sp', [(n, n ^ 1) for n in range(count)])  5.49 us
    pallas_call x1, Pallas kernels, rest(): pl.pallas_call(rest_kernel, in_specs=[pl.BlockSpec(memory_space=pltpu.VME...  4.56 us
  transfers between devices with their start and end apart: 23, of which 12 were waited for; matrix products, arithmetic and copies ran while one was open for 1% of the time, Pallas kernels for 18%

profile of v9, /device:TPU:8, one launch (start us, length us, event | category | flops | bytes accessed | tf_op | source)
XLA Modules:
  0.0 187.4 jit_solution(10585240215428163384)
XLA Ops:
  6.5 2.0 %weave.1 = bf16[64,4224]{1,0:T(8,128)(2,1)} custom-call(bf16[64,1408]{1,0:T(8,128)(2,1)} %g_hbm.1, bf16[64,1408]{1,0:T(8,128)(2,1)} %u_hbm.1, bf16[64,1408]{1,0:T(8,128)(2,1)} %bitcast.7), custom_call_target="tpu_custom_call" | custom-call | tf_op jit(solution)/shard_map/weave/pallas_call | solution.py:112
  8.6 0.0 all-gather.2.cloned.1.call-update
  8.6 0.1 add_convert_fusion.1
  8.7 0.2 multiply_sine_fusion
  9.0 0.1 negate_select_fusion.1
  9.0 0.8 pad_maximum_fusion
  9.8 4.1 %prepare.1 = (bf16[1024,128]{1,0:T(8,128)(2,1)}, bf16[512,256]{1,0:T(8,128)(2,1)}, bf16[256,2048]{1,0:T(8,128)(2,1)}, bf16[128,2048]{1,0:T(8,128)(2,1)}) custom-call(s32[1]{0:T(128)} %bitcast.1.core, bf16[512,256]{1,0:T(8,128)(2,1)} %q_hbm.1, bf16[512,128]{1,0:T(8,128)(2,1)} %k_hbm.1, bf16[512,128]{1,0:T(8,128)(2,1)} %v_hbm.1, bf16[256,2048]{1,0:T(8,128)(2,1)} %w_hbm.1, ...), custom_call_target="tpu_custom_call" | custom-call | tf_op jit(solution)/shard_map/prepare/pallas_call | solution.py:131
  13.9 0.0 copy-start
  13.9 0.4 collective-permute-start.2
  14.4 1.7 collective-permute-start.1
  16.0 3.5 %collective-permute-start = (bf16[512,256]{1,0:T(8,128)(2,1)}, bf16[512,256]{1,0:T(8,128)(2,1)S(1)}, u32[]{:S(2)}, u32[]{:S(2)}) collective-permute-start(bf16[512,256]{1,0:T(8,128)(2,1)} %get-tuple-element.39.refs_0_), channel_id=1, source_target_pairs={{0,16},{4,68},{8,24},{12,76},{16,0},{20,84},{24,8},{28,92},{32,48}... | collective-permute-start | bytes 786440 | tf_op jit(solution)/shard_map/ppermute | solution.py:396
  19.5 1.0 collective-permute-done.2.refs_3_
  20.6 1.5 collective-permute-done.1.refs_2_
  22.1 3.2 %collective-permute-done.refs_1_ = bf16[512,256]{1,0:T(8,128)(2,1)S(1)} collective-permute-done((bf16[512,256]{1,0:T(8,128)(2,1)}, bf16[512,256]{1,0:T(8,128)(2,1)S(1)}, u32[]{:S(2)}, u32[]{:S(2)}) %collective-permute-start) | collective-permute-done | bytes 262176 | tf_op jit(solution)/shard_map/ppermute | solution.py:396
  25.3 0.9 copy-done.1
  26.2 0.1 lines.1.refs_1_
  26.3 3.9 %collective-permute-start.3 = (bf16[2048,256]{1,0:T(8,128)(2,1)S(1)}, bf16[2048,256]{1,0:T(8,128)(2,1)S(1)}, u32[]{:S(2)}, u32[]{:S(2)}) collective-permute-start(bf16[2048,256]{1,0:T(8,128)(2,1)S(1)} %lines.1.refs_1_), channel_id=1, source_target_pairs={{0,4},{4,0},{8,12},{12,8},{16,20},{20,16},{24,28},{28,24},{32,36},... | collective-permute-start | bytes 3145736 | tf_op jit(solution)/shard_map/ppermute | solution.py:401
  30.2 2.4 %collective-permute-start.5 = (bf16[2048,256]{1,0:T(8,128)(2,1)S(1)}, bf16[2048,256]{1,0:T(8,128)(2,1)S(1)}, u32[]{:S(2)}, u32[]{:S(2)}) collective-permute-start(bf16[2048,256]{1,0:T(8,128)(2,1)S(1)} %lines.1.refs_1_), channel_id=1, source_target_pairs={{0,96},{4,28},{8,104},{12,4},{16,112},{20,12},{24,120},{28,20},{32... | collective-permute-start | bytes 3145736 | tf_op jit(solution)/shard_map/ppermute | solution.py:396
  32.6 0.0 collective-permute-start.4
  32.6 0.0 collective-permute-done.3.refs_2_
  32.6 0.9 copy-done.3
  33.6 6.2 %shard_map.109 = (f32[1024,128]{1,0:T(8,128)S(1)}, f32[1024,256]{1,0:T(8,128)S(1)}) custom-call(bf16[1024,128]{1,0:T(8,128)(2,1)S(1)} %copy-done.3, bf16[2048,256]{1,0:T(8,128)(2,1)S(1)} %lines.1.refs_1_, bf16[2048,256]{1,0:T(8,128)(2,1)S(1)} %collective-permute-done.3.refs_2_), custom_call_target="tpu_custom_call" | custom-call | flops 2147483648 | bytes 2097152 | tf_op jit(solution)/shard_map/pallas_call | solution.py:205
  39.8 7.7 %collective-permute-done.5.refs_2_ = bf16[2048,256]{1,0:T(8,128)(2,1)S(1)} collective-permute-done((bf16[2048,256]{1,0:T(8,128)(2,1)S(1)}, bf16[2048,256]{1,0:T(8,128)(2,1)S(1)}, u32[]{:S(2)}, u32[]{:S(2)}) %collective-permute-start.5) | collective-permute-done | bytes 1048608 | tf_op jit(solution)/shard_map/ppermute | solution.py:396
  47.5 2.6 %collective-permute-done.4.refs_1_ = bf16[2048,256]{1,0:T(8,128)(2,1)S(1)} collective-permute-done((bf16[2048,256]{1,0:T(8,128)(2,1)S(1)}, bf16[2048,256]{1,0:T(8,128)(2,1)S(1)}, u32[]{:S(2)}, u32[]{:S(2)}) %collective-permute-start.4) | collective-permute-done | bytes 1048608 | tf_op jit(solution)/shard_map/ppermute | solution.py:396
  50.1 0.0 collective-permute-start.6
  50.1 0.5 collective-permute-start.7
  50.6 1.5 collective-permute-start.11
  52.1 2.7 %collective-permute-start.10 = (bf16[256,2048]{1,0:T(8,128)(2,1)}, bf16[256,2048]{1,0:T(8,128)(2,1)}, u32[]{:S(2)}, u32[]{:S(2)}) collective-permute-start(bf16[256,2048]{1,0:T(8,128)(2,1)} %get-tuple-element.56.refs_4_), channel_id=1, source_target_pairs={{0,2},{1,3},{2,0},{3,1},{4,6},{5,7},{6,4},{7,5},{8,10},{9,11},{10,... | collective-permute-start | bytes 3145736 | tf_op jit(solution)/shard_map/ppermute | solution.py:378
  54.8 1.5 collective-permute-start.9
  56.2 0.0 collective-permute-done.6.refs_1_
  56.2 0.4 collective-permute-start.8
  56.7 6.9 %shard_map.110 = (f32[1024,128]{1,0:T(8,128)S(1)}, f32[1024,256]{1,0:T(8,128)S(1)}) custom-call(bf16[1024,128]{1,0:T(8,128)(2,1)S(1)} %copy-done.3, bf16[2048,256]{1,0:T(8,128)(2,1)S(1)} %collective-permute-done.4.refs_1_, bf16[2048,256]{1,0:T(8,128)(2,1)S(1)} %collective-permute-done.5.refs_2_, f32[1024,128]{1,0:T(8,128)S(1)} %get-tuple-element.44.refs_3_, ...), custom_call_target="tpu_custom_call" | custom-call | flops 2147483648 | bytes 2097152 | tf_op jit(solution)/shard_map/pallas_call | solution.py:205
  63.6 0.0 collective-permute-done.7.refs_2_
  63.6 6.9 %shard_map.111 = (f32[1024,128]{1,0:T(8,128)S(1)}, f32[1024,256]{1,0:T(8,128)S(1)}) custom-call(bf16[1024,128]{1,0:T(8,128)(2,1)S(1)} %copy-done.3, bf16[2048,256]{1,0:T(8,128)(2,1)S(1)} %collective-permute-done.6.refs_1_, bf16[2048,256]{1,0:T(8,128)(2,1)S(1)} %collective-permute-done.7.refs_2_, f32[1024,128]{1,0:T(8,128)S(1)} %get-tuple-element.46.refs_3_, ...), custom_call_target="tpu_custom_call" | custom-call | flops 2147483648 | bytes 2097152 | tf_op jit(solution)/shard_map/pallas_call | solution.py:205
  70.6 6.6 %collective-permute-done.11.refs_7_ = bf16[256,2048]{1,0:T(8,128)(2,1)S(1)} collective-permute-done((bf16[256,2048]{1,0:T(8,128)(2,1)}, bf16[256,2048]{1,0:T(8,128)(2,1)S(1)}, u32[]{:S(2)}, u32[]{:S(2)}) %collective-permute-start.11) | collective-permute-done | bytes 1048608 | tf_op jit(solution)/shard_map/ppermute | solution.py:378
  77.2 23.4 %collective-permute-done.10.refs_6_ = bf16[256,2048]{1,0:T(8,128)(2,1)} collective-permute-done((bf16[256,2048]{1,0:T(8,128)(2,1)}, bf16[256,2048]{1,0:T(8,128)(2,1)}, u32[]{:S(2)}, u32[]{:S(2)}) %collective-permute-start.10) | collective-permute-done | bytes 1048608 | tf_op jit(solution)/shard_map/ppermute | solution.py:378
  100.6 0.0 collective-permute-done.9.refs_5_
  100.6 0.0 collective-permute-done.8.refs_1_
  100.6 0.1 collective-permute-start.12
  100.7 0.5 collective-permute-start.16
  101.2 0.1 collective-permute-start.17
  101.3 0.4 collective-permute-start.18
  101.7 4.3 %shard_map.112 = (f32[1024,128]{1,0:T(8,128)S(1)}, f32[1024,256]{1,0:T(8,128)S(1)}) custom-call(bf16[1024,128]{1,0:T(8,128)(2,1)S(1)} %copy-done.3, bf16[2048,256]{1,0:T(8,128)(2,1)S(1)} %collective-permute-done.8.refs_1_, f32[1024,128]{1,0:T(8,128)S(1)} %get-tuple-element.52.refs_2_, f32[1024,256]{1,0:T(8,128)S(1)} %get-tuple-element.53.refs_3_), custom_call_target="tpu_custom_call" | custom-call | flops 1073741824 | bytes 1048576 | tf_op jit(solution)/shard_map/pallas_call | solution.py:205
  106.0 0.0 collective-permute-done.12.refs_1_
  106.0 4.4 %shard_map.113.refs_0_ = bf16[512,256]{1,0:T(8,128)(2,1)S(1)} custom-call(bf16[1024,128]{1,0:T(8,128)(2,1)S(1)} %copy-done.3, bf16[2048,256]{1,0:T(8,128)(2,1)S(1)} %collective-permute-done.12.refs_1_, f32[1024,128]{1,0:T(8,128)S(1)} %get-tuple-element.54.refs_2_, f32[1024,256]{1,0:T(8,128)S(1)} %get-tuple-element.55.refs_3_), custom_call_target="tpu_custom_call" | custom-call | flops 1073741824 | bytes 1048576 | tf_op jit(solution)/shard_map/pallas_call | solution.py:205
  110.4 1.3 collective-permute-start.15
  111.7 2.4 %collective-permute-start.14 = (bf16[512,256]{1,0:T(8,128)(2,1)S(1)}, bf16[512,256]{1,0:T(8,128)(2,1)S(1)}, u32[]{:S(2)}, u32[]{:S(2)}) collective-permute-start(bf16[512,256]{1,0:T(8,128)(2,1)S(1)} %shard_map.113.refs_0_), channel_id=1, source_target_pairs={{0,2},{1,3},{2,0},{3,1},{4,6},{5,7},{6,4},{7,5},{8,10},{9,11},{10,... | collective-permute-start | bytes 786440 | tf_op jit(solution)/shard_map/ppermute | solution.py:378
  114.1 0.0 collective-permute-done.16.refs_9_
  114.1 1.0 copy-done.6
  115.1 1.5 collective-permute-start.13
  116.6 0.1 pad_add_fusion.place
  116.7 0.0 collective-permute-done.17.refs_10_
  116.7 0.0 collective-permute-done.18.refs_11_
  116.7 3.8 %collective-permute-done.15.refs_3_ = bf16[512,256]{1,0:T(8,128)(2,1)S(1)} collective-permute-done((bf16[512,256]{1,0:T(8,128)(2,1)S(1)}, bf16[512,256]{1,0:T(8,128)(2,1)S(1)}, u32[]{:S(2)}, u32[]{:S(2)}) %collective-permute-start.15) | collective-permute-done | bytes 262176 | tf_op jit(solution)/shard_map/ppermute | solution.py:378
  120.5 5.5 %collective-permute-done.14.refs_2_ = bf16[512,256]{1,0:T(8,128)(2,1)S(1)} collective-permute-done((bf16[512,256]{1,0:T(8,128)(2,1)S(1)}, bf16[512,256]{1,0:T(8,128)(2,1)S(1)}, u32[]{:S(2)}, u32[]{:S(2)}) %collective-permute-start.14) | collective-permute-done | bytes 262176 | tf_op jit(solution)/shard_map/ppermute | solution.py:378
  126.0 0.3 collective-permute-done.13.refs_1_
  126.3 19.7 %layer.1 = (bf16[128,2048]{1,0:T(8,128)(2,1)S(1)}, bf16[128,2048]{1,0:T(8,128)(2,1)S(1)}, bf16[128,2048]{1,0:T(8,128)(2,1)S(1)}, bf16[256,1408]{1,0:T(8,128)(2,1)S(1)}) custom-call(s32[2]{0:T(128)S(1)} %pad_add_fusion.place, bf16[512,256]{1,0:T(8,128)(2,1)S(1)} %shard_map.113.refs_0_, bf16[512,256]{1,0:T(8,128)(2,1)S(1)} %collective-permute-done.13.refs_1_, ...), custom_call_target="tpu_custom_call" | custom-call | tf_op jit(solution)/shard_map/layer/pallas_call | solution.py:334
  146.0 4.6 %rest.1 = (bf16[128,2048]{1,0:T(8,128)(2,1)S(1)}, bf16[128,2048]{1,0:T(8,128)(2,1)S(1)}) custom-call(bf16[256,1408]{1,0:T(8,128)(2,1)S(1)} %get-tuple-element.62.h_ref, bf16[2048,4224]{1,0:T(8,128)(2,1)} %all-gather.2.cloned.1.call-done.refs_13_.w_hbm), custom_call_target="tpu_custom_call" | custom-call | tf_op jit(solution)/shard_map/rest/pallas_call | solution.py:317
  150.6 2.7 %collective-permute-start.21 = (bf16[128,2048]{1,0:T(8,128)(2,1)S(1)}, bf16[128,2048]{1,0:T(8,128)(2,1)S(1)}, u32[]{:S(2)}, u32[]{:S(2)}) collective-permute-start(bf16[128,2048]{1,0:T(8,128)(2,1)S(1)} %get-tuple-element.66), channel_id=1, source_target_pairs={{0,3},{1,0},{2,1},{3,2},{4,7},{5,4},{6,5},{7,6},{8,11},{9,8},{10,9... | collective-permute-start | bytes 1572872 | tf_op jit(solution)/shard_map/ppermute | solution.py:378
  153.3 1.9 %collective-permute-start.20 = (bf16[128,2048]{1,0:T(8,128)(2,1)S(1)}, bf16[128,2048]{1,0:T(8,128)(2,1)S(1)}, u32[]{:S(2)}, u32[]{:S(2)}) collective-permute-start(bf16[128,2048]{1,0:T(8,128)(2,1)S(1)} %get-tuple-element.65), channel_id=1, source_target_pairs={{0,2},{1,3},{2,0},{3,1},{4,6},{5,7},{6,4},{7,5},{8,10},{9,11},{10,... | collective-permute-start | bytes 1572872 | tf_op jit(solution)/shard_map/ppermute | solution.py:378
  155.1 20.7 %collective-permute-done.21 = bf16[128,2048]{1,0:T(8,128)(2,1)S(1)} collective-permute-done((bf16[128,2048]{1,0:T(8,128)(2,1)S(1)}, bf16[128,2048]{1,0:T(8,128)(2,1)S(1)}, u32[]{:S(2)}, u32[]{:S(2)}) %collective-permute-start.21) | collective-permute-done | bytes 524320 | tf_op jit(solution)/shard_map/ppermute | solution.py:378
  175.9 3.4 %collective-permute-done.19 = bf16[128,2048]{1,0:T(8,128)(2,1)S(1)} collective-permute-done((bf16[128,2048]{1,0:T(8,128)(2,1)S(1)}, bf16[128,2048]{1,0:T(8,128)(2,1)S(1)}, u32[]{:S(2)}, u32[]{:S(2)}) %collective-permute-start.19) | collective-permute-done | bytes 524320 | tf_op jit(solution)/shard_map/ppermute | solution.py:378
  179.3 0.0 collective-permute-done.20
  179.3 1.2 add_convert_fusion
  (17 shorter events, 0.1 us)
Async XLA Ops:
  6.5 119.7 %all-gather.2.cloned.1.call-start = ((), (), s32[]{:S(2)}) async-start(), calls=%async_computation | async-start | bytes 17842176 | tf_op jit(solution)/shard_map/all_gather | solution.py:422
  9.8 116.4 %copy-start.2 = (f32[2048]{0:T(1024)S(1)}, f32[2048]{0:T(1024)}, u32[]{:S(2)}) copy-start(f32[2048]{0:T(1024)} %param.18) | copy-start | bytes 24580
  13.9 112.3 %copy-start = (bf16[128,2048]{1,0:T(8,128)(2,1)S(1)}, bf16[128,2048]{1,0:T(8,128)(2,1)}, u32[]{:S(2)}) copy-start(bf16[128,2048]{1,0:T(8,128)(2,1)} %get-tuple-element.60.refs_8_) | copy-start | bytes 1572868
  13.9 6.7 %collective-permute-start.2 = (bf16[512,256]{1,0:T(8,128)(2,1)}, bf16[512,256]{1,0:T(8,128)(2,1)S(1)}, u32[]{:S(2)}, u32[]{:S(2)}) collective-permute-start(bf16[512,256]{1,0:T(8,128)(2,1)} %get-tuple-element.39.refs_0_), channel_id=1, source_target_pairs={{0,24},{4,100},{8,0},{12,108},{16,8},{20,116},{24,16},{28,124},{32... | collective-permute-start | bytes 786440 | tf_op jit(solution)/shard_map/ppermute | solution.py:396
  14.4 7.7 %collective-permute-start.1 = (bf16[512,256]{1,0:T(8,128)(2,1)}, bf16[512,256]{1,0:T(8,128)(2,1)S(1)}, u32[]{:S(2)}, u32[]{:S(2)}) collective-permute-start(bf16[512,256]{1,0:T(8,128)(2,1)} %get-tuple-element.39.refs_0_), channel_id=1, source_target_pairs={{0,8},{4,36},{8,16},{12,44},{16,24},{20,52},{24,0},{28,60},{32,40}... | collective-permute-start | bytes 786440 | tf_op jit(solution)/shard_map/ppermute | solution.py:396
  16.0 9.3 %collective-permute-start = (bf16[512,256]{1,0:T(8,128)(2,1)}, bf16[512,256]{1,0:T(8,128)(2,1)S(1)}, u32[]{:S(2)}, u32[]{:S(2)}) collective-permute-start(bf16[512,256]{1,0:T(8,128)(2,1)} %get-tuple-element.39.refs_0_), channel_id=1, source_target_pairs={{0,16},{4,68},{8,24},{12,76},{16,0},{20,84},{24,8},{28,92},{32,48}... | collective-permute-start | bytes 786440 | tf_op jit(solution)/shard_map/ppermute | solution.py:396
  25.3 1.0 copy-start.1
  26.3 6.3 %collective-permute-start.3 = (bf16[2048,256]{1,0:T(8,128)(2,1)S(1)}, bf16[2048,256]{1,0:T(8,128)(2,1)S(1)}, u32[]{:S(2)}, u32[]{:S(2)}) collective-permute-start(bf16[2048,256]{1,0:T(8,128)(2,1)S(1)} %lines.1.refs_1_), channel_id=1, source_target_pairs={{0,4},{4,0},{8,12},{12,8},{16,20},{20,16},{24,28},{28,24},{32,36},... | collective-permute-start | bytes 3145736 | tf_op jit(solution)/shard_map/ppermute | solution.py:401
  30.2 17.3 %collective-permute-start.5 = (bf16[2048,256]{1,0:T(8,128)(2,1)S(1)}, bf16[2048,256]{1,0:T(8,128)(2,1)S(1)}, u32[]{:S(2)}, u32[]{:S(2)}) collective-permute-start(bf16[2048,256]{1,0:T(8,128)(2,1)S(1)} %lines.1.refs_1_), channel_id=1, source_target_pairs={{0,96},{4,28},{8,104},{12,4},{16,112},{20,12},{24,120},{28,20},{32... | collective-permute-start | bytes 3145736 | tf_op jit(solution)/shard_map/ppermute | solution.py:396
  32.6 17.5 %collective-permute-start.4 = (bf16[2048,256]{1,0:T(8,128)(2,1)S(1)}, bf16[2048,256]{1,0:T(8,128)(2,1)S(1)}, u32[]{:S(2)}, u32[]{:S(2)}) collective-permute-start(bf16[2048,256]{1,0:T(8,128)(2,1)S(1)} %lines.1.refs_1_), channel_id=1, source_target_pairs={{0,32},{4,12},{8,40},{12,20},{16,48},{20,28},{24,56},{28,4},{32,64... | collective-permute-start | bytes 3145736 | tf_op jit(solution)/shard_map/ppermute | solution.py:396
  32.6 1.0 copy-start.3
  50.1 6.1 %collective-permute-start.6 = (bf16[2048,256]{1,0:T(8,128)(2,1)S(1)}, bf16[2048,256]{1,0:T(8,128)(2,1)S(1)}, u32[]{:S(2)}, u32[]{:S(2)}) collective-permute-start(bf16[2048,256]{1,0:T(8,128)(2,1)S(1)} %collective-permute-done.4.refs_1_), channel_id=1, source_target_pairs={{0,4},{4,0},{8,12},{12,8},{16,20},{20,16},{24,28},{28,24},{32,36},... | collective-permute-start | bytes 3145736 | tf_op jit(solution)/shard_map/ppermute | solution.py:401
  50.1 13.5 %collective-permute-start.7 = (bf16[2048,256]{1,0:T(8,128)(2,1)S(1)}, bf16[2048,256]{1,0:T(8,128)(2,1)S(1)}, u32[]{:S(2)}, u32[]{:S(2)}) collective-permute-start(bf16[2048,256]{1,0:T(8,128)(2,1)S(1)} %collective-permute-done.5.refs_2_), channel_id=1, source_target_pairs={{0,4},{4,0},{8,12},{12,8},{16,20},{20,16},{24,28},{28,24},{32,36},... | collective-permute-start | bytes 3145736 | tf_op jit(solution)/shard_map/ppermute | solution.py:401
  50.6 26.5 %collective-permute-start.11 = (bf16[256,2048]{1,0:T(8,128)(2,1)}, bf16[256,2048]{1,0:T(8,128)(2,1)S(1)}, u32[]{:S(2)}, u32[]{:S(2)}) collective-permute-start(bf16[256,2048]{1,0:T(8,128)(2,1)} %get-tuple-element.56.refs_4_), channel_id=1, source_target_pairs={{0,1},{1,2},{2,3},{3,0},{4,5},{5,6},{6,7},{7,4},{8,9},{9,10},{10,1... | collective-permute-start | bytes 3145736 | tf_op jit(solution)/shard_map/ppermute | solution.py:378
  52.1 48.5 %collective-permute-start.10 = (bf16[256,2048]{1,0:T(8,128)(2,1)}, bf16[256,2048]{1,0:T(8,128)(2,1)}, u32[]{:S(2)}, u32[]{:S(2)}) collective-permute-start(bf16[256,2048]{1,0:T(8,128)(2,1)} %get-tuple-element.56.refs_4_), channel_id=1, source_target_pairs={{0,2},{1,3},{2,0},{3,1},{4,6},{5,7},{6,4},{7,5},{8,10},{9,11},{10,... | collective-permute-start | bytes 3145736 | tf_op jit(solution)/shard_map/ppermute | solution.py:378
  54.8 45.8 %collective-permute-start.9 = (bf16[256,2048]{1,0:T(8,128)(2,1)}, bf16[256,2048]{1,0:T(8,128)(2,1)S(1)}, u32[]{:S(2)}, u32[]{:S(2)}) collective-permute-start(bf16[256,2048]{1,0:T(8,128)(2,1)} %get-tuple-element.56.refs_4_), channel_id=1, source_target_pairs={{0,3},{1,0},{2,1},{3,2},{4,7},{5,4},{6,5},{7,6},{8,11},{9,8},{10,9... | collective-permute-start | bytes 3145736 | tf_op jit(solution)/shard_map/ppermute | solution.py:378
  56.2 44.4 %collective-permute-start.8 = (bf16[2048,256]{1,0:T(8,128)(2,1)S(1)}, bf16[2048,256]{1,0:T(8,128)(2,1)S(1)}, u32[]{:S(2)}, u32[]{:S(2)}) collective-permute-start(bf16[2048,256]{1,0:T(8,128)(2,1)S(1)} %lines.1.refs_1_), channel_id=1, source_target_pairs={{0,64},{4,20},{8,72},{12,28},{16,80},{20,4},{24,88},{28,12},{32,96... | collective-permute-start | bytes 3145736 | tf_op jit(solution)/shard_map/ppermute | solution.py:396
  77.2 49.1 %copy-start.4 = (bf16[256,2048]{1,0:T(8,128)(2,1)}, bf16[256,2048]{1,0:T(8,128)(2,1)S(1)}, u32[]{:S(2)}) copy-start(bf16[256,2048]{1,0:T(8,128)(2,1)S(1)} %collective-permute-done.11.refs_7_) | copy-start | bytes 3145732
  100.6 13.5 %copy-start.5 = (bf16[256,2048]{1,0:T(8,128)(2,1)}, bf16[256,2048]{1,0:T(8,128)(2,1)S(1)}, u32[]{:S(2)}) copy-start(bf16[256,2048]{1,0:T(8,128)(2,1)S(1)} %collective-permute-done.9.refs_5_) | copy-start | bytes 3145732
  100.6 5.4 %collective-permute-start.12 = (bf16[2048,256]{1,0:T(8,128)(2,1)S(1)}, bf16[2048,256]{1,0:T(8,128)(2,1)S(1)}, u32[]{:S(2)}, u32[]{:S(2)}) collective-permute-start(bf16[2048,256]{1,0:T(8,128)(2,1)S(1)} %collective-permute-done.8.refs_1_), channel_id=1, source_target_pairs={{0,4},{4,0},{8,12},{12,8},{16,20},{20,16},{24,28},{28,24},{32,36},... | collective-permute-start | bytes 3145736 | tf_op jit(solution)/shard_map/ppermute | solution.py:401
  100.7 13.4 %collective-permute-start.16 = (bf16[256,2048]{1,0:T(8,128)(2,1)S(1)}, bf16[256,2048]{1,0:T(8,128)(2,1)S(1)}, u32[]{:S(2)}, u32[]{:S(2)}) collective-permute-start(bf16[256,2048]{1,0:T(8,128)(2,1)S(1)} %collective-permute-done.9.refs_5_), channel_id=1, source_target_pairs={{0,4},{4,0},{8,12},{12,8},{16,20},{20,16},{24,28},{28,24},{32,36},... | collective-permute-start | bytes 3145736 | tf_op jit(solution)/shard_map/ppermute | solution.py:401
  101.2 15.5 %collective-permute-start.17 = (bf16[256,2048]{1,0:T(8,128)(2,1)}, bf16[256,2048]{1,0:T(8,128)(2,1)}, u32[]{:S(2)}, u32[]{:S(2)}) collective-permute-start(bf16[256,2048]{1,0:T(8,128)(2,1)} %collective-permute-done.10.refs_6_), channel_id=1, source_target_pairs={{0,4},{4,0},{8,12},{12,8},{16,20},{20,16},{24,28},{28,24},{32,36},... | collective-permute-start | bytes 3145736 | tf_op jit(solution)/shard_map/ppermute | solution.py:401
  101.3 15.4 %collective-permute-start.18 = (bf16[256,2048]{1,0:T(8,128)(2,1)S(1)}, bf16[256,2048]{1,0:T(8,128)(2,1)}, u32[]{:S(2)}, u32[]{:S(2)}) collective-permute-start(bf16[256,2048]{1,0:T(8,128)(2,1)S(1)} %collective-permute-done.11.refs_7_), channel_id=1, source_target_pairs={{0,4},{4,0},{8,12},{12,8},{16,20},{20,16},{24,28},{28,24},{32,36},... | collective-permute-start | bytes 3145736 | tf_op jit(solution)/shard_map/ppermute | solution.py:401
  110.4 10.1 %collective-permute-start.15 = (bf16[512,256]{1,0:T(8,128)(2,1)S(1)}, bf16[512,256]{1,0:T(8,128)(2,1)S(1)}, u32[]{:S(2)}, u32[]{:S(2)}) collective-permute-start(bf16[512,256]{1,0:T(8,128)(2,1)S(1)} %shard_map.113.refs_0_), channel_id=1, source_target_pairs={{0,1},{1,2},{2,3},{3,0},{4,5},{5,6},{6,7},{7,4},{8,9},{9,10},{10,1... | collective-permute-start | bytes 786440 | tf_op jit(solution)/shard_map/ppermute | solution.py:378
  111.7 14.3 %collective-permute-start.14 = (bf16[512,256]{1,0:T(8,128)(2,1)S(1)}, bf16[512,256]{1,0:T(8,128)(2,1)S(1)}, u32[]{:S(2)}, u32[]{:S(2)}) collective-permute-start(bf16[512,256]{1,0:T(8,128)(2,1)S(1)} %shard_map.113.refs_0_), channel_id=1, source_target_pairs={{0,2},{1,3},{2,0},{3,1},{4,6},{5,7},{6,4},{7,5},{8,10},{9,11},{10,... | collective-permute-start | bytes 786440 | tf_op jit(solution)/shard_map/ppermute | solution.py:378
  114.1 1.0 copy-start.6
  115.1 11.1 %collective-permute-start.13 = (bf16[512,256]{1,0:T(8,128)(2,1)S(1)}, bf16[512,256]{1,0:T(8,128)(2,1)S(1)}, u32[]{:S(2)}, u32[]{:S(2)}) collective-permute-start(bf16[512,256]{1,0:T(8,128)(2,1)S(1)} %shard_map.113.refs_0_), channel_id=1, source_target_pairs={{0,3},{1,0},{2,1},{3,2},{4,7},{5,4},{6,5},{7,6},{8,11},{9,8},{10,9... | collective-permute-start | bytes 786440 | tf_op jit(solution)/shard_map/ppermute | solution.py:378
  150.6 25.3 %collective-permute-start.21 = (bf16[128,2048]{1,0:T(8,128)(2,1)S(1)}, bf16[128,2048]{1,0:T(8,128)(2,1)S(1)}, u32[]{:S(2)}, u32[]{:S(2)}) collective-permute-start(bf16[128,2048]{1,0:T(8,128)(2,1)S(1)} %get-tuple-element.66), channel_id=1, source_target_pairs={{0,3},{1,0},{2,1},{3,2},{4,7},{5,4},{6,5},{7,6},{8,11},{9,8},{10,9... | collective-permute-start | bytes 1572872 | tf_op jit(solution)/shard_map/ppermute | solution.py:378
  153.3 26.0 %collective-permute-start.19 = (bf16[128,2048]{1,0:T(8,128)(2,1)S(1)}, bf16[128,2048]{1,0:T(8,128)(2,1)S(1)}, u32[]{:S(2)}, u32[]{:S(2)}) collective-permute-start(bf16[128,2048]{1,0:T(8,128)(2,1)S(1)} %get-tuple-element.64), channel_id=1, source_target_pairs={{0,1},{1,2},{2,3},{3,0},{4,5},{5,6},{6,7},{7,4},{8,9},{9,10},{10,1... | collective-permute-start | bytes 1572872 | tf_op jit(solution)/shard_map/ppermute | solution.py:378
  153.3 26.0 %collective-permute-start.20 = (bf16[128,2048]{1,0:T(8,128)(2,1)S(1)}, bf16[128,2048]{1,0:T(8,128)(2,1)S(1)}, u32[]{:S(2)}, u32[]{:S(2)}) collective-permute-start(bf16[128,2048]{1,0:T(8,128)(2,1)S(1)} %get-tuple-element.65), channel_id=1, source_target_pairs={{0,2},{1,3},{2,0},{3,1},{4,6},{5,7},{6,4},{7,5},{8,10},{9,11},{10,... | collective-permute-start | bytes 1572872 | tf_op jit(solution)/shard_map/ppermute | solution.py:378
Sparse Core Ops, SparseCore 0:
  9.6 89.8 all-gather.1

commit v10 on v9

--- a/solution.py
+++ b/solution.py
@@ -430,7 +430,6 @@
     near = []
     for d in (1, -1):
         near.append(crossed(line, d, True))
-    far = crossed(line, 2, True)
 
     sent = [payload]
     for r in range(1, parts):
@@ -438,18 +437,27 @@
 
     state = flash(q, [line, other_core(line)], None, tok, False)
     state, near = lax.optimization_barrier((state, near))
-    near_swapped = [other_core(v) for v in near]
+    middle = line.shape[0] // 2
+    far = []
+    for v, d in ((near[0][:middle], 1), (near[1][middle:], -1)):
+        far.append(crossed(v, d, True))
+    near_swapped = []
+    for n in range(2):
+        near_swapped.append(other_core(near[n]))
     state = flash(q, near, state, tok, False)
     state = flash(q, near_swapped, state, tok, False)
-    state, far, sent = lax.optimization_barrier((state, far, sent))
-    far_swapped = other_core(far)
+    state, far = lax.optimization_barrier((state, far))
+    far_swapped = [other_core(v) for v in far]
+    state = flash(q, far, state, tok, False)
+    attended = flash(q, far_swapped, state, tok, True)
+
+    att_parts = [attended]
+    for r in range(1, parts):
+        att_parts.append(shifted(attended, -r))
+    att_parts[0], sent = lax.optimization_barrier((attended, sent))
     swapped = [kept]
     for r in range(1, parts):
         swapped.append(other_core(sent[r]))
-    state = flash(q, [far], state, tok, False)
-    attended = flash(q, [far_swapped], state, tok, True)
-
-    att_parts = [attended] + [shifted(attended, -r) for r in range(1, parts)]
     own_rows, part_1, part_2, hidden = layer(place, att_parts, sent, swapped, mix_gain, weights, units)
     part_0, part_3 = rest(hidden, weights)
     unit_sum = part_0.astype(f32)

time: 189 us -> 183 us (0.968)
  waiting for transfers between devices: 79.8 us -> 70.3 us
  starting transfers between devices: 29.3 us -> 31.4 us
    ppermute x9, waiting for transfers between devices: 63.7 us -> 54.2 us  [shifted(): lax.ppermute(value, 'tp', [(i, (i + by) % count) for i in range(count)])]
    ppermute x6 -> x7, starting transfers between devices: 8.4 us -> 10.1 us  [crossed(): return lax.ppermute(value, 'sp', pairs)]
    ppermute x6 -> x7, waiting for transfers between devices: 16.1 us -> 16 us  [crossed(): return lax.ppermute(value, 'sp', pairs)]
    ppermute x7 -> x8, starting transfers between devices: 5.49 us -> 5.5 us  [other_core(): return lax.ppermute(value, 'sp', [(n, n ^ 1) for n in range(count)])]
  transfers between devices with their start and end apart: 23 -> 25, of which waited for: 12 -> 12; matrix products, arithmetic and copies ran while one was open for 1% -> 1% of each run, Pallas kernels for 18% -> 18%
where the time goes in v10:
time: 183 us; the launch traced here: 180 us
  waiting for transfers between devices  70.3 us (38%)
  Pallas kernels  59.3 us (32%)
  starting transfers between devices  31.4 us (17%)
  between operations  13.7 us (7%)
  local copies, waits for them, and re-layouts  3.02 us (2%)
  other arithmetic  2.49 us (1%)
    ppermute x9, waiting for transfers between devices, shifted(): lax.ppermute(value, 'tp', [(i, (i + by) % count) for i in range(count)])  54.2 us
    pallas_call x5, Pallas kernels, flash(): pl.pallas_call(functools.partial(flash_kernel, pieces=pieces, scale=head_...  28.8 us
    pallas_call x1, Pallas kernels, layer(): pl.pallas_call(functools.partial(layer_kernel, parts=parts, tile=tile, su...  19.7 us
    ppermute x7, waiting for transfers between devices, crossed(): return lax.ppermute(value, 'sp', pairs)  16 us
    ppermute x9, starting transfers between devices, shifted(): lax.ppermute(value, 'tp', [(i, (i + by) % count) for i in range(count)])  15.8 us
    ppermute x7, starting transfers between devices, crossed(): return lax.ppermute(value, 'sp', pairs)  10.1 us
    ppermute x8, starting transfers between devices, other_core(): return lax.ppermute(value, 'sp', [(n, n ^ 1) for n in range(count)])  5.5 us
    pallas_call x1, Pallas kernels, rest(): pl.pallas_call(rest_kernel, in_specs=[pl.BlockSpec(memory_space=pltpu.VME...  4.56 us
  transfers between devices with their start and end apart: 25, of which 12 were waited for; matrix products, arithmetic and copies ran while one was open for 1% of the time, Pallas kernels for 18%

profile of v10, /device:TPU:8, one launch (start us, length us, event | category | flops | bytes accessed | tf_op | source)
XLA Modules:
  0.0 180.2 jit_solution(9216482466856435200)
XLA Ops:
  6.5 2.0 %weave.1 = bf16[64,4224]{1,0:T(8,128)(2,1)} custom-call(bf16[64,1408]{1,0:T(8,128)(2,1)} %g_hbm.1, bf16[64,1408]{1,0:T(8,128)(2,1)} %u_hbm.1, bf16[64,1408]{1,0:T(8,128)(2,1)} %bitcast.7), custom_call_target="tpu_custom_call" | custom-call | tf_op jit(solution)/shard_map/weave/pallas_call | solution.py:112
  8.6 0.0 all-gather.2.cloned.1.call-update
  8.6 0.1 add_convert_fusion.1
  8.7 0.2 multiply_sine_fusion
  9.0 0.1 negate_select_fusion.1
  9.0 0.8 pad_maximum_fusion
  9.8 4.1 %prepare.1 = (bf16[1024,128]{1,0:T(8,128)(2,1)}, bf16[512,256]{1,0:T(8,128)(2,1)}, bf16[256,2048]{1,0:T(8,128)(2,1)}, bf16[128,2048]{1,0:T(8,128)(2,1)}) custom-call(s32[1]{0:T(128)} %bitcast.1.core, bf16[512,256]{1,0:T(8,128)(2,1)} %q_hbm.1, bf16[512,128]{1,0:T(8,128)(2,1)} %k_hbm.1, bf16[512,128]{1,0:T(8,128)(2,1)} %v_hbm.1, bf16[256,2048]{1,0:T(8,128)(2,1)} %w_hbm.1, ...), custom_call_target="tpu_custom_call" | custom-call | tf_op jit(solution)/shard_map/prepare/pallas_call | solution.py:131
  14.0 0.4 collective-permute-start.2
  14.4 1.7 collective-permute-start.1
  16.1 3.5 %collective-permute-start = (bf16[512,256]{1,0:T(8,128)(2,1)}, bf16[512,256]{1,0:T(8,128)(2,1)S(1)}, u32[]{:S(2)}, u32[]{:S(2)}) collective-permute-start(bf16[512,256]{1,0:T(8,128)(2,1)} %get-tuple-element.41.refs_0_), channel_id=1, source_target_pairs={{0,16},{4,68},{8,24},{12,76},{16,0},{20,84},{24,8},{28,92},{32,48}... | collective-permute-start | bytes 786440 | tf_op jit(solution)/shard_map/ppermute | solution.py:396
  19.6 1.0 collective-permute-done.2.refs_3_
  20.6 1.5 collective-permute-done.1.refs_2_
  22.1 3.2 %collective-permute-done.refs_1_ = bf16[512,256]{1,0:T(8,128)(2,1)S(1)} collective-permute-done((bf16[512,256]{1,0:T(8,128)(2,1)}, bf16[512,256]{1,0:T(8,128)(2,1)S(1)}, u32[]{:S(2)}, u32[]{:S(2)}) %collective-permute-start) | collective-permute-done | bytes 262176 | tf_op jit(solution)/shard_map/ppermute | solution.py:396
  25.3 1.0 copy-done.1
  26.3 0.1 lines.1.refs_1_
  26.3 0.0 copy-start
  26.4 0.0 copy-start.2
  26.4 3.9 %collective-permute-start.3 = (bf16[2048,256]{1,0:T(8,128)(2,1)S(1)}, bf16[2048,256]{1,0:T(8,128)(2,1)S(1)}, u32[]{:S(2)}, u32[]{:S(2)}) collective-permute-start(bf16[2048,256]{1,0:T(8,128)(2,1)S(1)} %lines.1.refs_1_), channel_id=1, source_target_pairs={{0,4},{4,0},{8,12},{12,8},{16,20},{20,16},{24,28},{28,24},{32,36},... | collective-permute-start | bytes 3145736 | tf_op jit(solution)/shard_map/ppermute | solution.py:401
  30.3 2.4 %collective-permute-start.5 = (bf16[2048,256]{1,0:T(8,128)(2,1)S(1)}, bf16[2048,256]{1,0:T(8,128)(2,1)S(1)}, u32[]{:S(2)}, u32[]{:S(2)}) collective-permute-start(bf16[2048,256]{1,0:T(8,128)(2,1)S(1)} %lines.1.refs_1_), channel_id=1, source_target_pairs={{0,96},{4,28},{8,104},{12,4},{16,112},{20,12},{24,120},{28,20},{32... | collective-permute-start | bytes 3145736 | tf_op jit(solution)/shard_map/ppermute | solution.py:396
  32.6 0.0 collective-permute-start.4
  32.7 0.0 collective-permute-done.3.refs_2_
  32.7 0.9 copy-done.3
  33.6 6.2 %shard_map.109 = (f32[1024,128]{1,0:T(8,128)S(1)}, f32[1024,256]{1,0:T(8,128)S(1)}) custom-call(bf16[1024,128]{1,0:T(8,128)(2,1)S(1)} %copy-done.3, bf16[2048,256]{1,0:T(8,128)(2,1)S(1)} %lines.1.refs_1_, bf16[2048,256]{1,0:T(8,128)(2,1)S(1)} %collective-permute-done.3.refs_2_), custom_call_target="tpu_custom_call" | custom-call | flops 2147483648 | bytes 2097152 | tf_op jit(solution)/shard_map/pallas_call | solution.py:205
  39.9 7.7 %collective-permute-done.5.refs_2_ = bf16[2048,256]{1,0:T(8,128)(2,1)S(1)} collective-permute-done((bf16[2048,256]{1,0:T(8,128)(2,1)S(1)}, bf16[2048,256]{1,0:T(8,128)(2,1)S(1)}, u32[]{:S(2)}, u32[]{:S(2)}) %collective-permute-start.5) | collective-permute-done | bytes 1048608 | tf_op jit(solution)/shard_map/ppermute | solution.py:396
  47.6 2.5 %collective-permute-done.4.refs_1_ = bf16[2048,256]{1,0:T(8,128)(2,1)S(1)} collective-permute-done((bf16[2048,256]{1,0:T(8,128)(2,1)S(1)}, bf16[2048,256]{1,0:T(8,128)(2,1)S(1)}, u32[]{:S(2)}, u32[]{:S(2)}) %collective-permute-start.4) | collective-permute-done | bytes 1048608 | tf_op jit(solution)/shard_map/ppermute | solution.py:396
  50.1 0.0 collective-permute-start.6
  50.1 0.5 collective-permute-start.7
  50.7 0.6 collective-permute-start.9
  51.3 1.5 collective-permute-start.8
  52.8 1.5 collective-permute-start.14
  54.3 0.0 collective-permute-done.6.refs_1_
  54.3 2.7 %collective-permute-start.13 = (bf16[256,2048]{1,0:T(8,128)(2,1)}, bf16[256,2048]{1,0:T(8,128)(2,1)}, u32[]{:S(2)}, u32[]{:S(2)}) collective-permute-start(bf16[256,2048]{1,0:T(8,128)(2,1)} %get-tuple-element.60.refs_4_), channel_id=1, source_target_pairs={{0,2},{1,3},{2,0},{3,1},{4,6},{5,7},{6,4},{7,5},{8,10},{9,11},{10,... | collective-permute-start | bytes 3145736 | tf_op jit(solution)/shard_map/ppermute | solution.py:378
  57.0 0.0 collective-permute-done.7.refs_2_
  57.0 1.5 collective-permute-start.12
  58.4 1.0 copy-done.4
  59.5 6.9 %shard_map.110 = (f32[1024,128]{1,0:T(8,128)S(1)}, f32[1024,256]{1,0:T(8,128)S(1)}) custom-call(bf16[1024,128]{1,0:T(8,128)(2,1)S(1)} %copy-done.4, bf16[2048,256]{1,0:T(8,128)(2,1)S(1)} %collective-permute-done.4.refs_1_, bf16[2048,256]{1,0:T(8,128)(2,1)S(1)} %collective-permute-done.5.refs_2_, f32[1024,128]{1,0:T(8,128)S(1)} %get-tuple-element.46.refs_3_, ...), custom_call_target="tpu_custom_call" | custom-call | flops 2147483648 | bytes 2097152 | tf_op jit(solution)/shard_map/pallas_call | solution.py:205
  66.4 6.9 %shard_map.111 = (f32[1024,128]{1,0:T(8,128)S(1)}, f32[1024,256]{1,0:T(8,128)S(1)}) custom-call(bf16[1024,128]{1,0:T(8,128)(2,1)S(1)} %copy-done.4, bf16[2048,256]{1,0:T(8,128)(2,1)S(1)} %collective-permute-done.6.refs_1_, bf16[2048,256]{1,0:T(8,128)(2,1)S(1)} %collective-permute-done.7.refs_2_, f32[1024,128]{1,0:T(8,128)S(1)} %get-tuple-element.48.refs_3_, ...), custom_call_target="tpu_custom_call" | custom-call | flops 2147483648 | bytes 2097152 | tf_op jit(solution)/shard_map/pallas_call | solution.py:205
  73.3 0.0 collective-permute-done.9.refs_2_
  73.3 0.1 collective-permute-start.10
  73.4 0.5 collective-permute-start.11
  73.9 4.2 %shard_map.112 = (f32[1024,128]{1,0:T(8,128)S(1)}, f32[1024,256]{1,0:T(8,128)S(1)}) custom-call(bf16[1024,128]{1,0:T(8,128)(2,1)S(1)} %copy-done.4, bf16[1024,256]{1,0:T(8,128)(2,1)S(1)} %collective-permute-done.8.refs_1_, bf16[1024,256]{1,0:T(8,128)(2,1)S(1)} %collective-permute-done.9.refs_2_, f32[1024,128]{1,0:T(8,128)S(1)} %get-tuple-element.54.refs_3_, ...), custom_call_target="tpu_custom_call" | custom-call | flops 1073741824 | bytes 1048576 | tf_op jit(solution)/shard_map/pallas_call | solution.py:205
  78.2 0.0 collective-permute-done.10.refs_1_
  78.2 4.4 %shard_map.113.refs_0_ = bf16[512,256]{1,0:T(8,128)(2,1)S(1)} custom-call(bf16[1024,128]{1,0:T(8,128)(2,1)S(1)} %copy-done.4, bf16[1024,256]{1,0:T(8,128)(2,1)S(1)} %collective-permute-done.10.refs_1_, bf16[1024,256]{1,0:T(8,128)(2,1)S(1)} %collective-permute-done.11.refs_2_, f32[1024,128]{1,0:T(8,128)S(1)} %get-tuple-element.56.refs_3_, ...), custom_call_target="tpu_custom_call" | custom-call | flops 1073741824 | bytes 1048576 | tf_op jit(solution)/shard_map/pallas_call | solution.py:205
  82.6 0.0 collective-permute-done.14.refs_7_
  82.7 19.7 %collective-permute-done.13.refs_6_ = bf16[256,2048]{1,0:T(8,128)(2,1)} collective-permute-done((bf16[256,2048]{1,0:T(8,128)(2,1)}, bf16[256,2048]{1,0:T(8,128)(2,1)}, u32[]{:S(2)}, u32[]{:S(2)}) %collective-permute-start.13) | collective-permute-done | bytes 1048608 | tf_op jit(solution)/shard_map/ppermute | solution.py:378
  102.3 0.1 collective-permute-done.12.refs_5_
  102.4 0.0 collective-permute-start.18
  102.4 0.5 collective-permute-start.19
  102.9 0.0 collective-permute-start.20
  102.9 1.7 collective-permute-start.17
  104.6 2.4 %collective-permute-start.16 = (bf16[512,256]{1,0:T(8,128)(2,1)S(1)}, bf16[512,256]{1,0:T(8,128)(2,1)S(1)}, u32[]{:S(2)}, u32[]{:S(2)}) collective-permute-start(bf16[512,256]{1,0:T(8,128)(2,1)S(1)} %shard_map.113.refs_0_), channel_id=1, source_target_pairs={{0,2},{1,3},{2,0},{3,1},{4,6},{5,7},{6,4},{7,5},{8,10},{9,11},{10,... | collective-permute-start | bytes 786440 | tf_op jit(solution)/shard_map/ppermute | solution.py:378
  107.0 5.8 %collective-permute-done.17.refs_3_ = bf16[512,256]{1,0:T(8,128)(2,1)S(1)} collective-permute-done((bf16[512,256]{1,0:T(8,128)(2,1)S(1)}, bf16[512,256]{1,0:T(8,128)(2,1)S(1)}, u32[]{:S(2)}, u32[]{:S(2)}) %collective-permute-start.17) | collective-permute-done | bytes 262176 | tf_op jit(solution)/shard_map/ppermute | solution.py:378
  112.9 1.9 %collective-permute-start.15 = (bf16[512,256]{1,0:T(8,128)(2,1)S(1)}, bf16[512,256]{1,0:T(8,128)(2,1)S(1)}, u32[]{:S(2)}, u32[]{:S(2)}) collective-permute-start(bf16[512,256]{1,0:T(8,128)(2,1)S(1)} %shard_map.113.refs_0_), channel_id=1, source_target_pairs={{0,3},{1,0},{2,1},{3,2},{4,7},{5,4},{6,5},{7,6},{8,11},{9,8},{10,9... | collective-permute-start | bytes 786440 | tf_op jit(solution)/shard_map/ppermute | solution.py:378
  114.7 0.1 pad_add_fusion.place
  114.8 4.5 %collective-permute-done.16.refs_2_ = bf16[512,256]{1,0:T(8,128)(2,1)S(1)} collective-permute-done((bf16[512,256]{1,0:T(8,128)(2,1)S(1)}, bf16[512,256]{1,0:T(8,128)(2,1)S(1)}, u32[]{:S(2)}, u32[]{:S(2)}) %collective-permute-start.16) | collective-permute-done | bytes 262176 | tf_op jit(solution)/shard_map/ppermute | solution.py:378
  119.3 1.4 collective-permute-done.15.refs_1_
  120.7 0.0 all-gather.2.cloned.1.call-done.refs_13_.w_hbm
  120.8 19.7 %layer.1 = (bf16[128,2048]{1,0:T(8,128)(2,1)S(1)}, bf16[128,2048]{1,0:T(8,128)(2,1)S(1)}, bf16[128,2048]{1,0:T(8,128)(2,1)S(1)}, bf16[256,1408]{1,0:T(8,128)(2,1)S(1)}) custom-call(s32[2]{0:T(128)S(1)} %pad_add_fusion.place, bf16[512,256]{1,0:T(8,128)(2,1)S(1)} %shard_map.113.refs_0_, bf16[512,256]{1,0:T(8,128)(2,1)S(1)} %collective-permute-done.15.refs_1_, ...), custom_call_target="tpu_custom_call" | custom-call | tf_op jit(solution)/shard_map/layer/pallas_call | solution.py:334
  140.5 4.6 %rest.1 = (bf16[128,2048]{1,0:T(8,128)(2,1)S(1)}, bf16[128,2048]{1,0:T(8,128)(2,1)S(1)}) custom-call(bf16[256,1408]{1,0:T(8,128)(2,1)S(1)} %get-tuple-element.66.h_ref, bf16[2048,4224]{1,0:T(8,128)(2,1)} %all-gather.2.cloned.1.call-done.refs_13_.w_hbm), custom_call_target="tpu_custom_call" | custom-call | tf_op jit(solution)/shard_map/rest/pallas_call | solution.py:317
  145.1 2.7 %collective-permute-start.23 = (bf16[128,2048]{1,0:T(8,128)(2,1)S(1)}, bf16[128,2048]{1,0:T(8,128)(2,1)S(1)}, u32[]{:S(2)}, u32[]{:S(2)}) collective-permute-start(bf16[128,2048]{1,0:T(8,128)(2,1)S(1)} %get-tuple-element.70), channel_id=1, source_target_pairs={{0,3},{1,0},{2,1},{3,2},{4,7},{5,4},{6,5},{7,6},{8,11},{9,8},{10,9... | collective-permute-start | bytes 1572872 | tf_op jit(solution)/shard_map/ppermute | solution.py:378
  147.8 1.5 collective-permute-start.22
  149.3 19.4 %collective-permute-done.23 = bf16[128,2048]{1,0:T(8,128)(2,1)S(1)} collective-permute-done((bf16[128,2048]{1,0:T(8,128)(2,1)S(1)}, bf16[128,2048]{1,0:T(8,128)(2,1)S(1)}, u32[]{:S(2)}, u32[]{:S(2)}) %collective-permute-start.23) | collective-permute-done | bytes 524320 | tf_op jit(solution)/shard_map/ppermute | solution.py:378
  168.7 3.4 %collective-permute-done.21 = bf16[128,2048]{1,0:T(8,128)(2,1)S(1)} collective-permute-done((bf16[128,2048]{1,0:T(8,128)(2,1)S(1)}, bf16[128,2048]{1,0:T(8,128)(2,1)S(1)}, u32[]{:S(2)}, u32[]{:S(2)}) %collective-permute-start.21) | collective-permute-done | bytes 524320 | tf_op jit(solution)/shard_map/ppermute | solution.py:378
  172.1 1.2 add_convert_fusion
  (21 shorter events, 0.1 us)
Async XLA Ops:
  6.5 114.2 %all-gather.2.cloned.1.call-start = ((), (), s32[]{:S(2)}) async-start(), calls=%async_computation | async-start | bytes 17842176 | tf_op jit(solution)/shard_map/all_gather | solution.py:422
  14.0 6.7 %collective-permute-start.2 = (bf16[512,256]{1,0:T(8,128)(2,1)}, bf16[512,256]{1,0:T(8,128)(2,1)S(1)}, u32[]{:S(2)}, u32[]{:S(2)}) collective-permute-start(bf16[512,256]{1,0:T(8,128)(2,1)} %get-tuple-element.41.refs_0_), channel_id=1, source_target_pairs={{0,24},{4,100},{8,0},{12,108},{16,8},{20,116},{24,16},{28,124},{32... | collective-permute-start | bytes 786440 | tf_op jit(solution)/shard_map/ppermute | solution.py:396
  14.4 7.7 %collective-permute-start.1 = (bf16[512,256]{1,0:T(8,128)(2,1)}, bf16[512,256]{1,0:T(8,128)(2,1)S(1)}, u32[]{:S(2)}, u32[]{:S(2)}) collective-permute-start(bf16[512,256]{1,0:T(8,128)(2,1)} %get-tuple-element.41.refs_0_), channel_id=1, source_target_pairs={{0,8},{4,36},{8,16},{12,44},{16,24},{20,52},{24,0},{28,60},{32,40}... | collective-permute-start | bytes 786440 | tf_op jit(solution)/shard_map/ppermute | solution.py:396
  16.1 9.3 %collective-permute-start = (bf16[512,256]{1,0:T(8,128)(2,1)}, bf16[512,256]{1,0:T(8,128)(2,1)S(1)}, u32[]{:S(2)}, u32[]{:S(2)}) collective-permute-start(bf16[512,256]{1,0:T(8,128)(2,1)} %get-tuple-element.41.refs_0_), channel_id=1, source_target_pairs={{0,16},{4,68},{8,24},{12,76},{16,0},{20,84},{24,8},{28,92},{32,48}... | collective-permute-start | bytes 786440 | tf_op jit(solution)/shard_map/ppermute | solution.py:396
  25.3 1.0 copy-start.1
  26.3 94.4 %copy-start = (bf16[128,2048]{1,0:T(8,128)(2,1)S(1)}, bf16[128,2048]{1,0:T(8,128)(2,1)}, u32[]{:S(2)}) copy-start(bf16[128,2048]{1,0:T(8,128)(2,1)} %get-tuple-element.64.refs_8_) | copy-start | bytes 1572868
  26.4 94.4 %copy-start.2 = (f32[2048]{0:T(1024)S(1)}, f32[2048]{0:T(1024)}, u32[]{:S(2)}) copy-start(f32[2048]{0:T(1024)} %param.18) | copy-start | bytes 24580
  26.4 6.3 %collective-permute-start.3 = (bf16[2048,256]{1,0:T(8,128)(2,1)S(1)}, bf16[2048,256]{1,0:T(8,128)(2,1)S(1)}, u32[]{:S(2)}, u32[]{:S(2)}) collective-permute-start(bf16[2048,256]{1,0:T(8,128)(2,1)S(1)} %lines.1.refs_1_), channel_id=1, source_target_pairs={{0,4},{4,0},{8,12},{12,8},{16,20},{20,16},{24,28},{28,24},{32,36},... | collective-permute-start | bytes 3145736 | tf_op jit(solution)/shard_map/ppermute | solution.py:401
  30.3 17.3 %collective-permute-start.5 = (bf16[2048,256]{1,0:T(8,128)(2,1)S(1)}, bf16[2048,256]{1,0:T(8,128)(2,1)S(1)}, u32[]{:S(2)}, u32[]{:S(2)}) collective-permute-start(bf16[2048,256]{1,0:T(8,128)(2,1)S(1)} %lines.1.refs_1_), channel_id=1, source_target_pairs={{0,96},{4,28},{8,104},{12,4},{16,112},{20,12},{24,120},{28,20},{32... | collective-permute-start | bytes 3145736 | tf_op jit(solution)/shard_map/ppermute | solution.py:396
  32.6 17.5 %collective-permute-start.4 = (bf16[2048,256]{1,0:T(8,128)(2,1)S(1)}, bf16[2048,256]{1,0:T(8,128)(2,1)S(1)}, u32[]{:S(2)}, u32[]{:S(2)}) collective-permute-start(bf16[2048,256]{1,0:T(8,128)(2,1)S(1)} %lines.1.refs_1_), channel_id=1, source_target_pairs={{0,32},{4,12},{8,40},{12,20},{16,48},{20,28},{24,56},{28,4},{32,64... | collective-permute-start | bytes 3145736 | tf_op jit(solution)/shard_map/ppermute | solution.py:396
  32.7 1.0 copy-start.3
  50.1 4.2 %collective-permute-start.6 = (bf16[2048,256]{1,0:T(8,128)(2,1)S(1)}, bf16[2048,256]{1,0:T(8,128)(2,1)S(1)}, u32[]{:S(2)}, u32[]{:S(2)}) collective-permute-start(bf16[2048,256]{1,0:T(8,128)(2,1)S(1)} %collective-permute-done.4.refs_1_), channel_id=1, source_target_pairs={{0,4},{4,0},{8,12},{12,8},{16,20},{20,16},{24,28},{28,24},{32,36},... | collective-permute-start | bytes 3145736 | tf_op jit(solution)/shard_map/ppermute | solution.py:401
  50.1 6.8 %collective-permute-start.7 = (bf16[2048,256]{1,0:T(8,128)(2,1)S(1)}, bf16[2048,256]{1,0:T(8,128)(2,1)S(1)}, u32[]{:S(2)}, u32[]{:S(2)}) collective-permute-start(bf16[2048,256]{1,0:T(8,128)(2,1)S(1)} %collective-permute-done.5.refs_2_), channel_id=1, source_target_pairs={{0,4},{4,0},{8,12},{12,8},{16,20},{20,16},{24,28},{28,24},{32,36},... | collective-permute-start | bytes 3145736 | tf_op jit(solution)/shard_map/ppermute | solution.py:401
  50.7 22.6 %collective-permute-start.9 = (bf16[1024,256]{1,0:T(8,128)(2,1)S(1)}, bf16[1024,256]{1,0:T(8,128)(2,1)S(1)}, u32[]{:S(2)}, u32[]{:S(2)}) collective-permute-start(bf16[1024,256]{1,0:T(8,128)(2,1)S(1)} %slice.7), channel_id=1, source_target_pairs={{0,96},{4,28},{8,104},{12,4},{16,112},{20,12},{24,120},{28,20},{32... | collective-permute-start | bytes 1572872 | tf_op jit(solution)/shard_map/ppermute | solution.py:396
  51.3 22.0 %collective-permute-start.8 = (bf16[1024,256]{1,0:T(8,128)(2,1)S(1)}, bf16[1024,256]{1,0:T(8,128)(2,1)S(1)}, u32[]{:S(2)}, u32[]{:S(2)}) collective-permute-start(bf16[1024,256]{1,0:T(8,128)(2,1)S(1)} %slice.6), channel_id=1, source_target_pairs={{0,32},{4,12},{8,40},{12,20},{16,48},{20,28},{24,56},{28,4},{32,64... | collective-permute-start | bytes 1572872 | tf_op jit(solution)/shard_map/ppermute | solution.py:396
  52.8 29.8 %collective-permute-start.14 = (bf16[256,2048]{1,0:T(8,128)(2,1)}, bf16[256,2048]{1,0:T(8,128)(2,1)S(1)}, u32[]{:S(2)}, u32[]{:S(2)}) collective-permute-start(bf16[256,2048]{1,0:T(8,128)(2,1)} %get-tuple-element.60.refs_4_), channel_id=1, source_target_pairs={{0,1},{1,2},{2,3},{3,0},{4,5},{5,6},{6,7},{7,4},{8,9},{9,10},{10,1... | collective-permute-start | bytes 3145736 | tf_op jit(solution)/shard_map/ppermute | solution.py:378
  54.3 48.1 %collective-permute-start.13 = (bf16[256,2048]{1,0:T(8,128)(2,1)}, bf16[256,2048]{1,0:T(8,128)(2,1)}, u32[]{:S(2)}, u32[]{:S(2)}) collective-permute-start(bf16[256,2048]{1,0:T(8,128)(2,1)} %get-tuple-element.60.refs_4_), channel_id=1, source_target_pairs={{0,2},{1,3},{2,0},{3,1},{4,6},{5,7},{6,4},{7,5},{8,10},{9,11},{10,... | collective-permute-start | bytes 3145736 | tf_op jit(solution)/shard_map/ppermute | solution.py:378
  57.0 45.4 %collective-permute-start.12 = (bf16[256,2048]{1,0:T(8,128)(2,1)}, bf16[256,2048]{1,0:T(8,128)(2,1)}, u32[]{:S(2)}, u32[]{:S(2)}) collective-permute-start(bf16[256,2048]{1,0:T(8,128)(2,1)} %get-tuple-element.60.refs_4_), channel_id=1, source_target_pairs={{0,3},{1,0},{2,1},{3,2},{4,7},{5,4},{6,5},{7,6},{8,11},{9,8},{10,9... | collective-permute-start | bytes 3145736 | tf_op jit(solution)/shard_map/ppermute | solution.py:378
  58.4 1.0 copy-start.4
  73.3 4.8 %collective-permute-start.10 = (bf16[1024,256]{1,0:T(8,128)(2,1)S(1)}, bf16[1024,256]{1,0:T(8,128)(2,1)S(1)}, u32[]{:S(2)}, u32[]{:S(2)}) collective-permute-start(bf16[1024,256]{1,0:T(8,128)(2,1)S(1)} %collective-permute-done.8.refs_1_), channel_id=1, source_target_pairs={{0,4},{4,0},{8,12},{12,8},{16,20},{20,16},{24,28},{28,24},{32,36},... | collective-permute-start | bytes 1572872 | tf_op jit(solution)/shard_map/ppermute | solution.py:401
  73.4 4.8 %collective-permute-start.11 = (bf16[1024,256]{1,0:T(8,128)(2,1)S(1)}, bf16[1024,256]{1,0:T(8,128)(2,1)S(1)}, u32[]{:S(2)}, u32[]{:S(2)}) collective-permute-start(bf16[1024,256]{1,0:T(8,128)(2,1)S(1)} %collective-permute-done.9.refs_2_), channel_id=1, source_target_pairs={{0,4},{4,0},{8,12},{12,8},{16,20},{20,16},{24,28},{28,24},{32,36},... | collective-permute-start | bytes 1572872 | tf_op jit(solution)/shard_map/ppermute | solution.py:401
  82.6 38.1 %copy-start.5 = (bf16[256,2048]{1,0:T(8,128)(2,1)}, bf16[256,2048]{1,0:T(8,128)(2,1)S(1)}, u32[]{:S(2)}) copy-start(bf16[256,2048]{1,0:T(8,128)(2,1)S(1)} %collective-permute-done.14.refs_7_) | copy-start | bytes 3145732
  102.4 18.3 %collective-permute-start.18 = (bf16[256,2048]{1,0:T(8,128)(2,1)}, bf16[256,2048]{1,0:T(8,128)(2,1)}, u32[]{:S(2)}, u32[]{:S(2)}) collective-permute-start(bf16[256,2048]{1,0:T(8,128)(2,1)} %collective-permute-done.12.refs_5_), channel_id=1, source_target_pairs={{0,4},{4,0},{8,12},{12,8},{16,20},{20,16},{24,28},{28,24},{32,36},... | collective-permute-start | bytes 3145736 | tf_op jit(solution)/shard_map/ppermute | solution.py:401
  102.4 18.3 %collective-permute-start.19 = (bf16[256,2048]{1,0:T(8,128)(2,1)}, bf16[256,2048]{1,0:T(8,128)(2,1)}, u32[]{:S(2)}, u32[]{:S(2)}) collective-permute-start(bf16[256,2048]{1,0:T(8,128)(2,1)} %collective-permute-done.13.refs_6_), channel_id=1, source_target_pairs={{0,4},{4,0},{8,12},{12,8},{16,20},{20,16},{24,28},{28,24},{32,36},... | collective-permute-start | bytes 3145736 | tf_op jit(solution)/shard_map/ppermute | solution.py:401
  102.9 17.8 %collective-permute-start.20 = (bf16[256,2048]{1,0:T(8,128)(2,1)S(1)}, bf16[256,2048]{1,0:T(8,128)(2,1)}, u32[]{:S(2)}, u32[]{:S(2)}) collective-permute-start(bf16[256,2048]{1,0:T(8,128)(2,1)S(1)} %collective-permute-done.14.refs_7_), channel_id=1, source_target_pairs={{0,4},{4,0},{8,12},{12,8},{16,20},{20,16},{24,28},{28,24},{32,36},... | collective-permute-start | bytes 3145736 | tf_op jit(solution)/shard_map/ppermute | solution.py:401
  102.9 9.9 %collective-permute-start.17 = (bf16[512,256]{1,0:T(8,128)(2,1)S(1)}, bf16[512,256]{1,0:T(8,128)(2,1)S(1)}, u32[]{:S(2)}, u32[]{:S(2)}) collective-permute-start(bf16[512,256]{1,0:T(8,128)(2,1)S(1)} %shard_map.113.refs_0_), channel_id=1, source_target_pairs={{0,1},{1,2},{2,3},{3,0},{4,5},{5,6},{6,7},{7,4},{8,9},{9,10},{10,1... | collective-permute-start | bytes 786440 | tf_op jit(solution)/shard_map/ppermute | solution.py:378
  104.6 14.7 %collective-permute-start.16 = (bf16[512,256]{1,0:T(8,128)(2,1)S(1)}, bf16[512,256]{1,0:T(8,128)(2,1)S(1)}, u32[]{:S(2)}, u32[]{:S(2)}) collective-permute-start(bf16[512,256]{1,0:T(8,128)(2,1)S(1)} %shard_map.113.refs_0_), channel_id=1, source_target_pairs={{0,2},{1,3},{2,0},{3,1},{4,6},{5,7},{6,4},{7,5},{8,10},{9,11},{10,... | collective-permute-start | bytes 786440 | tf_op jit(solution)/shard_map/ppermute | solution.py:378
  112.9 7.9 %collective-permute-start.15 = (bf16[512,256]{1,0:T(8,128)(2,1)S(1)}, bf16[512,256]{1,0:T(8,128)(2,1)S(1)}, u32[]{:S(2)}, u32[]{:S(2)}) collective-permute-start(bf16[512,256]{1,0:T(8,128)(2,1)S(1)} %shard_map.113.refs_0_), channel_id=1, source_target_pairs={{0,3},{1,0},{2,1},{3,2},{4,7},{5,4},{6,5},{7,6},{8,11},{9,8},{10,9... | collective-permute-start | bytes 786440 | tf_op jit(solution)/shard_map/ppermute | solution.py:378
  145.1 23.6 %collective-permute-start.23 = (bf16[128,2048]{1,0:T(8,128)(2,1)S(1)}, bf16[128,2048]{1,0:T(8,128)(2,1)S(1)}, u32[]{:S(2)}, u32[]{:S(2)}) collective-permute-start(bf16[128,2048]{1,0:T(8,128)(2,1)S(1)} %get-tuple-element.70), channel_id=1, source_target_pairs={{0,3},{1,0},{2,1},{3,2},{4,7},{5,4},{6,5},{7,6},{8,11},{9,8},{10,9... | collective-permute-start | bytes 1572872 | tf_op jit(solution)/shard_map/ppermute | solution.py:378
  147.8 24.3 %collective-permute-start.21 = (bf16[128,2048]{1,0:T(8,128)(2,1)S(1)}, bf16[128,2048]{1,0:T(8,128)(2,1)S(1)}, u32[]{:S(2)}, u32[]{:S(2)}) collective-permute-start(bf16[128,2048]{1,0:T(8,128)(2,1)S(1)} %get-tuple-element.68), channel_id=1, source_target_pairs={{0,1},{1,2},{2,3},{3,0},{4,5},{5,6},{6,7},{7,4},{8,9},{9,10},{10,1... | collective-permute-start | bytes 1572872 | tf_op jit(solution)/shard_map/ppermute | solution.py:378
  147.8 24.3 %collective-permute-start.22 = (bf16[128,2048]{1,0:T(8,128)(2,1)S(1)}, bf16[128,2048]{1,0:T(8,128)(2,1)S(1)}, u32[]{:S(2)}, u32[]{:S(2)}) collective-permute-start(bf16[128,2048]{1,0:T(8,128)(2,1)S(1)} %get-tuple-element.69), channel_id=1, source_target_pairs={{0,2},{1,3},{2,0},{3,1},{4,6},{5,7},{6,4},{7,5},{8,10},{9,11},{10,... | collective-permute-start | bytes 1572872 | tf_op jit(solution)/shard_map/ppermute | solution.py:378
Sparse Core Ops, SparseCore 0:
  9.6 84.1 all-gather.1

commit v11 on v10

--- a/solution.py
+++ b/solution.py
@@ -38,19 +38,82 @@
     return placed(cosine, cosine), placed(-sine, sine)
 
 
-def prepare_kernel(
-    core, q_hbm, k_hbm, v_hbm, w_hbm, r_hbm, qg_ref, kg_ref, cos_ref, sin_ref,
-    q_out, kv_out, sent, kept,
-    q_ref, k_ref, v_ref, w_ref, r_ref, sems, *, rows, head_dim, heads,
+def rotated(ref_x, gain_ref, cos_ref, sin_ref, rows, head_dim, columns):
+    tok = rows * GRID
+
+    def spread(ref):
+        both = ref[0:rows, :][:, None, :] + ref[rows : rows + GRID, :][None, :, :]
+        return both.reshape(tok, head_dim)
+
+    cosine = spread(cos_ref)
+    sine = spread(sin_ref)
+    lane = lax.broadcasted_iota(jnp.int32, (tok, head_dim), 1)
+    first = (lane % (head_dim // 2)) < head_dim // 4
+    quarter = head_dim // 4
+    found = []
+    for part in columns:
+        x = ref_x[:, part].astype(f32)
+        x = x * lax.rsqrt(jnp.mean(x * x, axis=-1, keepdims=True) + norm_eps) * gain_ref[...]
+        partner = jnp.where(first, pltpu.roll(x, head_dim - quarter, 1), pltpu.roll(x, quarter, 1))
+        found.append((x * cosine + partner * sine).astype(bf16))
+    return found
+
+
+def keys_kernel(k_hbm, v_hbm, gain_ref, cos_ref, sin_ref, kv_out, k_ref, v_ref, sems, *, rows, head_dim):
+    copies = [
+        pltpu.make_async_copy(x, y, sems.at[n]) for n, (x, y) in enumerate(((k_hbm, k_ref), (v_hbm, v_ref)))
+    ]
+    for c in copies:
+        c.start()
+    for c in copies:
+        c.wait()
+    kv_out[:, 0:head_dim] = rotated(k_ref, gain_ref, cos_ref, sin_ref, rows, head_dim, [slice(0, head_dim)])[0]
+    kv_out[:, head_dim:] = v_ref[...]
+
+
+def prepare_keys(key_rows, value_rows, gain, cosine, sine):
+    tok, head_dim = key_rows.shape
+    hbm = pl.BlockSpec(memory_space=pltpu.HBM)
+    vmem = pl.BlockSpec(memory_space=pltpu.VMEM)
+    return pl.pallas_call(
+        functools.partial(keys_kernel, rows=tok // GRID, head_dim=head_dim),
+        in_specs=[hbm] * 2 + [vmem] * 3,
+        out_shape=jax.ShapeDtypeStruct((tok, 2 * head_dim), bf16),
+        scratch_shapes=[pltpu.VMEM((tok, head_dim), bf16)] * 2 + [pltpu.SemaphoreType.DMA((2,))],
+        compiler_params=pltpu.CompilerParams(vmem_limit_bytes=60 * 1024 * 1024),
+        name="keys",
+    )(key_rows, value_rows, gain[None, :], cosine, sine)
+
+
+def queries_kernel(q_ref, gain_ref, cos_ref, sin_ref, q_out, *, rows, head_dim, heads):
+    tok = rows * GRID
+    columns = [slice(h * head_dim, (h + 1) * head_dim) for h in range(heads)]
+    for h, x in enumerate(rotated(q_ref, gain_ref, cos_ref, sin_ref, rows, head_dim, columns)):
+        q_out[h * tok : (h + 1) * tok, :] = x
+
+
+def prepare_queries(query_rows, gain, cosine, sine):
+    tok, width = query_rows.shape
+    head_dim = gain.shape[0]
+    heads = width // head_dim
+    return pl.pallas_call(
+        functools.partial(queries_kernel, rows=tok // GRID, head_dim=head_dim, heads=heads),
+        out_shape=jax.ShapeDtypeStruct((tok * heads, head_dim), bf16),
+        compiler_params=pltpu.CompilerParams(vmem_limit_bytes=8 << 20),
+        name="queries",
+    )(query_rows, gain[None, :], cosine, sine)
+
+
+def weave_kernel(
+    core, g_hbm, u_hbm, d_hbm, w_hbm, r_hbm, woven, sent, kept, g_ref, u_ref, d_ref, w_ref, r_ref, sems, *, tile
 ):
-    tok = rows * GRID
     half = kept.shape[0]
     first_half = pl.ds(pl.multiple_of(core[0] * half, half), half)
     other_half = pl.ds(pl.multiple_of((1 - core[0]) * half, half), half)
     moves = [
-        (k_hbm, k_ref),
-        (v_hbm, v_ref),
-        (q_hbm, q_ref),
+        (g_hbm, g_ref),
+        (u_hbm, u_ref),
+        (d_hbm, d_ref),
         (w_hbm.at[first_half, :], w_ref.at[pl.ds(0, half), :]),
         (w_hbm.at[other_half, :], w_ref.at[pl.ds(half, half), :]),
         (r_hbm, r_ref),
@@ -61,43 +124,7 @@
     copies = [pltpu.make_async_copy(x, y, sems.at[n]) for n, (x, y) in enumerate(moves)]
     for c in copies[:6]:
         c.start()
-
-    def spread(ref):
-        both = ref[0:rows, :][:, None, :] + ref[rows : rows + GRID, :][None, :, :]
-        return both.reshape(tok, head_dim)
-
-    cosine = spread(cos_ref)
-    sine = spread(sin_ref)
-    lane = lax.broadcasted_iota(jnp.int32, (tok, head_dim), 1)
-    first = (lane % (head_dim // 2)) < head_dim // 4
-    quarter = head_dim // 4
-
-    def prepared(raw, gain):
-        x = raw.astype(f32)
-        x = x * lax.rsqrt(jnp.mean(x * x, axis=-1, keepdims=True) + norm_eps) * gain
-        partner = jnp.where(first, pltpu.roll(x, head_dim - quarter, 1), pltpu.roll(x, quarter, 1))
-        return (x * cosine + partner * sine).astype(bf16)
-
-    copies[0].wait()
-    copies[1].wait()
-    kv_out[:, 0:head_dim] = prepared(k_ref[...], kg_ref[...])
-    kv_out[:, head_dim:] = v_ref[...]
-    for n in (3, 4, 5):
-        copies[n].wait()
-        copies[n + 3].start()
-    copies[2].wait()
-    for h in range(heads):
-        q_out[h * tok : (h + 1) * tok, :] = prepared(q_ref[:, h * head_dim : (h + 1) * head_dim], qg_ref[...])
-    for n in (6, 7, 8):
-        copies[n].wait()
-
-
-def weave_kernel(g_hbm, u_hbm, d_hbm, woven, g_ref, u_ref, d_ref, sems, *, tile):
-    moves = ((g_hbm, g_ref), (u_hbm, u_ref), (d_hbm, d_ref))
-    copies = [pltpu.make_async_copy(x, y, sems.at[n]) for n, (x, y) in enumerate(moves)]
-    for c in copies:
-        c.start()
-    for c in copies:
+    for c in copies[:3]:
         c.wait()
     units = g_ref.shape[1]
     for n in range(units // tile):
@@ -105,45 +132,31 @@
         woven[:, 2 * n * tile : (2 * n + 1) * tile] = g_ref[:, part]
         woven[:, (2 * n + 1) * tile : (2 * n + 2) * tile] = u_ref[:, part]
     woven[:, 2 * units :] = d_ref[...]
-
-
-def interleaved(gate, up, down, tile=128):
-    big = (gate, up, down.T)
+    for n in (3, 4, 5):
+        copies[n].wait()
+        copies[n + 3].start()
+    for n in (6, 7, 8):
+        copies[n].wait()
+
+
+def weave(core, gate, up, down, out_weight, residual, tile=128):
+    big = (gate, up, down.T, out_weight, residual)
+    half = out_weight.shape[0] // 2
+    width = residual.shape[1]
+    hbm = pl.BlockSpec(memory_space=pltpu.HBM)
     return pl.pallas_call(
         functools.partial(weave_kernel, tile=tile),
-        in_specs=[pl.BlockSpec(memory_space=pltpu.HBM)] * 3,
-        out_shape=jax.ShapeDtypeStruct((gate.shape[0], 3 * gate.shape[1]), bf16),
-        scratch_shapes=[pltpu.VMEM(x.shape, bf16) for x in big] + [pltpu.SemaphoreType.DMA((3,))],
+        in_specs=[pl.BlockSpec(memory_space=pltpu.SMEM)] + [hbm] * 5,
+        out_specs=[pl.BlockSpec(memory_space=pltpu.VMEM), hbm, hbm],
+        out_shape=[
+            jax.ShapeDtypeStruct((gate.shape[0], 3 * gate.shape[1]), bf16),
+            jax.ShapeDtypeStruct((half + residual.shape[0], width), bf16),
+            jax.ShapeDtypeStruct((half, width), bf16),
+        ],
+        scratch_shapes=[pltpu.VMEM(x.shape, bf16) for x in big] + [pltpu.SemaphoreType.DMA((9,))],
         compiler_params=pltpu.CompilerParams(vmem_limit_bytes=60 * 1024 * 1024),
         name="weave",
-    )(*big)
-
-
-def prepare(query_rows, key_rows, value_rows, query_gain, key_gain, out_weight, residual):
-    tok, width = query_rows.shape
-    head_dim = query_gain.shape[0]
-    rows = tok // GRID
-    cosine, sine = angle_tables(lax.axis_index("sp") * rows, rows, head_dim)
-    hbm = pl.BlockSpec(memory_space=pltpu.HBM)
-    vmem = pl.BlockSpec(memory_space=pltpu.VMEM)
-    big = (query_rows, key_rows, value_rows, out_weight, residual)
-    half = out_weight.shape[0] // 2
-    return pl.pallas_call(
-        functools.partial(prepare_kernel, rows=rows, head_dim=head_dim, heads=width // head_dim),
-        in_specs=[pl.BlockSpec(memory_space=pltpu.SMEM)] + [hbm] * 5 + [vmem] * 4,
-        out_specs=[vmem] * 2 + [hbm] * 2,
-        out_shape=(
-            jax.ShapeDtypeStruct((tok * (width // head_dim), head_dim), bf16),
-            jax.ShapeDtypeStruct((tok, 2 * head_dim), bf16),
-            jax.ShapeDtypeStruct((half + residual.shape[0], residual.shape[1]), bf16),
-            jax.ShapeDtypeStruct((half, residual.shape[1]), bf16),
-        ),
-        scratch_shapes=[pltpu.VMEM(x.shape, bf16) for x in big] + [pltpu.SemaphoreType.DMA((9,))],
-        compiler_params=pltpu.CompilerParams(vmem_limit_bytes=60 * 1024 * 1024),
-        name="prepare",
-    )(
-        (lax.axis_index("sp") % 2)[None], *big, query_gain[None, :], key_gain[None, :], cosine, sine
-    )
+    )(core[None], *big)
 
 
 def flash_kernel(*refs, pieces, scale, first, last, block=1024):
@@ -241,9 +254,16 @@
             found.append(pltpu.make_async_copy(source, down_ref.at[n], sems.at[count + n]))
         return found
 
+    early = count * 2 // 3
+
     @pl.when(step == 0)
     def _():
-        for c in copies():
+        for c in copies()[:early]:
+            c.start()
+
+    @pl.when(step == 1)
+    def _():
+        for c in copies()[early:]:
             c.start()
 
     @pl.when(step == 0)
@@ -270,20 +290,21 @@
             x = x_ref[some, :].astype(f32)
             x = x * lax.rsqrt(jnp.mean(x * x, axis=-1, keepdims=True) + norm_eps)
             x_ref[some, :] = (x * gain_ref[...]).astype(bf16)
-        for c in copies():
-            c.wait()
 
         def product(n):
             return jnp.dot(x_ref[...], pair_ref[n], preferred_element_type=f32)
 
-        following = product(0)
-        for n in range(count):
-            r = following
-            if n + 1 < count:
-                following = product(n + 1)
-            gate = r[:, 0:unit_tile]
-            hidden = gate / (1.0 + jnp.exp(-gate)) * r[:, unit_tile:]
-            h_ref[:, n * unit_tile : (n + 1) * unit_tile] = hidden.astype(bf16)
+        for begin, end, arrived in ((0, early, copies()[:early]), (early, count, copies()[early:])):
+            for c in arrived:
+                c.wait()
+            following = product(begin)
+            for n in range(begin, end):
+                r = following
+                if n + 1 < end:
+                    following = product(n + 1)
+                gate = r[:, 0:unit_tile]
+                hidden = gate / (1.0 + jnp.exp(-gate)) * r[:, unit_tile:]
+                h_ref[:, n * unit_tile : (n + 1) * unit_tile] = hidden.astype(bf16)
         rest_ref[0:sub, :] = h_ref[0:sub, :]
         rest_ref[sub:, :] = h_ref[3 * sub :, :]
         down_products(h_ref[sub : 3 * sub, :], down_ref, (out_1, out_2))
@@ -419,8 +440,12 @@
     units = gate_weight.shape[1]
     core = lax.axis_index("sp") % 2
     place = jnp.stack([lax.axis_index("tp"), core])
-    weights = lax.all_gather(interleaved(gate_weight, up_weight, down_weight), "sp", axis=0, tiled=True)
-    q, kv, payload, kept = prepare(query_rows, key_rows, value_rows, query_gain, key_gain, out_weight, residual)
+    rows = tok // GRID
+    tables = angle_tables(lax.axis_index("sp") * rows, rows, query_gain.shape[0])
+    kv = prepare_keys(key_rows, value_rows, key_gain, *tables)
+    woven, payload, kept = weave(core, gate_weight, up_weight, down_weight, out_weight, residual)
+    weights = lax.all_gather(woven, "sp", axis=0, tiled=True)
+    q = prepare_queries(query_rows, query_gain, *tables)
 
     steps = (2, 1, -1)
     line = [kv]

time: 183 us -> 182 us (level)
    ppermute x7, waiting for transfers between devices: 16 us -> 14.1 us  [crossed(): return lax.ppermute(value, 'sp', pairs)]
    unnamed x12 -> x16, local copies, waits for them, and re-layouts: 2.95 us -> 4.11 us
    pallas_call x2 -> x3, Pallas kernels: 6.14 us -> 6.66 us  [the longest x1 3.36 us: weave(): pl.pallas_call(functools.partial(weave_kernel, tile=tile), in_specs=[pl.B...]
  transfers between devices with their start and end apart: 25 -> 25, of which waited for: 12 -> 13; matrix products, arithmetic and copies ran while one was open for 1% -> 1% of each run, Pallas kernels for 18% -> 18%
where the time goes in v11:
time: 182 us; the launch traced here: 180 us
  waiting for transfers between devices  68.9 us (38%)
  Pallas kernels  59.9 us (33%)
  starting transfers between devices  31.3 us (17%)
  between operations  13.6 us (7%)
  local copies, waits for them, and re-layouts  4.19 us (2%)
  other arithmetic  2.47 us (1%)
    ppermute x9, waiting for transfers between devices, shifted(): lax.ppermute(value, 'tp', [(i, (i + by) % count) for i in range(count)])  54.8 us
    pallas_call x5, Pallas kernels, flash(): pl.pallas_call(functools.partial(flash_kernel, pieces=pieces, scale=head_...  28.8 us
    pallas_call x1, Pallas kernels, layer(): pl.pallas_call(functools.partial(layer_kernel, parts=parts, tile=tile, su...  19.9 us
    ppermute x9, starting transfers between devices, shifted(): lax.ppermute(value, 'tp', [(i, (i + by) % count) for i in range(count)])  15.8 us
    ppermute x7, waiting for transfers between devices, crossed(): return lax.ppermute(value, 'sp', pairs)  14.1 us
    ppermute x7, starting transfers between devices, crossed(): return lax.ppermute(value, 'sp', pairs)  10.2 us
    ppermute x8, starting transfers between devices, other_core(): return lax.ppermute(value, 'sp', [(n, n ^ 1) for n in range(count)])  5.27 us
    pallas_call x1, Pallas kernels, rest(): pl.pallas_call(rest_kernel, in_specs=[pl.BlockSpec(memory_space=pltpu.VME...  4.54 us
  transfers between devices with their start and end apart: 25, of which 13 were waited for; matrix products, arithmetic and copies ran while one was open for 1% of the time, Pallas kernels for 18%

profile of v11, /device:TPU:8, one launch (start us, length us, event | category | flops | bytes accessed | tf_op | source)
XLA Modules:
  0.0 180.4 jit_solution(7943402526684322544)
XLA Ops:
  6.5 3.4 %weave.1 = (bf16[64,4224]{1,0:T(8,128)(2,1)}, bf16[256,2048]{1,0:T(8,128)(2,1)}, bf16[128,2048]{1,0:T(8,128)(2,1)}) custom-call(s32[1]{0:T(128)} %bitcast.1.core, bf16[64,1408]{1,0:T(8,128)(2,1)} %g_hbm.1, bf16[64,1408]{1,0:T(8,128)(2,1)} %u_hbm.1, bf16[64,1408]{1,0:T(8,128)(2,1)} %bitcast.8, bf16[256,2048]{1,0:T(8,128)(2,1)} %w_hbm.1, bf16[128,2048]{1,0:T(8,128)(2,1)} %r_hbm.1), custom_call_target="tpu_custom_call" | custom-call | tf_op jit(solution)/shard_map/weave/pallas_call | solution.py:147
  9.9 0.0 all-gather.2.cloned.1.call-update
  10.0 0.1 add_convert_fusion.1
  10.0 0.2 multiply_sine_fusion
  10.3 0.1 negate_select_fusion.1
  10.4 0.8 pad_maximum_fusion
  11.1 2.8 %keys.1.refs_0_ = bf16[512,256]{1,0:T(8,128)(2,1)} custom-call(bf16[512,128]{1,0:T(8,128)(2,1)} %k_hbm.1, bf16[512,128]{1,0:T(8,128)(2,1)} %v_hbm.1, f32[1,128]{1,0:T(1,128)} %bitcast.9, f32[72,128]{1,0:T(8,128)} %get-tuple-element.79.cos_ref, f32[72,128]{1,0:T(8,128)} %get-tuple-element.80.sin_ref), custom_call_target="tpu_custom_call" | custom-call | tf_op jit(solution)/shard_map/keys/pallas_call | solution.py:78
  13.9 0.4 collective-permute-start.2
  14.3 1.7 collective-permute-start.1
  16.0 3.5 %collective-permute-start = (bf16[512,256]{1,0:T(8,128)(2,1)}, bf16[512,256]{1,0:T(8,128)(2,1)S(1)}, u32[]{:S(2)}, u32[]{:S(2)}) collective-permute-start(bf16[512,256]{1,0:T(8,128)(2,1)} %keys.1.refs_0_), channel_id=1, source_target_pairs={{0,16},{4,68},{8,24},{12,76},{16,0},{20,84},{24,8},{28,92},{32,48}... | collective-permute-start | bytes 786440 | tf_op jit(solution)/shard_map/ppermute | solution.py:417
  19.5 1.0 collective-permute-done.2.refs_3_
  20.6 1.5 collective-permute-done.1.refs_2_
  22.0 2.3 %collective-permute-done.refs_1_ = bf16[512,256]{1,0:T(8,128)(2,1)S(1)} collective-permute-done((bf16[512,256]{1,0:T(8,128)(2,1)}, bf16[512,256]{1,0:T(8,128)(2,1)S(1)}, u32[]{:S(2)}, u32[]{:S(2)}) %collective-permute-start) | collective-permute-done | bytes 262176 | tf_op jit(solution)/shard_map/ppermute | solution.py:417
  24.4 0.9 copy-done
  25.3 0.1 lines.1.refs_1_
  25.4 0.0 copy-start.1
  25.4 3.7 %collective-permute-start.3 = (bf16[2048,256]{1,0:T(8,128)(2,1)S(1)}, bf16[2048,256]{1,0:T(8,128)(2,1)S(1)}, u32[]{:S(2)}, u32[]{:S(2)}) collective-permute-start(bf16[2048,256]{1,0:T(8,128)(2,1)S(1)} %lines.1.refs_1_), channel_id=1, source_target_pairs={{0,4},{4,0},{8,12},{12,8},{16,20},{20,16},{24,28},{28,24},{32,36},... | collective-permute-start | bytes 3145736 | tf_op jit(solution)/shard_map/ppermute | solution.py:422
  29.2 2.5 %collective-permute-start.5 = (bf16[2048,256]{1,0:T(8,128)(2,1)S(1)}, bf16[2048,256]{1,0:T(8,128)(2,1)S(1)}, u32[]{:S(2)}, u32[]{:S(2)}) collective-permute-start(bf16[2048,256]{1,0:T(8,128)(2,1)S(1)} %lines.1.refs_1_), channel_id=1, source_target_pairs={{0,96},{4,28},{8,104},{12,4},{16,112},{20,12},{24,120},{28,20},{32... | collective-permute-start | bytes 3145736 | tf_op jit(solution)/shard_map/ppermute | solution.py:417
  31.7 0.0 collective-permute-start.4
  31.7 0.8 copy-done.2
  32.4 0.8 copy-done.3
  33.2 1.0 copy-done.4
  34.2 0.7 copy-done.6
  34.8 0.5 queries.1.refs_0_
  35.4 0.0 collective-permute-done.3.refs_2_
  35.4 6.3 %shard_map.109 = (f32[1024,128]{1,0:T(8,128)S(1)}, f32[1024,256]{1,0:T(8,128)S(1)}) custom-call(bf16[1024,128]{1,0:T(8,128)(2,1)S(1)} %queries.1.refs_0_, bf16[2048,256]{1,0:T(8,128)(2,1)S(1)} %lines.1.refs_1_, bf16[2048,256]{1,0:T(8,128)(2,1)S(1)} %collective-permute-done.3.refs_2_), custom_call_target="tpu_custom_call" | custom-call | flops 2147483648 | bytes 2097152 | tf_op jit(solution)/shard_map/pallas_call | solution.py:218
  41.6 5.2 %collective-permute-done.5.refs_2_ = bf16[2048,256]{1,0:T(8,128)(2,1)S(1)} collective-permute-done((bf16[2048,256]{1,0:T(8,128)(2,1)S(1)}, bf16[2048,256]{1,0:T(8,128)(2,1)S(1)}, u32[]{:S(2)}, u32[]{:S(2)}) %collective-permute-start.5) | collective-permute-done | bytes 1048608 | tf_op jit(solution)/shard_map/ppermute | solution.py:417
  46.8 2.8 %collective-permute-done.4.refs_1_ = bf16[2048,256]{1,0:T(8,128)(2,1)S(1)} collective-permute-done((bf16[2048,256]{1,0:T(8,128)(2,1)S(1)}, bf16[2048,256]{1,0:T(8,128)(2,1)S(1)}, u32[]{:S(2)}, u32[]{:S(2)}) %collective-permute-start.4) | collective-permute-done | bytes 1048608 | tf_op jit(solution)/shard_map/ppermute | solution.py:417
  49.7 0.5 collective-permute-start.7
  50.3 1.0 collective-permute-start.9
  51.3 1.1 collective-permute-start.8
  52.4 1.5 collective-permute-start.14
  53.8 2.7 %collective-permute-start.13 = (bf16[256,2048]{1,0:T(8,128)(2,1)}, bf16[256,2048]{1,0:T(8,128)(2,1)}, u32[]{:S(2)}, u32[]{:S(2)}) collective-permute-start(bf16[256,2048]{1,0:T(8,128)(2,1)} %get-tuple-element.57.refs_4_), channel_id=1, source_target_pairs={{0,2},{1,3},{2,0},{3,1},{4,6},{5,7},{6,4},{7,5},{8,10},{9,11},{10,... | collective-permute-start | bytes 3145736 | tf_op jit(solution)/shard_map/ppermute | solution.py:399
  56.5 1.5 collective-permute-start.12
  58.0 6.9 %shard_map.110 = (f32[1024,128]{1,0:T(8,128)S(1)}, f32[1024,256]{1,0:T(8,128)S(1)}) custom-call(bf16[1024,128]{1,0:T(8,128)(2,1)S(1)} %queries.1.refs_0_, bf16[2048,256]{1,0:T(8,128)(2,1)S(1)} %collective-permute-done.4.refs_1_, bf16[2048,256]{1,0:T(8,128)(2,1)S(1)} %collective-permute-done.5.refs_2_, f32[1024,128]{1,0:T(8,128)S(1)} %get-tuple-element.43.refs_3_, ...), custom_call_target="tpu_custom_call" | custom-call | flops 2147483648 | bytes 2097152 | tf_op jit(solution)/shard_map/pallas_call | solution.py:218
  64.9 6.9 %shard_map.111 = (f32[1024,128]{1,0:T(8,128)S(1)}, f32[1024,256]{1,0:T(8,128)S(1)}) custom-call(bf16[1024,128]{1,0:T(8,128)(2,1)S(1)} %queries.1.refs_0_, bf16[2048,256]{1,0:T(8,128)(2,1)S(1)} %collective-permute-done.6.refs_1_, bf16[2048,256]{1,0:T(8,128)(2,1)S(1)} %collective-permute-done.7.refs_2_, f32[1024,128]{1,0:T(8,128)S(1)} %get-tuple-element.45.refs_3_, ...), custom_call_target="tpu_custom_call" | custom-call | flops 2147483648 | bytes 2097152 | tf_op jit(solution)/shard_map/pallas_call | solution.py:218
  71.8 0.0 collective-permute-done.9.refs_2_
  71.9 1.2 collective-permute-done.8.refs_1_
  73.0 0.0 collective-permute-start.10
  73.0 0.5 collective-permute-start.11
  73.5 4.2 %shard_map.112 = (f32[1024,128]{1,0:T(8,128)S(1)}, f32[1024,256]{1,0:T(8,128)S(1)}) custom-call(bf16[1024,128]{1,0:T(8,128)(2,1)S(1)} %queries.1.refs_0_, bf16[1024,256]{1,0:T(8,128)(2,1)S(1)} %collective-permute-done.8.refs_1_, bf16[1024,256]{1,0:T(8,128)(2,1)S(1)} %collective-permute-done.9.refs_2_, f32[1024,128]{1,0:T(8,128)S(1)} %get-tuple-element.51.refs_3_, ...), custom_call_target="tpu_custom_call" | custom-call | flops 1073741824 | bytes 1048576 | tf_op jit(solution)/shard_map/pallas_call | solution.py:218
  77.8 0.0 collective-permute-done.11.refs_2_
  77.8 4.4 %shard_map.113.refs_0_ = bf16[512,256]{1,0:T(8,128)(2,1)S(1)} custom-call(bf16[1024,128]{1,0:T(8,128)(2,1)S(1)} %queries.1.refs_0_, bf16[1024,256]{1,0:T(8,128)(2,1)S(1)} %collective-permute-done.10.refs_1_, bf16[1024,256]{1,0:T(8,128)(2,1)S(1)} %collective-permute-done.11.refs_2_, f32[1024,128]{1,0:T(8,128)S(1)} %get-tuple-element.53.refs_3_, ...), custom_call_target="tpu_custom_call" | custom-call | flops 1073741824 | bytes 1048576 | tf_op jit(solution)/shard_map/pallas_call | solution.py:218
  82.3 19.5 %collective-permute-done.13.refs_6_ = bf16[256,2048]{1,0:T(8,128)(2,1)} collective-permute-done((bf16[256,2048]{1,0:T(8,128)(2,1)}, bf16[256,2048]{1,0:T(8,128)(2,1)}, u32[]{:S(2)}, u32[]{:S(2)}) %collective-permute-start.13) | collective-permute-done | bytes 1048608 | tf_op jit(solution)/shard_map/ppermute | solution.py:399
  101.8 0.7 collective-permute-done.12.refs_5_
  102.5 0.0 collective-permute-start.18
  102.5 0.5 collective-permute-start.19
  103.0 0.0 collective-permute-start.20
  103.1 1.4 collective-permute-start.17
  104.5 2.7 %collective-permute-start.16 = (bf16[512,256]{1,0:T(8,128)(2,1)S(1)}, bf16[512,256]{1,0:T(8,128)(2,1)S(1)}, u32[]{:S(2)}, u32[]{:S(2)}) collective-permute-start(bf16[512,256]{1,0:T(8,128)(2,1)S(1)} %shard_map.113.refs_0_), channel_id=1, source_target_pairs={{0,2},{1,3},{2,0},{3,1},{4,6},{5,7},{6,4},{7,5},{8,10},{9,11},{10,... | collective-permute-start | bytes 786440 | tf_op jit(solution)/shard_map/ppermute | solution.py:399
  107.2 5.8 %collective-permute-done.17.refs_3_ = bf16[512,256]{1,0:T(8,128)(2,1)S(1)} collective-permute-done((bf16[512,256]{1,0:T(8,128)(2,1)S(1)}, bf16[512,256]{1,0:T(8,128)(2,1)S(1)}, u32[]{:S(2)}, u32[]{:S(2)}) %collective-permute-start.17) | collective-permute-done | bytes 262176 | tf_op jit(solution)/shard_map/ppermute | solution.py:399
  113.0 1.9 %collective-permute-start.15 = (bf16[512,256]{1,0:T(8,128)(2,1)S(1)}, bf16[512,256]{1,0:T(8,128)(2,1)S(1)}, u32[]{:S(2)}, u32[]{:S(2)}) collective-permute-start(bf16[512,256]{1,0:T(8,128)(2,1)S(1)} %shard_map.113.refs_0_), channel_id=1, source_target_pairs={{0,3},{1,0},{2,1},{3,2},{4,7},{5,4},{6,5},{7,6},{8,11},{9,8},{10,9... | collective-permute-start | bytes 786440 | tf_op jit(solution)/shard_map/ppermute | solution.py:399
  114.9 0.1 pad_add_fusion.place
  114.9 4.5 %collective-permute-done.16.refs_2_ = bf16[512,256]{1,0:T(8,128)(2,1)S(1)} collective-permute-done((bf16[512,256]{1,0:T(8,128)(2,1)S(1)}, bf16[512,256]{1,0:T(8,128)(2,1)S(1)}, u32[]{:S(2)}, u32[]{:S(2)}) %collective-permute-start.16) | collective-permute-done | bytes 262176 | tf_op jit(solution)/shard_map/ppermute | solution.py:399
  119.5 1.4 collective-permute-done.15.refs_1_
  120.8 0.0 collective-permute-done.19.refs_10_
  120.9 0.0 all-gather.2.cloned.1.call-done.refs_13_.w_hbm
  120.9 19.9 %layer.1 = (bf16[128,2048]{1,0:T(8,128)(2,1)S(1)}, bf16[128,2048]{1,0:T(8,128)(2,1)S(1)}, bf16[128,2048]{1,0:T(8,128)(2,1)S(1)}, bf16[256,1408]{1,0:T(8,128)(2,1)S(1)}) custom-call(s32[2]{0:T(128)S(1)} %pad_add_fusion.place, bf16[512,256]{1,0:T(8,128)(2,1)S(1)} %shard_map.113.refs_0_, bf16[512,256]{1,0:T(8,128)(2,1)S(1)} %collective-permute-done.15.refs_1_, ...), custom_call_target="tpu_custom_call" | custom-call | tf_op jit(solution)/shard_map/layer/pallas_call | solution.py:355
  140.8 4.5 %rest.1 = (bf16[128,2048]{1,0:T(8,128)(2,1)S(1)}, bf16[128,2048]{1,0:T(8,128)(2,1)S(1)}) custom-call(bf16[256,1408]{1,0:T(8,128)(2,1)S(1)} %get-tuple-element.64.h_ref, bf16[2048,4224]{1,0:T(8,128)(2,1)} %all-gather.2.cloned.1.call-done.refs_13_.w_hbm), custom_call_target="tpu_custom_call" | custom-call | tf_op jit(solution)/shard_map/rest/pallas_call | solution.py:338
  145.3 2.7 %collective-permute-start.23 = (bf16[128,2048]{1,0:T(8,128)(2,1)S(1)}, bf16[128,2048]{1,0:T(8,128)(2,1)S(1)}, u32[]{:S(2)}, u32[]{:S(2)}) collective-permute-start(bf16[128,2048]{1,0:T(8,128)(2,1)S(1)} %get-tuple-element.68), channel_id=1, source_target_pairs={{0,3},{1,0},{2,1},{3,2},{4,7},{5,4},{6,5},{7,6},{8,11},{9,8},{10,9... | collective-permute-start | bytes 1572872 | tf_op jit(solution)/shard_map/ppermute | solution.py:399
  148.0 1.5 collective-permute-start.22
  149.6 19.4 %collective-permute-done.23 = bf16[128,2048]{1,0:T(8,128)(2,1)S(1)} collective-permute-done((bf16[128,2048]{1,0:T(8,128)(2,1)S(1)}, bf16[128,2048]{1,0:T(8,128)(2,1)S(1)}, u32[]{:S(2)}, u32[]{:S(2)}) %collective-permute-start.23) | collective-permute-done | bytes 524320 | tf_op jit(solution)/shard_map/ppermute | solution.py:399
  169.0 3.4 %collective-permute-done.21 = bf16[128,2048]{1,0:T(8,128)(2,1)S(1)} collective-permute-done((bf16[128,2048]{1,0:T(8,128)(2,1)S(1)}, bf16[128,2048]{1,0:T(8,128)(2,1)S(1)}, u32[]{:S(2)}, u32[]{:S(2)}) %collective-permute-start.21) | collective-permute-done | bytes 524320 | tf_op jit(solution)/shard_map/ppermute | solution.py:399
  172.3 1.2 add_convert_fusion
  (26 shorter events, 0.1 us)
Async XLA Ops:
  6.5 114.3 %all-gather.2.cloned.1.call-start = ((), (), s32[]{:S(2)}) async-start(), calls=%async_computation | async-start | bytes 17842176 | tf_op jit(solution)/shard_map/all_gather | solution.py:447
  13.9 6.7 %collective-permute-start.2 = (bf16[512,256]{1,0:T(8,128)(2,1)}, bf16[512,256]{1,0:T(8,128)(2,1)S(1)}, u32[]{:S(2)}, u32[]{:S(2)}) collective-permute-start(bf16[512,256]{1,0:T(8,128)(2,1)} %keys.1.refs_0_), channel_id=1, source_target_pairs={{0,24},{4,100},{8,0},{12,108},{16,8},{20,116},{24,16},{28,124},{32... | collective-permute-start | bytes 786440 | tf_op jit(solution)/shard_map/ppermute | solution.py:417
  14.3 7.7 %collective-permute-start.1 = (bf16[512,256]{1,0:T(8,128)(2,1)}, bf16[512,256]{1,0:T(8,128)(2,1)S(1)}, u32[]{:S(2)}, u32[]{:S(2)}) collective-permute-start(bf16[512,256]{1,0:T(8,128)(2,1)} %keys.1.refs_0_), channel_id=1, source_target_pairs={{0,8},{4,36},{8,16},{12,44},{16,24},{20,52},{24,0},{28,60},{32,40}... | collective-permute-start | bytes 786440 | tf_op jit(solution)/shard_map/ppermute | solution.py:417
  16.0 8.4 %collective-permute-start = (bf16[512,256]{1,0:T(8,128)(2,1)}, bf16[512,256]{1,0:T(8,128)(2,1)S(1)}, u32[]{:S(2)}, u32[]{:S(2)}) collective-permute-start(bf16[512,256]{1,0:T(8,128)(2,1)} %keys.1.refs_0_), channel_id=1, source_target_pairs={{0,16},{4,68},{8,24},{12,76},{16,0},{20,84},{24,8},{28,92},{32,48}... | collective-permute-start | bytes 786440 | tf_op jit(solution)/shard_map/ppermute | solution.py:417
  24.4 1.0 copy-start
  25.3 95.6 %copy-start.5 = (f32[2048]{0:T(1024)S(1)}, f32[2048]{0:T(1024)}, u32[]{:S(2)}) copy-start(f32[2048]{0:T(1024)} %param.18) | copy-start | bytes 24580
  25.4 95.5 %copy-start.1 = (bf16[128,2048]{1,0:T(8,128)(2,1)S(1)}, bf16[128,2048]{1,0:T(8,128)(2,1)}, u32[]{:S(2)}) copy-start(bf16[128,2048]{1,0:T(8,128)(2,1)} %get-tuple-element.61.refs_8_) | copy-start | bytes 1572868
  25.4 9.9 %collective-permute-start.3 = (bf16[2048,256]{1,0:T(8,128)(2,1)S(1)}, bf16[2048,256]{1,0:T(8,128)(2,1)S(1)}, u32[]{:S(2)}, u32[]{:S(2)}) collective-permute-start(bf16[2048,256]{1,0:T(8,128)(2,1)S(1)} %lines.1.refs_1_), channel_id=1, source_target_pairs={{0,4},{4,0},{8,12},{12,8},{16,20},{20,16},{24,28},{28,24},{32,36},... | collective-permute-start | bytes 3145736 | tf_op jit(solution)/shard_map/ppermute | solution.py:422
  29.2 17.7 %collective-permute-start.5 = (bf16[2048,256]{1,0:T(8,128)(2,1)S(1)}, bf16[2048,256]{1,0:T(8,128)(2,1)S(1)}, u32[]{:S(2)}, u32[]{:S(2)}) collective-permute-start(bf16[2048,256]{1,0:T(8,128)(2,1)S(1)} %lines.1.refs_1_), channel_id=1, source_target_pairs={{0,96},{4,28},{8,104},{12,4},{16,112},{20,12},{24,120},{28,20},{32... | collective-permute-start | bytes 3145736 | tf_op jit(solution)/shard_map/ppermute | solution.py:417
  31.7 18.0 %collective-permute-start.4 = (bf16[2048,256]{1,0:T(8,128)(2,1)S(1)}, bf16[2048,256]{1,0:T(8,128)(2,1)S(1)}, u32[]{:S(2)}, u32[]{:S(2)}) collective-permute-start(bf16[2048,256]{1,0:T(8,128)(2,1)S(1)} %lines.1.refs_1_), channel_id=1, source_target_pairs={{0,32},{4,12},{8,40},{12,20},{16,48},{20,28},{24,56},{28,4},{32,64... | collective-permute-start | bytes 3145736 | tf_op jit(solution)/shard_map/ppermute | solution.py:417
  31.7 0.8 copy-start.2
  32.4 0.8 copy-start.3
  33.2 1.0 copy-start.4
  34.2 0.7 copy-start.6
  49.7 4.2 %collective-permute-start.6 = (bf16[2048,256]{1,0:T(8,128)(2,1)S(1)}, bf16[2048,256]{1,0:T(8,128)(2,1)S(1)}, u32[]{:S(2)}, u32[]{:S(2)}) collective-permute-start(bf16[2048,256]{1,0:T(8,128)(2,1)S(1)} %collective-permute-done.4.refs_1_), channel_id=1, source_target_pairs={{0,4},{4,0},{8,12},{12,8},{16,20},{20,16},{24,28},{28,24},{32,36},... | collective-permute-start | bytes 3145736 | tf_op jit(solution)/shard_map/ppermute | solution.py:422
  49.7 6.8 %collective-permute-start.7 = (bf16[2048,256]{1,0:T(8,128)(2,1)S(1)}, bf16[2048,256]{1,0:T(8,128)(2,1)S(1)}, u32[]{:S(2)}, u32[]{:S(2)}) collective-permute-start(bf16[2048,256]{1,0:T(8,128)(2,1)S(1)} %collective-permute-done.5.refs_2_), channel_id=1, source_target_pairs={{0,4},{4,0},{8,12},{12,8},{16,20},{20,16},{24,28},{28,24},{32,36},... | collective-permute-start | bytes 3145736 | tf_op jit(solution)/shard_map/ppermute | solution.py:422
  50.3 21.6 %collective-permute-start.9 = (bf16[1024,256]{1,0:T(8,128)(2,1)S(1)}, bf16[1024,256]{1,0:T(8,128)(2,1)S(1)}, u32[]{:S(2)}, u32[]{:S(2)}) collective-permute-start(bf16[1024,256]{1,0:T(8,128)(2,1)S(1)} %slice.7), channel_id=1, source_target_pairs={{0,96},{4,28},{8,104},{12,4},{16,112},{20,12},{24,120},{28,20},{32... | collective-permute-start | bytes 1572872 | tf_op jit(solution)/shard_map/ppermute | solution.py:417
  51.3 21.7 %collective-permute-start.8 = (bf16[1024,256]{1,0:T(8,128)(2,1)S(1)}, bf16[1024,256]{1,0:T(8,128)(2,1)S(1)}, u32[]{:S(2)}, u32[]{:S(2)}) collective-permute-start(bf16[1024,256]{1,0:T(8,128)(2,1)S(1)} %slice.6), channel_id=1, source_target_pairs={{0,32},{4,12},{8,40},{12,20},{16,48},{20,28},{24,56},{28,4},{32,64... | collective-permute-start | bytes 1572872 | tf_op jit(solution)/shard_map/ppermute | solution.py:417
  52.4 29.9 %collective-permute-start.14 = (bf16[256,2048]{1,0:T(8,128)(2,1)}, bf16[256,2048]{1,0:T(8,128)(2,1)S(1)}, u32[]{:S(2)}, u32[]{:S(2)}) collective-permute-start(bf16[256,2048]{1,0:T(8,128)(2,1)} %get-tuple-element.57.refs_4_), channel_id=1, source_target_pairs={{0,1},{1,2},{2,3},{3,0},{4,5},{5,6},{6,7},{7,4},{8,9},{9,10},{10,1... | collective-permute-start | bytes 3145736 | tf_op jit(solution)/shard_map/ppermute | solution.py:399
  53.8 48.0 %collective-permute-start.13 = (bf16[256,2048]{1,0:T(8,128)(2,1)}, bf16[256,2048]{1,0:T(8,128)(2,1)}, u32[]{:S(2)}, u32[]{:S(2)}) collective-permute-start(bf16[256,2048]{1,0:T(8,128)(2,1)} %get-tuple-element.57.refs_4_), channel_id=1, source_target_pairs={{0,2},{1,3},{2,0},{3,1},{4,6},{5,7},{6,4},{7,5},{8,10},{9,11},{10,... | collective-permute-start | bytes 3145736 | tf_op jit(solution)/shard_map/ppermute | solution.py:399
  56.5 46.0 %collective-permute-start.12 = (bf16[256,2048]{1,0:T(8,128)(2,1)}, bf16[256,2048]{1,0:T(8,128)(2,1)}, u32[]{:S(2)}, u32[]{:S(2)}) collective-permute-start(bf16[256,2048]{1,0:T(8,128)(2,1)} %get-tuple-element.57.refs_4_), channel_id=1, source_target_pairs={{0,3},{1,0},{2,1},{3,2},{4,7},{5,4},{6,5},{7,6},{8,11},{9,8},{10,9... | collective-permute-start | bytes 3145736 | tf_op jit(solution)/shard_map/ppermute | solution.py:399
  73.0 4.8 %collective-permute-start.10 = (bf16[1024,256]{1,0:T(8,128)(2,1)S(1)}, bf16[1024,256]{1,0:T(8,128)(2,1)S(1)}, u32[]{:S(2)}, u32[]{:S(2)}) collective-permute-start(bf16[1024,256]{1,0:T(8,128)(2,1)S(1)} %collective-permute-done.8.refs_1_), channel_id=1, source_target_pairs={{0,4},{4,0},{8,12},{12,8},{16,20},{20,16},{24,28},{28,24},{32,36},... | collective-permute-start | bytes 1572872 | tf_op jit(solution)/shard_map/ppermute | solution.py:422
  73.0 4.8 %collective-permute-start.11 = (bf16[1024,256]{1,0:T(8,128)(2,1)S(1)}, bf16[1024,256]{1,0:T(8,128)(2,1)S(1)}, u32[]{:S(2)}, u32[]{:S(2)}) collective-permute-start(bf16[1024,256]{1,0:T(8,128)(2,1)S(1)} %collective-permute-done.9.refs_2_), channel_id=1, source_target_pairs={{0,4},{4,0},{8,12},{12,8},{16,20},{20,16},{24,28},{28,24},{32,36},... | collective-permute-start | bytes 1572872 | tf_op jit(solution)/shard_map/ppermute | solution.py:422
  82.3 38.6 %copy-start.7 = (bf16[256,2048]{1,0:T(8,128)(2,1)}, bf16[256,2048]{1,0:T(8,128)(2,1)S(1)}, u32[]{:S(2)}) copy-start(bf16[256,2048]{1,0:T(8,128)(2,1)S(1)} %collective-permute-done.14.refs_7_) | copy-start | bytes 3145732
  102.5 18.3 %collective-permute-start.18 = (bf16[256,2048]{1,0:T(8,128)(2,1)}, bf16[256,2048]{1,0:T(8,128)(2,1)}, u32[]{:S(2)}, u32[]{:S(2)}) collective-permute-start(bf16[256,2048]{1,0:T(8,128)(2,1)} %collective-permute-done.12.refs_5_), channel_id=1, source_target_pairs={{0,4},{4,0},{8,12},{12,8},{16,20},{20,16},{24,28},{28,24},{32,36},... | collective-permute-start | bytes 3145736 | tf_op jit(solution)/shard_map/ppermute | solution.py:422
  102.5 18.3 %collective-permute-start.19 = (bf16[256,2048]{1,0:T(8,128)(2,1)}, bf16[256,2048]{1,0:T(8,128)(2,1)}, u32[]{:S(2)}, u32[]{:S(2)}) collective-permute-start(bf16[256,2048]{1,0:T(8,128)(2,1)} %collective-permute-done.13.refs_6_), channel_id=1, source_target_pairs={{0,4},{4,0},{8,12},{12,8},{16,20},{20,16},{24,28},{28,24},{32,36},... | collective-permute-start | bytes 3145736 | tf_op jit(solution)/shard_map/ppermute | solution.py:422
  103.0 17.8 %collective-permute-start.20 = (bf16[256,2048]{1,0:T(8,128)(2,1)S(1)}, bf16[256,2048]{1,0:T(8,128)(2,1)}, u32[]{:S(2)}, u32[]{:S(2)}) collective-permute-start(bf16[256,2048]{1,0:T(8,128)(2,1)S(1)} %collective-permute-done.14.refs_7_), channel_id=1, source_target_pairs={{0,4},{4,0},{8,12},{12,8},{16,20},{20,16},{24,28},{28,24},{32,36},... | collective-permute-start | bytes 3145736 | tf_op jit(solution)/shard_map/ppermute | solution.py:422
  103.1 9.9 %collective-permute-start.17 = (bf16[512,256]{1,0:T(8,128)(2,1)S(1)}, bf16[512,256]{1,0:T(8,128)(2,1)S(1)}, u32[]{:S(2)}, u32[]{:S(2)}) collective-permute-start(bf16[512,256]{1,0:T(8,128)(2,1)S(1)} %shard_map.113.refs_0_), channel_id=1, source_target_pairs={{0,1},{1,2},{2,3},{3,0},{4,5},{5,6},{6,7},{7,4},{8,9},{9,10},{10,1... | collective-permute-start | bytes 786440 | tf_op jit(solution)/shard_map/ppermute | solution.py:399
  104.5 15.0 %collective-permute-start.16 = (bf16[512,256]{1,0:T(8,128)(2,1)S(1)}, bf16[512,256]{1,0:T(8,128)(2,1)S(1)}, u32[]{:S(2)}, u32[]{:S(2)}) collective-permute-start(bf16[512,256]{1,0:T(8,128)(2,1)S(1)} %shard_map.113.refs_0_), channel_id=1, source_target_pairs={{0,2},{1,3},{2,0},{3,1},{4,6},{5,7},{6,4},{7,5},{8,10},{9,11},{10,... | collective-permute-start | bytes 786440 | tf_op jit(solution)/shard_map/ppermute | solution.py:399
  113.0 7.9 %collective-permute-start.15 = (bf16[512,256]{1,0:T(8,128)(2,1)S(1)}, bf16[512,256]{1,0:T(8,128)(2,1)S(1)}, u32[]{:S(2)}, u32[]{:S(2)}) collective-permute-start(bf16[512,256]{1,0:T(8,128)(2,1)S(1)} %shard_map.113.refs_0_), channel_id=1, source_target_pairs={{0,3},{1,0},{2,1},{3,2},{4,7},{5,4},{6,5},{7,6},{8,11},{9,8},{10,9... | collective-permute-start | bytes 786440 | tf_op jit(solution)/shard_map/ppermute | solution.py:399
  145.3 23.6 %collective-permute-start.23 = (bf16[128,2048]{1,0:T(8,128)(2,1)S(1)}, bf16[128,2048]{1,0:T(8,128)(2,1)S(1)}, u32[]{:S(2)}, u32[]{:S(2)}) collective-permute-start(bf16[128,2048]{1,0:T(8,128)(2,1)S(1)} %get-tuple-element.68), channel_id=1, source_target_pairs={{0,3},{1,0},{2,1},{3,2},{4,7},{5,4},{6,5},{7,6},{8,11},{9,8},{10,9... | collective-permute-start | bytes 1572872 | tf_op jit(solution)/shard_map/ppermute | solution.py:399
  148.0 24.3 %collective-permute-start.21 = (bf16[128,2048]{1,0:T(8,128)(2,1)S(1)}, bf16[128,2048]{1,0:T(8,128)(2,1)S(1)}, u32[]{:S(2)}, u32[]{:S(2)}) collective-permute-start(bf16[128,2048]{1,0:T(8,128)(2,1)S(1)} %get-tuple-element.66), channel_id=1, source_target_pairs={{0,1},{1,2},{2,3},{3,0},{4,5},{5,6},{6,7},{7,4},{8,9},{9,10},{10,1... | collective-permute-start | bytes 1572872 | tf_op jit(solution)/shard_map/ppermute | solution.py:399
  148.0 24.3 %collective-permute-start.22 = (bf16[128,2048]{1,0:T(8,128)(2,1)S(1)}, bf16[128,2048]{1,0:T(8,128)(2,1)S(1)}, u32[]{:S(2)}, u32[]{:S(2)}) collective-permute-start(bf16[128,2048]{1,0:T(8,128)(2,1)S(1)} %get-tuple-element.67), channel_id=1, source_target_pairs={{0,2},{1,3},{2,0},{3,1},{4,6},{5,7},{6,4},{7,5},{8,10},{9,11},{10,... | collective-permute-start | bytes 1572872 | tf_op jit(solution)/shard_map/ppermute | solution.py:399
Sparse Core Ops, SparseCore 0:
  10.1 83.8 all-gather.1

commit v12 on v11

--- a/solution.py
+++ b/solution.py
@@ -104,16 +104,38 @@
     )(query_rows, gain[None, :], cosine, sine)
 
 
-def weave_kernel(
-    core, g_hbm, u_hbm, d_hbm, w_hbm, r_hbm, woven, sent, kept, g_ref, u_ref, d_ref, w_ref, r_ref, sems, *, tile
-):
+def weave_kernel(g_hbm, u_hbm, d_hbm, woven, g_ref, u_ref, d_ref, sems, *, tile):
+    moves = ((g_hbm, g_ref), (u_hbm, u_ref), (d_hbm, d_ref))
+    copies = [pltpu.make_async_copy(x, y, sems.at[n]) for n, (x, y) in enumerate(moves)]
+    for c in copies:
+        c.start()
+    for c in copies:
+        c.wait()
+    units = g_ref.shape[1]
+    for n in range(units // tile):
+        part = slice(n * tile, (n + 1) * tile)
+        woven[:, 2 * n * tile : (2 * n + 1) * tile] = g_ref[:, part]
+        woven[:, (2 * n + 1) * tile : (2 * n + 2) * tile] = u_ref[:, part]
+    woven[:, 2 * units :] = d_ref[...]
+
+
+def weave(gate, up, down, tile=128):
+    big = (gate, up, down.T)
+    return pl.pallas_call(
+        functools.partial(weave_kernel, tile=tile),
+        in_specs=[pl.BlockSpec(memory_space=pltpu.HBM)] * 3,
+        out_shape=jax.ShapeDtypeStruct((gate.shape[0], 3 * gate.shape[1]), bf16),
+        scratch_shapes=[pltpu.VMEM(x.shape, bf16) for x in big] + [pltpu.SemaphoreType.DMA((3,))],
+        compiler_params=pltpu.CompilerParams(vmem_limit_bytes=60 * 1024 * 1024),
+        name="weave",
+    )(*big)
+
+
+def stage_kernel(core, w_hbm, r_hbm, sent, kept, w_ref, r_ref, sems):
     half = kept.shape[0]
     first_half = pl.ds(pl.multiple_of(core[0] * half, half), half)
     other_half = pl.ds(pl.multiple_of((1 - core[0]) * half, half), half)
     moves = [
-        (g_hbm, g_ref),
-        (u_hbm, u_ref),
-        (d_hbm, d_ref),
         (w_hbm.at[first_half, :], w_ref.at[pl.ds(0, half), :]),
         (w_hbm.at[other_half, :], w_ref.at[pl.ds(half, half), :]),
         (r_hbm, r_ref),
@@ -122,41 +144,28 @@
         (r_ref, sent.at[pl.ds(half, r_hbm.shape[0]), :]),
     ]
     copies = [pltpu.make_async_copy(x, y, sems.at[n]) for n, (x, y) in enumerate(moves)]
-    for c in copies[:6]:
+    for c in copies[:3]:
         c.start()
-    for c in copies[:3]:
-        c.wait()
-    units = g_ref.shape[1]
-    for n in range(units // tile):
-        part = slice(n * tile, (n + 1) * tile)
-        woven[:, 2 * n * tile : (2 * n + 1) * tile] = g_ref[:, part]
-        woven[:, (2 * n + 1) * tile : (2 * n + 2) * tile] = u_ref[:, part]
-    woven[:, 2 * units :] = d_ref[...]
-    for n in (3, 4, 5):
+    for n in range(3):
         copies[n].wait()
         copies[n + 3].start()
-    for n in (6, 7, 8):
-        copies[n].wait()
-
-
-def weave(core, gate, up, down, out_weight, residual, tile=128):
-    big = (gate, up, down.T, out_weight, residual)
+    for c in copies[3:]:
+        c.wait()
+
+
+def staged(core, out_weight, residual):
     half = out_weight.shape[0] // 2
-    width = residual.shape[1]
+    rows, width = residual.shape
     hbm = pl.BlockSpec(memory_space=pltpu.HBM)
     return pl.pallas_call(
-        functools.partial(weave_kernel, tile=tile),
-        in_specs=[pl.BlockSpec(memory_space=pltpu.SMEM)] + [hbm] * 5,
-        out_specs=[pl.BlockSpec(memory_space=pltpu.VMEM), hbm, hbm],
-        out_shape=[
-            jax.ShapeDtypeStruct((gate.shape[0], 3 * gate.shape[1]), bf16),
-            jax.ShapeDtypeStruct((half + residual.shape[0], width), bf16),
-            jax.ShapeDtypeStruct((half, width), bf16),
-        ],
-        scratch_shapes=[pltpu.VMEM(x.shape, bf16) for x in big] + [pltpu.SemaphoreType.DMA((9,))],
+        stage_kernel,
+        in_specs=[pl.BlockSpec(memory_space=pltpu.SMEM), hbm, hbm],
+        out_specs=[hbm, hbm],
+        out_shape=[jax.ShapeDtypeStruct((half + rows, width), bf16), jax.ShapeDtypeStruct((half, width), bf16)],
+        scratch_shapes=[pltpu.VMEM(x.shape, bf16) for x in (out_weight, residual)] + [pltpu.SemaphoreType.DMA((6,))],
         compiler_params=pltpu.CompilerParams(vmem_limit_bytes=60 * 1024 * 1024),
-        name="weave",
-    )(core[None], *big)
+        name="stage",
+    )(core[None], out_weight, residual)
 
 
 def flash_kernel(*refs, pieces, scale, first, last, block=1024):
@@ -291,20 +300,24 @@
             x = x * lax.rsqrt(jnp.mean(x * x, axis=-1, keepdims=True) + norm_eps)
             x_ref[some, :] = (x * gain_ref[...]).astype(bf16)
 
-        def product(n):
-            return jnp.dot(x_ref[...], pair_ref[n], preferred_element_type=f32)
+        def product(tiles):
+            both = jnp.concatenate([pair_ref[n] for n in tiles], axis=1)
+            return jnp.dot(x_ref[...], both, preferred_element_type=f32)
 
         for begin, end, arrived in ((0, early, copies()[:early]), (early, count, copies()[early:])):
             for c in arrived:
                 c.wait()
-            following = product(begin)
-            for n in range(begin, end):
+            runs = [range(n, min(n + 2, end)) for n in range(begin, end, 2)]
+            following = product(runs[0])
+            for k, tiles in enumerate(runs):
                 r = following
-                if n + 1 < end:
-                    following = product(n + 1)
-                gate = r[:, 0:unit_tile]
-                hidden = gate / (1.0 + jnp.exp(-gate)) * r[:, unit_tile:]
-                h_ref[:, n * unit_tile : (n + 1) * unit_tile] = hidden.astype(bf16)
+                if k + 1 < len(runs):
+                    following = product(runs[k + 1])
+                for m, n in enumerate(tiles):
+                    gate = r[:, 2 * m * unit_tile : (2 * m + 1) * unit_tile]
+                    up = r[:, (2 * m + 1) * unit_tile : (2 * m + 2) * unit_tile]
+                    hidden = gate / (1.0 + jnp.exp(-gate)) * up
+                    h_ref[:, n * unit_tile : (n + 1) * unit_tile] = hidden.astype(bf16)
         rest_ref[0:sub, :] = h_ref[0:sub, :]
         rest_ref[sub:, :] = h_ref[3 * sub :, :]
         down_products(h_ref[sub : 3 * sub, :], down_ref, (out_1, out_2))
@@ -443,8 +456,8 @@
     rows = tok // GRID
     tables = angle_tables(lax.axis_index("sp") * rows, rows, query_gain.shape[0])
     kv = prepare_keys(key_rows, value_rows, key_gain, *tables)
-    woven, payload, kept = weave(core, gate_weight, up_weight, down_weight, out_weight, residual)
-    weights = lax.all_gather(woven, "sp", axis=0, tiled=True)
+    weights = lax.all_gather(weave(gate_weight, up_weight, down_weight), "sp", axis=0, tiled=True)
+    payload, kept = staged(core, out_weight, residual)
     q = prepare_queries(query_rows, query_gain, *tables)
 
     steps = (2, 1, -1)

time: 182 us -> 185 us (1.016)
  local copies, waits for them, and re-layouts: 4.19 us -> 9.07 us
  waiting for transfers between devices: 68.9 us -> 64.4 us
  Pallas kernels: 59.9 us -> 64.3 us
  starting transfers between devices: 31.3 us -> 29.1 us
    ppermute x9, waiting for transfers between devices: 54.8 us -> 50.9 us  [shifted(): lax.ppermute(value, 'tp', [(i, (i + by) % count) for i in range(count)])]
    pallas_call x5, Pallas kernels: 28.8 us -> 32.2 us  [flash(): pl.pallas_call(functools.partial(flash_kernel, pieces=pieces, scale=head_...]
    unnamed x16 -> x24, local copies, waits for them, and re-layouts: 4.11 us -> 7.38 us
    pallas_call x0 -> x1, Pallas kernels: none -> 2.28 us  [staged(): pl.pallas_call(stage_kernel, in_specs=[pl.BlockSpec(memory_space=pltpu.SM...]
  transfers between devices with their start and end apart: 25 -> 25, of which waited for: 13 -> 11; matrix products, arithmetic and copies ran while one was open for 1% -> 2% of each run, Pallas kernels for 18% -> 21%
where the time goes in v12:
time: 185 us; the launch traced here: 183 us
  waiting for transfers between devices  64.4 us (35%)
  Pallas kernels  64.3 us (35%)
  starting transfers between devices  29.1 us (16%)
  between operations  13.7 us (7%)
  local copies, waits for them, and re-layouts  9.07 us (5%)
  other arithmetic  2.46 us (1%)
    ppermute x9, waiting for transfers between devices, shifted(): lax.ppermute(value, 'tp', [(i, (i + by) % count) for i in range(count)])  50.9 us
    pallas_call x5, Pallas kernels, flash(): pl.pallas_call(functools.partial(flash_kernel, pieces=pieces, scale=head_...  32.2 us
    pallas_call x1, Pallas kernels, layer(): pl.pallas_call(functools.partial(layer_kernel, parts=parts, tile=tile, su...  19.9 us
    ppermute x9, starting transfers between devices, shifted(): lax.ppermute(value, 'tp', [(i, (i + by) % count) for i in range(count)])  15.1 us
    ppermute x7, waiting for transfers between devices, crossed(): return lax.ppermute(value, 'sp', pairs)  13.4 us
    ppermute x7, starting transfers between devices, crossed(): return lax.ppermute(value, 'sp', pairs)  9.65 us
    unnamed x24, local copies, waits for them, and re-layouts  7.38 us
    pallas_call x1, Pallas kernels, rest(): pl.pallas_call(rest_kernel, in_specs=[pl.BlockSpec(memory_space=pltpu.VME...  4.53 us
  transfers between devices with their start and end apart: 25, of which 11 were waited for; matrix products, arithmetic and copies ran while one was open for 2% of the time, Pallas kernels for 21%

profile of v12, /device:TPU:8, one launch (start us, length us, event | category | flops | bytes accessed | tf_op | source)
XLA Modules:
  0.0 183.0 jit_solution(1200862641196682327)
XLA Ops:
  6.5 2.0 %weave.1 = bf16[64,4224]{1,0:T(8,128)(2,1)} custom-call(bf16[64,1408]{1,0:T(8,128)(2,1)} %g_hbm.1, bf16[64,1408]{1,0:T(8,128)(2,1)} %u_hbm.1, bf16[64,1408]{1,0:T(8,128)(2,1)} %bitcast.8), custom_call_target="tpu_custom_call" | custom-call | tf_op jit(solution)/shard_map/weave/pallas_call | solution.py:124
  8.6 0.0 all-gather.2.cloned.1.call-update
  8.7 0.1 add_convert_fusion.1
  8.7 0.2 multiply_sine_fusion
  9.0 0.1 negate_select_fusion.1
  9.1 0.8 pad_maximum_fusion
  9.8 2.8 %keys.1.refs_0_ = bf16[512,256]{1,0:T(8,128)(2,1)} custom-call(bf16[512,128]{1,0:T(8,128)(2,1)} %k_hbm.1, bf16[512,128]{1,0:T(8,128)(2,1)} %v_hbm.1, f32[1,128]{1,0:T(1,128)} %bitcast.9, f32[72,128]{1,0:T(8,128)} %get-tuple-element.77.cos_ref, f32[72,128]{1,0:T(8,128)} %get-tuple-element.78.sin_ref), custom_call_target="tpu_custom_call" | custom-call | tf_op jit(solution)/shard_map/keys/pallas_call | solution.py:78
  12.6 0.4 collective-permute-start.2
  13.0 1.7 collective-permute-start.1
  14.7 3.5 %collective-permute-start = (bf16[512,256]{1,0:T(8,128)(2,1)}, bf16[512,256]{1,0:T(8,128)(2,1)S(1)}, u32[]{:S(2)}, u32[]{:S(2)}) collective-permute-start(bf16[512,256]{1,0:T(8,128)(2,1)} %keys.1.refs_0_), channel_id=1, source_target_pairs={{0,16},{4,68},{8,24},{12,76},{16,0},{20,84},{24,8},{28,92},{32,48}... | collective-permute-start | bytes 786440 | tf_op jit(solution)/shard_map/ppermute | solution.py:430
  18.2 1.0 collective-permute-done.2.refs_3_
  19.3 1.5 collective-permute-done.1.refs_2_
  20.7 2.3 %collective-permute-done.refs_1_ = bf16[512,256]{1,0:T(8,128)(2,1)S(1)} collective-permute-done((bf16[512,256]{1,0:T(8,128)(2,1)}, bf16[512,256]{1,0:T(8,128)(2,1)S(1)}, u32[]{:S(2)}, u32[]{:S(2)}) %collective-permute-start) | collective-permute-done | bytes 262176 | tf_op jit(solution)/shard_map/ppermute | solution.py:430
  23.1 1.0 copy-done
  24.0 0.1 lines.1.refs_1_
  24.1 2.7 %collective-permute-start.3 = (bf16[2048,256]{1,0:T(8,128)(2,1)S(1)}, bf16[2048,256]{1,0:T(8,128)(2,1)S(1)}, u32[]{:S(2)}, u32[]{:S(2)}) collective-permute-start(bf16[2048,256]{1,0:T(8,128)(2,1)S(1)} %lines.1.refs_1_), channel_id=1, source_target_pairs={{0,4},{4,0},{8,12},{12,8},{16,20},{20,16},{24,28},{28,24},{32,36},... | collective-permute-start | bytes 3145736 | tf_op jit(solution)/shard_map/ppermute | solution.py:435
  26.8 1.8 %collective-permute-start.5 = (bf16[2048,256]{1,0:T(8,128)(2,1)S(1)}, bf16[2048,256]{1,0:T(8,128)(2,1)S(1)}, u32[]{:S(2)}, u32[]{:S(2)}) collective-permute-start(bf16[2048,256]{1,0:T(8,128)(2,1)S(1)} %lines.1.refs_1_), channel_id=1, source_target_pairs={{0,96},{4,28},{8,104},{12,4},{16,112},{20,12},{24,120},{28,20},{32... | collective-permute-start | bytes 3145736 | tf_op jit(solution)/shard_map/ppermute | solution.py:430
  28.7 0.2 collective-permute-start.4
  28.9 0.8 copy-done.2
  29.6 0.8 copy-done.3
  30.4 1.0 copy-done.4
  31.3 0.7 copy-done.6
  32.0 0.5 queries.1.refs_0_
  32.5 0.0 copy-start.5
  32.6 0.0 collective-permute-done.3.refs_2_
  32.6 6.4 %shard_map.109 = (f32[1024,128]{1,0:T(8,128)S(1)}, f32[1024,256]{1,0:T(8,128)S(1)}) custom-call(bf16[1024,128]{1,0:T(8,128)(2,1)S(1)} %queries.1.refs_0_, bf16[2048,256]{1,0:T(8,128)(2,1)S(1)} %lines.1.refs_1_, bf16[2048,256]{1,0:T(8,128)(2,1)S(1)} %collective-permute-done.3.refs_2_), custom_call_target="tpu_custom_call" | custom-call | flops 2147483648 | bytes 2097152 | tf_op jit(solution)/shard_map/pallas_call | solution.py:227
  39.0 6.8 %collective-permute-done.5.refs_2_ = bf16[2048,256]{1,0:T(8,128)(2,1)S(1)} collective-permute-done((bf16[2048,256]{1,0:T(8,128)(2,1)S(1)}, bf16[2048,256]{1,0:T(8,128)(2,1)S(1)}, u32[]{:S(2)}, u32[]{:S(2)}) %collective-permute-start.5) | collective-permute-done | bytes 1048608 | tf_op jit(solution)/shard_map/ppermute | solution.py:430
  45.8 1.7 collective-permute-done.4.refs_1_
  47.6 0.5 collective-permute-start.7
  48.1 0.8 slice.6
  48.9 0.9 slice.7
  49.8 1.7 collective-permute-start.9
  51.5 0.3 collective-permute-start.8
  51.8 2.3 %stage.1 = (bf16[256,2048]{1,0:T(8,128)(2,1)}, bf16[128,2048]{1,0:T(8,128)(2,1)}) custom-call(s32[1]{0:T(128)} %bitcast.1.core, bf16[256,2048]{1,0:T(8,128)(2,1)} %w_hbm.1, bf16[128,2048]{1,0:T(8,128)(2,1)} %r_hbm.1), custom_call_target="tpu_custom_call" | custom-call | tf_op jit(solution)/shard_map/stage/pallas_call | solution.py:160
  54.1 1.6 collective-permute-start.14
  55.7 2.8 %collective-permute-start.13 = (bf16[256,2048]{1,0:T(8,128)(2,1)}, bf16[256,2048]{1,0:T(8,128)(2,1)}, u32[]{:S(2)}, u32[]{:S(2)}) collective-permute-start(bf16[256,2048]{1,0:T(8,128)(2,1)} %get-tuple-element.56.refs_4_), channel_id=1, source_target_pairs={{0,2},{1,3},{2,0},{3,1},{4,6},{5,7},{6,4},{7,5},{8,10},{9,11},{10,... | collective-permute-start | bytes 3145736 | tf_op jit(solution)/shard_map/ppermute | solution.py:412
  58.5 1.4 collective-permute-start.12
  59.9 1.2 copy-done.8
  61.1 1.0 copy-done.10
  62.2 7.3 %shard_map.110 = (f32[1024,128]{1,0:T(8,128)S(1)}, f32[1024,256]{1,0:T(8,128)S(1)}) custom-call(bf16[1024,128]{1,0:T(8,128)(2,1)S(1)} %queries.1.refs_0_, bf16[2048,256]{1,0:T(8,128)(2,1)S(1)} %collective-permute-done.4.refs_1_, bf16[2048,256]{1,0:T(8,128)(2,1)S(1)} %collective-permute-done.5.refs_2_, f32[1024,128]{1,0:T(8,128)S(1)} %copy-done.10, ...), custom_call_target="tpu_custom_call" | custom-call | flops 2147483648 | bytes 2097152 | tf_op jit(solution)/shard_map/pallas_call | solution.py:227
  69.5 8.7 %shard_map.111 = (f32[1024,128]{1,0:T(8,128)S(1)}, f32[1024,256]{1,0:T(8,128)S(1)}) custom-call(bf16[1024,128]{1,0:T(8,128)(2,1)S(1)} %queries.1.refs_0_, bf16[2048,256]{1,0:T(8,128)(2,1)} %collective-permute-done.6.refs_1_, bf16[2048,256]{1,0:T(8,128)(2,1)} %collective-permute-done.7.refs_2_, f32[1024,128]{1,0:T(8,128)S(1)} %get-tuple-element.44.refs_3_, ...), custom_call_target="tpu_custom_call" | custom-call | flops 2147483648 | bytes 2097152 | tf_op jit(solution)/shard_map/pallas_call | solution.py:227
  78.2 0.1 collective-permute-start.10
  78.3 0.5 collective-permute-start.11
  78.8 5.4 %shard_map.112 = (f32[1024,128]{1,0:T(8,128)S(1)}, f32[1024,256]{1,0:T(8,128)S(1)}) custom-call(bf16[1024,128]{1,0:T(8,128)(2,1)S(1)} %queries.1.refs_0_, bf16[1024,256]{1,0:T(8,128)(2,1)} %collective-permute-done.8.refs_1_, bf16[1024,256]{1,0:T(8,128)(2,1)S(1)} %collective-permute-done.9.refs_2_, f32[1024,128]{1,0:T(8,128)S(1)} %get-tuple-element.50.refs_3_, ...), custom_call_target="tpu_custom_call" | custom-call | flops 1073741824 | bytes 1048576 | tf_op jit(solution)/shard_map/pallas_call | solution.py:227
  84.2 4.5 %shard_map.113.refs_0_ = bf16[512,256]{1,0:T(8,128)(2,1)S(1)} custom-call(bf16[1024,128]{1,0:T(8,128)(2,1)S(1)} %queries.1.refs_0_, bf16[1024,256]{1,0:T(8,128)(2,1)S(1)} %collective-permute-done.10.refs_1_, bf16[1024,256]{1,0:T(8,128)(2,1)S(1)} %collective-permute-done.11.refs_2_, f32[1024,128]{1,0:T(8,128)S(1)} %get-tuple-element.52.refs_3_, ...), custom_call_target="tpu_custom_call" | custom-call | flops 1073741824 | bytes 1048576 | tf_op jit(solution)/shard_map/pallas_call | solution.py:227
  88.7 15.8 %collective-permute-done.13.refs_6_ = bf16[256,2048]{1,0:T(8,128)(2,1)} collective-permute-done((bf16[256,2048]{1,0:T(8,128)(2,1)}, bf16[256,2048]{1,0:T(8,128)(2,1)}, u32[]{:S(2)}, u32[]{:S(2)}) %collective-permute-start.13) | collective-permute-done | bytes 1048608 | tf_op jit(solution)/shard_map/ppermute | solution.py:412
  104.4 0.5 collective-permute-start.19
  104.9 0.0 collective-permute-start.20
  104.9 1.4 collective-permute-start.17
  106.3 2.4 %collective-permute-start.16 = (bf16[512,256]{1,0:T(8,128)(2,1)S(1)}, bf16[512,256]{1,0:T(8,128)(2,1)S(1)}, u32[]{:S(2)}, u32[]{:S(2)}) collective-permute-start(bf16[512,256]{1,0:T(8,128)(2,1)S(1)} %shard_map.113.refs_0_), channel_id=1, source_target_pairs={{0,2},{1,3},{2,0},{3,1},{4,6},{5,7},{6,4},{7,5},{8,10},{9,11},{10,... | collective-permute-start | bytes 786440 | tf_op jit(solution)/shard_map/ppermute | solution.py:412
  108.7 6.1 %collective-permute-done.17.refs_3_ = bf16[512,256]{1,0:T(8,128)(2,1)S(1)} collective-permute-done((bf16[512,256]{1,0:T(8,128)(2,1)S(1)}, bf16[512,256]{1,0:T(8,128)(2,1)S(1)}, u32[]{:S(2)}, u32[]{:S(2)}) %collective-permute-start.17) | collective-permute-done | bytes 262176 | tf_op jit(solution)/shard_map/ppermute | solution.py:412
  114.9 1.6 collective-permute-start.15
  116.4 0.1 pad_add_fusion.place
  116.5 4.5 %collective-permute-done.16.refs_2_ = bf16[512,256]{1,0:T(8,128)(2,1)S(1)} collective-permute-done((bf16[512,256]{1,0:T(8,128)(2,1)S(1)}, bf16[512,256]{1,0:T(8,128)(2,1)S(1)}, u32[]{:S(2)}, u32[]{:S(2)}) %collective-permute-start.16) | collective-permute-done | bytes 262176 | tf_op jit(solution)/shard_map/ppermute | solution.py:412
  121.0 1.7 collective-permute-done.15.refs_1_
  122.8 0.0 all-gather.2.cloned.1.call-done.refs_13_.w_hbm
  122.8 1.0 copy-done.11
  123.8 19.9 %layer.1 = (bf16[128,2048]{1,0:T(8,128)(2,1)S(1)}, bf16[128,2048]{1,0:T(8,128)(2,1)S(1)}, bf16[128,2048]{1,0:T(8,128)(2,1)S(1)}, bf16[256,1408]{1,0:T(8,128)(2,1)S(1)}) custom-call(s32[2]{0:T(128)S(1)} %pad_add_fusion.place, bf16[512,256]{1,0:T(8,128)(2,1)S(1)} %shard_map.113.refs_0_, bf16[512,256]{1,0:T(8,128)(2,1)S(1)} %collective-permute-done.15.refs_1_, ...), custom_call_target="tpu_custom_call" | custom-call | tf_op jit(solution)/shard_map/layer/pallas_call | solution.py:368
  143.7 4.5 %rest.1 = (bf16[128,2048]{1,0:T(8,128)(2,1)S(1)}, bf16[128,2048]{1,0:T(8,128)(2,1)S(1)}) custom-call(bf16[256,1408]{1,0:T(8,128)(2,1)S(1)} %get-tuple-element.62.h_ref, bf16[2048,4224]{1,0:T(8,128)(2,1)} %all-gather.2.cloned.1.call-done.refs_13_.w_hbm), custom_call_target="tpu_custom_call" | custom-call | tf_op jit(solution)/shard_map/rest/pallas_call | solution.py:351
  148.2 2.4 %collective-permute-start.23 = (bf16[128,2048]{1,0:T(8,128)(2,1)S(1)}, bf16[128,2048]{1,0:T(8,128)(2,1)S(1)}, u32[]{:S(2)}, u32[]{:S(2)}) collective-permute-start(bf16[128,2048]{1,0:T(8,128)(2,1)S(1)} %get-tuple-element.66), channel_id=1, source_target_pairs={{0,3},{1,0},{2,1},{3,2},{4,7},{5,4},{6,5},{7,6},{8,11},{9,8},{10,9... | collective-permute-start | bytes 1572872 | tf_op jit(solution)/shard_map/ppermute | solution.py:412
  150.6 1.5 collective-permute-start.22
  152.1 19.4 %collective-permute-done.23 = bf16[128,2048]{1,0:T(8,128)(2,1)S(1)} collective-permute-done((bf16[128,2048]{1,0:T(8,128)(2,1)S(1)}, bf16[128,2048]{1,0:T(8,128)(2,1)S(1)}, u32[]{:S(2)}, u32[]{:S(2)}) %collective-permute-start.23) | collective-permute-done | bytes 524320 | tf_op jit(solution)/shard_map/ppermute | solution.py:412
  171.5 3.4 %collective-permute-done.21 = bf16[128,2048]{1,0:T(8,128)(2,1)S(1)} collective-permute-done((bf16[128,2048]{1,0:T(8,128)(2,1)S(1)}, bf16[128,2048]{1,0:T(8,128)(2,1)S(1)}, u32[]{:S(2)}, u32[]{:S(2)}) %collective-permute-start.21) | collective-permute-done | bytes 524320 | tf_op jit(solution)/shard_map/ppermute | solution.py:412
  174.9 1.2 add_convert_fusion
  (35 shorter events, 0.1 us)
Async XLA Ops:
  6.5 116.2 %all-gather.2.cloned.1.call-start = ((), (), s32[]{:S(2)}) async-start(), calls=%async_computation | async-start | bytes 17842176 | tf_op jit(solution)/shard_map/all_gather | solution.py:459
  12.6 6.7 %collective-permute-start.2 = (bf16[512,256]{1,0:T(8,128)(2,1)}, bf16[512,256]{1,0:T(8,128)(2,1)S(1)}, u32[]{:S(2)}, u32[]{:S(2)}) collective-permute-start(bf16[512,256]{1,0:T(8,128)(2,1)} %keys.1.refs_0_), channel_id=1, source_target_pairs={{0,24},{4,100},{8,0},{12,108},{16,8},{20,116},{24,16},{28,124},{32... | collective-permute-start | bytes 786440 | tf_op jit(solution)/shard_map/ppermute | solution.py:430
  13.0 7.7 %collective-permute-start.1 = (bf16[512,256]{1,0:T(8,128)(2,1)}, bf16[512,256]{1,0:T(8,128)(2,1)S(1)}, u32[]{:S(2)}, u32[]{:S(2)}) collective-permute-start(bf16[512,256]{1,0:T(8,128)(2,1)} %keys.1.refs_0_), channel_id=1, source_target_pairs={{0,8},{4,36},{8,16},{12,44},{16,24},{20,52},{24,0},{28,60},{32,40}... | collective-permute-start | bytes 786440 | tf_op jit(solution)/shard_map/ppermute | solution.py:430
  14.7 8.4 %collective-permute-start = (bf16[512,256]{1,0:T(8,128)(2,1)}, bf16[512,256]{1,0:T(8,128)(2,1)S(1)}, u32[]{:S(2)}, u32[]{:S(2)}) collective-permute-start(bf16[512,256]{1,0:T(8,128)(2,1)} %keys.1.refs_0_), channel_id=1, source_target_pairs={{0,16},{4,68},{8,24},{12,76},{16,0},{20,84},{24,8},{28,92},{32,48}... | collective-permute-start | bytes 786440 | tf_op jit(solution)/shard_map/ppermute | solution.py:430
  23.1 1.0 copy-start
  24.1 8.5 %collective-permute-start.3 = (bf16[2048,256]{1,0:T(8,128)(2,1)S(1)}, bf16[2048,256]{1,0:T(8,128)(2,1)S(1)}, u32[]{:S(2)}, u32[]{:S(2)}) collective-permute-start(bf16[2048,256]{1,0:T(8,128)(2,1)S(1)} %lines.1.refs_1_), channel_id=1, source_target_pairs={{0,4},{4,0},{8,12},{12,8},{16,20},{20,16},{24,28},{28,24},{32,36},... | collective-permute-start | bytes 3145736 | tf_op jit(solution)/shard_map/ppermute | solution.py:435
  26.8 19.0 %collective-permute-start.5 = (bf16[2048,256]{1,0:T(8,128)(2,1)S(1)}, bf16[2048,256]{1,0:T(8,128)(2,1)S(1)}, u32[]{:S(2)}, u32[]{:S(2)}) collective-permute-start(bf16[2048,256]{1,0:T(8,128)(2,1)S(1)} %lines.1.refs_1_), channel_id=1, source_target_pairs={{0,96},{4,28},{8,104},{12,4},{16,112},{20,12},{24,120},{28,20},{32... | collective-permute-start | bytes 3145736 | tf_op jit(solution)/shard_map/ppermute | solution.py:430
  28.7 18.9 %collective-permute-start.4 = (bf16[2048,256]{1,0:T(8,128)(2,1)S(1)}, bf16[2048,256]{1,0:T(8,128)(2,1)S(1)}, u32[]{:S(2)}, u32[]{:S(2)}) collective-permute-start(bf16[2048,256]{1,0:T(8,128)(2,1)S(1)} %lines.1.refs_1_), channel_id=1, source_target_pairs={{0,32},{4,12},{8,40},{12,20},{16,48},{20,28},{24,56},{28,4},{32,64... | collective-permute-start | bytes 3145736 | tf_op jit(solution)/shard_map/ppermute | solution.py:430
  28.9 0.8 copy-start.2
  29.6 0.8 copy-start.3
  30.4 1.0 copy-start.4
  31.3 0.7 copy-start.6
  32.5 91.2 %copy-start.5 = (f32[2048]{0:T(1024)S(1)}, f32[2048]{0:T(1024)}, u32[]{:S(2)}) copy-start(f32[2048]{0:T(1024)} %param.18) | copy-start | bytes 24580
  39.0 9.9 %copy-start.7 = (f32[1024,256]{1,0:T(8,128)}, f32[1024,256]{1,0:T(8,128)S(1)}, u32[]{:S(2)}) copy-start(f32[1024,256]{1,0:T(8,128)S(1)} %get-tuple-element.43.refs_4_) | copy-start | bytes 3145732
  39.0 10.8 %copy-start.9 = (f32[1024,128]{1,0:T(8,128)}, f32[1024,128]{1,0:T(8,128)S(1)}, u32[]{:S(2)}) copy-start(f32[1024,128]{1,0:T(8,128)S(1)} %get-tuple-element.42.refs_3_) | copy-start | bytes 1572868
  47.6 8.1 %collective-permute-start.6 = (bf16[2048,256]{1,0:T(8,128)(2,1)S(1)}, bf16[2048,256]{1,0:T(8,128)(2,1)}, u32[]{:S(2)}, u32[]{:S(2)}) collective-permute-start(bf16[2048,256]{1,0:T(8,128)(2,1)S(1)} %collective-permute-done.4.refs_1_), channel_id=1, source_target_pairs={{0,4},{4,0},{8,12},{12,8},{16,20},{20,16},{24,28},{28,24},{32,36},... | collective-permute-start | bytes 3145736 | tf_op jit(solution)/shard_map/ppermute | solution.py:435
  47.6 11.0 %collective-permute-start.7 = (bf16[2048,256]{1,0:T(8,128)(2,1)S(1)}, bf16[2048,256]{1,0:T(8,128)(2,1)}, u32[]{:S(2)}, u32[]{:S(2)}) collective-permute-start(bf16[2048,256]{1,0:T(8,128)(2,1)S(1)} %collective-permute-done.5.refs_2_), channel_id=1, source_target_pairs={{0,4},{4,0},{8,12},{12,8},{16,20},{20,16},{24,28},{28,24},{32,36},... | collective-permute-start | bytes 3145736 | tf_op jit(solution)/shard_map/ppermute | solution.py:435
  49.8 28.4 %collective-permute-start.9 = (bf16[1024,256]{1,0:T(8,128)(2,1)}, bf16[1024,256]{1,0:T(8,128)(2,1)S(1)}, u32[]{:S(2)}, u32[]{:S(2)}) collective-permute-start(bf16[1024,256]{1,0:T(8,128)(2,1)} %slice.7), channel_id=1, source_target_pairs={{0,96},{4,28},{8,104},{12,4},{16,112},{20,12},{24,120},{28,20},{32... | collective-permute-start | bytes 1572872 | tf_op jit(solution)/shard_map/ppermute | solution.py:430
  51.5 26.7 %collective-permute-start.8 = (bf16[1024,256]{1,0:T(8,128)(2,1)}, bf16[1024,256]{1,0:T(8,128)(2,1)}, u32[]{:S(2)}, u32[]{:S(2)}) collective-permute-start(bf16[1024,256]{1,0:T(8,128)(2,1)} %slice.6), channel_id=1, source_target_pairs={{0,32},{4,12},{8,40},{12,20},{16,48},{20,28},{24,56},{28,4},{32,64... | collective-permute-start | bytes 1572872 | tf_op jit(solution)/shard_map/ppermute | solution.py:430
  54.1 69.7 %copy-start.1 = (bf16[128,2048]{1,0:T(8,128)(2,1)S(1)}, bf16[128,2048]{1,0:T(8,128)(2,1)}, u32[]{:S(2)}) copy-start(bf16[128,2048]{1,0:T(8,128)(2,1)} %get-tuple-element.60.refs_8_) | copy-start | bytes 1572868
  54.1 34.6 %collective-permute-start.14 = (bf16[256,2048]{1,0:T(8,128)(2,1)}, bf16[256,2048]{1,0:T(8,128)(2,1)}, u32[]{:S(2)}, u32[]{:S(2)}) collective-permute-start(bf16[256,2048]{1,0:T(8,128)(2,1)} %get-tuple-element.56.refs_4_), channel_id=1, source_target_pairs={{0,1},{1,2},{2,3},{3,0},{4,5},{5,6},{6,7},{7,4},{8,9},{9,10},{10,1... | collective-permute-start | bytes 3145736 | tf_op jit(solution)/shard_map/ppermute | solution.py:412
  55.7 48.7 %collective-permute-start.13 = (bf16[256,2048]{1,0:T(8,128)(2,1)}, bf16[256,2048]{1,0:T(8,128)(2,1)}, u32[]{:S(2)}, u32[]{:S(2)}) collective-permute-start(bf16[256,2048]{1,0:T(8,128)(2,1)} %get-tuple-element.56.refs_4_), channel_id=1, source_target_pairs={{0,2},{1,3},{2,0},{3,1},{4,6},{5,7},{6,4},{7,5},{8,10},{9,11},{10,... | collective-permute-start | bytes 3145736 | tf_op jit(solution)/shard_map/ppermute | solution.py:412
  58.5 45.9 %collective-permute-start.12 = (bf16[256,2048]{1,0:T(8,128)(2,1)}, bf16[256,2048]{1,0:T(8,128)(2,1)}, u32[]{:S(2)}, u32[]{:S(2)}) collective-permute-start(bf16[256,2048]{1,0:T(8,128)(2,1)} %get-tuple-element.56.refs_4_), channel_id=1, source_target_pairs={{0,3},{1,0},{2,1},{3,2},{4,7},{5,4},{6,5},{7,6},{8,11},{9,8},{10,9... | collective-permute-start | bytes 3145736 | tf_op jit(solution)/shard_map/ppermute | solution.py:412
  59.9 1.2 copy-start.8
  61.1 1.0 copy-start.10
  78.2 6.0 %collective-permute-start.10 = (bf16[1024,256]{1,0:T(8,128)(2,1)}, bf16[1024,256]{1,0:T(8,128)(2,1)S(1)}, u32[]{:S(2)}, u32[]{:S(2)}) collective-permute-start(bf16[1024,256]{1,0:T(8,128)(2,1)} %collective-permute-done.8.refs_1_), channel_id=1, source_target_pairs={{0,4},{4,0},{8,12},{12,8},{16,20},{20,16},{24,28},{28,24},{32,36},... | collective-permute-start | bytes 1572872 | tf_op jit(solution)/shard_map/ppermute | solution.py:435
  78.3 5.9 %collective-permute-start.11 = (bf16[1024,256]{1,0:T(8,128)(2,1)S(1)}, bf16[1024,256]{1,0:T(8,128)(2,1)S(1)}, u32[]{:S(2)}, u32[]{:S(2)}) collective-permute-start(bf16[1024,256]{1,0:T(8,128)(2,1)S(1)} %collective-permute-done.9.refs_2_), channel_id=1, source_target_pairs={{0,4},{4,0},{8,12},{12,8},{16,20},{20,16},{24,28},{28,24},{32,36},... | collective-permute-start | bytes 1572872 | tf_op jit(solution)/shard_map/ppermute | solution.py:435
  104.4 18.3 %collective-permute-start.18 = (bf16[256,2048]{1,0:T(8,128)(2,1)}, bf16[256,2048]{1,0:T(8,128)(2,1)S(1)}, u32[]{:S(2)}, u32[]{:S(2)}) collective-permute-start(bf16[256,2048]{1,0:T(8,128)(2,1)} %collective-permute-done.12.refs_5_), channel_id=1, source_target_pairs={{0,4},{4,0},{8,12},{12,8},{16,20},{20,16},{24,28},{28,24},{32,36},... | collective-permute-start | bytes 3145736 | tf_op jit(solution)/shard_map/ppermute | solution.py:435
  104.4 18.3 %collective-permute-start.19 = (bf16[256,2048]{1,0:T(8,128)(2,1)}, bf16[256,2048]{1,0:T(8,128)(2,1)}, u32[]{:S(2)}, u32[]{:S(2)}) collective-permute-start(bf16[256,2048]{1,0:T(8,128)(2,1)} %collective-permute-done.13.refs_6_), channel_id=1, source_target_pairs={{0,4},{4,0},{8,12},{12,8},{16,20},{20,16},{24,28},{28,24},{32,36},... | collective-permute-start | bytes 3145736 | tf_op jit(solution)/shard_map/ppermute | solution.py:435
  104.9 17.8 %collective-permute-start.20 = (bf16[256,2048]{1,0:T(8,128)(2,1)}, bf16[256,2048]{1,0:T(8,128)(2,1)}, u32[]{:S(2)}, u32[]{:S(2)}) collective-permute-start(bf16[256,2048]{1,0:T(8,128)(2,1)} %collective-permute-done.14.refs_7_), channel_id=1, source_target_pairs={{0,4},{4,0},{8,12},{12,8},{16,20},{20,16},{24,28},{28,24},{32,36},... | collective-permute-start | bytes 3145736 | tf_op jit(solution)/shard_map/ppermute | solution.py:435
  104.9 9.9 %collective-permute-start.17 = (bf16[512,256]{1,0:T(8,128)(2,1)S(1)}, bf16[512,256]{1,0:T(8,128)(2,1)S(1)}, u32[]{:S(2)}, u32[]{:S(2)}) collective-permute-start(bf16[512,256]{1,0:T(8,128)(2,1)S(1)} %shard_map.113.refs_0_), channel_id=1, source_target_pairs={{0,1},{1,2},{2,3},{3,0},{4,5},{5,6},{6,7},{7,4},{8,9},{9,10},{10,1... | collective-permute-start | bytes 786440 | tf_op jit(solution)/shard_map/ppermute | solution.py:412
  106.3 14.7 %collective-permute-start.16 = (bf16[512,256]{1,0:T(8,128)(2,1)S(1)}, bf16[512,256]{1,0:T(8,128)(2,1)S(1)}, u32[]{:S(2)}, u32[]{:S(2)}) collective-permute-start(bf16[512,256]{1,0:T(8,128)(2,1)S(1)} %shard_map.113.refs_0_), channel_id=1, source_target_pairs={{0,2},{1,3},{2,0},{3,1},{4,6},{5,7},{6,4},{7,5},{8,10},{9,11},{10,... | collective-permute-start | bytes 786440 | tf_op jit(solution)/shard_map/ppermute | solution.py:412
  114.9 7.9 %collective-permute-start.15 = (bf16[512,256]{1,0:T(8,128)(2,1)S(1)}, bf16[512,256]{1,0:T(8,128)(2,1)S(1)}, u32[]{:S(2)}, u32[]{:S(2)}) collective-permute-start(bf16[512,256]{1,0:T(8,128)(2,1)S(1)} %shard_map.113.refs_0_), channel_id=1, source_target_pairs={{0,3},{1,0},{2,1},{3,2},{4,7},{5,4},{6,5},{7,6},{8,11},{9,8},{10,9... | collective-permute-start | bytes 786440 | tf_op jit(solution)/shard_map/ppermute | solution.py:412
  122.7 1.0 copy-start.11
  148.2 23.3 %collective-permute-start.23 = (bf16[128,2048]{1,0:T(8,128)(2,1)S(1)}, bf16[128,2048]{1,0:T(8,128)(2,1)S(1)}, u32[]{:S(2)}, u32[]{:S(2)}) collective-permute-start(bf16[128,2048]{1,0:T(8,128)(2,1)S(1)} %get-tuple-element.66), channel_id=1, source_target_pairs={{0,3},{1,0},{2,1},{3,2},{4,7},{5,4},{6,5},{7,6},{8,11},{9,8},{10,9... | collective-permute-start | bytes 1572872 | tf_op jit(solution)/shard_map/ppermute | solution.py:412
  150.6 24.3 %collective-permute-start.21 = (bf16[128,2048]{1,0:T(8,128)(2,1)S(1)}, bf16[128,2048]{1,0:T(8,128)(2,1)S(1)}, u32[]{:S(2)}, u32[]{:S(2)}) collective-permute-start(bf16[128,2048]{1,0:T(8,128)(2,1)S(1)} %get-tuple-element.64), channel_id=1, source_target_pairs={{0,1},{1,2},{2,3},{3,0},{4,5},{5,6},{6,7},{7,4},{8,9},{9,10},{10,1... | collective-permute-start | bytes 1572872 | tf_op jit(solution)/shard_map/ppermute | solution.py:412
  150.6 24.3 %collective-permute-start.22 = (bf16[128,2048]{1,0:T(8,128)(2,1)S(1)}, bf16[128,2048]{1,0:T(8,128)(2,1)S(1)}, u32[]{:S(2)}, u32[]{:S(2)}) collective-permute-start(bf16[128,2048]{1,0:T(8,128)(2,1)S(1)} %get-tuple-element.65), channel_id=1, source_target_pairs={{0,2},{1,3},{2,0},{3,1},{4,6},{5,7},{6,4},{7,5},{8,10},{9,11},{10,... | collective-permute-start | bytes 1572872 | tf_op jit(solution)/shard_map/ppermute | solution.py:412
Sparse Core Ops, SparseCore 0:
  9.6 83.4 all-gather.1

commit v13 on v12

--- a/solution.py
+++ b/solution.py
@@ -232,7 +232,7 @@
         + ([] if first else held),
         out_specs=pl.BlockSpec((tile, head_dim), lambda i: (i % tiles, i // tiles)) if last else tuple(held),
         out_shape=jax.ShapeDtypeStruct((tok, heads * head_dim), bf16) if last else held_shape,
-        compiler_params=pltpu.CompilerParams(dimension_semantics=("arbitrary",), vmem_limit_bytes=12 << 20),
+        compiler_params=pltpu.CompilerParams(dimension_semantics=("arbitrary",), vmem_limit_bytes=20 << 20),
         cost_estimate=pl.CostEstimate(
             flops=4 * rows * piece[0] * pieces * head_dim,
             bytes_accessed=4 * piece[0] * pieces * head_dim,
@@ -486,8 +486,8 @@
     state = flash(q, near_swapped, state, tok, False)
     state, far = lax.optimization_barrier((state, far))
     far_swapped = [other_core(v) for v in far]
-    state = flash(q, far, state, tok, False)
-    attended = flash(q, far_swapped, state, tok, True)
+    state = flash(q, far, state, tok, False, tile=512)
+    attended = flash(q, far_swapped, state, tok, True, tile=512)
 
     att_parts = [attended]
     for r in range(1, parts):

time: 185 us -> 185 us (level)
  no operation moved by 1% of the time
where the time goes in v13:
time: 185 us; the launch traced here: 183 us
  waiting for transfers between devices  64.7 us (35%)
  Pallas kernels  64 us (35%)
  starting transfers between devices  29.1 us (16%)
  between operations  13.7 us (7%)
  local copies, waits for them, and re-layouts  9.07 us (5%)
  other arithmetic  2.46 us (1%)
    ppermute x9, waiting for transfers between devices, shifted(): lax.ppermute(value, 'tp', [(i, (i + by) % count) for i in range(count)])  51.2 us
    pallas_call x5, Pallas kernels, flash(): pl.pallas_call(functools.partial(flash_kernel, pieces=pieces, scale=head_...  31.9 us
    pallas_call x1, Pallas kernels, layer(): pl.pallas_call(functools.partial(layer_kernel, parts=parts, tile=tile, su...  19.9 us
    ppermute x9, starting transfers between devices, shifted(): lax.ppermute(value, 'tp', [(i, (i + by) % count) for i in range(count)])  15.1 us
    ppermute x7, waiting for transfers between devices, crossed(): return lax.ppermute(value, 'sp', pairs)  13.4 us
    ppermute x7, starting transfers between devices, crossed(): return lax.ppermute(value, 'sp', pairs)  9.65 us
    unnamed x24, local copies, waits for them, and re-layouts  7.38 us
    pallas_call x1, Pallas kernels, rest(): pl.pallas_call(rest_kernel, in_specs=[pl.BlockSpec(memory_space=pltpu.VME...  4.53 us
  transfers between devices with their start and end apart: 25, of which 11 were waited for; matrix products, arithmetic and copies ran while one was open for 2% of the time, Pallas kernels for 21%

profile of v13, /device:TPU:8, one launch (start us, length us, event | category | flops | bytes accessed | tf_op | source)
XLA Modules:
  0.0 183.0 jit_solution(13221489970342214781)
XLA Ops:
  6.5 2.0 %weave.1 = bf16[64,4224]{1,0:T(8,128)(2,1)} custom-call(bf16[64,1408]{1,0:T(8,128)(2,1)} %g_hbm.1, bf16[64,1408]{1,0:T(8,128)(2,1)} %u_hbm.1, bf16[64,1408]{1,0:T(8,128)(2,1)} %bitcast.8), custom_call_target="tpu_custom_call" | custom-call | tf_op jit(solution)/shard_map/weave/pallas_call | solution.py:124
  8.6 0.0 all-gather.2.cloned.1.call-update
  8.7 0.1 add_convert_fusion.1
  8.7 0.2 multiply_sine_fusion
  9.0 0.1 negate_select_fusion.1
  9.1 0.8 pad_maximum_fusion
  9.8 2.8 %keys.1.refs_0_ = bf16[512,256]{1,0:T(8,128)(2,1)} custom-call(bf16[512,128]{1,0:T(8,128)(2,1)} %k_hbm.1, bf16[512,128]{1,0:T(8,128)(2,1)} %v_hbm.1, f32[1,128]{1,0:T(1,128)} %bitcast.9, f32[72,128]{1,0:T(8,128)} %get-tuple-element.77.cos_ref, f32[72,128]{1,0:T(8,128)} %get-tuple-element.78.sin_ref), custom_call_target="tpu_custom_call" | custom-call | tf_op jit(solution)/shard_map/keys/pallas_call | solution.py:78
  12.6 0.4 collective-permute-start.2
  13.0 1.7 collective-permute-start.1
  14.7 3.5 %collective-permute-start = (bf16[512,256]{1,0:T(8,128)(2,1)}, bf16[512,256]{1,0:T(8,128)(2,1)S(1)}, u32[]{:S(2)}, u32[]{:S(2)}) collective-permute-start(bf16[512,256]{1,0:T(8,128)(2,1)} %keys.1.refs_0_), channel_id=1, source_target_pairs={{0,16},{4,68},{8,24},{12,76},{16,0},{20,84},{24,8},{28,92},{32,48}... | collective-permute-start | bytes 786440 | tf_op jit(solution)/shard_map/ppermute | solution.py:430
  18.2 1.0 collective-permute-done.2.refs_3_
  19.3 1.5 collective-permute-done.1.refs_2_
  20.7 2.3 %collective-permute-done.refs_1_ = bf16[512,256]{1,0:T(8,128)(2,1)S(1)} collective-permute-done((bf16[512,256]{1,0:T(8,128)(2,1)}, bf16[512,256]{1,0:T(8,128)(2,1)S(1)}, u32[]{:S(2)}, u32[]{:S(2)}) %collective-permute-start) | collective-permute-done | bytes 262176 | tf_op jit(solution)/shard_map/ppermute | solution.py:430
  23.1 1.0 copy-done
  24.0 0.1 lines.1.refs_1_
  24.1 2.7 %collective-permute-start.3 = (bf16[2048,256]{1,0:T(8,128)(2,1)S(1)}, bf16[2048,256]{1,0:T(8,128)(2,1)S(1)}, u32[]{:S(2)}, u32[]{:S(2)}) collective-permute-start(bf16[2048,256]{1,0:T(8,128)(2,1)S(1)} %lines.1.refs_1_), channel_id=1, source_target_pairs={{0,4},{4,0},{8,12},{12,8},{16,20},{20,16},{24,28},{28,24},{32,36},... | collective-permute-start | bytes 3145736 | tf_op jit(solution)/shard_map/ppermute | solution.py:435
  26.8 1.8 %collective-permute-start.5 = (bf16[2048,256]{1,0:T(8,128)(2,1)S(1)}, bf16[2048,256]{1,0:T(8,128)(2,1)S(1)}, u32[]{:S(2)}, u32[]{:S(2)}) collective-permute-start(bf16[2048,256]{1,0:T(8,128)(2,1)S(1)} %lines.1.refs_1_), channel_id=1, source_target_pairs={{0,96},{4,28},{8,104},{12,4},{16,112},{20,12},{24,120},{28,20},{32... | collective-permute-start | bytes 3145736 | tf_op jit(solution)/shard_map/ppermute | solution.py:430
  28.7 0.2 collective-permute-start.4
  28.9 0.8 copy-done.2
  29.6 0.8 copy-done.3
  30.4 1.0 copy-done.4
  31.3 0.7 copy-done.6
  32.0 0.5 queries.1.refs_0_
  32.5 0.0 copy-start.5
  32.6 0.0 collective-permute-done.3.refs_2_
  32.6 6.4 %shard_map.109 = (f32[1024,128]{1,0:T(8,128)S(1)}, f32[1024,256]{1,0:T(8,128)S(1)}) custom-call(bf16[1024,128]{1,0:T(8,128)(2,1)S(1)} %queries.1.refs_0_, bf16[2048,256]{1,0:T(8,128)(2,1)S(1)} %lines.1.refs_1_, bf16[2048,256]{1,0:T(8,128)(2,1)S(1)} %collective-permute-done.3.refs_2_), custom_call_target="tpu_custom_call" | custom-call | flops 2147483648 | bytes 2097152 | tf_op jit(solution)/shard_map/pallas_call | solution.py:227
  39.0 6.8 %collective-permute-done.5.refs_2_ = bf16[2048,256]{1,0:T(8,128)(2,1)S(1)} collective-permute-done((bf16[2048,256]{1,0:T(8,128)(2,1)S(1)}, bf16[2048,256]{1,0:T(8,128)(2,1)S(1)}, u32[]{:S(2)}, u32[]{:S(2)}) %collective-permute-start.5) | collective-permute-done | bytes 1048608 | tf_op jit(solution)/shard_map/ppermute | solution.py:430
  45.8 1.7 collective-permute-done.4.refs_1_
  47.6 0.5 collective-permute-start.7
  48.1 0.8 slice.6
  48.9 0.9 slice.7
  49.8 1.7 collective-permute-start.9
  51.5 0.3 collective-permute-start.8
  51.8 2.3 %stage.1 = (bf16[256,2048]{1,0:T(8,128)(2,1)}, bf16[128,2048]{1,0:T(8,128)(2,1)}) custom-call(s32[1]{0:T(128)} %bitcast.1.core, bf16[256,2048]{1,0:T(8,128)(2,1)} %w_hbm.1, bf16[128,2048]{1,0:T(8,128)(2,1)} %r_hbm.1), custom_call_target="tpu_custom_call" | custom-call | tf_op jit(solution)/shard_map/stage/pallas_call | solution.py:160
  54.1 1.6 collective-permute-start.14
  55.7 2.8 %collective-permute-start.13 = (bf16[256,2048]{1,0:T(8,128)(2,1)}, bf16[256,2048]{1,0:T(8,128)(2,1)}, u32[]{:S(2)}, u32[]{:S(2)}) collective-permute-start(bf16[256,2048]{1,0:T(8,128)(2,1)} %get-tuple-element.56.refs_4_), channel_id=1, source_target_pairs={{0,2},{1,3},{2,0},{3,1},{4,6},{5,7},{6,4},{7,5},{8,10},{9,11},{10,... | collective-permute-start | bytes 3145736 | tf_op jit(solution)/shard_map/ppermute | solution.py:412
  58.5 1.4 collective-permute-start.12
  59.9 1.2 copy-done.8
  61.1 1.0 copy-done.10
  62.2 7.3 %shard_map.110 = (f32[1024,128]{1,0:T(8,128)S(1)}, f32[1024,256]{1,0:T(8,128)S(1)}) custom-call(bf16[1024,128]{1,0:T(8,128)(2,1)S(1)} %queries.1.refs_0_, bf16[2048,256]{1,0:T(8,128)(2,1)S(1)} %collective-permute-done.4.refs_1_, bf16[2048,256]{1,0:T(8,128)(2,1)S(1)} %collective-permute-done.5.refs_2_, f32[1024,128]{1,0:T(8,128)S(1)} %copy-done.10, ...), custom_call_target="tpu_custom_call" | custom-call | flops 2147483648 | bytes 2097152 | tf_op jit(solution)/shard_map/pallas_call | solution.py:227
  69.5 8.7 %shard_map.111 = (f32[1024,128]{1,0:T(8,128)S(1)}, f32[1024,256]{1,0:T(8,128)S(1)}) custom-call(bf16[1024,128]{1,0:T(8,128)(2,1)S(1)} %queries.1.refs_0_, bf16[2048,256]{1,0:T(8,128)(2,1)} %collective-permute-done.6.refs_1_, bf16[2048,256]{1,0:T(8,128)(2,1)} %collective-permute-done.7.refs_2_, f32[1024,128]{1,0:T(8,128)S(1)} %get-tuple-element.44.refs_3_, ...), custom_call_target="tpu_custom_call" | custom-call | flops 2147483648 | bytes 2097152 | tf_op jit(solution)/shard_map/pallas_call | solution.py:227
  78.2 0.1 collective-permute-start.10
  78.3 0.5 collective-permute-start.11
  78.8 5.3 %shard_map.112 = (f32[1024,128]{1,0:T(8,128)S(1)}, f32[1024,256]{1,0:T(8,128)S(1)}) custom-call(bf16[1024,128]{1,0:T(8,128)(2,1)S(1)} %queries.1.refs_0_, bf16[1024,256]{1,0:T(8,128)(2,1)} %collective-permute-done.8.refs_1_, bf16[1024,256]{1,0:T(8,128)(2,1)S(1)} %collective-permute-done.9.refs_2_, f32[1024,128]{1,0:T(8,128)S(1)} %get-tuple-element.50.refs_3_, ...), custom_call_target="tpu_custom_call" | custom-call | flops 1073741824 | bytes 1048576 | tf_op jit(solution)/shard_map/pallas_call | solution.py:227
  84.1 4.3 %shard_map.113.refs_0_ = bf16[512,256]{1,0:T(8,128)(2,1)S(1)} custom-call(bf16[1024,128]{1,0:T(8,128)(2,1)S(1)} %queries.1.refs_0_, bf16[1024,256]{1,0:T(8,128)(2,1)S(1)} %collective-permute-done.10.refs_1_, bf16[1024,256]{1,0:T(8,128)(2,1)S(1)} %collective-permute-done.11.refs_2_, f32[1024,128]{1,0:T(8,128)S(1)} %get-tuple-element.52.refs_3_, ...), custom_call_target="tpu_custom_call" | custom-call | flops 1073741824 | bytes 1048576 | tf_op jit(solution)/shard_map/pallas_call | solution.py:227
  88.4 16.0 %collective-permute-done.13.refs_6_ = bf16[256,2048]{1,0:T(8,128)(2,1)} collective-permute-done((bf16[256,2048]{1,0:T(8,128)(2,1)}, bf16[256,2048]{1,0:T(8,128)(2,1)}, u32[]{:S(2)}, u32[]{:S(2)}) %collective-permute-start.13) | collective-permute-done | bytes 1048608 | tf_op jit(solution)/shard_map/ppermute | solution.py:412
  104.4 0.5 collective-permute-start.19
  104.9 0.0 collective-permute-start.20
  104.9 1.4 collective-permute-start.17
  106.3 2.4 %collective-permute-start.16 = (bf16[512,256]{1,0:T(8,128)(2,1)S(1)}, bf16[512,256]{1,0:T(8,128)(2,1)S(1)}, u32[]{:S(2)}, u32[]{:S(2)}) collective-permute-start(bf16[512,256]{1,0:T(8,128)(2,1)S(1)} %shard_map.113.refs_0_), channel_id=1, source_target_pairs={{0,2},{1,3},{2,0},{3,1},{4,6},{5,7},{6,4},{7,5},{8,10},{9,11},{10,... | collective-permute-start | bytes 786440 | tf_op jit(solution)/shard_map/ppermute | solution.py:412
  108.7 6.1 %collective-permute-done.17.refs_3_ = bf16[512,256]{1,0:T(8,128)(2,1)S(1)} collective-permute-done((bf16[512,256]{1,0:T(8,128)(2,1)S(1)}, bf16[512,256]{1,0:T(8,128)(2,1)S(1)}, u32[]{:S(2)}, u32[]{:S(2)}) %collective-permute-start.17) | collective-permute-done | bytes 262176 | tf_op jit(solution)/shard_map/ppermute | solution.py:412
  114.9 1.6 collective-permute-start.15
  116.4 0.1 pad_add_fusion.place
  116.5 4.5 %collective-permute-done.16.refs_2_ = bf16[512,256]{1,0:T(8,128)(2,1)S(1)} collective-permute-done((bf16[512,256]{1,0:T(8,128)(2,1)S(1)}, bf16[512,256]{1,0:T(8,128)(2,1)S(1)}, u32[]{:S(2)}, u32[]{:S(2)}) %collective-permute-start.16) | collective-permute-done | bytes 262176 | tf_op jit(solution)/shard_map/ppermute | solution.py:412
  121.0 1.7 collective-permute-done.15.refs_1_
  122.8 0.0 all-gather.2.cloned.1.call-done.refs_13_.w_hbm
  122.8 1.0 copy-done.11
  123.8 19.9 %layer.1 = (bf16[128,2048]{1,0:T(8,128)(2,1)S(1)}, bf16[128,2048]{1,0:T(8,128)(2,1)S(1)}, bf16[128,2048]{1,0:T(8,128)(2,1)S(1)}, bf16[256,1408]{1,0:T(8,128)(2,1)S(1)}) custom-call(s32[2]{0:T(128)S(1)} %pad_add_fusion.place, bf16[512,256]{1,0:T(8,128)(2,1)S(1)} %shard_map.113.refs_0_, bf16[512,256]{1,0:T(8,128)(2,1)S(1)} %collective-permute-done.15.refs_1_, ...), custom_call_target="tpu_custom_call" | custom-call | tf_op jit(solution)/shard_map/layer/pallas_call | solution.py:368
  143.7 4.5 %rest.1 = (bf16[128,2048]{1,0:T(8,128)(2,1)S(1)}, bf16[128,2048]{1,0:T(8,128)(2,1)S(1)}) custom-call(bf16[256,1408]{1,0:T(8,128)(2,1)S(1)} %get-tuple-element.62.h_ref, bf16[2048,4224]{1,0:T(8,128)(2,1)} %all-gather.2.cloned.1.call-done.refs_13_.w_hbm), custom_call_target="tpu_custom_call" | custom-call | tf_op jit(solution)/shard_map/rest/pallas_call | solution.py:351
  148.2 2.4 %collective-permute-start.23 = (bf16[128,2048]{1,0:T(8,128)(2,1)S(1)}, bf16[128,2048]{1,0:T(8,128)(2,1)S(1)}, u32[]{:S(2)}, u32[]{:S(2)}) collective-permute-start(bf16[128,2048]{1,0:T(8,128)(2,1)S(1)} %get-tuple-element.66), channel_id=1, source_target_pairs={{0,3},{1,0},{2,1},{3,2},{4,7},{5,4},{6,5},{7,6},{8,11},{9,8},{10,9... | collective-permute-start | bytes 1572872 | tf_op jit(solution)/shard_map/ppermute | solution.py:412
  150.6 1.5 collective-permute-start.22
  152.1 19.4 %collective-permute-done.23 = bf16[128,2048]{1,0:T(8,128)(2,1)S(1)} collective-permute-done((bf16[128,2048]{1,0:T(8,128)(2,1)S(1)}, bf16[128,2048]{1,0:T(8,128)(2,1)S(1)}, u32[]{:S(2)}, u32[]{:S(2)}) %collective-permute-start.23) | collective-permute-done | bytes 524320 | tf_op jit(solution)/shard_map/ppermute | solution.py:412
  171.5 3.4 %collective-permute-done.21 = bf16[128,2048]{1,0:T(8,128)(2,1)S(1)} collective-permute-done((bf16[128,2048]{1,0:T(8,128)(2,1)S(1)}, bf16[128,2048]{1,0:T(8,128)(2,1)S(1)}, u32[]{:S(2)}, u32[]{:S(2)}) %collective-permute-start.21) | collective-permute-done | bytes 524320 | tf_op jit(solution)/shard_map/ppermute | solution.py:412
  174.9 1.2 add_convert_fusion
  (35 shorter events, 0.1 us)
Async XLA Ops:
  6.5 116.2 %all-gather.2.cloned.1.call-start = ((), (), s32[]{:S(2)}) async-start(), calls=%async_computation | async-start | bytes 17842176 | tf_op jit(solution)/shard_map/all_gather | solution.py:459
  12.6 6.7 %collective-permute-start.2 = (bf16[512,256]{1,0:T(8,128)(2,1)}, bf16[512,256]{1,0:T(8,128)(2,1)S(1)}, u32[]{:S(2)}, u32[]{:S(2)}) collective-permute-start(bf16[512,256]{1,0:T(8,128)(2,1)} %keys.1.refs_0_), channel_id=1, source_target_pairs={{0,24},{4,100},{8,0},{12,108},{16,8},{20,116},{24,16},{28,124},{32... | collective-permute-start | bytes 786440 | tf_op jit(solution)/shard_map/ppermute | solution.py:430
  13.0 7.7 %collective-permute-start.1 = (bf16[512,256]{1,0:T(8,128)(2,1)}, bf16[512,256]{1,0:T(8,128)(2,1)S(1)}, u32[]{:S(2)}, u32[]{:S(2)}) collective-permute-start(bf16[512,256]{1,0:T(8,128)(2,1)} %keys.1.refs_0_), channel_id=1, source_target_pairs={{0,8},{4,36},{8,16},{12,44},{16,24},{20,52},{24,0},{28,60},{32,40}... | collective-permute-start | bytes 786440 | tf_op jit(solution)/shard_map/ppermute | solution.py:430
  14.7 8.4 %collective-permute-start = (bf16[512,256]{1,0:T(8,128)(2,1)}, bf16[512,256]{1,0:T(8,128)(2,1)S(1)}, u32[]{:S(2)}, u32[]{:S(2)}) collective-permute-start(bf16[512,256]{1,0:T(8,128)(2,1)} %keys.1.refs_0_), channel_id=1, source_target_pairs={{0,16},{4,68},{8,24},{12,76},{16,0},{20,84},{24,8},{28,92},{32,48}... | collective-permute-start | bytes 786440 | tf_op jit(solution)/shard_map/ppermute | solution.py:430
  23.1 1.0 copy-start
  24.1 8.5 %collective-permute-start.3 = (bf16[2048,256]{1,0:T(8,128)(2,1)S(1)}, bf16[2048,256]{1,0:T(8,128)(2,1)S(1)}, u32[]{:S(2)}, u32[]{:S(2)}) collective-permute-start(bf16[2048,256]{1,0:T(8,128)(2,1)S(1)} %lines.1.refs_1_), channel_id=1, source_target_pairs={{0,4},{4,0},{8,12},{12,8},{16,20},{20,16},{24,28},{28,24},{32,36},... | collective-permute-start | bytes 3145736 | tf_op jit(solution)/shard_map/ppermute | solution.py:435
  26.8 19.0 %collective-permute-start.5 = (bf16[2048,256]{1,0:T(8,128)(2,1)S(1)}, bf16[2048,256]{1,0:T(8,128)(2,1)S(1)}, u32[]{:S(2)}, u32[]{:S(2)}) collective-permute-start(bf16[2048,256]{1,0:T(8,128)(2,1)S(1)} %lines.1.refs_1_), channel_id=1, source_target_pairs={{0,96},{4,28},{8,104},{12,4},{16,112},{20,12},{24,120},{28,20},{32... | collective-permute-start | bytes 3145736 | tf_op jit(solution)/shard_map/ppermute | solution.py:430
  28.7 18.9 %collective-permute-start.4 = (bf16[2048,256]{1,0:T(8,128)(2,1)S(1)}, bf16[2048,256]{1,0:T(8,128)(2,1)S(1)}, u32[]{:S(2)}, u32[]{:S(2)}) collective-permute-start(bf16[2048,256]{1,0:T(8,128)(2,1)S(1)} %lines.1.refs_1_), channel_id=1, source_target_pairs={{0,32},{4,12},{8,40},{12,20},{16,48},{20,28},{24,56},{28,4},{32,64... | collective-permute-start | bytes 3145736 | tf_op jit(solution)/shard_map/ppermute | solution.py:430
  28.9 0.8 copy-start.2
  29.6 0.8 copy-start.3
  30.4 1.0 copy-start.4
  31.3 0.7 copy-start.6
  32.5 91.2 %copy-start.5 = (f32[2048]{0:T(1024)S(1)}, f32[2048]{0:T(1024)}, u32[]{:S(2)}) copy-start(f32[2048]{0:T(1024)} %param.18) | copy-start | bytes 24580
  39.0 9.9 %copy-start.7 = (f32[1024,256]{1,0:T(8,128)}, f32[1024,256]{1,0:T(8,128)S(1)}, u32[]{:S(2)}) copy-start(f32[1024,256]{1,0:T(8,128)S(1)} %get-tuple-element.43.refs_4_) | copy-start | bytes 3145732
  39.0 10.8 %copy-start.9 = (f32[1024,128]{1,0:T(8,128)}, f32[1024,128]{1,0:T(8,128)S(1)}, u32[]{:S(2)}) copy-start(f32[1024,128]{1,0:T(8,128)S(1)} %get-tuple-element.42.refs_3_) | copy-start | bytes 1572868
  47.6 8.1 %collective-permute-start.6 = (bf16[2048,256]{1,0:T(8,128)(2,1)S(1)}, bf16[2048,256]{1,0:T(8,128)(2,1)}, u32[]{:S(2)}, u32[]{:S(2)}) collective-permute-start(bf16[2048,256]{1,0:T(8,128)(2,1)S(1)} %collective-permute-done.4.refs_1_), channel_id=1, source_target_pairs={{0,4},{4,0},{8,12},{12,8},{16,20},{20,16},{24,28},{28,24},{32,36},... | collective-permute-start | bytes 3145736 | tf_op jit(solution)/shard_map/ppermute | solution.py:435
  47.6 11.0 %collective-permute-start.7 = (bf16[2048,256]{1,0:T(8,128)(2,1)S(1)}, bf16[2048,256]{1,0:T(8,128)(2,1)}, u32[]{:S(2)}, u32[]{:S(2)}) collective-permute-start(bf16[2048,256]{1,0:T(8,128)(2,1)S(1)} %collective-permute-done.5.refs_2_), channel_id=1, source_target_pairs={{0,4},{4,0},{8,12},{12,8},{16,20},{20,16},{24,28},{28,24},{32,36},... | collective-permute-start | bytes 3145736 | tf_op jit(solution)/shard_map/ppermute | solution.py:435
  49.8 28.4 %collective-permute-start.9 = (bf16[1024,256]{1,0:T(8,128)(2,1)}, bf16[1024,256]{1,0:T(8,128)(2,1)S(1)}, u32[]{:S(2)}, u32[]{:S(2)}) collective-permute-start(bf16[1024,256]{1,0:T(8,128)(2,1)} %slice.7), channel_id=1, source_target_pairs={{0,96},{4,28},{8,104},{12,4},{16,112},{20,12},{24,120},{28,20},{32... | collective-permute-start | bytes 1572872 | tf_op jit(solution)/shard_map/ppermute | solution.py:430
  51.5 26.7 %collective-permute-start.8 = (bf16[1024,256]{1,0:T(8,128)(2,1)}, bf16[1024,256]{1,0:T(8,128)(2,1)}, u32[]{:S(2)}, u32[]{:S(2)}) collective-permute-start(bf16[1024,256]{1,0:T(8,128)(2,1)} %slice.6), channel_id=1, source_target_pairs={{0,32},{4,12},{8,40},{12,20},{16,48},{20,28},{24,56},{28,4},{32,64... | collective-permute-start | bytes 1572872 | tf_op jit(solution)/shard_map/ppermute | solution.py:430
  54.1 69.7 %copy-start.1 = (bf16[128,2048]{1,0:T(8,128)(2,1)S(1)}, bf16[128,2048]{1,0:T(8,128)(2,1)}, u32[]{:S(2)}) copy-start(bf16[128,2048]{1,0:T(8,128)(2,1)} %get-tuple-element.60.refs_8_) | copy-start | bytes 1572868
  54.1 34.3 %collective-permute-start.14 = (bf16[256,2048]{1,0:T(8,128)(2,1)}, bf16[256,2048]{1,0:T(8,128)(2,1)}, u32[]{:S(2)}, u32[]{:S(2)}) collective-permute-start(bf16[256,2048]{1,0:T(8,128)(2,1)} %get-tuple-element.56.refs_4_), channel_id=1, source_target_pairs={{0,1},{1,2},{2,3},{3,0},{4,5},{5,6},{6,7},{7,4},{8,9},{9,10},{10,1... | collective-permute-start | bytes 3145736 | tf_op jit(solution)/shard_map/ppermute | solution.py:412
  55.7 48.7 %collective-permute-start.13 = (bf16[256,2048]{1,0:T(8,128)(2,1)}, bf16[256,2048]{1,0:T(8,128)(2,1)}, u32[]{:S(2)}, u32[]{:S(2)}) collective-permute-start(bf16[256,2048]{1,0:T(8,128)(2,1)} %get-tuple-element.56.refs_4_), channel_id=1, source_target_pairs={{0,2},{1,3},{2,0},{3,1},{4,6},{5,7},{6,4},{7,5},{8,10},{9,11},{10,... | collective-permute-start | bytes 3145736 | tf_op jit(solution)/shard_map/ppermute | solution.py:412
  58.5 45.9 %collective-permute-start.12 = (bf16[256,2048]{1,0:T(8,128)(2,1)}, bf16[256,2048]{1,0:T(8,128)(2,1)}, u32[]{:S(2)}, u32[]{:S(2)}) collective-permute-start(bf16[256,2048]{1,0:T(8,128)(2,1)} %get-tuple-element.56.refs_4_), channel_id=1, source_target_pairs={{0,3},{1,0},{2,1},{3,2},{4,7},{5,4},{6,5},{7,6},{8,11},{9,8},{10,9... | collective-permute-start | bytes 3145736 | tf_op jit(solution)/shard_map/ppermute | solution.py:412
  59.9 1.2 copy-start.8
  61.1 1.0 copy-start.10
  78.2 5.9 %collective-permute-start.10 = (bf16[1024,256]{1,0:T(8,128)(2,1)}, bf16[1024,256]{1,0:T(8,128)(2,1)S(1)}, u32[]{:S(2)}, u32[]{:S(2)}) collective-permute-start(bf16[1024,256]{1,0:T(8,128)(2,1)} %collective-permute-done.8.refs_1_), channel_id=1, source_target_pairs={{0,4},{4,0},{8,12},{12,8},{16,20},{20,16},{24,28},{28,24},{32,36},... | collective-permute-start | bytes 1572872 | tf_op jit(solution)/shard_map/ppermute | solution.py:435
  78.3 5.8 %collective-permute-start.11 = (bf16[1024,256]{1,0:T(8,128)(2,1)S(1)}, bf16[1024,256]{1,0:T(8,128)(2,1)S(1)}, u32[]{:S(2)}, u32[]{:S(2)}) collective-permute-start(bf16[1024,256]{1,0:T(8,128)(2,1)S(1)} %collective-permute-done.9.refs_2_), channel_id=1, source_target_pairs={{0,4},{4,0},{8,12},{12,8},{16,20},{20,16},{24,28},{28,24},{32,36},... | collective-permute-start | bytes 1572872 | tf_op jit(solution)/shard_map/ppermute | solution.py:435
  104.4 18.3 %collective-permute-start.18 = (bf16[256,2048]{1,0:T(8,128)(2,1)}, bf16[256,2048]{1,0:T(8,128)(2,1)S(1)}, u32[]{:S(2)}, u32[]{:S(2)}) collective-permute-start(bf16[256,2048]{1,0:T(8,128)(2,1)} %collective-permute-done.12.refs_5_), channel_id=1, source_target_pairs={{0,4},{4,0},{8,12},{12,8},{16,20},{20,16},{24,28},{28,24},{32,36},... | collective-permute-start | bytes 3145736 | tf_op jit(solution)/shard_map/ppermute | solution.py:435
  104.4 18.3 %collective-permute-start.19 = (bf16[256,2048]{1,0:T(8,128)(2,1)}, bf16[256,2048]{1,0:T(8,128)(2,1)}, u32[]{:S(2)}, u32[]{:S(2)}) collective-permute-start(bf16[256,2048]{1,0:T(8,128)(2,1)} %collective-permute-done.13.refs_6_), channel_id=1, source_target_pairs={{0,4},{4,0},{8,12},{12,8},{16,20},{20,16},{24,28},{28,24},{32,36},... | collective-permute-start | bytes 3145736 | tf_op jit(solution)/shard_map/ppermute | solution.py:435
  104.9 17.8 %collective-permute-start.20 = (bf16[256,2048]{1,0:T(8,128)(2,1)}, bf16[256,2048]{1,0:T(8,128)(2,1)}, u32[]{:S(2)}, u32[]{:S(2)}) collective-permute-start(bf16[256,2048]{1,0:T(8,128)(2,1)} %collective-permute-done.14.refs_7_), channel_id=1, source_target_pairs={{0,4},{4,0},{8,12},{12,8},{16,20},{20,16},{24,28},{28,24},{32,36},... | collective-permute-start | bytes 3145736 | tf_op jit(solution)/shard_map/ppermute | solution.py:435
  104.9 9.9 %collective-permute-start.17 = (bf16[512,256]{1,0:T(8,128)(2,1)S(1)}, bf16[512,256]{1,0:T(8,128)(2,1)S(1)}, u32[]{:S(2)}, u32[]{:S(2)}) collective-permute-start(bf16[512,256]{1,0:T(8,128)(2,1)S(1)} %shard_map.113.refs_0_), channel_id=1, source_target_pairs={{0,1},{1,2},{2,3},{3,0},{4,5},{5,6},{6,7},{7,4},{8,9},{9,10},{10,1... | collective-permute-start | bytes 786440 | tf_op jit(solution)/shard_map/ppermute | solution.py:412
  106.3 14.7 %collective-permute-start.16 = (bf16[512,256]{1,0:T(8,128)(2,1)S(1)}, bf16[512,256]{1,0:T(8,128)(2,1)S(1)}, u32[]{:S(2)}, u32[]{:S(2)}) collective-permute-start(bf16[512,256]{1,0:T(8,128)(2,1)S(1)} %shard_map.113.refs_0_), channel_id=1, source_target_pairs={{0,2},{1,3},{2,0},{3,1},{4,6},{5,7},{6,4},{7,5},{8,10},{9,11},{10,... | collective-permute-start | bytes 786440 | tf_op jit(solution)/shard_map/ppermute | solution.py:412
  114.9 7.9 %collective-permute-start.15 = (bf16[512,256]{1,0:T(8,128)(2,1)S(1)}, bf16[512,256]{1,0:T(8,128)(2,1)S(1)}, u32[]{:S(2)}, u32[]{:S(2)}) collective-permute-start(bf16[512,256]{1,0:T(8,128)(2,1)S(1)} %shard_map.113.refs_0_), channel_id=1, source_target_pairs={{0,3},{1,0},{2,1},{3,2},{4,7},{5,4},{6,5},{7,6},{8,11},{9,8},{10,9... | collective-permute-start | bytes 786440 | tf_op jit(solution)/shard_map/ppermute | solution.py:412
  122.7 1.0 copy-start.11
  148.2 23.3 %collective-permute-start.23 = (bf16[128,2048]{1,0:T(8,128)(2,1)S(1)}, bf16[128,2048]{1,0:T(8,128)(2,1)S(1)}, u32[]{:S(2)}, u32[]{:S(2)}) collective-permute-start(bf16[128,2048]{1,0:T(8,128)(2,1)S(1)} %get-tuple-element.66), channel_id=1, source_target_pairs={{0,3},{1,0},{2,1},{3,2},{4,7},{5,4},{6,5},{7,6},{8,11},{9,8},{10,9... | collective-permute-start | bytes 1572872 | tf_op jit(solution)/shard_map/ppermute | solution.py:412
  150.6 24.3 %collective-permute-start.21 = (bf16[128,2048]{1,0:T(8,128)(2,1)S(1)}, bf16[128,2048]{1,0:T(8,128)(2,1)S(1)}, u32[]{:S(2)}, u32[]{:S(2)}) collective-permute-start(bf16[128,2048]{1,0:T(8,128)(2,1)S(1)} %get-tuple-element.64), channel_id=1, source_target_pairs={{0,1},{1,2},{2,3},{3,0},{4,5},{5,6},{6,7},{7,4},{8,9},{9,10},{10,1... | collective-permute-start | bytes 1572872 | tf_op jit(solution)/shard_map/ppermute | solution.py:412
  150.6 24.3 %collective-permute-start.22 = (bf16[128,2048]{1,0:T(8,128)(2,1)S(1)}, bf16[128,2048]{1,0:T(8,128)(2,1)S(1)}, u32[]{:S(2)}, u32[]{:S(2)}) collective-permute-start(bf16[128,2048]{1,0:T(8,128)(2,1)S(1)} %get-tuple-element.65), channel_id=1, source_target_pairs={{0,2},{1,3},{2,0},{3,1},{4,6},{5,7},{6,4},{7,5},{8,10},{9,11},{10,... | collective-permute-start | bytes 1572872 | tf_op jit(solution)/shard_map/ppermute | solution.py:412
Sparse Core Ops, SparseCore 0:
  9.6 83.4 all-gather.1
